TPU v7x, 512 devices: a whole 4x4x16 slice. The times are simulated.
512 devices in a mesh: fs: 64 (over z, y), tp: 8 (over x, core).
Axes of the slice: x: 4, y: 4, z: 16, core: 2. Of those that a mesh axis runs over, the one named last changes fastest.
Arguments:
- tokens: bfloat16 [32768, 2048], P('fs', 'tp'), may hold values from -6 to 6
- norm_gain: bfloat16 [2048], P('tp'), may hold values from 0.099609375 to 1.8984375
- proj_u: bfloat16 [2048, 2048], P('fs', 'tp'), may hold values from -0.125 to 0.125
- proj_v: bfloat16 [2048, 2048], P('fs', 'tp'), may hold values from -0.125 to 0.125
- layer_gain: bfloat16 [2048], P('tp'), may hold values from 0.099609375 to 1.8984375
- layer_shift: bfloat16 [2048], P('tp'), may hold values from -3 to 3
- mix_weight: bfloat16 [16, 128, 128], P('tp'), may hold values from -0.5 to 0.5
- mix_bias: bfloat16 [16, 128], P('tp'), may hold values from 0.099609375 to 1.8984375
- proj_out: bfloat16 [2048, 2048], P('tp', 'fs'), may hold values from -0.375 to 0.375
- ffn_gain: bfloat16 [2048], P('tp'), may hold values from 0.099609375 to 1.8984375
- ffn_gate: bfloat16 [2048, 4096], P('fs', 'tp'), may hold values from -0.125 to 0.125
- ffn_value: bfloat16 [2048, 4096], P('fs', 'tp'), may hold values from -0.125 to 0.125
- conv_gate: bfloat16 [3, 4096], P(None, 'tp'), may hold values from -3 to 3
- conv_value: bfloat16 [3, 4096], P(None, 'tp'), may hold values from -3 to 3
- proj_down: bfloat16 [4096, 2048], P('tp', 'fs'), may hold values from -0.25 to 0.25
Outputs:
- result: bfloat16 [32768, 2048], P('fs', 'tp')
All inputs are finite; a program needn't handle non-finite values.
Results may differ from a plain program's by a relative error of at most 0.017.
Values may be sent and summed in bfloat16 or wider, within the bound.
No kernel may reach another device: no remote copies, remote signals or barrier semaphores. Data moves between devices by JAX's collectives and lax.ppermute only.
A program may use at most 64 MiB of HBM per device.

v0:
```python
import jax
import jax.numpy as jnp
from jax import lax
from jax.sharding import Mesh
from jax.sharding import PartitionSpec as P

GROUP_DIM = 128
BLOCK = 128
SEGMENT = 64
KERNEL = 3
SEQ_LEN = 256
FS = ("z", "y")
TP = ("x", "c")
EPS = 1e-06
F32 = jnp.float32
BF16 = jnp.bfloat16
SWAP = [(0, 1), (1, 0)]


def everyones(shard, axis):
    copies = jnp.broadcast_to(shard, (lax.axis_size(axis), *shard.shape))
    return lax.all_to_all(copies, axis, split_axis=0, concat_axis=0, tiled=True)


def other_core(value):
    return lax.ppermute(value, "c", SWAP)


def after(value, *first):
    return lax.optimization_barrier((value, *first))[0]


def by_permutes(shard, axis):
    size = lax.axis_size(axis)
    here = lax.axis_index(axis).astype(jnp.uint32)
    parts = [shard]
    for step in (1, 3, 2):
        parts.append(lax.ppermute(shard, axis, [(i, (i + step) % size) for i in range(size)]))
    filled = jnp.zeros((size, *shard.shape), shard.dtype)
    for step, part in zip((0, 1, 3, 2), parts):
        origin = (here + jnp.uint32(size - step)) & jnp.uint32(size - 1)
        filled = lax.dynamic_update_slice(filled, part[None], (origin, *([jnp.uint32(0)] * shard.ndim)))
    return filled


def matmul(operand, matrix):
    return jnp.dot(operand, matrix, preferred_element_type=F32)


def matmul_t(operand, matrix):
    return lax.dot_general(operand, matrix, (((1,), (1,)), ((), ())), preferred_element_type=F32)


def whole_rows(shard, gather=everyones):
    n, w = shard.shape
    mine = gather(shard, "x")
    other = other_core(mine)
    first = lax.axis_index("c") == 0
    both = jnp.stack([jnp.where(first, mine, other), jnp.where(first, other, mine)], axis=1)
    return both.reshape(-1, n, w).transpose(1, 0, 2).reshape(n, -1)


def rms(values, gain):
    v = values.astype(F32)
    scale = lax.rsqrt(jnp.mean(v * v, axis=1, keepdims=True) + EPS)
    return (v * scale * gain.astype(F32)).astype(BF16)


def causal_taps(values, weights):
    seq_count = values.shape[0] // SEQ_LEN
    shaped = values.reshape(seq_count, SEQ_LEN, values.shape[1])
    padded = jnp.pad(shaped, ((0, 0), (KERNEL - 1, 0), (0, 0)))
    summed = jnp.zeros(shaped.shape, F32)
    for k in range(KERNEL):
        summed = summed + padded[:, k : k + SEQ_LEN].astype(F32) * weights[k].astype(F32)
    return summed.reshape(values.shape[0], values.shape[1])


def product_at_owner(rows, matrix):
    blocks = matrix.reshape(lax.axis_size("x"), 2, -1, matrix.shape[1])
    first = lax.axis_index("c") == 0
    keep = jnp.where(first, blocks[:, 0], blocks[:, 1])
    give = jnp.where(first, blocks[:, 1], blocks[:, 0])
    width = keep.shape[1]

    def split(w):
        return matmul_t(rows, w.reshape(-1, w.shape[2])).astype(BF16)

    came = other_core(split(give))
    pair = (split(keep).astype(F32) + came.astype(F32)).astype(BF16)
    parts = pair.reshape(rows.shape[0], -1, width).transpose(1, 0, 2)
    arrived = lax.all_to_all(parts, "x", split_axis=0, concat_axis=0, tiled=True)
    return arrived.astype(F32).sum(axis=0)


def on_device(
    tokens,
    norm_gain,
    proj_u,
    proj_v,
    layer_gain,
    layer_shift,
    mix_weight,
    mix_bias,
    proj_out,
    ffn_gain,
    ffn_gate,
    ffn_value,
    conv_gate,
    conv_value,
    proj_down,
):
    da = proj_u.shape[1]
    ff = ffn_gate.shape[1]
    row_count = tokens.shape[0]

    early = jnp.concatenate([proj_u, proj_v, proj_out.T], axis=1)
    early_z = everyones(early, "z")
    late = jnp.concatenate([ffn_gate, ffn_value, proj_down.T], axis=1)
    late_y = by_permutes(late, "y").reshape(-1, late.shape[1])
    late_all = lax.all_gather(after(late_y, early_z), "z", axis=0, tiled=True)

    packed = jnp.concatenate([tokens, jnp.broadcast_to(norm_gain, (8, da)), jnp.broadcast_to(ffn_gain, (8, da))], axis=0)
    whole = whole_rows(packed, by_permutes)
    normed = rms(whole[:row_count], whole[row_count])
    gain_two = whole[row_count + 8]
    early_all = everyones(early_z, "y").transpose(1, 0, 2, 3).reshape(-1, early.shape[1])

    act_v = jax.nn.gelu(matmul(normed, early_all[:, da : 2 * da]), approximate=False)
    sums = jnp.stack([jnp.sum(act_v, axis=1), jnp.sum(act_v * act_v, axis=1)])
    totals = everyones(sums.reshape(-1), TP).sum(axis=0).reshape(2, -1)
    act_u = jax.nn.gelu(matmul(normed, early_all[:, :da]), approximate=False)
    full_width = da * lax.axis_size(TP)
    center = totals[0] / full_width
    spread = totals[1] / full_width - center * center
    mixed_in = (
        (act_v - center[:, None]) * lax.rsqrt(spread + EPS)[:, None] * layer_gain.astype(F32) + layer_shift.astype(F32)
    ).astype(BF16)
    groups = da // GROUP_DIM
    blocks = mixed_in.reshape(row_count // BLOCK, BLOCK, groups, GROUP_DIM)
    segment = jnp.arange(BLOCK) // SEGMENT
    visible = segment[None, :] <= segment[:, None]
    masked = jnp.where(visible[None], mix_weight, jnp.zeros_like(mix_weight))
    spatial = (
        jnp.einsum("gij,njgc->nigc", masked, blocks, preferred_element_type=F32)
        + mix_bias.astype(F32).T[None, :, :, None]
    )
    gated = (act_u * spatial.reshape(row_count, da)).astype(BF16)
    stream = (tokens.astype(F32) + product_at_owner(gated, early_all[:, 2 * da :])).astype(BF16)
    normed_two = rms(whole_rows(stream), gain_two)
    pre_gate = matmul(normed_two, late_all[:, :ff]).astype(BF16)
    pre_value = matmul(normed_two, late_all[:, ff : 2 * ff]).astype(BF16)
    conv_g = causal_taps(pre_gate, conv_gate)
    conv_v = causal_taps(pre_value, conv_value)
    hidden = (jax.nn.silu(conv_g) * conv_v).astype(BF16)
    return (stream.astype(F32) + product_at_owner(hidden, late_all[:, 2 * ff :])).astype(BF16)


def solution(mesh):
    split = Mesh(mesh.devices.reshape(16, 4, 4, 2), ("z", "y", "x", "c"))
    placed = (
        P(FS, TP),
        P(TP),
        P(FS, TP),
        P(FS, TP),
        P(TP),
        P(TP),
        P(TP, None, None),
        P(TP, None),
        P(TP, FS),
        P(TP),
        P(FS, TP),
        P(FS, TP),
        P(None, TP),
        P(None, TP),
        P(TP, FS),
    )

    return jax.shard_map(on_device, mesh=split, in_specs=placed, out_specs=P(FS, TP), check_vma=False)
```

profile of v0, /device:TPU:1, one launch (start us, length us, event | category | flops | bytes accessed | tf_op | source)
XLA Modules:
  0.0 227.3 jit_solution(9421366425100502881)
XLA Ops:
  6.6 0.8 pad_maximum_fusion.3
  7.4 1.0 broadcast_in_dim.86
  8.3 15.7 %all-to-all-start = ((bf16[16,32,768]{2,1,0:T(8,128)(2,1)}), bf16[16,32,768]{2,1,0:T(8,128)(2,1)S(1)}, u32[]{:S(2)}, u32[]{:S(2)}) async-start(bf16[16,32,768]{2,1,0:T(8,128)(2,1)} %broadcast_in_dim.86), calls=%async_computation | async-start | bytes 1572864 | tf_op jit(solution)/shard_map/all_to_all | solution.py:22
  24.2 0.7 pad_maximum_fusion.1
  24.9 3.1 %collective-permute-start = (bf16[528,256]{1,0:T(8,128)(2,1)}, bf16[528,256]{1,0:T(8,128)(2,1)S(1)}, u32[]{:S(2)}, u32[]{:S(2)}) collective-permute-start(bf16[528,256]{1,0:T(8,128)(2,1)} %pad_maximum_fusion.1), channel_id=1, source_target_pairs={{0,2},{2,4},{4,6},{6,0},{1,3},{3,5},{5,7},{7,1},{8,10},{10,12},{12... | collective-permute-start | bytes 811016 | tf_op jit(solution)/shard_map/ppermute | solution.py:38
  28.0 3.4 %collective-permute-start.1 = (bf16[528,256]{1,0:T(8,128)(2,1)}, bf16[528,256]{1,0:T(8,128)(2,1)S(1)}, u32[]{:S(2)}, u32[]{:S(2)}) collective-permute-start(bf16[528,256]{1,0:T(8,128)(2,1)} %pad_maximum_fusion.1), channel_id=1, source_target_pairs={{0,6},{2,0},{4,2},{6,4},{1,7},{3,1},{5,3},{7,5},{8,14},{10,8},{12,... | collective-permute-start | bytes 811016 | tf_op jit(solution)/shard_map/ppermute | solution.py:38
  31.4 3.4 %collective-permute-start.2 = (bf16[528,256]{1,0:T(8,128)(2,1)}, bf16[528,256]{1,0:T(8,128)(2,1)S(1)}, u32[]{:S(2)}, u32[]{:S(2)}) collective-permute-start(bf16[528,256]{1,0:T(8,128)(2,1)} %pad_maximum_fusion.1), channel_id=1, source_target_pairs={{0,4},{2,6},{4,0},{6,2},{1,5},{3,7},{5,1},{7,3},{8,12},{10,14},{12... | collective-permute-start | bytes 811016 | tf_op jit(solution)/shard_map/ppermute | solution.py:38
  34.9 3.2 %collective-permute-start.6 = (bf16[32,1536]{1,0:T(8,128)(2,1)S(1)}, bf16[32,1536]{1,0:T(8,128)(2,1)}, u32[]{:S(2)}, u32[]{:S(2)}) collective-permute-start(bf16[32,1536]{1,0:T(8,128)(2,1)S(1)} %pad_maximum_fusion.2), channel_id=1, source_target_pairs={{0,8},{8,16},{16,24},{24,0},{1,9},{9,17},{17,25},{25,1},{2,10},{10... | collective-permute-start | bytes 294920 | tf_op jit(solution)/shard_map/ppermute | solution.py:38
  38.1 3.4 %collective-permute-start.7 = (bf16[32,1536]{1,0:T(8,128)(2,1)S(1)}, bf16[32,1536]{1,0:T(8,128)(2,1)}, u32[]{:S(2)}, u32[]{:S(2)}) collective-permute-start(bf16[32,1536]{1,0:T(8,128)(2,1)S(1)} %pad_maximum_fusion.2), channel_id=1, source_target_pairs={{0,24},{8,0},{16,8},{24,16},{1,25},{9,1},{17,9},{25,17},{2,26},{10... | collective-permute-start | bytes 294920 | tf_op jit(solution)/shard_map/ppermute | solution.py:38
  41.7 0.1 collective-permute-done.6
  41.8 3.5 %collective-permute-start.8 = (bf16[32,1536]{1,0:T(8,128)(2,1)S(1)}, bf16[32,1536]{1,0:T(8,128)(2,1)S(1)}, u32[]{:S(2)}, u32[]{:S(2)}) collective-permute-start(bf16[32,1536]{1,0:T(8,128)(2,1)S(1)} %pad_maximum_fusion.2), channel_id=1, source_target_pairs={{0,16},{8,24},{16,0},{24,8},{1,17},{9,25},{17,1},{25,9},{2,18},{10... | collective-permute-start | bytes 294920 | tf_op jit(solution)/shard_map/ppermute | solution.py:38
  45.4 0.9 bitcast_dynamic-update-slice_fusion.6
  46.3 0.9 bitcast_dynamic-update-slice_fusion.5
  47.3 4.9 %collective-permute-start.3 = (bf16[4,528,256]{2,1,0:T(8,128)(2,1)S(1)}, bf16[4,528,256]{2,1,0:T(8,128)(2,1)}, u32[]{:S(2)}, u32[]{:S(2)}) collective-permute-start(bf16[4,528,256]{2,1,0:T(8,128)(2,1)S(1)} %bitcast_dynamic-update-slice_fusion), channel_id=1, source_target_pairs={{0,1},{1,0},{2,3},{3,2},{4,5},{5,4},{6,7},{7,6},{8,9},{9,8},{10,11... | collective-permute-start | bytes 3244040 | tf_op jit(solution)/shard_map/ppermute | solution.py:26
  52.3 6.4 %all-to-all-done = bf16[16,32,768]{2,1,0:T(8,128)(2,1)S(1)} async-done(((bf16[16,32,768]{2,1,0:T(8,128)(2,1)}), bf16[16,32,768]{2,1,0:T(8,128)(2,1)S(1)}, u32[]{:S(2)}, u32[]{:S(2)}) %all-to-all-start) | async-done | bytes 786464 | tf_op jit(solution)/shard_map/all_to_all | solution.py:22
  58.9 2.0 broadcast_in_dim.87
  60.9 4.8 %all-to-all-start.1 = ((bf16[4,16,32,768]{3,2,1,0:T(8,128)(2,1)}), bf16[4,16,32,768]{3,2,1,0:T(8,128)(2,1)}, u32[]{:S(2)}, u32[]{:S(2)}) async-start(bf16[4,16,32,768]{3,2,1,0:T(8,128)(2,1)} %broadcast_in_dim.87), calls=%async_computation.1 | async-start | bytes 6291456 | tf_op jit(solution)/shard_map/all_to_all | solution.py:22
  65.7 1.4 select_bitcast_fusion.1
  67.1 0.2 pad_maximum_fusion
  67.3 2.4 %slice_convert_fusion = f32[512,8,256]{2,0,1:T(8,128)} fusion(bf16[528,8,256]{2,0,1:T(8,128)(2,1)S(1)} %bitcast.115), kind=kLoop, calls=%fused_computation.13 | loop fusion | flops 1048576 | bytes 6291456 | tf_op jit(solution)/shard_map/convert_element_type | solution.py:64
  69.8 5.4 %copy.51 = f32[512,8,256]{0,2,1:T(8,128)} copy(f32[512,8,256]{2,0,1:T(8,128)} %slice_convert_fusion) | data formatting | bytes 8388608 | tf_op jit(solution)/shard_map/convert_element_type | solution.py:64
  75.1 0.5 multiply_reduce_fusion.1
  75.6 4.1 %fusion.3 = bf16[512,2048]{0,1:T(8,128)(2,1)} fusion(f32[512,8,256]{0,2,1:T(8,128)} %copy.51, f32[2048]{0:T(1024)S(1)} %bitcast.141, f32[512]{0:T(512)S(1)} %add_rsqrt_fusion.2), kind=kLoop, calls=%fused_computation.5 | loop fusion | flops 3145728 | bytes 6301696 | tf_op jit(solution)/shard_map/convert_element_type | solution.py:66
  79.7 18.3 %all-to-all-done.1 = bf16[4,16,32,768]{3,2,1,0:T(8,128)(2,1)} async-done(((bf16[4,16,32,768]{3,2,1,0:T(8,128)(2,1)}), bf16[4,16,32,768]{3,2,1,0:T(8,128)(2,1)}, u32[]{:S(2)}, u32[]{:S(2)}) %all-to-all-start.1) | async-done | bytes 3145760 | tf_op jit(solution)/shard_map/all_to_all | solution.py:22
  98.0 2.2 copy.52
  100.2 1.0 slice.115
  101.3 0.9 copy-done.2
  102.2 2.6 %fusion.49 = (f32[512]{0:T(512)S(1)}, f32[512]{0:T(512)S(1)}, f32[512,256]{1,0:T(8,128)}) fusion(bf16[512,2048]{0,1:T(8,128)(2,1)S(1)} %copy-done.2, bf16[2048,768]{1,0:T(8,128)(2,1)S(1)} %bitcast.121), kind=kOutput, calls=%fused_computation.120 | convolution fusion | flops 545651712 | bytes 3674112 | tf_op jit(solution)/shard_map/dot_general | solution.py:47
  104.9 0.6 broadcast_in_dim.89
  105.5 10.5 %all-to-all-start.2 = ((f32[8,1,1024]{2,1,0:T(1,128)}), f32[8,1,1024]{2,1,0:T(1,128)S(1)}, u32[]{:S(2)}, u32[]{:S(2)}) async-start(f32[8,1,1024]{2,1,0:T(1,128)} %broadcast_in_dim.89), calls=%async_computation.2 | async-start | bytes 65536 | tf_op jit(solution)/shard_map/all_to_all | solution.py:22
  116.0 2.4 %broadcast_select_fusion.3 = (bf16[4,1,256,256]{3,2,1,0:T(8,128)(2,1)}, bf16[4,1,256,256]{3,2,1,0:T(8,128)(2,1)}) fusion(pred[]{:T(512)S(6)} %eq.2, bf16[4,2,256,256]{3,2,1,0:T(8,128)(2,1)} %bitcast.123), kind=kLoop, calls=%fused_computation.79 | loop fusion | flops 524288 | bytes 2097153 | tf_op jit(solution)/shard_map/jit(_where)/select_n | solution.py:82
  118.4 2.4 %all-to-all-done.2 = f32[8,1,1024]{2,1,0:T(1,128)S(1)} async-done(((f32[8,1,1024]{2,1,0:T(1,128)}), f32[8,1,1024]{2,1,0:T(1,128)S(1)}, u32[]{:S(2)}, u32[]{:S(2)}) %all-to-all-start.2) | async-done | bytes 32800 | tf_op jit(solution)/shard_map/all_to_all | solution.py:22
  120.8 2.0 add_convert_fusion.4
  122.8 1.7 reshape.216
  124.5 2.0 fusion.14
  126.6 2.0 copy.57
  128.6 3.5 %fusion.22 = bf16[512,256]{1,0:T(8,128)(2,1)S(1)} fusion(f32[64,8,2,128]{3,2,1,0:T(2,128)} %bitcast.137, bf16[512,2048]{0,1:T(8,128)(2,1)} %fusion.3, bf16[2048,768]{1,0:T(8,128)(2,1)S(1)} %bitcast.122), kind=kOutput, calls=%fused_computation.45 | convolution fusion | flops 545521664 | bytes 3932160 | tf_op jit(solution)/shard_map/dot_general | solution.py:47
  132.1 0.5 convolution_convert_fusion
  132.6 2.6 %collective-permute-start.4 = (bf16[512,1024]{1,0:T(8,128)(2,1)S(1)}, bf16[512,1024]{1,0:T(8,128)(2,1)S(1)}, u32[]{:S(2)}, u32[]{:S(2)}) collective-permute-start(bf16[512,1024]{1,0:T(8,128)(2,1)S(1)} %convolution_convert_fusion), channel_id=1, source_target_pairs={{0,1},{1,0},{2,3},{3,2},{4,5},{5,4},{6,7},{7,6},{8,9},{9,8},{10,11... | collective-permute-start | bytes 3145736 | tf_op jit(solution)/shard_map/ppermute | solution.py:26
  135.2 2.3 collective-permute-done.4
  137.5 0.5 add_convert_fusion.1
  138.1 17.2 %all_to_all.31 = bf16[4,512,256]{2,1,0:T(8,128)(2,1)S(1)} all-to-all(bf16[4,512,256]{2,1,0:T(8,128)(2,1)S(1)} %bitcast.124), channel_id=1, replica_groups=mesh['z'=16,'y'=4,'x'=4,'c'=2] {'x'}, dimensions={0} | all-to-all | bytes 2097152 | tf_op jit(solution)/shard_map/all_to_all | solution.py:92
  155.3 0.1 convert_reduce_fusion.1
  155.6 16.4 %all_to_all.32 = bf16[4,512,256]{2,1,0:T(8,128)(2,1)S(1)} all-to-all(bf16[4,512,256]{2,1,0:T(8,128)(2,1)S(1)} %broadcast_in_dim.92), channel_id=1, replica_groups=mesh['z'=16,'y'=4,'x'=4,'c'=2] {'x'}, dimensions={0} | all-to-all | bytes 2097152 | tf_op jit(solution)/shard_map/all_to_all | solution.py:22
  172.0 4.2 %collective-permute-start.5 = (bf16[4,512,256]{2,1,0:T(8,128)(2,1)S(1)}, bf16[4,512,256]{2,1,0:T(8,128)(2,1)S(1)}, u32[]{:S(2)}, u32[]{:S(2)}) collective-permute-start(bf16[4,512,256]{2,1,0:T(8,128)(2,1)S(1)} %all_to_all.32), channel_id=1, source_target_pairs={{0,1},{1,0},{2,3},{3,2},{4,5},{5,4},{6,7},{7,6},{8,9},{9,8},{10,11... | collective-permute-start | bytes 3145736 | tf_op jit(solution)/shard_map/ppermute | solution.py:26
  176.2 2.0 collective-permute-done.5
  178.2 0.1 select_bitcast_fusion.3
  178.4 2.3 %maximum_convert_fusion = f32[4,2,512,256]{3,2,1,0:T(8,128)} fusion(bf16[4,1,512,256]{3,2,1,0:T(8,128)(2,1)S(1)} %get-tuple-element.16, bf16[4,1,512,256]{3,2,1,0:T(8,128)(2,1)S(1)} %get-tuple-element.15), kind=kLoop, calls=%fused_computation.14 | loop fusion | flops 2097152 | bytes 6291456 | tf_op jit(solution)/shard_map/convert_element_type | solution.py:64
  180.7 5.3 %copy.60 = f32[512,8,256]{0,2,1:T(8,128)} copy(f32[512,8,256]{2,0,1:T(8,128)} %bitcast.118) | data formatting | bytes 8388608 | tf_op jit(solution)/shard_map/convert_element_type | solution.py:64
  186.1 0.5 multiply_reduce_fusion
  186.6 2.6 %fusion.1 = bf16[512,2048]{0,1:T(8,128)(2,1)S(1)} fusion(f32[512,8,256]{0,2,1:T(8,128)} %copy.60, f32[2048]{0:T(1024)S(1)} %bitcast.140, f32[512]{0:T(512)S(1)} %add_rsqrt_fusion), kind=kLoop, calls=%fused_computation.2 | loop fusion | flops 3145728 | bytes 6301696 | tf_op jit(solution)/shard_map/convert_element_type | solution.py:66
  189.2 1.6 slice-done
  190.8 0.1 broadcast_select_fusion.1
  191.0 1.7 copy-done
  192.7 1.3 fusion.8
  193.9 1.3 fusion.11
  195.2 0.9 multiply_convert_fusion
  196.1 0.8 convolution_convert_fusion.2
  196.9 2.3 %collective-permute-start.9 = (bf16[512,1024]{1,0:T(8,128)(2,1)S(1)}, bf16[512,1024]{1,0:T(8,128)(2,1)S(1)}, u32[]{:S(2)}, u32[]{:S(2)}) collective-permute-start(bf16[512,1024]{1,0:T(8,128)(2,1)S(1)} %convolution_convert_fusion.2), channel_id=1, source_target_pairs={{0,1},{1,0},{2,3},{3,2},{4,5},{5,4},{6,7},{7,6},{8,9},{9,8},{10,11... | collective-permute-start | bytes 3145736 | tf_op jit(solution)/shard_map/ppermute | solution.py:26
  199.2 2.3 collective-permute-done.9
  201.5 0.8 add_convert_fusion
  202.3 17.2 %all_to_all.33 = bf16[4,512,256]{2,1,0:T(8,128)(2,1)S(1)} all-to-all(bf16[4,512,256]{2,1,0:T(8,128)(2,1)S(1)} %bitcast.125), channel_id=1, replica_groups=mesh['z'=16,'y'=4,'x'=4,'c'=2] {'x'}, dimensions={0} | all-to-all | bytes 2097152 | tf_op jit(solution)/shard_map/all_to_all | solution.py:92
  219.5 0.1 convert_reduce_fusion
  219.7 0.8 add_convert_fusion.2
  (71 shorter events, 0.9 us)
Async XLA Ops:
  6.5 17.6 %copy-start.12 = (bf16[256]{0:T(256)(128)(2,1)S(1)}, bf16[256]{0:T(256)(128)(2,1)}, u32[]{:S(2)}) copy-start(bf16[256]{0:T(256)(128)(2,1)} %param.16) | copy-start | bytes 1540
  6.5 17.6 %copy-start.13 = (bf16[256]{0:T(256)(128)(2,1)S(1)}, bf16[256]{0:T(256)(128)(2,1)}, u32[]{:S(2)}) copy-start(bf16[256]{0:T(256)(128)(2,1)} %param.24) | copy-start | bytes 1540
  6.5 17.6 %copy-start.1 = (bf16[512,256]{1,0:T(8,128)(2,1)S(1)}, bf16[512,256]{1,0:T(8,128)(2,1)}, u32[]{:S(2)}) copy-start(bf16[512,256]{1,0:T(8,128)(2,1)} %param.15) | copy-start | bytes 786436
  6.5 28.3 %copy-start.6 = (bf16[512,32]{0,1:T(8,128)(2,1)S(1)}, bf16[512,32]{0,1:T(8,128)(2,1)}, u32[]{:S(2)}) copy-start(bf16[512,32]{0,1:T(8,128)(2,1)} %param.29) | copy-start | bytes 98308
  6.5 28.3 %copy-start.8 = (bf16[32,512]{1,0:T(8,128)(2,1)S(1)}, bf16[32,512]{1,0:T(8,128)(2,1)}, u32[]{:S(2)}) copy-start(bf16[32,512]{1,0:T(8,128)(2,1)} %param.25) | copy-start | bytes 98308
  6.5 28.3 %copy-start.7 = (bf16[32,512]{1,0:T(8,128)(2,1)S(1)}, bf16[32,512]{1,0:T(8,128)(2,1)}, u32[]{:S(2)}) copy-start(bf16[32,512]{1,0:T(8,128)(2,1)} %param.26) | copy-start | bytes 98308
  8.3 50.4 %all-to-all-start = ((bf16[16,32,768]{2,1,0:T(8,128)(2,1)}), bf16[16,32,768]{2,1,0:T(8,128)(2,1)S(1)}, u32[]{:S(2)}, u32[]{:S(2)}) async-start(bf16[16,32,768]{2,1,0:T(8,128)(2,1)} %broadcast_in_dim.86), calls=%async_computation | async-start | bytes 1572864 | tf_op jit(solution)/shard_map/all_to_all | solution.py:22
  24.1 165.2 %all-gather.2.cloned.1.call-start = ((), (), s32[]{:S(2)}) async-start(), calls=%async_computation.6 | async-start | bytes 6684672 | tf_op jit(solution)/shard_map/all_gather | solution.py:121
  24.9 22.3 %collective-permute-start = (bf16[528,256]{1,0:T(8,128)(2,1)}, bf16[528,256]{1,0:T(8,128)(2,1)S(1)}, u32[]{:S(2)}, u32[]{:S(2)}) collective-permute-start(bf16[528,256]{1,0:T(8,128)(2,1)} %pad_maximum_fusion.1), channel_id=1, source_target_pairs={{0,2},{2,4},{4,6},{6,0},{1,3},{3,5},{5,7},{7,1},{8,10},{10,12},{12... | collective-permute-start | bytes 811016 | tf_op jit(solution)/shard_map/ppermute | solution.py:38
  28.0 19.2 %collective-permute-start.1 = (bf16[528,256]{1,0:T(8,128)(2,1)}, bf16[528,256]{1,0:T(8,128)(2,1)S(1)}, u32[]{:S(2)}, u32[]{:S(2)}) collective-permute-start(bf16[528,256]{1,0:T(8,128)(2,1)} %pad_maximum_fusion.1), channel_id=1, source_target_pairs={{0,6},{2,0},{4,2},{6,4},{1,7},{3,1},{5,3},{7,5},{8,14},{10,8},{12,... | collective-permute-start | bytes 811016 | tf_op jit(solution)/shard_map/ppermute | solution.py:38
  31.4 15.9 %collective-permute-start.2 = (bf16[528,256]{1,0:T(8,128)(2,1)}, bf16[528,256]{1,0:T(8,128)(2,1)S(1)}, u32[]{:S(2)}, u32[]{:S(2)}) collective-permute-start(bf16[528,256]{1,0:T(8,128)(2,1)} %pad_maximum_fusion.1), channel_id=1, source_target_pairs={{0,4},{2,6},{4,0},{6,2},{1,5},{3,7},{5,1},{7,3},{8,12},{10,14},{12... | collective-permute-start | bytes 811016 | tf_op jit(solution)/shard_map/ppermute | solution.py:38
  34.9 6.9 %collective-permute-start.6 = (bf16[32,1536]{1,0:T(8,128)(2,1)S(1)}, bf16[32,1536]{1,0:T(8,128)(2,1)}, u32[]{:S(2)}, u32[]{:S(2)}) collective-permute-start(bf16[32,1536]{1,0:T(8,128)(2,1)S(1)} %pad_maximum_fusion.2), channel_id=1, source_target_pairs={{0,8},{8,16},{16,24},{24,0},{1,9},{9,17},{17,25},{25,1},{2,10},{10... | collective-permute-start | bytes 294920 | tf_op jit(solution)/shard_map/ppermute | solution.py:38
  38.1 8.2 %collective-permute-start.7 = (bf16[32,1536]{1,0:T(8,128)(2,1)S(1)}, bf16[32,1536]{1,0:T(8,128)(2,1)}, u32[]{:S(2)}, u32[]{:S(2)}) collective-permute-start(bf16[32,1536]{1,0:T(8,128)(2,1)S(1)} %pad_maximum_fusion.2), channel_id=1, source_target_pairs={{0,24},{8,0},{16,8},{24,16},{1,25},{9,1},{17,9},{25,17},{2,26},{10... | collective-permute-start | bytes 294920 | tf_op jit(solution)/shard_map/ppermute | solution.py:38
  41.5 17.2 %copy-start.14 = (bf16[256]{0:T(256)(128)(2,1)S(1)}, bf16[256]{0:T(256)(128)(2,1)}, u32[]{:S(2)}) copy-start(bf16[256]{0:T(256)(128)(2,1)} %param.19) | copy-start | bytes 1540
  41.6 17.2 %copy-start.15 = (bf16[256]{0:T(256)(128)(2,1)S(1)}, bf16[256]{0:T(256)(128)(2,1)}, u32[]{:S(2)}) copy-start(bf16[256]{0:T(256)(128)(2,1)} %param.20) | copy-start | bytes 1540
  41.8 10.4 %collective-permute-start.8 = (bf16[32,1536]{1,0:T(8,128)(2,1)S(1)}, bf16[32,1536]{1,0:T(8,128)(2,1)S(1)}, u32[]{:S(2)}, u32[]{:S(2)}) collective-permute-start(bf16[32,1536]{1,0:T(8,128)(2,1)S(1)} %pad_maximum_fusion.2), channel_id=1, source_target_pairs={{0,16},{8,24},{16,0},{24,8},{1,17},{9,25},{17,1},{25,9},{2,18},{10... | collective-permute-start | bytes 294920 | tf_op jit(solution)/shard_map/ppermute | solution.py:38
  47.3 18.4 %collective-permute-start.3 = (bf16[4,528,256]{2,1,0:T(8,128)(2,1)S(1)}, bf16[4,528,256]{2,1,0:T(8,128)(2,1)}, u32[]{:S(2)}, u32[]{:S(2)}) collective-permute-start(bf16[4,528,256]{2,1,0:T(8,128)(2,1)S(1)} %bitcast_dynamic-update-slice_fusion), channel_id=1, source_target_pairs={{0,1},{1,0},{2,3},{3,2},{4,5},{5,4},{6,7},{7,6},{8,9},{9,8},{10,11... | collective-permute-start | bytes 3244040 | tf_op jit(solution)/shard_map/ppermute | solution.py:26
  52.3 6.4 %copy-start.5 = (bf16[4,32,1536]{2,1,0:T(8,128)(2,1)}, bf16[4,32,1536]{2,1,0:T(8,128)(2,1)S(1)}, u32[]{:S(2)}) copy-start(bf16[4,32,1536]{2,1,0:T(8,128)(2,1)S(1)} %bitcast_dynamic-update-slice_fusion.4) | copy-start | bytes 1179652
  60.9 4.8 %copy-start.16 = (bf16[2,128]{1,0:T(2,128)(2,1)S(1)}, bf16[2,128]{1,0:T(2,128)(2,1)}, u32[]{:S(2)}) copy-start(bf16[2,128]{1,0:T(2,128)(2,1)} %param.22) | copy-start | bytes 1540
  60.9 37.1 %all-to-all-start.1 = ((bf16[4,16,32,768]{3,2,1,0:T(8,128)(2,1)}), bf16[4,16,32,768]{3,2,1,0:T(8,128)(2,1)}, u32[]{:S(2)}, u32[]{:S(2)}) async-start(bf16[4,16,32,768]{3,2,1,0:T(8,128)(2,1)} %broadcast_in_dim.87), calls=%async_computation.1 | async-start | bytes 6291456 | tf_op jit(solution)/shard_map/all_to_all | solution.py:22
  100.2 2.0 copy-start.2
  104.8 19.7 %copy-start.9 = (bf16[2,128,128]{2,1,0:T(8,128)(2,1)S(1)}, bf16[2,128,128]{2,1,0:T(8,128)(2,1)}, u32[]{:S(2)}) copy-start(bf16[2,128,128]{2,1,0:T(8,128)(2,1)} %param.21) | copy-start | bytes 196612
  105.5 15.3 %all-to-all-start.2 = ((f32[8,1,1024]{2,1,0:T(1,128)}), f32[8,1,1024]{2,1,0:T(1,128)S(1)}, u32[]{:S(2)}, u32[]{:S(2)}) async-start(f32[8,1,1024]{2,1,0:T(1,128)} %broadcast_in_dim.89), calls=%async_computation.2 | async-start | bytes 65536 | tf_op jit(solution)/shard_map/all_to_all | solution.py:22
  128.6 3.5 %copy-start.3 = (bf16[4,1,256,256]{3,2,1,0:T(8,128)(2,1)S(1)}, bf16[4,1,256,256]{3,2,1,0:T(8,128)(2,1)}, u32[]{:S(2)}) copy-start(bf16[4,1,256,256]{3,2,1,0:T(8,128)(2,1)} %get-tuple-element.18) | copy-start | bytes 1572868
  132.1 5.4 %copy-start.4 = (bf16[4,1,256,256]{3,2,1,0:T(8,128)(2,1)S(1)}, bf16[4,1,256,256]{3,2,1,0:T(8,128)(2,1)}, u32[]{:S(2)}) copy-start(bf16[4,1,256,256]{3,2,1,0:T(8,128)(2,1)} %get-tuple-element.17) | copy-start | bytes 1572868
  132.6 4.9 %collective-permute-start.4 = (bf16[512,1024]{1,0:T(8,128)(2,1)S(1)}, bf16[512,1024]{1,0:T(8,128)(2,1)S(1)}, u32[]{:S(2)}, u32[]{:S(2)}) collective-permute-start(bf16[512,1024]{1,0:T(8,128)(2,1)S(1)} %convolution_convert_fusion), channel_id=1, source_target_pairs={{0,1},{1,0},{2,3},{3,2},{4,5},{5,4},{6,7},{7,6},{8,9},{9,8},{10,11... | collective-permute-start | bytes 3145736 | tf_op jit(solution)/shard_map/ppermute | solution.py:26
  155.4 20.7 %copy-start.10 = (bf16[3,512]{1,0:T(4,128)(2,1)S(1)}, bf16[3,512]{1,0:T(4,128)(2,1)}, u32[]{:S(2)}) copy-start(bf16[3,512]{1,0:T(4,128)(2,1)} %param.27) | copy-start | bytes 9220
  155.5 20.7 %copy-start.11 = (bf16[3,512]{1,0:T(4,128)(2,1)S(1)}, bf16[3,512]{1,0:T(4,128)(2,1)}, u32[]{:S(2)}) copy-start(bf16[3,512]{1,0:T(4,128)(2,1)} %param.28) | copy-start | bytes 9220
  172.0 6.3 %collective-permute-start.5 = (bf16[4,512,256]{2,1,0:T(8,128)(2,1)S(1)}, bf16[4,512,256]{2,1,0:T(8,128)(2,1)S(1)}, u32[]{:S(2)}, u32[]{:S(2)}) collective-permute-start(bf16[4,512,256]{2,1,0:T(8,128)(2,1)S(1)} %all_to_all.32), channel_id=1, source_target_pairs={{0,1},{1,0},{2,3},{3,2},{4,5},{5,4},{6,7},{7,6},{8,9},{9,8},{10,11... | collective-permute-start | bytes 3145736 | tf_op jit(solution)/shard_map/ppermute | solution.py:26
  189.2 1.6 slice-start
  189.2 3.4 %copy-start = (bf16[2048,1536]{1,0:T(8,128)(2,1)S(1)}, bf16[2048,1536]{1,0:T(8,128)(2,1)}, u32[]{:S(2)}) copy-start(bf16[2048,1536]{1,0:T(8,128)(2,1)} %all-gather.2.cloned.1.call-done) | copy-start | bytes 18874372
  196.9 4.6 %collective-permute-start.9 = (bf16[512,1024]{1,0:T(8,128)(2,1)S(1)}, bf16[512,1024]{1,0:T(8,128)(2,1)S(1)}, u32[]{:S(2)}, u32[]{:S(2)}) collective-permute-start(bf16[512,1024]{1,0:T(8,128)(2,1)S(1)} %convolution_convert_fusion.2), channel_id=1, source_target_pairs={{0,1},{1,0},{2,3},{3,2},{4,5},{5,4},{6,7},{7,6},{8,9},{9,8},{10,11... | collective-permute-start | bytes 3145736 | tf_op jit(solution)/shard_map/ppermute | solution.py:26
Sparse Core Ops, SparseCore 0:
  58.9 84.5 all-gather.1
where the time goes:
time: 229 us; the launch traced here: 227 us
  starting transfers between devices  65.1 us (28%)
  blocking collectives  50.9 us (22%)
  waiting for transfers between devices  33.9 us (15%)
  local copies, waits for them, and re-layouts  27.8 us (12%)
  other arithmetic  22.4 us (10%)
  between operations  14 us (6%)
  matrix products  13.1 us (6%)
    all_to_all x2, blocking collectives, product_at_owner(): lax.all_to_all(parts, 'x', split_axis=0, concat_axis=0, tiled=True)  34.5 us
    all_to_all x3, starting transfers between devices, everyones(): return lax.all_to_all(copies, axis, split_axis=0, concat_axis=0, tiled=True)  31 us
    all_to_all x3, waiting for transfers between devices, everyones(): return lax.all_to_all(copies, axis, split_axis=0, concat_axis=0, tiled=True)  27.1 us
    ppermute x6, starting transfers between devices, by_permutes(): lax.ppermute(shard, axis, [(i, (i + step) % size) for i in range(size)])  20 us
    all_to_all x1, blocking collectives, everyones(): return lax.all_to_all(copies, axis, split_axis=0, concat_axis=0, tiled=True)  16.4 us
    ppermute x4, starting transfers between devices, other_core(): return lax.ppermute(value, 'c', SWAP)  14 us
    convert_element_type x2, local copies, waits for them, and re-layouts, rms(): v = values.astype(F32)  10.7 us
    dot_general x4, matrix products, matmul(): return jnp.dot(operand, matrix, preferred_element_type=F32)  8.68 us
  transfers between devices with their start and end apart: 14, of which 7 were waited for; matrix products, arithmetic and copies ran while one was open for 23% of the time, Pallas kernels for 0%

commit v1 on v0

v1 whole, which is shorter than its diff:
```python
import jax
import jax.numpy as jnp
from jax import lax
from jax.experimental import pallas as pl
from jax.experimental.pallas import tpu as pltpu
from jax.sharding import Mesh
from jax.sharding import PartitionSpec as P

GROUP_DIM = 128
BLOCK = 128
SEGMENT = 64
SEQ_LEN = 256
FS = ("z", "y")
TP = ("x", "c")
EPS = 1e-06
F32 = jnp.float32
BF16 = jnp.bfloat16
SWAP = [(0, 1), (1, 0)]
SQRT_HALF = 0.7071067811865476
VMEM = pl.BlockSpec(memory_space=pltpu.VMEM)
SMEM = pl.BlockSpec(memory_space=pltpu.SMEM)


def everyones(shard, axis):
    copies = jnp.broadcast_to(shard, (lax.axis_size(axis), *shard.shape))
    return lax.all_to_all(copies, axis, split_axis=0, concat_axis=0, tiled=True)


def other_core(value):
    return lax.ppermute(value, "c", SWAP)


def after(value, *first):
    return lax.optimization_barrier((value, *first))[0]


def by_permutes(shard, axis):
    size = lax.axis_size(axis)
    here = lax.axis_index(axis).astype(jnp.uint32)
    parts = [shard]
    for step in (1, 3, 2):
        parts.append(lax.ppermute(shard, axis, [(i, (i + step) % size) for i in range(size)]))
    filled = jnp.zeros((size, *shard.shape), shard.dtype)
    for step, part in zip((0, 1, 3, 2), parts):
        origin = (here + jnp.uint32(size - step)) & jnp.uint32(size - 1)
        filled = lax.dynamic_update_slice(filled, part[None], (origin, *([jnp.uint32(0)] * shard.ndim)))
    return filled


def rms(values, gain):
    v = values.astype(F32)
    scale = lax.rsqrt(jnp.mean(v * v, axis=1, keepdims=True) + EPS)
    return (v * scale * gain.astype(F32)).astype(BF16)


def stats_kernel(normed, early, act, sums, weight):
    near = early.shape[0]
    piece = 32
    width = act.shape[1]
    for far in range(early.shape[1] // piece):
        for y in range(near):
            weight[pl.ds((far * near + y) * piece, piece), :] = early[y, pl.ds(far * piece, piece), width : 2 * width]
    for part in range(normed.shape[0] // SEQ_LEN):
        rows = pl.ds(part * SEQ_LEN, SEQ_LEN)
        value = gelu(jnp.dot(normed[rows, :], weight[...], preferred_element_type=F32))
        act[rows, :] = value
        once = sum(value[:, k : k + 128] for k in range(0, width, 128))
        twice = sum(value[:, k : k + 128] * value[:, k : k + 128] for k in range(0, width, 128))
        sums[0:1, rows] = jnp.sum(once.T, axis=0, keepdims=True)
        sums[1:2, rows] = jnp.sum(twice.T, axis=0, keepdims=True)


def gate_kernel(normed, early, act, weight):
    near = early.shape[0]
    piece = 32
    width = act.shape[1]
    for far in range(early.shape[1] // piece):
        for y in range(near):
            weight[pl.ds((far * near + y) * piece, piece), :] = early[y, pl.ds(far * piece, piece), 0:width]
    for part in range(normed.shape[0] // SEQ_LEN):
        rows = pl.ds(part * SEQ_LEN, SEQ_LEN)
        act[rows, :] = gelu(jnp.dot(normed[rows, :], weight[...], preferred_element_type=F32))


def mix_kernel(core, act_v, act_u, stats, gain, shift, mix, bias, early, give, keep, weight, gated):
    near = early.shape[0]
    piece = 32
    width = act_v.shape[1]
    for far in range(early.shape[1] // piece):
        for y in range(near):
            weight[pl.ds((far * near + y) * piece, piece), :] = early[y, pl.ds(far * piece, piece), 2 * width : 3 * width]
    full = width * stats.shape[0]
    i = lax.broadcasted_iota(jnp.int32, (BLOCK, BLOCK), 0)
    j = lax.broadcasted_iota(jnp.int32, (BLOCK, BLOCK), 1)
    visible = (i >= SEGMENT) | (j < SEGMENT)
    total = stats[0]
    for k in range(1, stats.shape[0]):
        total = total + stats[k]
    center_row = total[0:1] / full
    spread_row = total[1:2] / full - center_row * center_row
    scale_row = lax.rsqrt(spread_row + EPS)
    for block in range(act_v.shape[0] // BLOCK):
        rows = pl.ds(block * BLOCK, BLOCK)
        at = slice(block * BLOCK, (block + 1) * BLOCK)
        center = jnp.broadcast_to(center_row[:, at], (BLOCK, BLOCK)).T
        scale = jnp.broadcast_to(scale_row[:, at], (BLOCK, BLOCK)).T
        for g in range(width // GROUP_DIM):
            cols = slice(g * GROUP_DIM, (g + 1) * GROUP_DIM)
            mixed = ((act_v[rows, cols] - center) * scale * gain[:, cols] + shift[:, cols]).astype(BF16)
            seen = jnp.where(visible, mix[g].astype(F32), 0.0).astype(BF16)
            spatial = jnp.dot(seen, mixed, preferred_element_type=F32) + bias[:, g : g + 1]
            gated[rows, cols] = (act_u[rows, cols] * spatial).astype(BF16)
    c = core[0]
    for out, side in ((give, 1 - c), (keep, c)):
        for x in range(out.shape[0]):
            start = pl.multiple_of((2 * x + side) * width, width)
            columns = weight[pl.ds(start, width), :]
            out[x] = lax.dot_general(
                gated[...], columns, (((1,), (1,)), ((), ())), preferred_element_type=F32
            ).astype(BF16)


def shifted(value, by):
    row = lax.broadcasted_iota(jnp.int32, value.shape, 0)
    return jnp.where(row >= by, pltpu.roll(value, by, 0), 0.0)


def taps(value, weights):
    value = value.astype(BF16).astype(F32)
    return (shifted(value, 2) * weights[0:1] + shifted(value, 1) * weights[1:2]) + value * weights[2:3]


def ffn_kernel(core, mine, other, gain, late, conv_gate, conv_value, give, keep, normed, hidden):
    width = mine.shape[2]
    ff = conv_gate.shape[1]
    c = core[0]
    for part in range(mine.shape[1] // SEQ_LEN):
        rows = pl.ds(part * SEQ_LEN, SEQ_LEN)
        squares = jnp.zeros((SEQ_LEN, 1), F32)
        for x in range(mine.shape[0]):
            for ref in (mine, other):
                value = ref[x, rows, :].astype(F32)
                squares = squares + jnp.sum(value * value, axis=1, keepdims=True)
        scale = lax.rsqrt(squares / (2 * mine.shape[0] * width) + EPS)

        def fill(ref, side):
            for x in range(mine.shape[0]):
                at = pl.ds((2 * x + side) * width, width)
                normed[:, at] = (ref[x, rows, :].astype(F32) * scale * gain[:, at]).astype(BF16)

        @pl.when(c == 0)
        def _():
            fill(mine, 0)
            fill(other, 1)

        @pl.when(c == 1)
        def _():
            fill(other, 0)
            fill(mine, 1)

        gate = jnp.dot(normed[...], late[:, 0:ff], preferred_element_type=F32)
        value = jnp.dot(normed[...], late[:, ff : 2 * ff], preferred_element_type=F32)
        conv_g = taps(gate, conv_gate[...])
        conv_v = taps(value, conv_value[...])
        hidden[rows, :] = (conv_g * jax.nn.sigmoid(conv_g) * conv_v).astype(BF16)
    for out, side in ((give, 1 - c), (keep, c)):
        for x in range(out.shape[0]):
            start = pl.multiple_of((2 * x + side) * width, width)
            columns = late[pl.ds(start, width), 2 * ff : 3 * ff]
            out[x] = lax.dot_general(
                hidden[...], columns, (((1,), (1,)), ((), ())), preferred_element_type=F32
            ).astype(BF16)


def gelu(value):
    return 0.5 * value * (1.0 + lax.erf(value * SQRT_HALF))


def shape(dims, dtype):
    return jax.ShapeDtypeStruct(dims, dtype)


def summed_at_owner(give, keep):
    pair = (keep.astype(F32) + other_core(give).astype(F32)).astype(BF16)
    arrived = lax.all_to_all(pair, "x", split_axis=0, concat_axis=0, tiled=True)
    return arrived.astype(F32).sum(axis=0)


def on_device(
    tokens,
    norm_gain,
    proj_u,
    proj_v,
    layer_gain,
    layer_shift,
    mix_weight,
    mix_bias,
    proj_out,
    ffn_gain,
    ffn_gate,
    ffn_value,
    conv_gate,
    conv_value,
    proj_down,
):
    da = proj_u.shape[1]
    ff = ffn_gate.shape[1]
    row_count = tokens.shape[0]

    early = jnp.concatenate([proj_u, proj_v, proj_out.T], axis=1)
    early_z = everyones(early, "z")
    late = jnp.concatenate([ffn_gate, ffn_value, proj_down.T], axis=1)
    late_y = by_permutes(late, "y").reshape(-1, late.shape[1])
    late_all = lax.all_gather(after(late_y, early_z), "z", axis=0, tiled=True)

    packed = jnp.concatenate([tokens, jnp.broadcast_to(norm_gain, (8, da)), jnp.broadcast_to(ffn_gain, (8, da))], axis=0)
    mine = by_permutes(packed, "x")
    other = other_core(mine)
    first = lax.axis_index("c") == 0
    both = jnp.stack([jnp.where(first, mine, other), jnp.where(first, other, mine)], axis=1)
    whole = both.reshape(-1, *packed.shape).transpose(1, 0, 2).reshape(packed.shape[0], -1)
    normed = rms(whole[:row_count], whole[row_count])
    gain_two = whole[row_count + 8]
    early_all = everyones(early_z, "y").reshape(4, -1, early.shape[1])
    core = lax.axis_index("c").astype(jnp.int32).reshape(1)
    model = proj_u.shape[0] * lax.axis_size(FS)

    act_v, sums = pl.pallas_call(
        stats_kernel,
        in_specs=[VMEM] * 2,
        out_specs=[VMEM] * 2,
        out_shape=[shape((row_count, da), F32), shape((2, row_count), F32)],
        scratch_shapes=[pltpu.VMEM((model, da), BF16)],
        name="stats",
    )(normed, early_all)
    stats = everyones(sums, TP)
    act_u = pl.pallas_call(
        gate_kernel,
        in_specs=[VMEM] * 2,
        out_specs=VMEM,
        out_shape=shape((row_count, da), F32),
        scratch_shapes=[pltpu.VMEM((model, da), BF16)],
        name="gate",
    )(normed, early_all)
    blocks = [shape((lax.axis_size("x"), row_count, da), BF16)] * 2
    give, keep = pl.pallas_call(
        mix_kernel,
        in_specs=[SMEM] + [VMEM] * 8,
        out_specs=[VMEM] * 2,
        out_shape=blocks,
        scratch_shapes=[pltpu.VMEM((model, da), BF16), pltpu.VMEM((row_count, da), BF16)],
        name="mix",
    )(
        core,
        act_v,
        act_u,
        stats,
        layer_gain.astype(F32)[None],
        layer_shift.astype(F32)[None],
        mix_weight,
        mix_bias.astype(F32).T,
        early_all,
    )
    stream = (tokens.astype(F32) + summed_at_owner(give, keep)).astype(BF16)
    mine = everyones(stream, "x")
    give, keep = pl.pallas_call(
        ffn_kernel,
        in_specs=[SMEM] + [VMEM] * 6,
        out_specs=[VMEM] * 2,
        out_shape=blocks,
        scratch_shapes=[pltpu.VMEM((SEQ_LEN, model), BF16), pltpu.VMEM((row_count, ff), BF16)],
        name="ffn",
    )(
        core,
        mine,
        other_core(mine),
        gain_two.astype(F32)[None],
        late_all,
        conv_gate.astype(F32),
        conv_value.astype(F32),
    )
    return (stream.astype(F32) + summed_at_owner(give, keep)).astype(BF16)


def solution(mesh):
    split = Mesh(mesh.devices.reshape(16, 4, 4, 2), ("z", "y", "x", "c"))
    placed = (
        P(FS, TP),
        P(TP),
        P(FS, TP),
        P(FS, TP),
        P(TP),
        P(TP),
        P(TP, None, None),
        P(TP, None),
        P(TP, FS),
        P(TP),
        P(FS, TP),
        P(FS, TP),
        P(None, TP),
        P(None, TP),
        P(TP, FS),
    )

    return jax.shard_map(on_device, mesh=split, in_specs=placed, out_specs=P(FS, TP), check_vma=False)
```

time: 229 us -> 240 us (1.048)
  waiting for transfers between devices: 33.9 us -> 66.8 us
  Pallas kernels: 0 us -> 22.2 us
  local copies, waits for them, and re-layouts: 27.8 us -> 12.6 us
  matrix products: 13.1 us -> 0 us
  other arithmetic: 22.4 us -> 13.1 us
  starting transfers between devices: 65.1 us -> 59.4 us
    all_to_all x3, waiting for transfers between devices: 27.1 us -> 52.8 us  [everyones(): return lax.all_to_all(copies, axis, split_axis=0, concat_axis=0, tiled=True)]
    pallas_call x0 -> x4, Pallas kernels: none -> 22.2 us  [the longest x1 9.56 us: on_device(): pl.pallas_call(ffn_kernel, in_specs=[SMEM] + [VMEM] * 6, out_specs=[VMEM]...]
    dot_general x9 -> x0, matrix products: 13.1 us -> none  [the longest x4 8.68 us: matmul(): return jnp.dot(operand, matrix, preferred_element_type=F32)]
    convert_element_type x2 -> x1, local copies, waits for them, and re-layouts: 10.7 us -> 0.6 us  [rms(): v = values.astype(F32)]
    ppermute x6, waiting for transfers between devices: 0.16 us -> 8.37 us  [by_permutes(): lax.ppermute(shard, axis, [(i, (i + step) % size) for i in range(size)])]
    all_to_all x3, starting transfers between devices: 31 us -> 24.3 us  [everyones(): return lax.all_to_all(copies, axis, split_axis=0, concat_axis=0, tiled=True)]
    convert_element_type x3 -> x1, other arithmetic: 6.73 us -> 1.72 us  [rms(): return (v * scale * gain.astype(F32)).astype(BF16)]
    convert_element_type x10 -> x7, other arithmetic: 8.5 us -> 5.64 us  [the longest x2 3.02 us: summed_at_owner(): pair = (keep.astype(F32) + other_core(give).astype(F32)).astype(BF16)]
  transfers between devices with their start and end apart: 14 -> 14, of which waited for: 7 -> 7; matrix products, arithmetic and copies ran while one was open for 23% -> 8% of each run, Pallas kernels for 0% -> 5%
where the time goes in v1:
time: 240 us; the launch traced here: 239 us
  waiting for transfers between devices  66.8 us (28%)
  starting transfers between devices  59.4 us (25%)
  blocking collectives  51.3 us (21%)
  Pallas kernels  22.2 us (9%)
  between operations  13.8 us (6%)
  other arithmetic  13.1 us (5%)
  local copies, waits for them, and re-layouts  12.6 us (5%)
    all_to_all x3, waiting for transfers between devices, everyones(): return lax.all_to_all(copies, axis, split_axis=0, concat_axis=0, tiled=True)  52.8 us
    all_to_all x2, blocking collectives, summed_at_owner(): arrived = lax.all_to_all(pair, 'x', split_axis=0, concat_axis=0, tiled=True)  35.5 us
    all_to_all x3, starting transfers between devices, everyones(): return lax.all_to_all(copies, axis, split_axis=0, concat_axis=0, tiled=True)  24.3 us
    ppermute x6, starting transfers between devices, by_permutes(): lax.ppermute(shard, axis, [(i, (i + step) % size) for i in range(size)])  20 us
    all_to_all x1, blocking collectives, everyones(): return lax.all_to_all(copies, axis, split_axis=0, concat_axis=0, tiled=True)  15.8 us
    ppermute x4, starting transfers between devices, other_core(): return lax.ppermute(value, 'c', SWAP)  15 us
    pallas_call x1, Pallas kernels, on_device(): pl.pallas_call(ffn_kernel, in_specs=[SMEM] + [VMEM] * 6, out_specs=[VMEM]...  9.56 us
    ppermute x6, waiting for transfers between devices, by_permutes(): lax.ppermute(shard, axis, [(i, (i + step) % size) for i in range(size)])  8.37 us
  transfers between devices with their start and end apart: 14, of which 7 were waited for; matrix products, arithmetic and copies ran while one was open for 8% of the time, Pallas kernels for 5%

profile of v1, /device:TPU:1, one launch (start us, length us, event | category | flops | bytes accessed | tf_op | source)
XLA Modules:
  0.0 239.3 jit_solution(2357978480518314185)
XLA Ops:
  6.5 0.8 pad_maximum_fusion.3
  7.3 1.0 broadcast_in_dim.68
  8.3 15.7 %all-to-all-start = ((bf16[16,32,768]{2,1,0:T(8,128)(2,1)}), bf16[16,32,768]{2,1,0:T(8,128)(2,1)S(1)}, u32[]{:S(2)}, u32[]{:S(2)}) async-start(bf16[16,32,768]{2,1,0:T(8,128)(2,1)} %broadcast_in_dim.68), calls=%async_computation | async-start | bytes 1572864 | tf_op jit(solution)/shard_map/all_to_all | solution.py:26
  24.0 0.0 all-gather.2.cloned.1.call-start
  24.1 3.2 %collective-permute-start.6 = (bf16[32,1536]{1,0:T(8,128)(2,1)S(1)}, bf16[32,1536]{1,0:T(8,128)(2,1)S(1)}, u32[]{:S(2)}, u32[]{:S(2)}) collective-permute-start(bf16[32,1536]{1,0:T(8,128)(2,1)S(1)} %pad_maximum_fusion.2), channel_id=1, source_target_pairs={{0,8},{8,16},{16,24},{24,0},{1,9},{9,17},{17,25},{25,1},{2,10},{10... | collective-permute-start | bytes 294920 | tf_op jit(solution)/shard_map/ppermute | solution.py:42
  27.3 3.4 %collective-permute-start.7 = (bf16[32,1536]{1,0:T(8,128)(2,1)S(1)}, bf16[32,1536]{1,0:T(8,128)(2,1)S(1)}, u32[]{:S(2)}, u32[]{:S(2)}) collective-permute-start(bf16[32,1536]{1,0:T(8,128)(2,1)S(1)} %pad_maximum_fusion.2), channel_id=1, source_target_pairs={{0,24},{8,0},{16,8},{24,16},{1,25},{9,1},{17,9},{25,17},{2,26},{10... | collective-permute-start | bytes 294920 | tf_op jit(solution)/shard_map/ppermute | solution.py:42
  30.7 3.5 %collective-permute-start.8 = (bf16[32,1536]{1,0:T(8,128)(2,1)S(1)}, bf16[32,1536]{1,0:T(8,128)(2,1)S(1)}, u32[]{:S(2)}, u32[]{:S(2)}) collective-permute-start(bf16[32,1536]{1,0:T(8,128)(2,1)S(1)} %pad_maximum_fusion.2), channel_id=1, source_target_pairs={{0,16},{8,24},{16,0},{24,8},{1,17},{9,25},{17,1},{25,9},{2,18},{10... | collective-permute-start | bytes 294920 | tf_op jit(solution)/shard_map/ppermute | solution.py:42
  34.4 0.0 collective-permute-done.7
  34.4 3.5 %collective-permute-done.8 = bf16[32,1536]{1,0:T(8,128)(2,1)S(1)} collective-permute-done((bf16[32,1536]{1,0:T(8,128)(2,1)S(1)}, bf16[32,1536]{1,0:T(8,128)(2,1)S(1)}, u32[]{:S(2)}, u32[]{:S(2)}) %collective-permute-start.8) | collective-permute-done | bytes 98336 | tf_op jit(solution)/shard_map/ppermute | solution.py:42
  37.9 20.8 %all-to-all-done = bf16[16,32,768]{2,1,0:T(8,128)(2,1)S(1)} async-done(((bf16[16,32,768]{2,1,0:T(8,128)(2,1)}), bf16[16,32,768]{2,1,0:T(8,128)(2,1)S(1)}, u32[]{:S(2)}, u32[]{:S(2)}) %all-to-all-start) | async-done | bytes 786464 | tf_op jit(solution)/shard_map/all_to_all | solution.py:26
  58.7 0.0 all-gather.2.cloned.1.call-update
  58.8 3.1 %collective-permute-start = (bf16[528,256]{1,0:T(8,128)(2,1)S(1)}, bf16[528,256]{1,0:T(8,128)(2,1)S(1)}, u32[]{:S(2)}, u32[]{:S(2)}) collective-permute-start(bf16[528,256]{1,0:T(8,128)(2,1)S(1)} %pad_maximum_fusion.1), channel_id=1, source_target_pairs={{0,2},{2,4},{4,6},{6,0},{1,3},{3,5},{5,7},{7,1},{8,10},{10,12},{12... | collective-permute-start | bytes 811016 | tf_op jit(solution)/shard_map/ppermute | solution.py:42
  61.9 3.4 %collective-permute-start.1 = (bf16[528,256]{1,0:T(8,128)(2,1)S(1)}, bf16[528,256]{1,0:T(8,128)(2,1)S(1)}, u32[]{:S(2)}, u32[]{:S(2)}) collective-permute-start(bf16[528,256]{1,0:T(8,128)(2,1)S(1)} %pad_maximum_fusion.1), channel_id=1, source_target_pairs={{0,6},{2,0},{4,2},{6,4},{1,7},{3,1},{5,3},{7,5},{8,14},{10,8},{12,... | collective-permute-start | bytes 811016 | tf_op jit(solution)/shard_map/ppermute | solution.py:42
  65.3 3.4 %collective-permute-start.2 = (bf16[528,256]{1,0:T(8,128)(2,1)S(1)}, bf16[528,256]{1,0:T(8,128)(2,1)S(1)}, u32[]{:S(2)}, u32[]{:S(2)}) collective-permute-start(bf16[528,256]{1,0:T(8,128)(2,1)S(1)} %pad_maximum_fusion.1), channel_id=1, source_target_pairs={{0,4},{2,6},{4,0},{6,2},{1,5},{3,7},{5,1},{7,3},{8,12},{10,14},{12... | collective-permute-start | bytes 811016 | tf_op jit(solution)/shard_map/ppermute | solution.py:42
  68.8 1.1 broadcast_in_dim.61
  69.8 0.7 bitcast_dynamic-update-slice_fusion.3
  70.6 0.7 bitcast_dynamic-update-slice_fusion.2
  71.3 0.7 bitcast_dynamic-update-slice_fusion.1
  72.0 4.9 %collective-permute-done.2 = bf16[528,256]{1,0:T(8,128)(2,1)S(1)} collective-permute-done((bf16[528,256]{1,0:T(8,128)(2,1)S(1)}, bf16[528,256]{1,0:T(8,128)(2,1)S(1)}, u32[]{:S(2)}, u32[]{:S(2)}) %collective-permute-start.2) | collective-permute-done | bytes 270368 | tf_op jit(solution)/shard_map/ppermute | solution.py:42
  76.9 0.7 bitcast_dynamic-update-slice_fusion
  77.6 6.1 %collective-permute-start.3 = (bf16[4,528,256]{2,1,0:T(8,128)(2,1)}, bf16[4,528,256]{2,1,0:T(8,128)(2,1)}, u32[]{:S(2)}, u32[]{:S(2)}) collective-permute-start(bf16[4,528,256]{2,1,0:T(8,128)(2,1)} %bitcast_dynamic-update-slice_fusion), channel_id=1, source_target_pairs={{0,1},{1,0},{2,3},{3,2},{4,5},{5,4},{6,7},{7,6},{8,9},{9,8},{10,11... | collective-permute-start | bytes 3244040 | tf_op jit(solution)/shard_map/ppermute | solution.py:30
  83.7 2.1 broadcast_in_dim.69
  85.8 4.2 %all-to-all-start.1 = ((bf16[4,16,32,768]{3,2,1,0:T(8,128)(2,1)}), bf16[4,16,32,768]{3,2,1,0:T(8,128)(2,1)S(1)}, u32[]{:S(2)}, u32[]{:S(2)}) async-start(bf16[4,16,32,768]{3,2,1,0:T(8,128)(2,1)} %broadcast_in_dim.69), calls=%async_computation.1 | async-start | bytes 6291456 | tf_op jit(solution)/shard_map/all_to_all | solution.py:26
  90.0 1.7 select_bitcast_fusion.1
  91.7 0.2 pad_maximum_fusion
  91.9 0.1 copy.19
  92.1 0.4 convert_bitcast_fusion
  92.5 0.6 copy.22
  93.1 0.5 fusion
  93.6 1.7 multiply_convert_fusion.normed
  95.3 32.0 %all-to-all-done.1 = bf16[4,16,32,768]{3,2,1,0:T(8,128)(2,1)S(1)} async-done(((bf16[4,16,32,768]{3,2,1,0:T(8,128)(2,1)}), bf16[4,16,32,768]{3,2,1,0:T(8,128)(2,1)S(1)}, u32[]{:S(2)}, u32[]{:S(2)}) %all-to-all-start.1) | async-done | bytes 3145760 | tf_op jit(solution)/shard_map/all_to_all | solution.py:26
  127.4 1.7 copy-done
  129.1 4.2 %stats.1 = (f32[512,256]{1,0:T(8,128)}, f32[2,512]{1,0:T(2,128)}) custom-call(bf16[512,2048]{1,0:T(8,128)(2,1)} %multiply_convert_fusion.normed, bf16[4,512,768]{2,1,0:T(8,128)(2,1)} %bitcast.37), custom_call_target="tpu_custom_call" | custom-call | tf_op jit(solution)/shard_map/stats/pallas_call | solution.py:228
  133.2 1.3 broadcast_in_dim.70
  134.5 4.4 %all-to-all-start.2 = ((f32[8,2,512]{2,1,0:T(2,128)}), f32[8,2,512]{2,1,0:T(2,128)S(1)}, u32[]{:S(2)}, u32[]{:S(2)}) async-start(f32[8,2,512]{2,1,0:T(2,128)} %broadcast_in_dim.70), calls=%async_computation.2 | async-start | bytes 65536 | tf_op jit(solution)/shard_map/all_to_all | solution.py:26
  138.9 0.7 copy.21
  139.7 0.5 broadcast_in_dim.81
  140.2 0.6 broadcast_in_dim.82
  140.8 4.1 %gate.1.act_u = f32[512,256]{1,0:T(8,128)} custom-call(bf16[512,2048]{1,0:T(8,128)(2,1)} %multiply_convert_fusion.normed, bf16[4,512,768]{2,1,0:T(8,128)(2,1)} %bitcast.38), custom_call_target="tpu_custom_call" | custom-call | tf_op jit(solution)/shard_map/gate/pallas_call | solution.py:237
  144.9 0.6 copy-done.5
  145.5 4.4 %mix.2 = (bf16[4,512,256]{2,1,0:T(8,128)(2,1)}, bf16[4,512,256]{2,1,0:T(8,128)(2,1)}) custom-call(s32[1]{0:T(128)} %bitcast.core, f32[512,256]{1,0:T(8,128)} %get-tuple-element.12.act_v, f32[512,256]{1,0:T(8,128)} %gate.1.act_u, f32[8,2,512]{2,1,0:T(2,128)} %copy-done.5, f32[1,256]{1,0:T(1,128)} %bitcast.51, f32[1,256]{1,0:T(1,128)} %bitcast.52, ...), custom_call_target="tpu_custom_call" | custom-call | tf_op jit(solution)/shard_map/mix/pallas_call | solution.py:246
  149.9 2.1 collective-permute-start.4
  152.0 2.7 %collective-permute-done.4 = bf16[4,512,256]{2,1,0:T(8,128)(2,1)S(1)} collective-permute-done((bf16[4,512,256]{2,1,0:T(8,128)(2,1)}, bf16[4,512,256]{2,1,0:T(8,128)(2,1)S(1)}, u32[]{:S(2)}, u32[]{:S(2)}) %collective-permute-start.4) | collective-permute-done | bytes 1048608 | tf_op jit(solution)/shard_map/ppermute | solution.py:30
  154.7 1.5 add_convert_fusion.1
  156.2 18.2 %all_to_all.30 = bf16[4,512,256]{2,1,0:T(8,128)(2,1)S(1)} all-to-all(bf16[4,512,256]{2,1,0:T(8,128)(2,1)S(1)} %add_convert_fusion.1), channel_id=1, replica_groups=mesh['z'=16,'y'=4,'x'=4,'c'=2] {'x'}, dimensions={0} | all-to-all | bytes 2097152 | tf_op jit(solution)/shard_map/all_to_all | solution.py:185
  174.4 0.1 convert_reduce_fusion.1
  174.6 0.0 copy-start.9
  174.6 0.0 copy-start.10
  174.6 0.1 add_convert_fusion.3
  174.7 0.1 broadcast_in_dim.75
  174.7 15.8 %all_to_all.31.mine = bf16[4,512,256]{2,1,0:T(8,128)(2,1)S(1)} all-to-all(bf16[4,512,256]{2,1,0:T(8,128)(2,1)S(1)} %broadcast_in_dim.75), channel_id=1, replica_groups=mesh['z'=16,'y'=4,'x'=4,'c'=2] {'x'}, dimensions={0} | all-to-all | bytes 2097152 | tf_op jit(solution)/shard_map/all_to_all | solution.py:26
  190.5 4.6 %collective-permute-start.5 = (bf16[4,512,256]{2,1,0:T(8,128)(2,1)S(1)}, bf16[4,512,256]{2,1,0:T(8,128)(2,1)S(1)}, u32[]{:S(2)}, u32[]{:S(2)}) collective-permute-start(bf16[4,512,256]{2,1,0:T(8,128)(2,1)S(1)} %all_to_all.31.mine), channel_id=1, source_target_pairs={{0,1},{1,0},{2,3},{3,2},{4,5},{5,4},{6,7},{7,6},{8,9},{9,8},{10,11... | collective-permute-start | bytes 3145736 | tf_op jit(solution)/shard_map/ppermute | solution.py:30
  195.1 0.6 convert_element_type.103.conv_gate
  195.7 0.6 convert_element_type.104.conv_value
  196.3 0.6 convert.6.gain
  196.9 0.4 collective-permute-done.5.other
  197.4 1.1 copy-done.4
  198.4 9.6 %ffn.1 = (bf16[4,512,256]{2,1,0:T(8,128)(2,1)}, bf16[4,512,256]{2,1,0:T(8,128)(2,1)}) custom-call(s32[1]{0:T(128)} %bitcast.core, bf16[4,512,256]{2,1,0:T(8,128)(2,1)} %copy-done.1, bf16[4,512,256]{2,1,0:T(8,128)(2,1)} %copy-done.4, f32[1,2048]{1,0:T(1,128)} %convert.6.gain, bf16[2048,1536]{1,0:T(8,128)(2,1)} %all-gather.2.cloned.1.call-done.late, ...), custom_call_target="tpu_custom_call" | custom-call | tf_op jit(solution)/shard_map/ffn/pallas_call | solution.py:266
  208.0 2.3 collective-permute-start.9
  210.3 2.5 %collective-permute-done.9 = bf16[4,512,256]{2,1,0:T(8,128)(2,1)S(1)} collective-permute-done((bf16[4,512,256]{2,1,0:T(8,128)(2,1)}, bf16[4,512,256]{2,1,0:T(8,128)(2,1)S(1)}, u32[]{:S(2)}, u32[]{:S(2)}) %collective-permute-start.9) | collective-permute-done | bytes 1048608 | tf_op jit(solution)/shard_map/ppermute | solution.py:30
  212.8 1.5 add_convert_fusion
  214.3 17.2 %all_to_all.32 = bf16[4,512,256]{2,1,0:T(8,128)(2,1)S(1)} all-to-all(bf16[4,512,256]{2,1,0:T(8,128)(2,1)S(1)} %add_convert_fusion), channel_id=1, replica_groups=mesh['z'=16,'y'=4,'x'=4,'c'=2] {'x'}, dimensions={0} | all-to-all | bytes 2097152 | tf_op jit(solution)/shard_map/all_to_all | solution.py:185
  231.5 0.1 convert_reduce_fusion
  231.7 0.8 add_convert_fusion.2
  (44 shorter events, 0.2 us)
Async XLA Ops:
  6.5 17.6 %copy-start.6 = (bf16[512,32]{0,1:T(8,128)(2,1)S(1)}, bf16[512,32]{0,1:T(8,128)(2,1)}, u32[]{:S(2)}) copy-start(bf16[512,32]{0,1:T(8,128)(2,1)} %param.29) | copy-start | bytes 98308
  6.5 17.6 %copy-start.8 = (bf16[32,512]{1,0:T(8,128)(2,1)S(1)}, bf16[32,512]{1,0:T(8,128)(2,1)}, u32[]{:S(2)}) copy-start(bf16[32,512]{1,0:T(8,128)(2,1)} %param.25) | copy-start | bytes 98308
  6.5 17.6 %copy-start.7 = (bf16[32,512]{1,0:T(8,128)(2,1)S(1)}, bf16[32,512]{1,0:T(8,128)(2,1)}, u32[]{:S(2)}) copy-start(bf16[32,512]{1,0:T(8,128)(2,1)} %param.26) | copy-start | bytes 98308
  7.3 51.4 %copy-start.12 = (bf16[256]{0:T(256)(128)(2,1)S(1)}, bf16[256]{0:T(256)(128)(2,1)}, u32[]{:S(2)}) copy-start(bf16[256]{0:T(256)(128)(2,1)} %param.16) | copy-start | bytes 1540
  7.3 51.4 %copy-start.13 = (bf16[256]{0:T(256)(128)(2,1)S(1)}, bf16[256]{0:T(256)(128)(2,1)}, u32[]{:S(2)}) copy-start(bf16[256]{0:T(256)(128)(2,1)} %param.24) | copy-start | bytes 1540
  7.3 51.4 %copy-start.2 = (bf16[512,256]{1,0:T(8,128)(2,1)S(1)}, bf16[512,256]{1,0:T(8,128)(2,1)}, u32[]{:S(2)}) copy-start(bf16[512,256]{1,0:T(8,128)(2,1)} %param.15) | copy-start | bytes 786436
  8.3 50.4 %all-to-all-start = ((bf16[16,32,768]{2,1,0:T(8,128)(2,1)}), bf16[16,32,768]{2,1,0:T(8,128)(2,1)S(1)}, u32[]{:S(2)}, u32[]{:S(2)}) async-start(bf16[16,32,768]{2,1,0:T(8,128)(2,1)} %broadcast_in_dim.68), calls=%async_computation | async-start | bytes 1572864 | tf_op jit(solution)/shard_map/all_to_all | solution.py:26
  24.0 173.3 %all-gather.2.cloned.1.call-start = ((), (), s32[]{:S(2)}) async-start(), calls=%async_computation.6 | async-start | bytes 6684672 | tf_op jit(solution)/shard_map/all_gather | solution.py:214
  24.1 10.2 %collective-permute-start.6 = (bf16[32,1536]{1,0:T(8,128)(2,1)S(1)}, bf16[32,1536]{1,0:T(8,128)(2,1)S(1)}, u32[]{:S(2)}, u32[]{:S(2)}) collective-permute-start(bf16[32,1536]{1,0:T(8,128)(2,1)S(1)} %pad_maximum_fusion.2), channel_id=1, source_target_pairs={{0,8},{8,16},{16,24},{24,0},{1,9},{9,17},{17,25},{25,1},{2,10},{10... | collective-permute-start | bytes 294920 | tf_op jit(solution)/shard_map/ppermute | solution.py:42
  27.3 7.0 %collective-permute-start.7 = (bf16[32,1536]{1,0:T(8,128)(2,1)S(1)}, bf16[32,1536]{1,0:T(8,128)(2,1)S(1)}, u32[]{:S(2)}, u32[]{:S(2)}) collective-permute-start(bf16[32,1536]{1,0:T(8,128)(2,1)S(1)} %pad_maximum_fusion.2), channel_id=1, source_target_pairs={{0,24},{8,0},{16,8},{24,16},{1,25},{9,1},{17,9},{25,17},{2,26},{10... | collective-permute-start | bytes 294920 | tf_op jit(solution)/shard_map/ppermute | solution.py:42
  30.7 7.2 %collective-permute-start.8 = (bf16[32,1536]{1,0:T(8,128)(2,1)S(1)}, bf16[32,1536]{1,0:T(8,128)(2,1)S(1)}, u32[]{:S(2)}, u32[]{:S(2)}) collective-permute-start(bf16[32,1536]{1,0:T(8,128)(2,1)S(1)} %pad_maximum_fusion.2), channel_id=1, source_target_pairs={{0,16},{8,24},{16,0},{24,8},{1,17},{9,25},{17,1},{25,9},{2,18},{10... | collective-permute-start | bytes 294920 | tf_op jit(solution)/shard_map/ppermute | solution.py:42
  37.9 20.8 %copy-start.3 = (bf16[4,32,1536]{2,1,0:T(8,128)(2,1)}, bf16[4,32,1536]{2,1,0:T(8,128)(2,1)S(1)}, u32[]{:S(2)}) copy-start(bf16[4,32,1536]{2,1,0:T(8,128)(2,1)S(1)} %bitcast_dynamic-update-slice_fusion.4) | copy-start | bytes 1179652
  58.8 11.8 %collective-permute-start = (bf16[528,256]{1,0:T(8,128)(2,1)S(1)}, bf16[528,256]{1,0:T(8,128)(2,1)S(1)}, u32[]{:S(2)}, u32[]{:S(2)}) collective-permute-start(bf16[528,256]{1,0:T(8,128)(2,1)S(1)} %pad_maximum_fusion.1), channel_id=1, source_target_pairs={{0,2},{2,4},{4,6},{6,0},{1,3},{3,5},{5,7},{7,1},{8,10},{10,12},{12... | collective-permute-start | bytes 811016 | tf_op jit(solution)/shard_map/ppermute | solution.py:42
  61.9 9.4 %collective-permute-start.1 = (bf16[528,256]{1,0:T(8,128)(2,1)S(1)}, bf16[528,256]{1,0:T(8,128)(2,1)S(1)}, u32[]{:S(2)}, u32[]{:S(2)}) collective-permute-start(bf16[528,256]{1,0:T(8,128)(2,1)S(1)} %pad_maximum_fusion.1), channel_id=1, source_target_pairs={{0,6},{2,0},{4,2},{6,4},{1,7},{3,1},{5,3},{7,5},{8,14},{10,8},{12,... | collective-permute-start | bytes 811016 | tf_op jit(solution)/shard_map/ppermute | solution.py:42
  65.3 11.6 %collective-permute-start.2 = (bf16[528,256]{1,0:T(8,128)(2,1)S(1)}, bf16[528,256]{1,0:T(8,128)(2,1)S(1)}, u32[]{:S(2)}, u32[]{:S(2)}) collective-permute-start(bf16[528,256]{1,0:T(8,128)(2,1)S(1)} %pad_maximum_fusion.1), channel_id=1, source_target_pairs={{0,4},{2,6},{4,0},{6,2},{1,5},{3,7},{5,1},{7,3},{8,12},{10,14},{12... | collective-permute-start | bytes 811016 | tf_op jit(solution)/shard_map/ppermute | solution.py:42
  77.6 12.4 %collective-permute-start.3 = (bf16[4,528,256]{2,1,0:T(8,128)(2,1)}, bf16[4,528,256]{2,1,0:T(8,128)(2,1)}, u32[]{:S(2)}, u32[]{:S(2)}) collective-permute-start(bf16[4,528,256]{2,1,0:T(8,128)(2,1)} %bitcast_dynamic-update-slice_fusion), channel_id=1, source_target_pairs={{0,1},{1,0},{2,3},{3,2},{4,5},{5,4},{6,7},{7,6},{8,9},{9,8},{10,11... | collective-permute-start | bytes 3244040 | tf_op jit(solution)/shard_map/ppermute | solution.py:30
  85.8 41.6 %all-to-all-start.1 = ((bf16[4,16,32,768]{3,2,1,0:T(8,128)(2,1)}), bf16[4,16,32,768]{3,2,1,0:T(8,128)(2,1)S(1)}, u32[]{:S(2)}, u32[]{:S(2)}) async-start(bf16[4,16,32,768]{3,2,1,0:T(8,128)(2,1)} %broadcast_in_dim.69), calls=%async_computation.1 | async-start | bytes 6291456 | tf_op jit(solution)/shard_map/all_to_all | solution.py:26
  127.4 1.7 copy-start
  129.1 9.9 %copy-start.11 = (bf16[2,128]{1,0:T(2,128)(2,1)S(1)}, bf16[2,128]{1,0:T(2,128)(2,1)}, u32[]{:S(2)}) copy-start(bf16[2,128]{1,0:T(2,128)(2,1)} %param.22) | copy-start | bytes 1540
  129.1 10.6 %copy-start.14 = (bf16[256]{0:T(256)(128)(2,1)S(1)}, bf16[256]{0:T(256)(128)(2,1)}, u32[]{:S(2)}) copy-start(bf16[256]{0:T(256)(128)(2,1)} %param.19) | copy-start | bytes 1540
  129.1 11.2 %copy-start.15 = (bf16[256]{0:T(256)(128)(2,1)S(1)}, bf16[256]{0:T(256)(128)(2,1)}, u32[]{:S(2)}) copy-start(bf16[256]{0:T(256)(128)(2,1)} %param.20) | copy-start | bytes 1540
  134.5 10.3 %all-to-all-start.2 = ((f32[8,2,512]{2,1,0:T(2,128)}), f32[8,2,512]{2,1,0:T(2,128)S(1)}, u32[]{:S(2)}, u32[]{:S(2)}) async-start(f32[8,2,512]{2,1,0:T(2,128)} %broadcast_in_dim.70), calls=%async_computation.2 | async-start | bytes 65536 | tf_op jit(solution)/shard_map/all_to_all | solution.py:26
  144.9 0.6 copy-start.5
  149.9 4.8 %collective-permute-start.4 = (bf16[4,512,256]{2,1,0:T(8,128)(2,1)}, bf16[4,512,256]{2,1,0:T(8,128)(2,1)S(1)}, u32[]{:S(2)}, u32[]{:S(2)}) collective-permute-start(bf16[4,512,256]{2,1,0:T(8,128)(2,1)} %get-tuple-element.15), channel_id=1, source_target_pairs={{0,1},{1,0},{2,3},{3,2},{4,5},{5,4},{6,7},{7,6},{8,9},{9,8},{10,11... | collective-permute-start | bytes 3145736 | tf_op jit(solution)/shard_map/ppermute | solution.py:30
  174.6 20.5 %copy-start.9 = (bf16[3,512]{1,0:T(4,128)(2,1)S(1)}, bf16[3,512]{1,0:T(4,128)(2,1)}, u32[]{:S(2)}) copy-start(bf16[3,512]{1,0:T(4,128)(2,1)} %param.27) | copy-start | bytes 9220
  174.6 21.1 %copy-start.10 = (bf16[3,512]{1,0:T(4,128)(2,1)S(1)}, bf16[3,512]{1,0:T(4,128)(2,1)}, u32[]{:S(2)}) copy-start(bf16[3,512]{1,0:T(4,128)(2,1)} %param.28) | copy-start | bytes 9220
  190.5 6.8 %copy-start.1 = (bf16[4,512,256]{2,1,0:T(8,128)(2,1)}, bf16[4,512,256]{2,1,0:T(8,128)(2,1)S(1)}, u32[]{:S(2)}) copy-start(bf16[4,512,256]{2,1,0:T(8,128)(2,1)S(1)} %all_to_all.31.mine) | copy-start | bytes 3145732
  190.5 6.8 %collective-permute-start.5 = (bf16[4,512,256]{2,1,0:T(8,128)(2,1)S(1)}, bf16[4,512,256]{2,1,0:T(8,128)(2,1)S(1)}, u32[]{:S(2)}, u32[]{:S(2)}) collective-permute-start(bf16[4,512,256]{2,1,0:T(8,128)(2,1)S(1)} %all_to_all.31.mine), channel_id=1, source_target_pairs={{0,1},{1,0},{2,3},{3,2},{4,5},{5,4},{6,7},{7,6},{8,9},{9,8},{10,11... | collective-permute-start | bytes 3145736 | tf_op jit(solution)/shard_map/ppermute | solution.py:30
  197.4 1.1 copy-start.4
  208.0 4.8 %collective-permute-start.9 = (bf16[4,512,256]{2,1,0:T(8,128)(2,1)}, bf16[4,512,256]{2,1,0:T(8,128)(2,1)S(1)}, u32[]{:S(2)}, u32[]{:S(2)}) collective-permute-start(bf16[4,512,256]{2,1,0:T(8,128)(2,1)} %get-tuple-element.18), channel_id=1, source_target_pairs={{0,1},{1,0},{2,3},{3,2},{4,5},{5,4},{6,7},{7,6},{8,9},{9,8},{10,11... | collective-permute-start | bytes 3145736 | tf_op jit(solution)/shard_map/ppermute | solution.py:30
Sparse Core Ops, SparseCore 0:
  58.8 84.5 all-gather.1

commit v2 on v1

--- a/solution.py
+++ b/solution.py
@@ -16,6 +16,7 @@
 F32 = jnp.float32
 BF16 = jnp.bfloat16
 SWAP = [(0, 1), (1, 0)]
+RING = (0, 1, 3, 2)
 SQRT_HALF = 0.7071067811865476
 VMEM = pl.BlockSpec(memory_space=pltpu.VMEM)
 SMEM = pl.BlockSpec(memory_space=pltpu.SMEM)
@@ -34,23 +35,43 @@
     return lax.optimization_barrier((value, *first))[0]
 
 
-def by_permutes(shard, axis):
-    size = lax.axis_size(axis)
+def round_ring(shard, axis):
+    return [shard] + [lax.ppermute(shard, axis, [(i, (i + step) % 4) for i in range(4)]) for step in RING[1:]]
+
+
+def in_order(parts, axis):
     here = lax.axis_index(axis).astype(jnp.uint32)
-    parts = [shard]
-    for step in (1, 3, 2):
-        parts.append(lax.ppermute(shard, axis, [(i, (i + step) % size) for i in range(size)]))
-    filled = jnp.zeros((size, *shard.shape), shard.dtype)
-    for step, part in zip((0, 1, 3, 2), parts):
-        origin = (here + jnp.uint32(size - step)) & jnp.uint32(size - 1)
-        filled = lax.dynamic_update_slice(filled, part[None], (origin, *([jnp.uint32(0)] * shard.ndim)))
+    filled = jnp.zeros((4, *parts[0].shape), parts[0].dtype)
+    for step, part in zip(RING, parts):
+        at = (here + jnp.uint32(4 - step)) & jnp.uint32(3)
+        filled = lax.dynamic_update_slice(filled, part[None], (at, *([jnp.uint32(0)] * part.ndim)))
     return filled
 
 
-def rms(values, gain):
-    v = values.astype(F32)
-    scale = lax.rsqrt(jnp.mean(v * v, axis=1, keepdims=True) + EPS)
-    return (v * scale * gain.astype(F32)).astype(BF16)
+def norm_kernel(place, *refs):
+    parts, (out, gain_two) = refs[:8], refs[8:]
+    count, width = parts[0].shape[0] - 16, parts[0].shape[1]
+    x, c = place[0], place[1]
+    for part in range(count // BLOCK):
+        rows = pl.ds(part * BLOCK, BLOCK)
+        squares = jnp.zeros((BLOCK, width), F32)
+        for ref in parts:
+            value = ref[rows, :].astype(F32)
+            squares = squares + value * value
+        scale = lax.rsqrt(jnp.sum(squares, axis=1, keepdims=True) / (8 * width) + EPS)
+        for at, ref in enumerate(parts):
+            block = origin(x, RING[at % 4]) * 2 + (c if at < 4 else 1 - c)
+            gain = ref[count : count + 1, :].astype(F32)
+            out[rows, pl.ds(pl.multiple_of(block * width, width), width)] = (
+                ref[rows, :].astype(F32) * scale * gain
+            ).astype(BF16)
+    for at, ref in enumerate(parts):
+        block = origin(x, RING[at % 4]) * 2 + (c if at < 4 else 1 - c)
+        gain_two[block] = ref[count + 8 : count + 16, :]
+
+
+def origin(here, step):
+    return (here + (4 - step)) & 3
 
 
 def stats_kernel(normed, early, act, sums, weight):
@@ -99,6 +120,7 @@
     center_row = total[0:1] / full
     spread_row = total[1:2] / full - center_row * center_row
     scale_row = lax.rsqrt(spread_row + EPS)
+    biases = [jnp.broadcast_to(bias[g : g + 1, :].astype(F32), (BLOCK, BLOCK)).T for g in range(width // GROUP_DIM)]
     for block in range(act_v.shape[0] // BLOCK):
         rows = pl.ds(block * BLOCK, BLOCK)
         at = slice(block * BLOCK, (block + 1) * BLOCK)
@@ -106,9 +128,9 @@
         scale = jnp.broadcast_to(scale_row[:, at], (BLOCK, BLOCK)).T
         for g in range(width // GROUP_DIM):
             cols = slice(g * GROUP_DIM, (g + 1) * GROUP_DIM)
-            mixed = ((act_v[rows, cols] - center) * scale * gain[:, cols] + shift[:, cols]).astype(BF16)
+            mixed = ((act_v[rows, cols] - center) * scale * gain[:, cols].astype(F32) + shift[:, cols].astype(F32)).astype(BF16)
             seen = jnp.where(visible, mix[g].astype(F32), 0.0).astype(BF16)
-            spatial = jnp.dot(seen, mixed, preferred_element_type=F32) + bias[:, g : g + 1]
+            spatial = jnp.dot(seen, mixed, preferred_element_type=F32) + biases[g]
             gated[rows, cols] = (act_u[rows, cols] * spatial).astype(BF16)
     c = core[0]
     for out, side in ((give, 1 - c), (keep, c)):
@@ -146,7 +168,8 @@
         def fill(ref, side):
             for x in range(mine.shape[0]):
                 at = pl.ds((2 * x + side) * width, width)
-                normed[:, at] = (ref[x, rows, :].astype(F32) * scale * gain[:, at]).astype(BF16)
+                row = gain[2 * x + side, 0:1, :].astype(F32)
+                normed[:, at] = (ref[x, rows, :].astype(F32) * scale * row).astype(BF16)
 
         @pl.when(c == 0)
         def _():
@@ -160,8 +183,8 @@
 
         gate = jnp.dot(normed[...], late[:, 0:ff], preferred_element_type=F32)
         value = jnp.dot(normed[...], late[:, ff : 2 * ff], preferred_element_type=F32)
-        conv_g = taps(gate, conv_gate[...])
-        conv_v = taps(value, conv_value[...])
+        conv_g = taps(gate, conv_gate[...].astype(F32))
+        conv_v = taps(value, conv_value[...].astype(F32))
         hidden[rows, :] = (conv_g * jax.nn.sigmoid(conv_g) * conv_v).astype(BF16)
     for out, side in ((give, 1 - c), (keep, c)):
         for x in range(out.shape[0]):
@@ -178,6 +201,10 @@
 
 def shape(dims, dtype):
     return jax.ShapeDtypeStruct(dims, dtype)
+
+
+def room(mebibytes):
+    return pltpu.CompilerParams(vmem_limit_bytes=mebibytes << 20)
 
 
 def summed_at_owner(give, keep):
@@ -210,20 +237,26 @@
     early = jnp.concatenate([proj_u, proj_v, proj_out.T], axis=1)
     early_z = everyones(early, "z")
     late = jnp.concatenate([ffn_gate, ffn_value, proj_down.T], axis=1)
-    late_y = by_permutes(late, "y").reshape(-1, late.shape[1])
+    late_y = in_order(round_ring(late, "y"), "y").reshape(-1, late.shape[1])
     late_all = lax.all_gather(after(late_y, early_z), "z", axis=0, tiled=True)
 
     packed = jnp.concatenate([tokens, jnp.broadcast_to(norm_gain, (8, da)), jnp.broadcast_to(ffn_gain, (8, da))], axis=0)
-    mine = by_permutes(packed, "x")
-    other = other_core(mine)
-    first = lax.axis_index("c") == 0
-    both = jnp.stack([jnp.where(first, mine, other), jnp.where(first, other, mine)], axis=1)
-    whole = both.reshape(-1, *packed.shape).transpose(1, 0, 2).reshape(packed.shape[0], -1)
-    normed = rms(whole[:row_count], whole[row_count])
-    gain_two = whole[row_count + 8]
+    mine = round_ring(packed, "x")
+    other = [other_core(part) for part in mine]
     early_all = everyones(early_z, "y").reshape(4, -1, early.shape[1])
-    core = lax.axis_index("c").astype(jnp.int32).reshape(1)
+    core = lax.axis_index("c").astype(jnp.int32)
+    place = jnp.stack([lax.axis_index("x").astype(jnp.int32), core])
+    core = core.reshape(1)
     model = proj_u.shape[0] * lax.axis_size(FS)
+    tp = lax.axis_size(TP)
+    normed, gain_two = pl.pallas_call(
+        norm_kernel,
+        in_specs=[SMEM] + [VMEM] * 8,
+        out_specs=[VMEM] * 2,
+        out_shape=[shape((row_count, model), BF16), shape((tp, 8, da), BF16)],
+        name="norm",
+        compiler_params=room(12),
+    )(place, *mine, *other)
 
     act_v, sums = pl.pallas_call(
         stats_kernel,
@@ -232,6 +265,7 @@
         out_shape=[shape((row_count, da), F32), shape((2, row_count), F32)],
         scratch_shapes=[pltpu.VMEM((model, da), BF16)],
         name="stats",
+        compiler_params=room(14),
     )(normed, early_all)
     stats = everyones(sums, TP)
     act_u = pl.pallas_call(
@@ -241,6 +275,7 @@
         out_shape=shape((row_count, da), F32),
         scratch_shapes=[pltpu.VMEM((model, da), BF16)],
         name="gate",
+        compiler_params=room(14),
     )(normed, early_all)
     blocks = [shape((lax.axis_size("x"), row_count, da), BF16)] * 2
     give, keep = pl.pallas_call(
@@ -250,15 +285,16 @@
         out_shape=blocks,
         scratch_shapes=[pltpu.VMEM((model, da), BF16), pltpu.VMEM((row_count, da), BF16)],
         name="mix",
+        compiler_params=room(16),
     )(
         core,
         act_v,
         act_u,
         stats,
-        layer_gain.astype(F32)[None],
-        layer_shift.astype(F32)[None],
+        layer_gain[None],
+        layer_shift[None],
         mix_weight,
-        mix_bias.astype(F32).T,
+        mix_bias,
         early_all,
     )
     stream = (tokens.astype(F32) + summed_at_owner(give, keep)).astype(BF16)
@@ -270,14 +306,15 @@
         out_shape=blocks,
         scratch_shapes=[pltpu.VMEM((SEQ_LEN, model), BF16), pltpu.VMEM((row_count, ff), BF16)],
         name="ffn",
+        compiler_params=room(26),
     )(
         core,
         mine,
         other_core(mine),
-        gain_two.astype(F32)[None],
+        gain_two,
         late_all,
-        conv_gate.astype(F32),
-        conv_value.astype(F32),
+        conv_gate,
+        conv_value,
     )
     return (stream.astype(F32) + summed_at_owner(give, keep)).astype(BF16)
 

time: 240 us -> 205 us (0.85)
  waiting for transfers between devices: 66.8 us -> 35.1 us
  starting transfers between devices: 59.4 us -> 74.4 us
  Pallas kernels: 22.2 us -> 10.4 us
  other arithmetic: 13.1 us -> 3.49 us
    all_to_all x3, waiting for transfers between devices: 52.8 us -> 23 us  [everyones(): return lax.all_to_all(copies, axis, split_axis=0, concat_axis=0, tiled=True)]
    ppermute x4 -> x7, starting transfers between devices: 15 us -> 23.5 us  [other_core(): return lax.ppermute(value, 'c', SWAP)]
    unnamed x32 -> x42, local copies, waits for them, and re-layouts: 3.43 us -> 11 us
    all_to_all x3, starting transfers between devices: 24.3 us -> 30.9 us  [everyones(): return lax.all_to_all(copies, axis, split_axis=0, concat_axis=0, tiled=True)]
    ppermute x6, waiting for transfers between devices: 8.37 us -> 3.49 us  [round_ring(): lax.ppermute(shard, axis, [(i, (i + step) % 4) for i in range(4)])]
    pallas_call x1, Pallas kernels: 9.56 us -> 5.19 us  [on_device(): pl.pallas_call(ffn_kernel, in_specs=[SMEM] + [VMEM] * 6, out_specs=[VMEM]...]
    convert_element_type x4 -> x0, other arithmetic: 3.52 us -> none  [the longest x1 1.72 us: rms(): return (v * scale * gain.astype(F32)).astype(BF16)]
    pallas_call x1, Pallas kernels: 4.43 us -> 1.02 us  [on_device(): pl.pallas_call(mix_kernel, in_specs=[SMEM] + [VMEM] * 8, out_specs=[VMEM]...]
  transfers between devices with their start and end apart: 14 -> 17, of which waited for: 7 -> 8; matrix products, arithmetic and copies ran while one was open for 8% -> 2% of each run, Pallas kernels for 5% -> 3%
where the time goes in v2:
time: 205 us; the launch traced here: 203 us
  starting transfers between devices  74.4 us (36%)
  blocking collectives  51 us (25%)
  waiting for transfers between devices  35.1 us (17%)
  local copies, waits for them, and re-layouts  14.9 us (7%)
  between operations  13.8 us (7%)
  Pallas kernels  10.4 us (5%)
  other arithmetic  3.49 us (2%)
    all_to_all x2, blocking collectives, summed_at_owner(): arrived = lax.all_to_all(pair, 'x', split_axis=0, concat_axis=0, tiled=True)  34.6 us
    all_to_all x3, starting transfers between devices, everyones(): return lax.all_to_all(copies, axis, split_axis=0, concat_axis=0, tiled=True)  30.9 us
    ppermute x7, starting transfers between devices, other_core(): return lax.ppermute(value, 'c', SWAP)  23.5 us
    all_to_all x3, waiting for transfers between devices, everyones(): return lax.all_to_all(copies, axis, split_axis=0, concat_axis=0, tiled=True)  23 us
    ppermute x6, starting transfers between devices, round_ring(): lax.ppermute(shard, axis, [(i, (i + step) % 4) for i in range(4)])  20 us
    all_to_all x1, blocking collectives, everyones(): return lax.all_to_all(copies, axis, split_axis=0, concat_axis=0, tiled=True)  16.4 us
    unnamed x42, local copies, waits for them, and re-layouts  11 us
    ppermute x7, waiting for transfers between devices, other_core(): return lax.ppermute(value, 'c', SWAP)  8.59 us
  transfers between devices with their start and end apart: 17, of which 8 were waited for; matrix products, arithmetic and copies ran while one was open for 2% of the time, Pallas kernels for 3%

profile of v2, /device:TPU:1, one launch (start us, length us, event | category | flops | bytes accessed | tf_op | source)
XLA Modules:
  0.0 203.1 jit_solution(4272036624573191749)
XLA Ops:
  6.5 0.8 pad_maximum_fusion.2
  7.3 1.0 broadcast_in_dim.41
  8.3 15.7 %all-to-all-start = ((bf16[16,32,768]{2,1,0:T(8,128)(2,1)}), bf16[16,32,768]{2,1,0:T(8,128)(2,1)S(1)}, u32[]{:S(2)}, u32[]{:S(2)}) async-start(bf16[16,32,768]{2,1,0:T(8,128)(2,1)} %broadcast_in_dim.41), calls=%async_computation | async-start | bytes 1572864 | tf_op jit(solution)/shard_map/all_to_all | solution.py:27
  24.0 0.0 all-gather.2.cloned.1.call-start
  24.1 3.2 %collective-permute-start.9 = (bf16[32,1536]{1,0:T(8,128)(2,1)S(1)}, bf16[32,1536]{1,0:T(8,128)(2,1)S(1)}, u32[]{:S(2)}, u32[]{:S(2)}) collective-permute-start(bf16[32,1536]{1,0:T(8,128)(2,1)S(1)} %pad_maximum_fusion.1), channel_id=1, source_target_pairs={{0,8},{8,16},{16,24},{24,0},{1,9},{9,17},{17,25},{25,1},{2,10},{10... | collective-permute-start | bytes 294920 | tf_op jit(solution)/shard_map/ppermute | solution.py:39
  27.3 3.4 %collective-permute-start.10 = (bf16[32,1536]{1,0:T(8,128)(2,1)S(1)}, bf16[32,1536]{1,0:T(8,128)(2,1)S(1)}, u32[]{:S(2)}, u32[]{:S(2)}) collective-permute-start(bf16[32,1536]{1,0:T(8,128)(2,1)S(1)} %pad_maximum_fusion.1), channel_id=1, source_target_pairs={{0,24},{8,0},{16,8},{24,16},{1,25},{9,1},{17,9},{25,17},{2,26},{10... | collective-permute-start | bytes 294920 | tf_op jit(solution)/shard_map/ppermute | solution.py:39
  30.7 3.5 %collective-permute-start.11 = (bf16[32,1536]{1,0:T(8,128)(2,1)S(1)}, bf16[32,1536]{1,0:T(8,128)(2,1)S(1)}, u32[]{:S(2)}, u32[]{:S(2)}) collective-permute-start(bf16[32,1536]{1,0:T(8,128)(2,1)S(1)} %pad_maximum_fusion.1), channel_id=1, source_target_pairs={{0,16},{8,24},{16,0},{24,8},{1,17},{9,25},{17,1},{25,9},{2,18},{10... | collective-permute-start | bytes 294920 | tf_op jit(solution)/shard_map/ppermute | solution.py:39
  34.3 0.0 collective-permute-done.9
  34.3 0.0 collective-permute-done.10
  34.4 3.5 %collective-permute-done.11 = bf16[32,1536]{1,0:T(8,128)(2,1)S(1)} collective-permute-done((bf16[32,1536]{1,0:T(8,128)(2,1)S(1)}, bf16[32,1536]{1,0:T(8,128)(2,1)S(1)}, u32[]{:S(2)}, u32[]{:S(2)}) %collective-permute-start.11) | collective-permute-done | bytes 98336 | tf_op jit(solution)/shard_map/ppermute | solution.py:39
  37.9 20.8 %all-to-all-done = bf16[16,32,768]{2,1,0:T(8,128)(2,1)S(1)} async-done(((bf16[16,32,768]{2,1,0:T(8,128)(2,1)}), bf16[16,32,768]{2,1,0:T(8,128)(2,1)S(1)}, u32[]{:S(2)}, u32[]{:S(2)}) %all-to-all-start) | async-done | bytes 786464 | tf_op jit(solution)/shard_map/all_to_all | solution.py:27
  58.7 0.0 all-gather.2.cloned.1.call-update
  58.7 2.1 %broadcast_in_dim.42 = bf16[4,16,32,768]{3,2,1,0:T(8,128)(2,1)} broadcast(bf16[16,32,768]{2,1,0:T(8,128)(2,1)S(1)} %all-to-all-done), dimensions={1,2,3} | broadcast | bytes 3932160 | tf_op jit(solution)/shard_map/broadcast_in_dim | solution.py:26
  60.8 4.3 %all-to-all-start.1 = ((bf16[4,16,32,768]{3,2,1,0:T(8,128)(2,1)}), bf16[4,16,32,768]{3,2,1,0:T(8,128)(2,1)S(1)}, u32[]{:S(2)}, u32[]{:S(2)}) async-start(bf16[4,16,32,768]{3,2,1,0:T(8,128)(2,1)} %broadcast_in_dim.42), calls=%async_computation.1 | async-start | bytes 6291456 | tf_op jit(solution)/shard_map/all_to_all | solution.py:27
  65.1 1.0 pad_maximum_fusion.refs_0_
  66.1 3.1 %collective-permute-start = (bf16[528,256]{1,0:T(8,128)(2,1)S(1)}, bf16[528,256]{1,0:T(8,128)(2,1)}, u32[]{:S(2)}, u32[]{:S(2)}) collective-permute-start(bf16[528,256]{1,0:T(8,128)(2,1)S(1)} %pad_maximum_fusion.refs_0_), channel_id=1, source_target_pairs={{0,2},{2,4},{4,6},{6,0},{1,3},{3,5},{5,7},{7,1},{8,10},{10,12},{12... | collective-permute-start | bytes 811016 | tf_op jit(solution)/shard_map/ppermute | solution.py:39
  69.2 3.4 %collective-permute-start.1 = (bf16[528,256]{1,0:T(8,128)(2,1)S(1)}, bf16[528,256]{1,0:T(8,128)(2,1)}, u32[]{:S(2)}, u32[]{:S(2)}) collective-permute-start(bf16[528,256]{1,0:T(8,128)(2,1)S(1)} %pad_maximum_fusion.refs_0_), channel_id=1, source_target_pairs={{0,6},{2,0},{4,2},{6,4},{1,7},{3,1},{5,3},{7,5},{8,14},{10,8},{12,... | collective-permute-start | bytes 811016 | tf_op jit(solution)/shard_map/ppermute | solution.py:39
  72.6 3.4 %collective-permute-start.2 = (bf16[528,256]{1,0:T(8,128)(2,1)S(1)}, bf16[528,256]{1,0:T(8,128)(2,1)}, u32[]{:S(2)}, u32[]{:S(2)}) collective-permute-start(bf16[528,256]{1,0:T(8,128)(2,1)S(1)} %pad_maximum_fusion.refs_0_), channel_id=1, source_target_pairs={{0,4},{2,6},{4,0},{6,2},{1,5},{3,7},{5,1},{7,3},{8,12},{10,14},{12... | collective-permute-start | bytes 811016 | tf_op jit(solution)/shard_map/ppermute | solution.py:39
  76.1 8.4 %collective-permute-start.3 = (bf16[528,256]{1,0:T(8,128)(2,1)S(1)}, bf16[528,256]{1,0:T(8,128)(2,1)}, u32[]{:S(2)}, u32[]{:S(2)}) collective-permute-start(bf16[528,256]{1,0:T(8,128)(2,1)S(1)} %pad_maximum_fusion.refs_0_), channel_id=1, source_target_pairs={{0,1},{1,0},{2,3},{3,2},{4,5},{5,4},{6,7},{7,6},{8,9},{9,8},{10,11... | collective-permute-start | bytes 811016 | tf_op jit(solution)/shard_map/ppermute | solution.py:31
  84.5 0.0 collective-permute-done.refs_1_
  84.5 1.9 collective-permute-start.4
  86.4 0.0 collective-permute-done.1.refs_2_
  86.4 2.4 %collective-permute-start.5 = (bf16[528,256]{1,0:T(8,128)(2,1)}, bf16[528,256]{1,0:T(8,128)(2,1)}, u32[]{:S(2)}, u32[]{:S(2)}) collective-permute-start(bf16[528,256]{1,0:T(8,128)(2,1)} %collective-permute-done.1.refs_2_), channel_id=1, source_target_pairs={{0,1},{1,0},{2,3},{3,2},{4,5},{5,4},{6,7},{7,6},{8,9},{9,8},{10,11... | collective-permute-start | bytes 811016 | tf_op jit(solution)/shard_map/ppermute | solution.py:31
  88.8 0.0 collective-permute-done.2.refs_3_
  88.8 1.9 collective-permute-start.6
  90.8 0.1 pad_add_fusion.place
  90.9 0.0 collective-permute-done.3.refs_4_
  90.9 1.8 collective-permute-done.6.refs_7_
  92.6 2.5 %norm.1 = (bf16[512,2048]{1,0:T(8,128)(2,1)S(1)}, bf16[8,8,256]{2,1,0:T(8,128)(2,1)S(1)}) custom-call(s32[2]{0:T(128)S(1)} %pad_add_fusion.place, bf16[528,256]{1,0:T(8,128)(2,1)S(1)} %pad_maximum_fusion.refs_0_, bf16[528,256]{1,0:T(8,128)(2,1)} %collective-permute-done.refs_1_, bf16[528,256]{1,0:T(8,128)(2,1)} %collective-permute-done.1.refs_2_, ...), custom_call_target="tpu_custom_call" | custom-call | tf_op jit(solution)/shard_map/norm/pallas_call | solution.py:252
  95.2 1.3 copy-done
  96.5 0.6 all-to-all-done.1
  97.1 1.6 copy-done.1
  98.7 0.9 stats.1
  99.6 0.8 copy-done.6
  100.4 0.6 broadcast_in_dim.43
  101.1 10.8 %all-to-all-start.2 = ((f32[8,2,512]{2,1,0:T(2,128)}), f32[8,2,512]{2,1,0:T(2,128)S(1)}, u32[]{:S(2)}, u32[]{:S(2)}) async-start(f32[8,2,512]{2,1,0:T(2,128)} %broadcast_in_dim.43), calls=%async_computation.2 | async-start | bytes 65536 | tf_op jit(solution)/shard_map/all_to_all | solution.py:27
  111.9 1.6 copy-done.2
  113.5 0.7 gate.1.act_u
  114.3 0.8 copy-done.4
  115.0 1.6 all-to-all-done.2.stats
  116.7 1.1 copy-done.5
  117.7 1.1 copy-done.7
  118.8 1.0 mix.2
  119.8 2.6 %collective-permute-start.7 = (bf16[4,512,256]{2,1,0:T(8,128)(2,1)S(1)}, bf16[4,512,256]{2,1,0:T(8,128)(2,1)S(1)}, u32[]{:S(2)}, u32[]{:S(2)}) collective-permute-start(bf16[4,512,256]{2,1,0:T(8,128)(2,1)S(1)} %get-tuple-element.18), channel_id=1, source_target_pairs={{0,1},{1,0},{2,3},{3,2},{4,5},{5,4},{6,7},{7,6},{8,9},{9,8},{10,11... | collective-permute-start | bytes 3145736 | tf_op jit(solution)/shard_map/ppermute | solution.py:31
  122.4 2.3 %collective-permute-done.7 = bf16[4,512,256]{2,1,0:T(8,128)(2,1)S(1)} collective-permute-done((bf16[4,512,256]{2,1,0:T(8,128)(2,1)S(1)}, bf16[4,512,256]{2,1,0:T(8,128)(2,1)S(1)}, u32[]{:S(2)}, u32[]{:S(2)}) %collective-permute-start.7) | collective-permute-done | bytes 1048608 | tf_op jit(solution)/shard_map/ppermute | solution.py:31
  124.6 0.2 add_convert_fusion.1
  124.9 0.0 copy-start.13
  124.9 17.4 %all_to_all.30 = bf16[4,512,256]{2,1,0:T(8,128)(2,1)S(1)} all-to-all(bf16[4,512,256]{2,1,0:T(8,128)(2,1)S(1)} %add_convert_fusion.1), channel_id=1, replica_groups=mesh['z'=16,'y'=4,'x'=4,'c'=2] {'x'}, dimensions={0} | all-to-all | bytes 2097152 | tf_op jit(solution)/shard_map/all_to_all | solution.py:212
  142.3 0.1 convert_reduce_fusion.1
  142.4 0.0 copy-start.9
  142.4 0.0 copy-start.10
  142.4 0.1 add_convert_fusion.3
  142.5 0.1 broadcast_in_dim.46
  142.6 16.4 %all_to_all.31.mine = bf16[4,512,256]{2,1,0:T(8,128)(2,1)S(1)} all-to-all(bf16[4,512,256]{2,1,0:T(8,128)(2,1)S(1)} %broadcast_in_dim.46), channel_id=1, replica_groups=mesh['z'=16,'y'=4,'x'=4,'c'=2] {'x'}, dimensions={0} | all-to-all | bytes 2097152 | tf_op jit(solution)/shard_map/all_to_all | solution.py:27
  159.0 4.0 %collective-permute-start.8 = (bf16[4,512,256]{2,1,0:T(8,128)(2,1)S(1)}, bf16[4,512,256]{2,1,0:T(8,128)(2,1)S(1)}, u32[]{:S(2)}, u32[]{:S(2)}) collective-permute-start(bf16[4,512,256]{2,1,0:T(8,128)(2,1)S(1)} %all_to_all.31.mine), channel_id=1, source_target_pairs={{0,1},{1,0},{2,3},{3,2},{4,5},{5,4},{6,7},{7,6},{8,9},{9,8},{10,11... | collective-permute-start | bytes 3145736 | tf_op jit(solution)/shard_map/ppermute | solution.py:31
  163.0 2.3 %collective-permute-done.8.other = bf16[4,512,256]{2,1,0:T(8,128)(2,1)S(1)} collective-permute-done((bf16[4,512,256]{2,1,0:T(8,128)(2,1)S(1)}, bf16[4,512,256]{2,1,0:T(8,128)(2,1)S(1)}, u32[]{:S(2)}, u32[]{:S(2)}) %collective-permute-start.8) | collective-permute-done | bytes 1048608 | tf_op jit(solution)/shard_map/ppermute | solution.py:31
  165.2 2.8 %copy-done.3 = bf16[2048,1536]{1,0:T(8,128)(2,1)S(1)} copy-done((bf16[2048,1536]{1,0:T(8,128)(2,1)S(1)}, bf16[2048,1536]{1,0:T(8,128)(2,1)}, u32[]{:S(2)}) %copy-start.3) | copy-done | bytes 6291480
  168.0 5.2 %ffn.1 = (bf16[4,512,256]{2,1,0:T(8,128)(2,1)S(1)}, bf16[4,512,256]{2,1,0:T(8,128)(2,1)S(1)}) custom-call(s32[1]{0:T(128)} %bitcast.core, bf16[4,512,256]{2,1,0:T(8,128)(2,1)S(1)} %all_to_all.31.mine, bf16[4,512,256]{2,1,0:T(8,128)(2,1)S(1)} %collective-permute-done.8.other, bf16[8,8,256]{2,1,0:T(8,128)(2,1)S(1)} %get-tuple-element.19.gain, ...), custom_call_target="tpu_custom_call" | custom-call | tf_op jit(solution)/shard_map/ffn/pallas_call | solution.py:302
  173.2 2.3 %collective-permute-start.12 = (bf16[4,512,256]{2,1,0:T(8,128)(2,1)S(1)}, bf16[4,512,256]{2,1,0:T(8,128)(2,1)S(1)}, u32[]{:S(2)}, u32[]{:S(2)}) collective-permute-start(bf16[4,512,256]{2,1,0:T(8,128)(2,1)S(1)} %get-tuple-element.22), channel_id=1, source_target_pairs={{0,1},{1,0},{2,3},{3,2},{4,5},{5,4},{6,7},{7,6},{8,9},{9,8},{10,11... | collective-permute-start | bytes 3145736 | tf_op jit(solution)/shard_map/ppermute | solution.py:31
  175.5 2.3 %collective-permute-done.12 = bf16[4,512,256]{2,1,0:T(8,128)(2,1)S(1)} collective-permute-done((bf16[4,512,256]{2,1,0:T(8,128)(2,1)S(1)}, bf16[4,512,256]{2,1,0:T(8,128)(2,1)S(1)}, u32[]{:S(2)}, u32[]{:S(2)}) %collective-permute-start.12) | collective-permute-done | bytes 1048608 | tf_op jit(solution)/shard_map/ppermute | solution.py:31
  177.8 0.3 add_convert_fusion
  178.1 17.3 %all_to_all.32 = bf16[4,512,256]{2,1,0:T(8,128)(2,1)S(1)} all-to-all(bf16[4,512,256]{2,1,0:T(8,128)(2,1)S(1)} %add_convert_fusion), channel_id=1, replica_groups=mesh['z'=16,'y'=4,'x'=4,'c'=2] {'x'}, dimensions={0} | all-to-all | bytes 2097152 | tf_op jit(solution)/shard_map/all_to_all | solution.py:212
  195.3 0.1 convert_reduce_fusion
  195.5 0.8 add_convert_fusion.2
  (44 shorter events, 0.2 us)
Async XLA Ops:
  6.5 17.5 %copy-start.14 = (bf16[512,32]{0,1:T(8,128)(2,1)S(1)}, bf16[512,32]{0,1:T(8,128)(2,1)}, u32[]{:S(2)}) copy-start(bf16[512,32]{0,1:T(8,128)(2,1)} %param.29) | copy-start | bytes 98308
  6.5 17.5 %copy-start.16 = (bf16[32,512]{1,0:T(8,128)(2,1)S(1)}, bf16[32,512]{1,0:T(8,128)(2,1)}, u32[]{:S(2)}) copy-start(bf16[32,512]{1,0:T(8,128)(2,1)} %param.25) | copy-start | bytes 98308
  6.5 17.6 %copy-start.15 = (bf16[32,512]{1,0:T(8,128)(2,1)S(1)}, bf16[32,512]{1,0:T(8,128)(2,1)}, u32[]{:S(2)}) copy-start(bf16[32,512]{1,0:T(8,128)(2,1)} %param.26) | copy-start | bytes 98308
  8.3 50.4 %all-to-all-start = ((bf16[16,32,768]{2,1,0:T(8,128)(2,1)}), bf16[16,32,768]{2,1,0:T(8,128)(2,1)S(1)}, u32[]{:S(2)}, u32[]{:S(2)}) async-start(bf16[16,32,768]{2,1,0:T(8,128)(2,1)} %broadcast_in_dim.41), calls=%async_computation | async-start | bytes 1572864 | tf_op jit(solution)/shard_map/all_to_all | solution.py:27
  24.0 141.2 %all-gather.2.cloned.1.call-start = ((), (), s32[]{:S(2)}) async-start(), calls=%async_computation.6 | async-start | bytes 6684672 | tf_op jit(solution)/shard_map/all_gather | solution.py:241
  24.1 10.2 %collective-permute-start.9 = (bf16[32,1536]{1,0:T(8,128)(2,1)S(1)}, bf16[32,1536]{1,0:T(8,128)(2,1)S(1)}, u32[]{:S(2)}, u32[]{:S(2)}) collective-permute-start(bf16[32,1536]{1,0:T(8,128)(2,1)S(1)} %pad_maximum_fusion.1), channel_id=1, source_target_pairs={{0,8},{8,16},{16,24},{24,0},{1,9},{9,17},{17,25},{25,1},{2,10},{10... | collective-permute-start | bytes 294920 | tf_op jit(solution)/shard_map/ppermute | solution.py:39
  27.3 7.0 %collective-permute-start.10 = (bf16[32,1536]{1,0:T(8,128)(2,1)S(1)}, bf16[32,1536]{1,0:T(8,128)(2,1)S(1)}, u32[]{:S(2)}, u32[]{:S(2)}) collective-permute-start(bf16[32,1536]{1,0:T(8,128)(2,1)S(1)} %pad_maximum_fusion.1), channel_id=1, source_target_pairs={{0,24},{8,0},{16,8},{24,16},{1,25},{9,1},{17,9},{25,17},{2,26},{10... | collective-permute-start | bytes 294920 | tf_op jit(solution)/shard_map/ppermute | solution.py:39
  30.7 7.2 %collective-permute-start.11 = (bf16[32,1536]{1,0:T(8,128)(2,1)S(1)}, bf16[32,1536]{1,0:T(8,128)(2,1)S(1)}, u32[]{:S(2)}, u32[]{:S(2)}) collective-permute-start(bf16[32,1536]{1,0:T(8,128)(2,1)S(1)} %pad_maximum_fusion.1), channel_id=1, source_target_pairs={{0,16},{8,24},{16,0},{24,8},{1,17},{9,25},{17,1},{25,9},{2,18},{10... | collective-permute-start | bytes 294920 | tf_op jit(solution)/shard_map/ppermute | solution.py:39
  37.9 20.8 %copy-start.12 = (bf16[4,32,1536]{2,1,0:T(8,128)(2,1)}, bf16[4,32,1536]{2,1,0:T(8,128)(2,1)S(1)}, u32[]{:S(2)}) copy-start(bf16[4,32,1536]{2,1,0:T(8,128)(2,1)S(1)} %bitcast_dynamic-update-slice_fusion) | copy-start | bytes 1179652
  60.8 4.3 %copy-start.17 = (bf16[256]{0:T(256)(128)(2,1)S(1)}, bf16[256]{0:T(256)(128)(2,1)}, u32[]{:S(2)}) copy-start(bf16[256]{0:T(256)(128)(2,1)} %param.16) | copy-start | bytes 1540
  60.8 4.3 %copy-start.18 = (bf16[256]{0:T(256)(128)(2,1)S(1)}, bf16[256]{0:T(256)(128)(2,1)}, u32[]{:S(2)}) copy-start(bf16[256]{0:T(256)(128)(2,1)} %param.24) | copy-start | bytes 1540
  60.8 36.3 %all-to-all-start.1 = ((bf16[4,16,32,768]{3,2,1,0:T(8,128)(2,1)}), bf16[4,16,32,768]{3,2,1,0:T(8,128)(2,1)S(1)}, u32[]{:S(2)}, u32[]{:S(2)}) async-start(bf16[4,16,32,768]{3,2,1,0:T(8,128)(2,1)} %broadcast_in_dim.42), calls=%async_computation.1 | async-start | bytes 6291456 | tf_op jit(solution)/shard_map/all_to_all | solution.py:27
  66.1 18.4 %collective-permute-start = (bf16[528,256]{1,0:T(8,128)(2,1)S(1)}, bf16[528,256]{1,0:T(8,128)(2,1)}, u32[]{:S(2)}, u32[]{:S(2)}) collective-permute-start(bf16[528,256]{1,0:T(8,128)(2,1)S(1)} %pad_maximum_fusion.refs_0_), channel_id=1, source_target_pairs={{0,2},{2,4},{4,6},{6,0},{1,3},{3,5},{5,7},{7,1},{8,10},{10,12},{12... | collective-permute-start | bytes 811016 | tf_op jit(solution)/shard_map/ppermute | solution.py:39
  69.2 17.2 %collective-permute-start.1 = (bf16[528,256]{1,0:T(8,128)(2,1)S(1)}, bf16[528,256]{1,0:T(8,128)(2,1)}, u32[]{:S(2)}, u32[]{:S(2)}) collective-permute-start(bf16[528,256]{1,0:T(8,128)(2,1)S(1)} %pad_maximum_fusion.refs_0_), channel_id=1, source_target_pairs={{0,6},{2,0},{4,2},{6,4},{1,7},{3,1},{5,3},{7,5},{8,14},{10,8},{12,... | collective-permute-start | bytes 811016 | tf_op jit(solution)/shard_map/ppermute | solution.py:39
  72.6 16.2 %collective-permute-start.2 = (bf16[528,256]{1,0:T(8,128)(2,1)S(1)}, bf16[528,256]{1,0:T(8,128)(2,1)}, u32[]{:S(2)}, u32[]{:S(2)}) collective-permute-start(bf16[528,256]{1,0:T(8,128)(2,1)S(1)} %pad_maximum_fusion.refs_0_), channel_id=1, source_target_pairs={{0,4},{2,6},{4,0},{6,2},{1,5},{3,7},{5,1},{7,3},{8,12},{10,14},{12... | collective-permute-start | bytes 811016 | tf_op jit(solution)/shard_map/ppermute | solution.py:39
  76.1 14.8 %collective-permute-start.3 = (bf16[528,256]{1,0:T(8,128)(2,1)S(1)}, bf16[528,256]{1,0:T(8,128)(2,1)}, u32[]{:S(2)}, u32[]{:S(2)}) collective-permute-start(bf16[528,256]{1,0:T(8,128)(2,1)S(1)} %pad_maximum_fusion.refs_0_), channel_id=1, source_target_pairs={{0,1},{1,0},{2,3},{3,2},{4,5},{5,4},{6,7},{7,6},{8,9},{9,8},{10,11... | collective-permute-start | bytes 811016 | tf_op jit(solution)/shard_map/ppermute | solution.py:31
  84.5 6.4 %collective-permute-start.4 = (bf16[528,256]{1,0:T(8,128)(2,1)}, bf16[528,256]{1,0:T(8,128)(2,1)}, u32[]{:S(2)}, u32[]{:S(2)}) collective-permute-start(bf16[528,256]{1,0:T(8,128)(2,1)} %collective-permute-done.refs_1_), channel_id=1, source_target_pairs={{0,1},{1,0},{2,3},{3,2},{4,5},{5,4},{6,7},{7,6},{8,9},{9,8},{10,11... | collective-permute-start | bytes 811016 | tf_op jit(solution)/shard_map/ppermute | solution.py:31
  86.4 4.4 %collective-permute-start.5 = (bf16[528,256]{1,0:T(8,128)(2,1)}, bf16[528,256]{1,0:T(8,128)(2,1)}, u32[]{:S(2)}, u32[]{:S(2)}) collective-permute-start(bf16[528,256]{1,0:T(8,128)(2,1)} %collective-permute-done.1.refs_2_), channel_id=1, source_target_pairs={{0,1},{1,0},{2,3},{3,2},{4,5},{5,4},{6,7},{7,6},{8,9},{9,8},{10,11... | collective-permute-start | bytes 811016 | tf_op jit(solution)/shard_map/ppermute | solution.py:31
  88.8 3.8 %collective-permute-start.6 = (bf16[528,256]{1,0:T(8,128)(2,1)}, bf16[528,256]{1,0:T(8,128)(2,1)}, u32[]{:S(2)}, u32[]{:S(2)}) collective-permute-start(bf16[528,256]{1,0:T(8,128)(2,1)} %collective-permute-done.2.refs_3_), channel_id=1, source_target_pairs={{0,1},{1,0},{2,3},{3,2},{4,5},{5,4},{6,7},{7,6},{8,9},{9,8},{10,11... | collective-permute-start | bytes 811016 | tf_op jit(solution)/shard_map/ppermute | solution.py:31
  95.2 1.3 copy-start
  97.1 1.6 copy-start.1
  98.7 13.2 %copy-start.19 = (bf16[256]{0:T(256)(128)(2,1)S(1)}, bf16[256]{0:T(256)(128)(2,1)}, u32[]{:S(2)}) copy-start(bf16[256]{0:T(256)(128)(2,1)} %param.19) | copy-start | bytes 1540
  98.7 13.2 %copy-start.20 = (bf16[256]{0:T(256)(128)(2,1)S(1)}, bf16[256]{0:T(256)(128)(2,1)}, u32[]{:S(2)}) copy-start(bf16[256]{0:T(256)(128)(2,1)} %param.20) | copy-start | bytes 1540
  99.6 0.8 copy-start.6
  101.1 15.6 %all-to-all-start.2 = ((f32[8,2,512]{2,1,0:T(2,128)}), f32[8,2,512]{2,1,0:T(2,128)S(1)}, u32[]{:S(2)}, u32[]{:S(2)}) async-start(f32[8,2,512]{2,1,0:T(2,128)} %broadcast_in_dim.43), calls=%async_computation.2 | async-start | bytes 65536 | tf_op jit(solution)/shard_map/all_to_all | solution.py:27
  111.9 1.6 copy-start.2
  113.5 3.1 %copy-start.8 = (bf16[2,128,128]{2,1,0:T(8,128)(2,1)S(1)}, bf16[2,128,128]{2,1,0:T(8,128)(2,1)}, u32[]{:S(2)}) copy-start(bf16[2,128,128]{2,1,0:T(8,128)(2,1)} %mix.3) | copy-start | bytes 196612
  113.5 3.1 %copy-start.11 = (bf16[2,128]{1,0:T(2,128)(2,1)S(1)}, bf16[2,128]{1,0:T(2,128)(2,1)}, u32[]{:S(2)}) copy-start(bf16[2,128]{1,0:T(2,128)(2,1)} %bias.1) | copy-start | bytes 1540
  114.3 0.8 copy-start.4
  116.7 1.1 copy-start.5
  117.7 1.1 copy-start.7
  119.8 4.8 %collective-permute-start.7 = (bf16[4,512,256]{2,1,0:T(8,128)(2,1)S(1)}, bf16[4,512,256]{2,1,0:T(8,128)(2,1)S(1)}, u32[]{:S(2)}, u32[]{:S(2)}) collective-permute-start(bf16[4,512,256]{2,1,0:T(8,128)(2,1)S(1)} %get-tuple-element.18), channel_id=1, source_target_pairs={{0,1},{1,0},{2,3},{3,2},{4,5},{5,4},{6,7},{7,6},{8,9},{9,8},{10,11... | collective-permute-start | bytes 3145736 | tf_op jit(solution)/shard_map/ppermute | solution.py:31
  124.9 17.5 %copy-start.13 = (bf16[512,256]{1,0:T(8,128)(2,1)S(1)}, bf16[512,256]{1,0:T(8,128)(2,1)}, u32[]{:S(2)}) copy-start(bf16[512,256]{1,0:T(8,128)(2,1)} %param.15) | copy-start | bytes 786436
  142.4 22.8 %copy-start.9 = (bf16[3,512]{1,0:T(4,128)(2,1)S(1)}, bf16[3,512]{1,0:T(4,128)(2,1)}, u32[]{:S(2)}) copy-start(bf16[3,512]{1,0:T(4,128)(2,1)} %conv_gate.1) | copy-start | bytes 9220
  142.4 22.8 %copy-start.10 = (bf16[3,512]{1,0:T(4,128)(2,1)S(1)}, bf16[3,512]{1,0:T(4,128)(2,1)}, u32[]{:S(2)}) copy-start(bf16[3,512]{1,0:T(4,128)(2,1)} %conv_value.1) | copy-start | bytes 9220
  159.0 6.3 %collective-permute-start.8 = (bf16[4,512,256]{2,1,0:T(8,128)(2,1)S(1)}, bf16[4,512,256]{2,1,0:T(8,128)(2,1)S(1)}, u32[]{:S(2)}, u32[]{:S(2)}) collective-permute-start(bf16[4,512,256]{2,1,0:T(8,128)(2,1)S(1)} %all_to_all.31.mine), channel_id=1, source_target_pairs={{0,1},{1,0},{2,3},{3,2},{4,5},{5,4},{6,7},{7,6},{8,9},{9,8},{10,11... | collective-permute-start | bytes 3145736 | tf_op jit(solution)/shard_map/ppermute | solution.py:31
  165.2 2.8 %copy-start.3 = (bf16[2048,1536]{1,0:T(8,128)(2,1)S(1)}, bf16[2048,1536]{1,0:T(8,128)(2,1)}, u32[]{:S(2)}) copy-start(bf16[2048,1536]{1,0:T(8,128)(2,1)} %all-gather.2.cloned.1.call-done.late) | copy-start | bytes 18874372
  173.2 4.6 %collective-permute-start.12 = (bf16[4,512,256]{2,1,0:T(8,128)(2,1)S(1)}, bf16[4,512,256]{2,1,0:T(8,128)(2,1)S(1)}, u32[]{:S(2)}, u32[]{:S(2)}) collective-permute-start(bf16[4,512,256]{2,1,0:T(8,128)(2,1)S(1)} %get-tuple-element.22), channel_id=1, source_target_pairs={{0,1},{1,0},{2,3},{3,2},{4,5},{5,4},{6,7},{7,6},{8,9},{9,8},{10,11... | collective-permute-start | bytes 3145736 | tf_op jit(solution)/shard_map/ppermute | solution.py:31
Sparse Core Ops, SparseCore 0:
  58.8 84.5 all-gather.1

commit v3 on v2

--- a/solution.py
+++ b/solution.py
@@ -17,6 +17,8 @@
 BF16 = jnp.bfloat16
 SWAP = [(0, 1), (1, 0)]
 RING = (0, 1, 3, 2)
+PIECE = 32
+ANY = pl.BlockSpec(memory_space=pl.ANY)
 SQRT_HALF = 0.7071067811865476
 VMEM = pl.BlockSpec(memory_space=pltpu.VMEM)
 SMEM = pl.BlockSpec(memory_space=pltpu.SMEM)
@@ -74,13 +76,17 @@
     return (here + (4 - step)) & 3
 
 
-def stats_kernel(normed, early, act, sums, weight):
-    near = early.shape[0]
-    piece = 32
+def fill_rows(weight, parts, y, cols):
+    for step, part in zip(RING, parts):
+        near = origin(y, step)
+        for far in range(part.shape[0] // PIECE):
+            start = pl.multiple_of((far * 4 + near) * PIECE, PIECE)
+            weight[pl.ds(start, PIECE), :] = part[far * PIECE : (far + 1) * PIECE, cols]
+
+
+def stats_kernel(place, normed, p0, p1, p2, p3, act, sums, weight):
     width = act.shape[1]
-    for far in range(early.shape[1] // piece):
-        for y in range(near):
-            weight[pl.ds((far * near + y) * piece, piece), :] = early[y, pl.ds(far * piece, piece), width : 2 * width]
+    fill_rows(weight, (p0, p1, p2, p3), place[2], slice(width, 2 * width))
     for part in range(normed.shape[0] // SEQ_LEN):
         rows = pl.ds(part * SEQ_LEN, SEQ_LEN)
         value = gelu(jnp.dot(normed[rows, :], weight[...], preferred_element_type=F32))
@@ -91,25 +97,16 @@
         sums[1:2, rows] = jnp.sum(twice.T, axis=0, keepdims=True)
 
 
-def gate_kernel(normed, early, act, weight):
-    near = early.shape[0]
-    piece = 32
-    width = act.shape[1]
-    for far in range(early.shape[1] // piece):
-        for y in range(near):
-            weight[pl.ds((far * near + y) * piece, piece), :] = early[y, pl.ds(far * piece, piece), 0:width]
+def gate_kernel(place, normed, p0, p1, p2, p3, act, weight):
+    fill_rows(weight, (p0, p1, p2, p3), place[2], slice(0, act.shape[1]))
     for part in range(normed.shape[0] // SEQ_LEN):
         rows = pl.ds(part * SEQ_LEN, SEQ_LEN)
         act[rows, :] = gelu(jnp.dot(normed[rows, :], weight[...], preferred_element_type=F32))
 
 
-def mix_kernel(core, act_v, act_u, stats, gain, shift, mix, bias, early, give, keep, weight, gated):
-    near = early.shape[0]
-    piece = 32
+def mix_kernel(place, act_v, act_u, stats, gain, shift, mix, bias, p0, p1, p2, p3, give, keep, weight, gated):
     width = act_v.shape[1]
-    for far in range(early.shape[1] // piece):
-        for y in range(near):
-            weight[pl.ds((far * near + y) * piece, piece), :] = early[y, pl.ds(far * piece, piece), 2 * width : 3 * width]
+    fill_rows(weight, (p0, p1, p2, p3), place[2], slice(0, width))
     full = width * stats.shape[0]
     i = lax.broadcasted_iota(jnp.int32, (BLOCK, BLOCK), 0)
     j = lax.broadcasted_iota(jnp.int32, (BLOCK, BLOCK), 1)
@@ -132,7 +129,7 @@
             seen = jnp.where(visible, mix[g].astype(F32), 0.0).astype(BF16)
             spatial = jnp.dot(seen, mixed, preferred_element_type=F32) + biases[g]
             gated[rows, cols] = (act_u[rows, cols] * spatial).astype(BF16)
-    c = core[0]
+    c = place[1]
     for out, side in ((give, 1 - c), (keep, c)):
         for x in range(out.shape[0]):
             start = pl.multiple_of((2 * x + side) * width, width)
@@ -152,10 +149,16 @@
     return (shifted(value, 2) * weights[0:1] + shifted(value, 1) * weights[1:2]) + value * weights[2:3]
 
 
-def ffn_kernel(core, mine, other, gain, late, conv_gate, conv_value, give, keep, normed, hidden):
+def ffn_kernel(place, mine, other, gain, late_hbm, conv_gate, conv_value, give, keep, normed, hidden, late, done):
     width = mine.shape[2]
     ff = conv_gate.shape[1]
-    c = core[0]
+    c = place[1]
+    copies = [
+        pltpu.make_async_copy(late_hbm.at[:, pl.ds(k * ff, ff)], late.at[:, pl.ds(k * ff, ff)], done.at[k])
+        for k in range(3)
+    ]
+    for copy in copies:
+        copy.start()
     for part in range(mine.shape[1] // SEQ_LEN):
         rows = pl.ds(part * SEQ_LEN, SEQ_LEN)
         squares = jnp.zeros((SEQ_LEN, 1), F32)
@@ -181,11 +184,16 @@
             fill(other, 0)
             fill(mine, 1)
 
+        if part == 0:
+            copies[0].wait()
         gate = jnp.dot(normed[...], late[:, 0:ff], preferred_element_type=F32)
+        if part == 0:
+            copies[1].wait()
         value = jnp.dot(normed[...], late[:, ff : 2 * ff], preferred_element_type=F32)
         conv_g = taps(gate, conv_gate[...].astype(F32))
         conv_v = taps(value, conv_value[...].astype(F32))
         hidden[rows, :] = (conv_g * jax.nn.sigmoid(conv_g) * conv_v).astype(BF16)
+    copies[2].wait()
     for out, side in ((give, 1 - c), (keep, c)):
         for x in range(out.shape[0]):
             start = pl.multiple_of((2 * x + side) * width, width)
@@ -234,19 +242,19 @@
     ff = ffn_gate.shape[1]
     row_count = tokens.shape[0]
 
-    early = jnp.concatenate([proj_u, proj_v, proj_out.T], axis=1)
-    early_z = everyones(early, "z")
+    early = jnp.concatenate([proj_u, proj_v], axis=1)
+    early_z = everyones(early, "z").reshape(-1, early.shape[1])
     late = jnp.concatenate([ffn_gate, ffn_value, proj_down.T], axis=1)
     late_y = in_order(round_ring(late, "y"), "y").reshape(-1, late.shape[1])
     late_all = lax.all_gather(after(late_y, early_z), "z", axis=0, tiled=True)
 
     packed = jnp.concatenate([tokens, jnp.broadcast_to(norm_gain, (8, da)), jnp.broadcast_to(ffn_gain, (8, da))], axis=0)
     mine = round_ring(packed, "x")
+    early_parts = round_ring(early_z, "y")
+    out_z = everyones(proj_out.T, "z").reshape(-1, da)
     other = [other_core(part) for part in mine]
-    early_all = everyones(early_z, "y").reshape(4, -1, early.shape[1])
-    core = lax.axis_index("c").astype(jnp.int32)
-    place = jnp.stack([lax.axis_index("x").astype(jnp.int32), core])
-    core = core.reshape(1)
+    out_parts = round_ring(out_z, "y")
+    place = jnp.stack([lax.axis_index(name).astype(jnp.int32) for name in ("x", "c", "y")])
     model = proj_u.shape[0] * lax.axis_size(FS)
     tp = lax.axis_size(TP)
     normed, gain_two = pl.pallas_call(
@@ -260,34 +268,34 @@
 
     act_v, sums = pl.pallas_call(
         stats_kernel,
-        in_specs=[VMEM] * 2,
+        in_specs=[SMEM] + [VMEM] * 5,
         out_specs=[VMEM] * 2,
         out_shape=[shape((row_count, da), F32), shape((2, row_count), F32)],
         scratch_shapes=[pltpu.VMEM((model, da), BF16)],
         name="stats",
         compiler_params=room(14),
-    )(normed, early_all)
+    )(place, normed, *early_parts)
     stats = everyones(sums, TP)
     act_u = pl.pallas_call(
         gate_kernel,
-        in_specs=[VMEM] * 2,
+        in_specs=[SMEM] + [VMEM] * 5,
         out_specs=VMEM,
         out_shape=shape((row_count, da), F32),
         scratch_shapes=[pltpu.VMEM((model, da), BF16)],
         name="gate",
         compiler_params=room(14),
-    )(normed, early_all)
+    )(place, normed, *early_parts)
     blocks = [shape((lax.axis_size("x"), row_count, da), BF16)] * 2
     give, keep = pl.pallas_call(
         mix_kernel,
-        in_specs=[SMEM] + [VMEM] * 8,
+        in_specs=[SMEM] + [VMEM] * 11,
         out_specs=[VMEM] * 2,
         out_shape=blocks,
         scratch_shapes=[pltpu.VMEM((model, da), BF16), pltpu.VMEM((row_count, da), BF16)],
         name="mix",
         compiler_params=room(16),
     )(
-        core,
+        place,
         act_v,
         act_u,
         stats,
@@ -295,20 +303,20 @@
         layer_shift[None],
         mix_weight,
         mix_bias,
-        early_all,
+        *out_parts,
     )
     stream = (tokens.astype(F32) + summed_at_owner(give, keep)).astype(BF16)
     mine = everyones(stream, "x")
     give, keep = pl.pallas_call(
         ffn_kernel,
-        in_specs=[SMEM] + [VMEM] * 6,
+        in_specs=[SMEM] + [VMEM] * 3 + [ANY] + [VMEM] * 2,
         out_specs=[VMEM] * 2,
         out_shape=blocks,
-        scratch_shapes=[pltpu.VMEM((SEQ_LEN, model), BF16), pltpu.VMEM((row_count, ff), BF16)],
+        scratch_shapes=[pltpu.VMEM((SEQ_LEN, model), BF16), pltpu.VMEM((row_count, ff), BF16), pltpu.VMEM(late_all.shape, BF16), pltpu.SemaphoreType.DMA((3,))],
         name="ffn",
         compiler_params=room(26),
     )(
-        core,
+        place,
         mine,
         other_core(mine),
         gain_two,

time: 205 us -> 219 us (1.068)
  starting transfers between devices: 74.4 us -> 93.2 us
  waiting for transfers between devices: 35.1 us -> 20.6 us
  local copies, waits for them, and re-layouts: 14.9 us -> 20.5 us
  Pallas kernels: 10.4 us -> 14.6 us
    ppermute x6 -> x12, starting transfers between devices: 20 us -> 38.6 us  [round_ring(): lax.ppermute(shard, axis, [(i, (i + step) % 4) for i in range(4)])]
    all_to_all x3, waiting for transfers between devices: 23 us -> 10.3 us  [everyones(): return lax.all_to_all(copies, axis, split_axis=0, concat_axis=0, tiled=True)]
    unnamed x42 -> x68, local copies, waits for them, and re-layouts: 11 us -> 18.2 us
    pallas_call x4, Pallas kernels: 7.86 us -> 13 us  [the longest x1 6.58 us: on_device(): pl.pallas_call(ffn_kernel, in_specs=[SMEM] + [VMEM] * 3 + [ANY] + [VMEM]...]
    all_to_all x3, starting transfers between devices: 30.9 us -> 35 us  [everyones(): return lax.all_to_all(copies, axis, split_axis=0, concat_axis=0, tiled=True)]
    ppermute x7, starting transfers between devices: 23.5 us -> 19.6 us  [other_core(): return lax.ppermute(value, 'c', SWAP)]
  transfers between devices with their start and end apart: 17 -> 23, of which waited for: 8 -> 6; matrix products, arithmetic and copies ran while one was open for 2% -> 1% of each run, Pallas kernels for 3% -> 4%
where the time goes in v3:
time: 219 us; the launch traced here: 217 us
  starting transfers between devices  93.2 us (43%)
  blocking collectives  51 us (23%)
  waiting for transfers between devices  20.6 us (9%)
  local copies, waits for them, and re-layouts  20.5 us (9%)
  Pallas kernels  14.6 us (7%)
  between operations  14 us (6%)
  other arithmetic  3.32 us (2%)
    ppermute x12, starting transfers between devices, round_ring(): lax.ppermute(shard, axis, [(i, (i + step) % 4) for i in range(4)])  38.6 us
    all_to_all x3, starting transfers between devices, everyones(): return lax.all_to_all(copies, axis, split_axis=0, concat_axis=0, tiled=True)  35 us
    all_to_all x2, blocking collectives, summed_at_owner(): arrived = lax.all_to_all(pair, 'x', split_axis=0, concat_axis=0, tiled=True)  34.6 us
    ppermute x7, starting transfers between devices, other_core(): return lax.ppermute(value, 'c', SWAP)  19.6 us
    unnamed x68, local copies, waits for them, and re-layouts  18.2 us
    all_to_all x1, blocking collectives, everyones(): return lax.all_to_all(copies, axis, split_axis=0, concat_axis=0, tiled=True)  16.4 us
    all_to_all x3, waiting for transfers between devices, everyones(): return lax.all_to_all(copies, axis, split_axis=0, concat_axis=0, tiled=True)  10.3 us
    ppermute x7, waiting for transfers between devices, other_core(): return lax.ppermute(value, 'c', SWAP)  6.82 us
  transfers between devices with their start and end apart: 23, of which 6 were waited for; matrix products, arithmetic and copies ran while one was open for 1% of the time, Pallas kernels for 4%

profile of v3, /device:TPU:1, one launch (start us, length us, event | category | flops | bytes accessed | tf_op | source)
XLA Modules:
  0.0 217.3 jit_solution(16442684963679088689)
XLA Ops:
  6.5 0.8 pad_maximum_fusion.2
  7.3 0.9 broadcast_in_dim.41
  8.2 15.7 %all-to-all-start = ((bf16[16,32,512]{2,1,0:T(8,128)(2,1)}), bf16[16,32,512]{2,1,0:T(8,128)(2,1)S(1)}, u32[]{:S(2)}, u32[]{:S(2)}) async-start(bf16[16,32,512]{2,1,0:T(8,128)(2,1)} %broadcast_in_dim.41), calls=%async_computation | async-start | bytes 1048576 | tf_op jit(solution)/shard_map/all_to_all | solution.py:29
  24.0 0.8 pad_maximum_fusion.1
  24.8 3.2 %collective-permute-start.15 = (bf16[32,1536]{1,0:T(8,128)(2,1)S(1)}, bf16[32,1536]{1,0:T(8,128)(2,1)S(1)}, u32[]{:S(2)}, u32[]{:S(2)}) collective-permute-start(bf16[32,1536]{1,0:T(8,128)(2,1)S(1)} %pad_maximum_fusion.1), channel_id=1, source_target_pairs={{0,8},{8,16},{16,24},{24,0},{1,9},{9,17},{17,25},{25,1},{2,10},{10... | collective-permute-start | bytes 294920 | tf_op jit(solution)/shard_map/ppermute | solution.py:41
  28.0 3.4 %collective-permute-start.16 = (bf16[32,1536]{1,0:T(8,128)(2,1)S(1)}, bf16[32,1536]{1,0:T(8,128)(2,1)S(1)}, u32[]{:S(2)}, u32[]{:S(2)}) collective-permute-start(bf16[32,1536]{1,0:T(8,128)(2,1)S(1)} %pad_maximum_fusion.1), channel_id=1, source_target_pairs={{0,24},{8,0},{16,8},{24,16},{1,25},{9,1},{17,9},{25,17},{2,26},{10... | collective-permute-start | bytes 294920 | tf_op jit(solution)/shard_map/ppermute | solution.py:41
  31.3 3.5 %collective-permute-start.17 = (bf16[32,1536]{1,0:T(8,128)(2,1)S(1)}, bf16[32,1536]{1,0:T(8,128)(2,1)S(1)}, u32[]{:S(2)}, u32[]{:S(2)}) collective-permute-start(bf16[32,1536]{1,0:T(8,128)(2,1)S(1)} %pad_maximum_fusion.1), channel_id=1, source_target_pairs={{0,16},{8,24},{16,0},{24,8},{1,17},{9,25},{17,1},{25,9},{2,18},{10... | collective-permute-start | bytes 294920 | tf_op jit(solution)/shard_map/ppermute | solution.py:41
  35.0 3.4 %collective-permute-done.17 = bf16[32,1536]{1,0:T(8,128)(2,1)S(1)} collective-permute-done((bf16[32,1536]{1,0:T(8,128)(2,1)S(1)}, bf16[32,1536]{1,0:T(8,128)(2,1)S(1)}, u32[]{:S(2)}, u32[]{:S(2)}) %collective-permute-start.17) | collective-permute-done | bytes 98336 | tf_op jit(solution)/shard_map/ppermute | solution.py:41
  38.5 8.4 %all-to-all-done = bf16[16,32,512]{2,1,0:T(8,128)(2,1)S(1)} async-done(((bf16[16,32,512]{2,1,0:T(8,128)(2,1)}), bf16[16,32,512]{2,1,0:T(8,128)(2,1)S(1)}, u32[]{:S(2)}, u32[]{:S(2)}) %all-to-all-start) | async-done | bytes 524320 | tf_op jit(solution)/shard_map/all_to_all | solution.py:29
  47.0 0.7 broadcast_in_dim.45
  47.7 12.5 %all-to-all-start.2 = ((bf16[16,32,256]{2,1,0:T(8,128)(2,1)}), bf16[16,32,256]{2,1,0:T(8,128)(2,1)}, u32[]{:S(2)}, u32[]{:S(2)}) async-start(bf16[16,32,256]{2,1,0:T(8,128)(2,1)} %broadcast_in_dim.45), calls=%async_computation.2 | async-start | bytes 524288 | tf_op jit(solution)/shard_map/all_to_all | solution.py:29
  60.2 3.1 %collective-permute-start = (bf16[528,256]{1,0:T(8,128)(2,1)S(1)}, bf16[528,256]{1,0:T(8,128)(2,1)S(1)}, u32[]{:S(2)}, u32[]{:S(2)}) collective-permute-start(bf16[528,256]{1,0:T(8,128)(2,1)S(1)} %pad_maximum_fusion.refs_0_), channel_id=1, source_target_pairs={{0,2},{2,4},{4,6},{6,0},{1,3},{3,5},{5,7},{7,1},{8,10},{10,12},{12... | collective-permute-start | bytes 811016 | tf_op jit(solution)/shard_map/ppermute | solution.py:41
  63.4 3.4 %collective-permute-start.1 = (bf16[528,256]{1,0:T(8,128)(2,1)S(1)}, bf16[528,256]{1,0:T(8,128)(2,1)S(1)}, u32[]{:S(2)}, u32[]{:S(2)}) collective-permute-start(bf16[528,256]{1,0:T(8,128)(2,1)S(1)} %pad_maximum_fusion.refs_0_), channel_id=1, source_target_pairs={{0,6},{2,0},{4,2},{6,4},{1,7},{3,1},{5,3},{7,5},{8,14},{10,8},{12,... | collective-permute-start | bytes 811016 | tf_op jit(solution)/shard_map/ppermute | solution.py:41
  66.7 3.4 %collective-permute-start.2 = (bf16[528,256]{1,0:T(8,128)(2,1)S(1)}, bf16[528,256]{1,0:T(8,128)(2,1)S(1)}, u32[]{:S(2)}, u32[]{:S(2)}) collective-permute-start(bf16[528,256]{1,0:T(8,128)(2,1)S(1)} %pad_maximum_fusion.refs_0_), channel_id=1, source_target_pairs={{0,4},{2,6},{4,0},{6,2},{1,5},{3,7},{5,1},{7,3},{8,12},{10,14},{12... | collective-permute-start | bytes 811016 | tf_op jit(solution)/shard_map/ppermute | solution.py:41
  70.2 3.7 %collective-permute-start.3 = (bf16[528,256]{1,0:T(8,128)(2,1)S(1)}, bf16[528,256]{1,0:T(8,128)(2,1)S(1)}, u32[]{:S(2)}, u32[]{:S(2)}) collective-permute-start(bf16[528,256]{1,0:T(8,128)(2,1)S(1)} %pad_maximum_fusion.refs_0_), channel_id=1, source_target_pairs={{0,1},{1,0},{2,3},{3,2},{4,5},{5,4},{6,7},{7,6},{8,9},{9,8},{10,11... | collective-permute-start | bytes 811016 | tf_op jit(solution)/shard_map/ppermute | solution.py:33
  73.9 1.9 collective-permute-start.4
  75.8 0.7 copy-done.5
  76.5 3.2 %collective-permute-start.7 = (bf16[512,512]{1,0:T(8,128)(2,1)S(1)}, bf16[512,512]{1,0:T(8,128)(2,1)S(1)}, u32[]{:S(2)}, u32[]{:S(2)}) collective-permute-start(bf16[512,512]{1,0:T(8,128)(2,1)S(1)} %bitcast.16), channel_id=1, source_target_pairs={{0,8},{8,16},{16,24},{24,0},{1,9},{9,17},{17,25},{25,1},{2,10},{10... | collective-permute-start | bytes 1572872 | tf_op jit(solution)/shard_map/ppermute | solution.py:41
  79.7 3.4 %collective-permute-start.8 = (bf16[512,512]{1,0:T(8,128)(2,1)S(1)}, bf16[512,512]{1,0:T(8,128)(2,1)}, u32[]{:S(2)}, u32[]{:S(2)}) collective-permute-start(bf16[512,512]{1,0:T(8,128)(2,1)S(1)} %bitcast.17), channel_id=1, source_target_pairs={{0,24},{8,0},{16,8},{24,16},{1,25},{9,1},{17,9},{25,17},{2,26},{10... | collective-permute-start | bytes 1572872 | tf_op jit(solution)/shard_map/ppermute | solution.py:41
  83.1 3.5 %collective-permute-start.9 = (bf16[512,512]{1,0:T(8,128)(2,1)S(1)}, bf16[512,512]{1,0:T(8,128)(2,1)}, u32[]{:S(2)}, u32[]{:S(2)}) collective-permute-start(bf16[512,512]{1,0:T(8,128)(2,1)S(1)} %bitcast.18), channel_id=1, source_target_pairs={{0,16},{8,24},{16,0},{24,8},{1,17},{9,25},{17,1},{25,9},{2,18},{10... | collective-permute-start | bytes 1572872 | tf_op jit(solution)/shard_map/ppermute | solution.py:41
  86.7 0.7 copy-done.11
  87.4 3.2 %collective-permute-start.5 = (bf16[528,256]{1,0:T(8,128)(2,1)S(1)}, bf16[528,256]{1,0:T(8,128)(2,1)S(1)}, u32[]{:S(2)}, u32[]{:S(2)}) collective-permute-start(bf16[528,256]{1,0:T(8,128)(2,1)S(1)} %collective-permute-done.1.refs_2_), channel_id=1, source_target_pairs={{0,1},{1,0},{2,3},{3,2},{4,5},{5,4},{6,7},{7,6},{8,9},{9,8},{10,11... | collective-permute-start | bytes 811016 | tf_op jit(solution)/shard_map/ppermute | solution.py:33
  90.6 0.7 copy-done.7
  91.3 0.7 copy-done.13
  92.0 1.9 collective-permute-start.6
  94.0 0.7 copy-done.9
  94.7 0.7 copy-done.15
  95.4 2.3 %collective-permute-start.10 = (bf16[512,256]{1,0:T(8,128)(2,1)}, bf16[512,256]{1,0:T(8,128)(2,1)}, u32[]{:S(2)}, u32[]{:S(2)}) collective-permute-start(bf16[512,256]{1,0:T(8,128)(2,1)} %bitcast.5.p0), channel_id=1, source_target_pairs={{0,8},{8,16},{16,24},{24,0},{1,9},{9,17},{17,25},{25,1},{2,10},{10... | collective-permute-start | bytes 786440 | tf_op jit(solution)/shard_map/ppermute | solution.py:41
  97.7 0.7 copy-done.17
  98.4 4.2 %collective-permute-start.11 = (bf16[512,256]{1,0:T(8,128)(2,1)}, bf16[512,256]{1,0:T(8,128)(2,1)}, u32[]{:S(2)}, u32[]{:S(2)}) collective-permute-start(bf16[512,256]{1,0:T(8,128)(2,1)} %bitcast.5.p0), channel_id=1, source_target_pairs={{0,24},{8,0},{16,8},{24,16},{1,25},{9,1},{17,9},{25,17},{2,26},{10... | collective-permute-start | bytes 786440 | tf_op jit(solution)/shard_map/ppermute | solution.py:41
  102.6 2.0 collective-permute-start.12
  104.7 1.0 copy-done.6
  105.7 1.0 copy-done.8
  106.7 1.0 copy-done.10
  107.6 1.0 copy-done.12
  108.6 1.0 copy-done.14
  109.5 1.0 copy-done.16
  110.5 1.0 copy-done.18
  111.4 1.6 norm.1
  113.1 2.2 stats.1
  115.2 0.8 copy-done.3
  116.0 0.6 broadcast_in_dim.42
  116.6 6.8 %all-to-all-start.1 = ((f32[8,2,512]{2,1,0:T(2,128)}), f32[8,2,512]{2,1,0:T(2,128)S(1)}, u32[]{:S(2)}, u32[]{:S(2)}) async-start(f32[8,2,512]{2,1,0:T(2,128)} %broadcast_in_dim.42), calls=%async_computation.1 | async-start | bytes 65536 | tf_op jit(solution)/shard_map/all_to_all | solution.py:29
  123.5 2.0 gate.1.act_u
  125.5 0.8 copy-done.1
  126.3 1.9 all-to-all-done.1.stats
  128.2 1.1 copy-done.2
  129.3 1.0 copy-done.4
  130.3 2.2 %mix.2 = (bf16[4,512,256]{2,1,0:T(8,128)(2,1)S(1)}, bf16[4,512,256]{2,1,0:T(8,128)(2,1)S(1)}) custom-call(s32[3]{0:T(128)S(1)} %pad_add_fusion.place, f32[512,256]{1,0:T(8,128)S(1)} %copy-done.4, f32[512,256]{1,0:T(8,128)S(1)} %copy-done.2, f32[8,2,512]{2,1,0:T(2,128)S(1)} %all-to-all-done.1.stats, bf16[1,256]{1,0:T(2,128)(2,1)S(1)} %broadcast_in_dim.43.gain, ...), custom_call_target="tpu_custom_call" | custom-call | tf_op jit(solution)/shard_map/mix/pallas_call | solution.py:289
  132.6 2.6 %collective-permute-start.13 = (bf16[4,512,256]{2,1,0:T(8,128)(2,1)S(1)}, bf16[4,512,256]{2,1,0:T(8,128)(2,1)S(1)}, u32[]{:S(2)}, u32[]{:S(2)}) collective-permute-start(bf16[4,512,256]{2,1,0:T(8,128)(2,1)S(1)} %get-tuple-element.18), channel_id=1, source_target_pairs={{0,1},{1,0},{2,3},{3,2},{4,5},{5,4},{6,7},{7,6},{8,9},{9,8},{10,11... | collective-permute-start | bytes 3145736 | tf_op jit(solution)/shard_map/ppermute | solution.py:33
  135.2 2.3 %collective-permute-done.13 = bf16[4,512,256]{2,1,0:T(8,128)(2,1)S(1)} collective-permute-done((bf16[4,512,256]{2,1,0:T(8,128)(2,1)S(1)}, bf16[4,512,256]{2,1,0:T(8,128)(2,1)S(1)}, u32[]{:S(2)}, u32[]{:S(2)}) %collective-permute-start.13) | collective-permute-done | bytes 1048608 | tf_op jit(solution)/shard_map/ppermute | solution.py:33
  137.4 0.2 add_convert_fusion.1
  137.7 17.4 %all_to_all.30 = bf16[4,512,256]{2,1,0:T(8,128)(2,1)S(1)} all-to-all(bf16[4,512,256]{2,1,0:T(8,128)(2,1)S(1)} %add_convert_fusion.1), channel_id=1, replica_groups=mesh['z'=16,'y'=4,'x'=4,'c'=2] {'x'}, dimensions={0} | all-to-all | bytes 2097152 | tf_op jit(solution)/shard_map/all_to_all | solution.py:220
  155.4 16.4 %all_to_all.31.mine = bf16[4,512,256]{2,1,0:T(8,128)(2,1)S(1)} all-to-all(bf16[4,512,256]{2,1,0:T(8,128)(2,1)S(1)} %broadcast_in_dim.46), channel_id=1, replica_groups=mesh['z'=16,'y'=4,'x'=4,'c'=2] {'x'}, dimensions={0} | all-to-all | bytes 2097152 | tf_op jit(solution)/shard_map/all_to_all | solution.py:29
  171.8 4.0 %collective-permute-start.14 = (bf16[4,512,256]{2,1,0:T(8,128)(2,1)S(1)}, bf16[4,512,256]{2,1,0:T(8,128)(2,1)S(1)}, u32[]{:S(2)}, u32[]{:S(2)}) collective-permute-start(bf16[4,512,256]{2,1,0:T(8,128)(2,1)S(1)} %all_to_all.31.mine), channel_id=1, source_target_pairs={{0,1},{1,0},{2,3},{3,2},{4,5},{5,4},{6,7},{7,6},{8,9},{9,8},{10,11... | collective-permute-start | bytes 3145736 | tf_op jit(solution)/shard_map/ppermute | solution.py:33
  175.8 2.3 %collective-permute-done.14.other = bf16[4,512,256]{2,1,0:T(8,128)(2,1)S(1)} collective-permute-done((bf16[4,512,256]{2,1,0:T(8,128)(2,1)S(1)}, bf16[4,512,256]{2,1,0:T(8,128)(2,1)S(1)}, u32[]{:S(2)}, u32[]{:S(2)}) %collective-permute-start.14) | collective-permute-done | bytes 1048608 | tf_op jit(solution)/shard_map/ppermute | solution.py:33
  178.1 2.8 %copy-done = bf16[2048,1536]{1,0:T(8,128)(2,1)S(1)} copy-done((bf16[2048,1536]{1,0:T(8,128)(2,1)S(1)}, bf16[2048,1536]{1,0:T(8,128)(2,1)}, u32[]{:S(2)}) %copy-start) | copy-done | bytes 6291480
  180.8 6.6 %ffn.1 = (bf16[4,512,256]{2,1,0:T(8,128)(2,1)S(1)}, bf16[4,512,256]{2,1,0:T(8,128)(2,1)S(1)}) custom-call(s32[3]{0:T(128)S(1)} %pad_add_fusion.place, bf16[4,512,256]{2,1,0:T(8,128)(2,1)S(1)} %all_to_all.31.mine, bf16[4,512,256]{2,1,0:T(8,128)(2,1)S(1)} %collective-permute-done.14.other, bf16[8,8,256]{2,1,0:T(8,128)(2,1)S(1)} %get-tuple-element.19.gain, ...), custom_call_target="tpu_custom_call" | custom-call | tf_op jit(solution)/shard_map/ffn/pallas_call | solution.py:310
  187.4 2.3 %collective-permute-start.18 = (bf16[4,512,256]{2,1,0:T(8,128)(2,1)S(1)}, bf16[4,512,256]{2,1,0:T(8,128)(2,1)S(1)}, u32[]{:S(2)}, u32[]{:S(2)}) collective-permute-start(bf16[4,512,256]{2,1,0:T(8,128)(2,1)S(1)} %get-tuple-element.22), channel_id=1, source_target_pairs={{0,1},{1,0},{2,3},{3,2},{4,5},{5,4},{6,7},{7,6},{8,9},{9,8},{10,11... | collective-permute-start | bytes 3145736 | tf_op jit(solution)/shard_map/ppermute | solution.py:33
  189.7 2.3 %collective-permute-done.18 = bf16[4,512,256]{2,1,0:T(8,128)(2,1)S(1)} collective-permute-done((bf16[4,512,256]{2,1,0:T(8,128)(2,1)S(1)}, bf16[4,512,256]{2,1,0:T(8,128)(2,1)S(1)}, u32[]{:S(2)}, u32[]{:S(2)}) %collective-permute-start.18) | collective-permute-done | bytes 1048608 | tf_op jit(solution)/shard_map/ppermute | solution.py:33
  192.0 0.3 add_convert_fusion
  192.3 17.3 %all_to_all.32 = bf16[4,512,256]{2,1,0:T(8,128)(2,1)S(1)} all-to-all(bf16[4,512,256]{2,1,0:T(8,128)(2,1)S(1)} %add_convert_fusion), channel_id=1, replica_groups=mesh['z'=16,'y'=4,'x'=4,'c'=2] {'x'}, dimensions={0} | all-to-all | bytes 2097152 | tf_op jit(solution)/shard_map/all_to_all | solution.py:220
  209.5 0.1 convert_reduce_fusion
  209.7 0.8 add_convert_fusion.2
  (82 shorter events, 0.7 us)
Async XLA Ops:
  6.5 28.4 %copy-start.26 = (bf16[512,32]{0,1:T(8,128)(2,1)S(1)}, bf16[512,32]{0,1:T(8,128)(2,1)}, u32[]{:S(2)}) copy-start(bf16[512,32]{0,1:T(8,128)(2,1)} %param.29) | copy-start | bytes 98308
  6.5 28.4 %copy-start.28 = (bf16[32,512]{1,0:T(8,128)(2,1)S(1)}, bf16[32,512]{1,0:T(8,128)(2,1)}, u32[]{:S(2)}) copy-start(bf16[32,512]{1,0:T(8,128)(2,1)} %param.25) | copy-start | bytes 98308
  6.5 28.4 %copy-start.27 = (bf16[32,512]{1,0:T(8,128)(2,1)S(1)}, bf16[32,512]{1,0:T(8,128)(2,1)}, u32[]{:S(2)}) copy-start(bf16[32,512]{1,0:T(8,128)(2,1)} %param.26) | copy-start | bytes 98308
  6.5 40.4 %copy-start.29 = (bf16[256,32]{0,1:T(8,128)(2,1)S(1)}, bf16[256,32]{0,1:T(8,128)(2,1)}, u32[]{:S(2)}) copy-start(bf16[256,32]{0,1:T(8,128)(2,1)} %param.23) | copy-start | bytes 49156
  7.3 52.9 %copy-start.30 = (bf16[256]{0:T(256)(128)(2,1)S(1)}, bf16[256]{0:T(256)(128)(2,1)}, u32[]{:S(2)}) copy-start(bf16[256]{0:T(256)(128)(2,1)} %param.16) | copy-start | bytes 1540
  7.3 52.9 %copy-start.31 = (bf16[256]{0:T(256)(128)(2,1)S(1)}, bf16[256]{0:T(256)(128)(2,1)}, u32[]{:S(2)}) copy-start(bf16[256]{0:T(256)(128)(2,1)} %param.24) | copy-start | bytes 1540
  7.3 52.9 %copy-start.24 = (bf16[512,256]{1,0:T(8,128)(2,1)S(1)}, bf16[512,256]{1,0:T(8,128)(2,1)}, u32[]{:S(2)}) copy-start(bf16[512,256]{1,0:T(8,128)(2,1)} %param.15) | copy-start | bytes 786436
  8.2 38.7 %all-to-all-start = ((bf16[16,32,512]{2,1,0:T(8,128)(2,1)}), bf16[16,32,512]{2,1,0:T(8,128)(2,1)S(1)}, u32[]{:S(2)}, u32[]{:S(2)}) async-start(bf16[16,32,512]{2,1,0:T(8,128)(2,1)} %broadcast_in_dim.41), calls=%async_computation | async-start | bytes 1048576 | tf_op jit(solution)/shard_map/all_to_all | solution.py:29
  23.9 154.1 %all-gather.2.cloned.1.call-start = ((), (), s32[]{:S(2)}) async-start(), calls=%async_computation.6 | async-start | bytes 6684672 | tf_op jit(solution)/shard_map/all_gather | solution.py:249
  24.8 10.2 %collective-permute-start.15 = (bf16[32,1536]{1,0:T(8,128)(2,1)S(1)}, bf16[32,1536]{1,0:T(8,128)(2,1)S(1)}, u32[]{:S(2)}, u32[]{:S(2)}) collective-permute-start(bf16[32,1536]{1,0:T(8,128)(2,1)S(1)} %pad_maximum_fusion.1), channel_id=1, source_target_pairs={{0,8},{8,16},{16,24},{24,0},{1,9},{9,17},{17,25},{25,1},{2,10},{10... | collective-permute-start | bytes 294920 | tf_op jit(solution)/shard_map/ppermute | solution.py:41
  28.0 7.1 %collective-permute-start.16 = (bf16[32,1536]{1,0:T(8,128)(2,1)S(1)}, bf16[32,1536]{1,0:T(8,128)(2,1)S(1)}, u32[]{:S(2)}, u32[]{:S(2)}) collective-permute-start(bf16[32,1536]{1,0:T(8,128)(2,1)S(1)} %pad_maximum_fusion.1), channel_id=1, source_target_pairs={{0,24},{8,0},{16,8},{24,16},{1,25},{9,1},{17,9},{25,17},{2,26},{10... | collective-permute-start | bytes 294920 | tf_op jit(solution)/shard_map/ppermute | solution.py:41
  31.3 7.2 %collective-permute-start.17 = (bf16[32,1536]{1,0:T(8,128)(2,1)S(1)}, bf16[32,1536]{1,0:T(8,128)(2,1)S(1)}, u32[]{:S(2)}, u32[]{:S(2)}) collective-permute-start(bf16[32,1536]{1,0:T(8,128)(2,1)S(1)} %pad_maximum_fusion.1), channel_id=1, source_target_pairs={{0,16},{8,24},{16,0},{24,8},{1,17},{9,25},{17,1},{25,9},{2,18},{10... | collective-permute-start | bytes 294920 | tf_op jit(solution)/shard_map/ppermute | solution.py:41
  38.5 8.4 %copy-start.23 = (bf16[4,32,1536]{2,1,0:T(8,128)(2,1)}, bf16[4,32,1536]{2,1,0:T(8,128)(2,1)S(1)}, u32[]{:S(2)}) copy-start(bf16[4,32,1536]{2,1,0:T(8,128)(2,1)S(1)} %bitcast_dynamic-update-slice_fusion) | copy-start | bytes 1179652
  47.7 47.7 %all-to-all-start.2 = ((bf16[16,32,256]{2,1,0:T(8,128)(2,1)}), bf16[16,32,256]{2,1,0:T(8,128)(2,1)}, u32[]{:S(2)}, u32[]{:S(2)}) async-start(bf16[16,32,256]{2,1,0:T(8,128)(2,1)} %broadcast_in_dim.45), calls=%async_computation.2 | async-start | bytes 524288 | tf_op jit(solution)/shard_map/all_to_all | solution.py:29
  60.2 13.7 %collective-permute-start = (bf16[528,256]{1,0:T(8,128)(2,1)S(1)}, bf16[528,256]{1,0:T(8,128)(2,1)S(1)}, u32[]{:S(2)}, u32[]{:S(2)}) collective-permute-start(bf16[528,256]{1,0:T(8,128)(2,1)S(1)} %pad_maximum_fusion.refs_0_), channel_id=1, source_target_pairs={{0,2},{2,4},{4,6},{6,0},{1,3},{3,5},{5,7},{7,1},{8,10},{10,12},{12... | collective-permute-start | bytes 811016 | tf_op jit(solution)/shard_map/ppermute | solution.py:41
  63.4 16.4 %collective-permute-start.1 = (bf16[528,256]{1,0:T(8,128)(2,1)S(1)}, bf16[528,256]{1,0:T(8,128)(2,1)S(1)}, u32[]{:S(2)}, u32[]{:S(2)}) collective-permute-start(bf16[528,256]{1,0:T(8,128)(2,1)S(1)} %pad_maximum_fusion.refs_0_), channel_id=1, source_target_pairs={{0,6},{2,0},{4,2},{6,4},{1,7},{3,1},{5,3},{7,5},{8,14},{10,8},{12,... | collective-permute-start | bytes 811016 | tf_op jit(solution)/shard_map/ppermute | solution.py:41
  66.7 16.4 %collective-permute-start.2 = (bf16[528,256]{1,0:T(8,128)(2,1)S(1)}, bf16[528,256]{1,0:T(8,128)(2,1)S(1)}, u32[]{:S(2)}, u32[]{:S(2)}) collective-permute-start(bf16[528,256]{1,0:T(8,128)(2,1)S(1)} %pad_maximum_fusion.refs_0_), channel_id=1, source_target_pairs={{0,4},{2,6},{4,0},{6,2},{1,5},{3,7},{5,1},{7,3},{8,12},{10,14},{12... | collective-permute-start | bytes 811016 | tf_op jit(solution)/shard_map/ppermute | solution.py:41
  70.2 16.5 %collective-permute-start.3 = (bf16[528,256]{1,0:T(8,128)(2,1)S(1)}, bf16[528,256]{1,0:T(8,128)(2,1)S(1)}, u32[]{:S(2)}, u32[]{:S(2)}) collective-permute-start(bf16[528,256]{1,0:T(8,128)(2,1)S(1)} %pad_maximum_fusion.refs_0_), channel_id=1, source_target_pairs={{0,1},{1,0},{2,3},{3,2},{4,5},{5,4},{6,7},{7,6},{8,9},{9,8},{10,11... | collective-permute-start | bytes 811016 | tf_op jit(solution)/shard_map/ppermute | solution.py:33
  73.9 17.4 %collective-permute-start.4 = (bf16[528,256]{1,0:T(8,128)(2,1)S(1)}, bf16[528,256]{1,0:T(8,128)(2,1)S(1)}, u32[]{:S(2)}, u32[]{:S(2)}) collective-permute-start(bf16[528,256]{1,0:T(8,128)(2,1)S(1)} %collective-permute-done.refs_1_), channel_id=1, source_target_pairs={{0,1},{1,0},{2,3},{3,2},{4,5},{5,4},{6,7},{7,6},{8,9},{9,8},{10,11... | collective-permute-start | bytes 811016 | tf_op jit(solution)/shard_map/ppermute | solution.py:33
  75.8 0.7 copy-start.5
  76.5 26.1 %collective-permute-start.7 = (bf16[512,512]{1,0:T(8,128)(2,1)S(1)}, bf16[512,512]{1,0:T(8,128)(2,1)S(1)}, u32[]{:S(2)}, u32[]{:S(2)}) collective-permute-start(bf16[512,512]{1,0:T(8,128)(2,1)S(1)} %bitcast.16), channel_id=1, source_target_pairs={{0,8},{8,16},{16,24},{24,0},{1,9},{9,17},{17,25},{25,1},{2,10},{10... | collective-permute-start | bytes 1572872 | tf_op jit(solution)/shard_map/ppermute | solution.py:41
  79.7 33.3 %collective-permute-start.8 = (bf16[512,512]{1,0:T(8,128)(2,1)S(1)}, bf16[512,512]{1,0:T(8,128)(2,1)}, u32[]{:S(2)}, u32[]{:S(2)}) collective-permute-start(bf16[512,512]{1,0:T(8,128)(2,1)S(1)} %bitcast.17), channel_id=1, source_target_pairs={{0,24},{8,0},{16,8},{24,16},{1,25},{9,1},{17,9},{25,17},{2,26},{10... | collective-permute-start | bytes 1572872 | tf_op jit(solution)/shard_map/ppermute | solution.py:41
  83.1 29.9 %collective-permute-start.9 = (bf16[512,512]{1,0:T(8,128)(2,1)S(1)}, bf16[512,512]{1,0:T(8,128)(2,1)}, u32[]{:S(2)}, u32[]{:S(2)}) collective-permute-start(bf16[512,512]{1,0:T(8,128)(2,1)S(1)} %bitcast.18), channel_id=1, source_target_pairs={{0,16},{8,24},{16,0},{24,8},{1,17},{9,25},{17,1},{25,9},{2,18},{10... | collective-permute-start | bytes 1572872 | tf_op jit(solution)/shard_map/ppermute | solution.py:41
  86.7 0.7 copy-start.11
  87.4 7.3 %collective-permute-start.5 = (bf16[528,256]{1,0:T(8,128)(2,1)S(1)}, bf16[528,256]{1,0:T(8,128)(2,1)S(1)}, u32[]{:S(2)}, u32[]{:S(2)}) collective-permute-start(bf16[528,256]{1,0:T(8,128)(2,1)S(1)} %collective-permute-done.1.refs_2_), channel_id=1, source_target_pairs={{0,1},{1,0},{2,3},{3,2},{4,5},{5,4},{6,7},{7,6},{8,9},{9,8},{10,11... | collective-permute-start | bytes 811016 | tf_op jit(solution)/shard_map/ppermute | solution.py:33
  90.6 0.7 copy-start.7
  91.3 0.7 copy-start.13
  92.0 5.6 %collective-permute-start.6 = (bf16[528,256]{1,0:T(8,128)(2,1)S(1)}, bf16[528,256]{1,0:T(8,128)(2,1)S(1)}, u32[]{:S(2)}, u32[]{:S(2)}) collective-permute-start(bf16[528,256]{1,0:T(8,128)(2,1)S(1)} %collective-permute-done.2.refs_3_), channel_id=1, source_target_pairs={{0,1},{1,0},{2,3},{3,2},{4,5},{5,4},{6,7},{7,6},{8,9},{9,8},{10,11... | collective-permute-start | bytes 811016 | tf_op jit(solution)/shard_map/ppermute | solution.py:33
  93.9 0.7 copy-start.9
  94.6 0.7 copy-start.15
  95.4 31.0 %collective-permute-start.10 = (bf16[512,256]{1,0:T(8,128)(2,1)}, bf16[512,256]{1,0:T(8,128)(2,1)}, u32[]{:S(2)}, u32[]{:S(2)}) collective-permute-start(bf16[512,256]{1,0:T(8,128)(2,1)} %bitcast.5.p0), channel_id=1, source_target_pairs={{0,8},{8,16},{16,24},{24,0},{1,9},{9,17},{17,25},{25,1},{2,10},{10... | collective-permute-start | bytes 786440 | tf_op jit(solution)/shard_map/ppermute | solution.py:41
  97.7 0.7 copy-start.17
  98.4 27.9 %collective-permute-start.11 = (bf16[512,256]{1,0:T(8,128)(2,1)}, bf16[512,256]{1,0:T(8,128)(2,1)}, u32[]{:S(2)}, u32[]{:S(2)}) collective-permute-start(bf16[512,256]{1,0:T(8,128)(2,1)} %bitcast.5.p0), channel_id=1, source_target_pairs={{0,24},{8,0},{16,8},{24,16},{1,25},{9,1},{17,9},{25,17},{2,26},{10... | collective-permute-start | bytes 786440 | tf_op jit(solution)/shard_map/ppermute | solution.py:41
  102.6 23.7 %collective-permute-start.12 = (bf16[512,256]{1,0:T(8,128)(2,1)}, bf16[512,256]{1,0:T(8,128)(2,1)}, u32[]{:S(2)}, u32[]{:S(2)}) collective-permute-start(bf16[512,256]{1,0:T(8,128)(2,1)} %bitcast.5.p0), channel_id=1, source_target_pairs={{0,16},{8,24},{16,0},{24,8},{1,17},{9,25},{17,1},{25,9},{2,18},{10... | collective-permute-start | bytes 786440 | tf_op jit(solution)/shard_map/ppermute | solution.py:41
  104.7 1.0 copy-start.6
  105.7 1.0 copy-start.8
  106.6 1.0 copy-start.10
  107.6 1.0 copy-start.12
  108.6 1.0 copy-start.14
  109.5 1.0 copy-start.16
  110.5 1.0 copy-start.18
  113.0 10.4 %copy-start.32 = (bf16[256]{0:T(256)(128)(2,1)S(1)}, bf16[256]{0:T(256)(128)(2,1)}, u32[]{:S(2)}) copy-start(bf16[256]{0:T(256)(128)(2,1)} %param.19) | copy-start | bytes 1540
  113.1 10.4 %copy-start.33 = (bf16[256]{0:T(256)(128)(2,1)S(1)}, bf16[256]{0:T(256)(128)(2,1)}, u32[]{:S(2)}) copy-start(bf16[256]{0:T(256)(128)(2,1)} %param.20) | copy-start | bytes 1540
  115.2 0.8 copy-start.3
  116.6 11.6 %all-to-all-start.1 = ((f32[8,2,512]{2,1,0:T(2,128)}), f32[8,2,512]{2,1,0:T(2,128)S(1)}, u32[]{:S(2)}, u32[]{:S(2)}) async-start(f32[8,2,512]{2,1,0:T(2,128)} %broadcast_in_dim.42), calls=%async_computation.1 | async-start | bytes 65536 | tf_op jit(solution)/shard_map/all_to_all | solution.py:29
  123.5 4.8 %copy-start.19 = (bf16[2,128,128]{2,1,0:T(8,128)(2,1)S(1)}, bf16[2,128,128]{2,1,0:T(8,128)(2,1)}, u32[]{:S(2)}) copy-start(bf16[2,128,128]{2,1,0:T(8,128)(2,1)} %mix.3) | copy-start | bytes 196612
  123.5 4.8 %copy-start.22 = (bf16[2,128]{1,0:T(2,128)(2,1)S(1)}, bf16[2,128]{1,0:T(2,128)(2,1)}, u32[]{:S(2)}) copy-start(bf16[2,128]{1,0:T(2,128)(2,1)} %bias.1) | copy-start | bytes 1540
  125.5 0.8 copy-start.1
  128.2 1.1 copy-start.2
  129.3 1.0 copy-start.4
  132.6 4.9 %collective-permute-start.13 = (bf16[4,512,256]{2,1,0:T(8,128)(2,1)S(1)}, bf16[4,512,256]{2,1,0:T(8,128)(2,1)S(1)}, u32[]{:S(2)}, u32[]{:S(2)}) collective-permute-start(bf16[4,512,256]{2,1,0:T(8,128)(2,1)S(1)} %get-tuple-element.18), channel_id=1, source_target_pairs={{0,1},{1,0},{2,3},{3,2},{4,5},{5,4},{6,7},{7,6},{8,9},{9,8},{10,11... | collective-permute-start | bytes 3145736 | tf_op jit(solution)/shard_map/ppermute | solution.py:33
  137.7 17.5 %copy-start.25 = (bf16[512,256]{1,0:T(8,128)(2,1)S(1)}, bf16[512,256]{1,0:T(8,128)(2,1)}, u32[]{:S(2)}) copy-start(bf16[512,256]{1,0:T(8,128)(2,1)} %param.15) | copy-start | bytes 786436
  155.2 22.8 %copy-start.20 = (bf16[3,512]{1,0:T(4,128)(2,1)S(1)}, bf16[3,512]{1,0:T(4,128)(2,1)}, u32[]{:S(2)}) copy-start(bf16[3,512]{1,0:T(4,128)(2,1)} %conv_gate.1) | copy-start | bytes 9220
  155.2 22.8 %copy-start.21 = (bf16[3,512]{1,0:T(4,128)(2,1)S(1)}, bf16[3,512]{1,0:T(4,128)(2,1)}, u32[]{:S(2)}) copy-start(bf16[3,512]{1,0:T(4,128)(2,1)} %conv_value.1) | copy-start | bytes 9220
  171.8 6.3 %collective-permute-start.14 = (bf16[4,512,256]{2,1,0:T(8,128)(2,1)S(1)}, bf16[4,512,256]{2,1,0:T(8,128)(2,1)S(1)}, u32[]{:S(2)}, u32[]{:S(2)}) collective-permute-start(bf16[4,512,256]{2,1,0:T(8,128)(2,1)S(1)} %all_to_all.31.mine), channel_id=1, source_target_pairs={{0,1},{1,0},{2,3},{3,2},{4,5},{5,4},{6,7},{7,6},{8,9},{9,8},{10,11... | collective-permute-start | bytes 3145736 | tf_op jit(solution)/shard_map/ppermute | solution.py:33
  178.1 2.8 %copy-start = (bf16[2048,1536]{1,0:T(8,128)(2,1)S(1)}, bf16[2048,1536]{1,0:T(8,128)(2,1)}, u32[]{:S(2)}) copy-start(bf16[2048,1536]{1,0:T(8,128)(2,1)} %all-gather.2.cloned.1.call-done.late_hbm) | copy-start | bytes 18874372
  187.4 4.6 %collective-permute-start.18 = (bf16[4,512,256]{2,1,0:T(8,128)(2,1)S(1)}, bf16[4,512,256]{2,1,0:T(8,128)(2,1)S(1)}, u32[]{:S(2)}, u32[]{:S(2)}) collective-permute-start(bf16[4,512,256]{2,1,0:T(8,128)(2,1)S(1)} %get-tuple-element.22), channel_id=1, source_target_pairs={{0,1},{1,0},{2,3},{3,2},{4,5},{5,4},{6,7},{7,6},{8,9},{9,8},{10,11... | collective-permute-start | bytes 3145736 | tf_op jit(solution)/shard_map/ppermute | solution.py:33
Sparse Core Ops, SparseCore 0:
  47.1 90.6 all-gather.1

commit v4 on v3

--- a/solution.py
+++ b/solution.py
@@ -10,7 +10,8 @@
 BLOCK = 128
 SEGMENT = 64
 SEQ_LEN = 256
-FS = ("z", "y")
+Z = ("zh", "zl")
+FS = ("zh", "zl", "y")
 TP = ("x", "c")
 EPS = 1e-06
 F32 = jnp.float32
@@ -18,7 +19,7 @@
 SWAP = [(0, 1), (1, 0)]
 RING = (0, 1, 3, 2)
 PIECE = 32
-ANY = pl.BlockSpec(memory_space=pl.ANY)
+HBM = pl.BlockSpec(memory_space=pltpu.HBM)
 SQRT_HALF = 0.7071067811865476
 VMEM = pl.BlockSpec(memory_space=pltpu.VMEM)
 SMEM = pl.BlockSpec(memory_space=pltpu.SMEM)
@@ -38,7 +39,9 @@
 
 
 def round_ring(shard, axis):
-    return [shard] + [lax.ppermute(shard, axis, [(i, (i + step) % 4) for i in range(4)]) for step in RING[1:]]
+    size = lax.axis_size(axis)
+    steps = (1, size - 1, 2)
+    return [shard] + [lax.ppermute(shard, axis, [(i, (i + step) % size) for i in range(size)]) for step in steps]
 
 
 def in_order(parts, axis):
@@ -76,17 +79,18 @@
     return (here + (4 - step)) & 3
 
 
-def fill_rows(weight, parts, y, cols):
-    for step, part in zip(RING, parts):
-        near = origin(y, step)
-        for far in range(part.shape[0] // PIECE):
-            start = pl.multiple_of((far * 4 + near) * PIECE, PIECE)
-            weight[pl.ds(start, PIECE), :] = part[far * PIECE : (far + 1) * PIECE, cols]
-
-
-def stats_kernel(place, normed, p0, p1, p2, p3, act, sums, weight):
+def fill_rows(weight, early, near, cols):
+    for y in range(4):
+        for at, step in enumerate(RING):
+            for far in range(4):
+                start = pl.multiple_of(((far * 4 + origin(near, step)) * 4 + y) * PIECE, PIECE)
+                came = (at * 4 + far) * PIECE
+                weight[pl.ds(start, PIECE), :] = early[y, came : came + PIECE, cols]
+
+
+def stats_kernel(place, normed, early, act, sums, weight):
     width = act.shape[1]
-    fill_rows(weight, (p0, p1, p2, p3), place[2], slice(width, 2 * width))
+    fill_rows(weight, early, place[2], slice(width, 2 * width))
     for part in range(normed.shape[0] // SEQ_LEN):
         rows = pl.ds(part * SEQ_LEN, SEQ_LEN)
         value = gelu(jnp.dot(normed[rows, :], weight[...], preferred_element_type=F32))
@@ -97,16 +101,16 @@
         sums[1:2, rows] = jnp.sum(twice.T, axis=0, keepdims=True)
 
 
-def gate_kernel(place, normed, p0, p1, p2, p3, act, weight):
-    fill_rows(weight, (p0, p1, p2, p3), place[2], slice(0, act.shape[1]))
+def gate_kernel(place, normed, early, act, weight):
+    fill_rows(weight, early, place[2], slice(0, act.shape[1]))
     for part in range(normed.shape[0] // SEQ_LEN):
         rows = pl.ds(part * SEQ_LEN, SEQ_LEN)
         act[rows, :] = gelu(jnp.dot(normed[rows, :], weight[...], preferred_element_type=F32))
 
 
-def mix_kernel(place, act_v, act_u, stats, gain, shift, mix, bias, p0, p1, p2, p3, give, keep, weight, gated):
+def mix_kernel(place, act_v, act_u, stats, gain, shift, mix, bias, early, give, keep, weight, gated):
     width = act_v.shape[1]
-    fill_rows(weight, (p0, p1, p2, p3), place[2], slice(0, width))
+    fill_rows(weight, early, place[2], slice(2 * width, 3 * width))
     full = width * stats.shape[0]
     i = lax.broadcasted_iota(jnp.int32, (BLOCK, BLOCK), 0)
     j = lax.broadcasted_iota(jnp.int32, (BLOCK, BLOCK), 1)
@@ -242,19 +246,19 @@
     ff = ffn_gate.shape[1]
     row_count = tokens.shape[0]
 
-    early = jnp.concatenate([proj_u, proj_v], axis=1)
-    early_z = everyones(early, "z").reshape(-1, early.shape[1])
+    early = jnp.concatenate([proj_u, proj_v, proj_out.T], axis=1)
+    early_far = everyones(early, "zh").reshape(-1, early.shape[1])
+    early_z = jnp.stack(round_ring(early_far, Z))
+    early_all = everyones(early_z, "y").reshape(4, -1, early.shape[1])
+
     late = jnp.concatenate([ffn_gate, ffn_value, proj_down.T], axis=1)
     late_y = in_order(round_ring(late, "y"), "y").reshape(-1, late.shape[1])
-    late_all = lax.all_gather(after(late_y, early_z), "z", axis=0, tiled=True)
+    late_all = lax.all_gather(after(late_y, early_z), Z, axis=0, tiled=True)
 
     packed = jnp.concatenate([tokens, jnp.broadcast_to(norm_gain, (8, da)), jnp.broadcast_to(ffn_gain, (8, da))], axis=0)
     mine = round_ring(packed, "x")
-    early_parts = round_ring(early_z, "y")
-    out_z = everyones(proj_out.T, "z").reshape(-1, da)
     other = [other_core(part) for part in mine]
-    out_parts = round_ring(out_z, "y")
-    place = jnp.stack([lax.axis_index(name).astype(jnp.int32) for name in ("x", "c", "y")])
+    place = jnp.stack([lax.axis_index(name).astype(jnp.int32) for name in ("x", "c", "zl")])
     model = proj_u.shape[0] * lax.axis_size(FS)
     tp = lax.axis_size(TP)
     normed, gain_two = pl.pallas_call(
@@ -268,27 +272,27 @@
 
     act_v, sums = pl.pallas_call(
         stats_kernel,
-        in_specs=[SMEM] + [VMEM] * 5,
+        in_specs=[SMEM] + [VMEM] * 2,
         out_specs=[VMEM] * 2,
         out_shape=[shape((row_count, da), F32), shape((2, row_count), F32)],
         scratch_shapes=[pltpu.VMEM((model, da), BF16)],
         name="stats",
         compiler_params=room(14),
-    )(place, normed, *early_parts)
+    )(place, normed, early_all)
     stats = everyones(sums, TP)
     act_u = pl.pallas_call(
         gate_kernel,
-        in_specs=[SMEM] + [VMEM] * 5,
+        in_specs=[SMEM] + [VMEM] * 2,
         out_specs=VMEM,
         out_shape=shape((row_count, da), F32),
         scratch_shapes=[pltpu.VMEM((model, da), BF16)],
         name="gate",
         compiler_params=room(14),
-    )(place, normed, *early_parts)
+    )(place, normed, early_all)
     blocks = [shape((lax.axis_size("x"), row_count, da), BF16)] * 2
     give, keep = pl.pallas_call(
         mix_kernel,
-        in_specs=[SMEM] + [VMEM] * 11,
+        in_specs=[SMEM] + [VMEM] * 8,
         out_specs=[VMEM] * 2,
         out_shape=blocks,
         scratch_shapes=[pltpu.VMEM((model, da), BF16), pltpu.VMEM((row_count, da), BF16)],
@@ -303,18 +307,18 @@
         layer_shift[None],
         mix_weight,
         mix_bias,
-        *out_parts,
+        early_all,
     )
     stream = (tokens.astype(F32) + summed_at_owner(give, keep)).astype(BF16)
     mine = everyones(stream, "x")
     give, keep = pl.pallas_call(
         ffn_kernel,
-        in_specs=[SMEM] + [VMEM] * 3 + [ANY] + [VMEM] * 2,
+        in_specs=[SMEM] + [VMEM] * 3 + [HBM] + [VMEM] * 2,
         out_specs=[VMEM] * 2,
         out_shape=blocks,
         scratch_shapes=[pltpu.VMEM((SEQ_LEN, model), BF16), pltpu.VMEM((row_count, ff), BF16), pltpu.VMEM(late_all.shape, BF16), pltpu.SemaphoreType.DMA((3,))],
         name="ffn",
-        compiler_params=room(26),
+        compiler_params=room(47),
     )(
         place,
         mine,
@@ -328,7 +332,7 @@
 
 
 def solution(mesh):
-    split = Mesh(mesh.devices.reshape(16, 4, 4, 2), ("z", "y", "x", "c"))
+    split = Mesh(mesh.devices.reshape(4, 4, 4, 4, 2), ("zh", "zl", "y", "x", "c"))
     placed = (
         P(FS, TP),
         P(TP),

time: 219 us -> 214 us (0.977)
  waiting for transfers between devices: 20.6 us -> 36 us
  starting transfers between devices: 93.2 us -> 82 us
  local copies, waits for them, and re-layouts: 20.5 us -> 11.7 us
    unnamed x68 -> x34, local copies, waits for them, and re-layouts: 18.2 us -> 8.26 us
    all_to_all x3, starting transfers between devices: 35 us -> 26 us  [everyones(): return lax.all_to_all(copies, axis, split_axis=0, concat_axis=0, tiled=True)]
    all_to_all x3, waiting for transfers between devices: 10.3 us -> 18.4 us  [everyones(): return lax.all_to_all(copies, axis, split_axis=0, concat_axis=0, tiled=True)]
    ppermute x12 -> x9, waiting for transfers between devices: 3.48 us -> 8.93 us  [round_ring(): lax.ppermute(shard, axis, [(i, (i + step) % size) for i in range(size)])]
    ppermute x12 -> x9, starting transfers between devices: 38.6 us -> 33.6 us  [round_ring(): lax.ppermute(shard, axis, [(i, (i + step) % size) for i in range(size)])]
    ppermute x7, starting transfers between devices: 19.6 us -> 22.4 us  [other_core(): return lax.ppermute(value, 'c', SWAP)]
  transfers between devices with their start and end apart: 23 -> 20, of which waited for: 6 -> 9; matrix products, arithmetic and copies ran while one was open for 1% -> 3% of each run, Pallas kernels for 4% -> 3%
where the time goes in v4:
time: 214 us; the launch traced here: 213 us
  starting transfers between devices  82 us (38%)
  blocking collectives  50.1 us (23%)
  waiting for transfers between devices  36 us (17%)
  Pallas kernels  13.9 us (6%)
  between operations  13.8 us (6%)
  local copies, waits for them, and re-layouts  11.7 us (5%)
  other arithmetic  5.15 us (2%)
    all_to_all x2, blocking collectives, summed_at_owner(): arrived = lax.all_to_all(pair, 'x', split_axis=0, concat_axis=0, tiled=True)  34.2 us
    ppermute x9, starting transfers between devices, round_ring(): lax.ppermute(shard, axis, [(i, (i + step) % size) for i in range(size)])  33.6 us
    all_to_all x3, starting transfers between devices, everyones(): return lax.all_to_all(copies, axis, split_axis=0, concat_axis=0, tiled=True)  26 us
    ppermute x7, starting transfers between devices, other_core(): return lax.ppermute(value, 'c', SWAP)  22.4 us
    all_to_all x3, waiting for transfers between devices, everyones(): return lax.all_to_all(copies, axis, split_axis=0, concat_axis=0, tiled=True)  18.4 us
    all_to_all x1, blocking collectives, everyones(): return lax.all_to_all(copies, axis, split_axis=0, concat_axis=0, tiled=True)  15.8 us
    ppermute x9, waiting for transfers between devices, round_ring(): lax.ppermute(shard, axis, [(i, (i + step) % size) for i in range(size)])  8.93 us
    ppermute x7, waiting for transfers between devices, other_core(): return lax.ppermute(value, 'c', SWAP)  8.56 us
  transfers between devices with their start and end apart: 20, of which 9 were waited for; matrix products, arithmetic and copies ran while one was open for 3% of the time, Pallas kernels for 3%

profile of v4, /device:TPU:1, one launch (start us, length us, event | category | flops | bytes accessed | tf_op | source)
XLA Modules:
  0.0 212.6 jit_solution(14981283862749581588)
XLA Ops:
  6.5 0.8 pad_maximum_fusion.2
  7.3 4.0 %collective-permute-start.12 = (bf16[32,1536]{1,0:T(8,128)(2,1)S(1)}, bf16[32,1536]{1,0:T(8,128)(2,1)S(1)}, u32[]{:S(2)}, u32[]{:S(2)}) collective-permute-start(bf16[32,1536]{1,0:T(8,128)(2,1)S(1)} %pad_maximum_fusion.2), channel_id=1, source_target_pairs={{0,8},{8,16},{16,24},{24,0},{1,9},{9,17},{17,25},{25,1},{2,10},{10... | collective-permute-start | bytes 294920 | tf_op jit(solution)/shard_map/ppermute | solution.py:44
  11.4 3.4 %collective-permute-start.13 = (bf16[32,1536]{1,0:T(8,128)(2,1)S(1)}, bf16[32,1536]{1,0:T(8,128)(2,1)S(1)}, u32[]{:S(2)}, u32[]{:S(2)}) collective-permute-start(bf16[32,1536]{1,0:T(8,128)(2,1)S(1)} %pad_maximum_fusion.2), channel_id=1, source_target_pairs={{0,24},{8,0},{16,8},{24,16},{1,25},{9,1},{17,9},{25,17},{2,26},{10... | collective-permute-start | bytes 294920 | tf_op jit(solution)/shard_map/ppermute | solution.py:44
  14.7 3.5 %collective-permute-start.14 = (bf16[32,1536]{1,0:T(8,128)(2,1)S(1)}, bf16[32,1536]{1,0:T(8,128)(2,1)S(1)}, u32[]{:S(2)}, u32[]{:S(2)}) collective-permute-start(bf16[32,1536]{1,0:T(8,128)(2,1)S(1)} %pad_maximum_fusion.2), channel_id=1, source_target_pairs={{0,16},{8,24},{16,0},{24,8},{1,17},{9,25},{17,1},{25,9},{2,18},{10... | collective-permute-start | bytes 294920 | tf_op jit(solution)/shard_map/ppermute | solution.py:44
  18.3 0.8 pad_maximum_fusion.3
  19.0 0.7 broadcast_in_dim.41
  19.7 14.8 %all-to-all-start = ((bf16[4,32,768]{2,1,0:T(8,128)(2,1)}), bf16[4,32,768]{2,1,0:T(8,128)(2,1)S(1)}, u32[]{:S(2)}, u32[]{:S(2)}) async-start(bf16[4,32,768]{2,1,0:T(8,128)(2,1)} %broadcast_in_dim.41), calls=%async_computation | async-start | bytes 393216 | tf_op jit(solution)/shard_map/all_to_all | solution.py:30
  34.6 0.8 bitcast_dynamic-update-slice_fusion.3
  35.4 0.0 collective-permute-done.12
  35.4 11.8 %all-to-all-done = bf16[4,32,768]{2,1,0:T(8,128)(2,1)S(1)} async-done(((bf16[4,32,768]{2,1,0:T(8,128)(2,1)}), bf16[4,32,768]{2,1,0:T(8,128)(2,1)S(1)}, u32[]{:S(2)}, u32[]{:S(2)}) %all-to-all-start) | async-done | bytes 196640 | tf_op jit(solution)/shard_map/all_to_all | solution.py:30
  47.2 7.0 %collective-permute-start.7 = (bf16[128,768]{1,0:T(8,128)(2,1)S(1)}, bf16[128,768]{1,0:T(8,128)(2,1)S(1)}, u32[]{:S(2)}, u32[]{:S(2)}) collective-permute-start(bf16[128,768]{1,0:T(8,128)(2,1)S(1)} %bitcast.24), channel_id=1, source_target_pairs={{0,32},{32,64},{64,96},{96,128},{128,160},{160,192},{192,224},{224... | collective-permute-start | bytes 589832 | tf_op jit(solution)/shard_map/ppermute | solution.py:44
  54.2 1.9 collective-permute-start.8
  56.1 3.8 %collective-permute-start.9 = (bf16[128,768]{1,0:T(8,128)(2,1)S(1)}, bf16[128,768]{1,0:T(8,128)(2,1)S(1)}, u32[]{:S(2)}, u32[]{:S(2)}) collective-permute-start(bf16[128,768]{1,0:T(8,128)(2,1)S(1)} %bitcast.26), channel_id=1, source_target_pairs={{0,64},{32,96},{64,128},{96,160},{128,192},{160,224},{192,256},{22... | collective-permute-start | bytes 589832 | tf_op jit(solution)/shard_map/ppermute | solution.py:44
  60.0 0.6 collective-permute-done.8
  60.6 8.3 %collective-permute-done.9 = bf16[128,768]{1,0:T(8,128)(2,1)S(1)} collective-permute-done((bf16[128,768]{1,0:T(8,128)(2,1)S(1)}, bf16[128,768]{1,0:T(8,128)(2,1)S(1)}, u32[]{:S(2)}, u32[]{:S(2)}) %collective-permute-start.9) | collective-permute-done | bytes 196640 | tf_op jit(solution)/shard_map/ppermute | solution.py:44
  68.9 0.1 pad_maximum_fusion
  69.0 0.0 all-gather.2.cloned.1.call-update
  69.1 2.0 broadcast_in_dim.42
  71.1 3.8 %all-to-all-start.1 = ((bf16[4,4,128,768]{3,2,1,0:T(8,128)(2,1)}), bf16[4,4,128,768]{3,2,1,0:T(8,128)(2,1)S(1)}, u32[]{:S(2)}, u32[]{:S(2)}) async-start(bf16[4,4,128,768]{3,2,1,0:T(8,128)(2,1)} %broadcast_in_dim.42), calls=%async_computation.1 | async-start | bytes 6291456 | tf_op jit(solution)/shard_map/all_to_all | solution.py:30
  75.0 1.0 pad_maximum_fusion.1.refs_0_
  75.9 3.1 %collective-permute-start = (bf16[528,256]{1,0:T(8,128)(2,1)S(1)}, bf16[528,256]{1,0:T(8,128)(2,1)}, u32[]{:S(2)}, u32[]{:S(2)}) collective-permute-start(bf16[528,256]{1,0:T(8,128)(2,1)S(1)} %pad_maximum_fusion.1.refs_0_), channel_id=1, source_target_pairs={{0,2},{2,4},{4,6},{6,0},{1,3},{3,5},{5,7},{7,1},{8,10},{10,12},{12... | collective-permute-start | bytes 811016 | tf_op jit(solution)/shard_map/ppermute | solution.py:44
  79.1 3.4 %collective-permute-start.1 = (bf16[528,256]{1,0:T(8,128)(2,1)S(1)}, bf16[528,256]{1,0:T(8,128)(2,1)}, u32[]{:S(2)}, u32[]{:S(2)}) collective-permute-start(bf16[528,256]{1,0:T(8,128)(2,1)S(1)} %pad_maximum_fusion.1.refs_0_), channel_id=1, source_target_pairs={{0,6},{2,0},{4,2},{6,4},{1,7},{3,1},{5,3},{7,5},{8,14},{10,8},{12,... | collective-permute-start | bytes 811016 | tf_op jit(solution)/shard_map/ppermute | solution.py:44
  82.4 3.4 %collective-permute-start.2 = (bf16[528,256]{1,0:T(8,128)(2,1)S(1)}, bf16[528,256]{1,0:T(8,128)(2,1)}, u32[]{:S(2)}, u32[]{:S(2)}) collective-permute-start(bf16[528,256]{1,0:T(8,128)(2,1)S(1)} %pad_maximum_fusion.1.refs_0_), channel_id=1, source_target_pairs={{0,4},{2,6},{4,0},{6,2},{1,5},{3,7},{5,1},{7,3},{8,12},{10,14},{12... | collective-permute-start | bytes 811016 | tf_op jit(solution)/shard_map/ppermute | solution.py:44
  85.9 5.0 %collective-permute-start.3 = (bf16[528,256]{1,0:T(8,128)(2,1)S(1)}, bf16[528,256]{1,0:T(8,128)(2,1)}, u32[]{:S(2)}, u32[]{:S(2)}) collective-permute-start(bf16[528,256]{1,0:T(8,128)(2,1)S(1)} %pad_maximum_fusion.1.refs_0_), channel_id=1, source_target_pairs={{0,1},{1,0},{2,3},{3,2},{4,5},{5,4},{6,7},{7,6},{8,9},{9,8},{10,11... | collective-permute-start | bytes 811016 | tf_op jit(solution)/shard_map/ppermute | solution.py:34
  90.9 1.9 collective-permute-start.4
  92.9 4.1 %collective-permute-start.5 = (bf16[528,256]{1,0:T(8,128)(2,1)}, bf16[528,256]{1,0:T(8,128)(2,1)}, u32[]{:S(2)}, u32[]{:S(2)}) collective-permute-start(bf16[528,256]{1,0:T(8,128)(2,1)} %collective-permute-done.1.refs_2_), channel_id=1, source_target_pairs={{0,1},{1,0},{2,3},{3,2},{4,5},{5,4},{6,7},{7,6},{8,9},{9,8},{10,11... | collective-permute-start | bytes 811016 | tf_op jit(solution)/shard_map/ppermute | solution.py:34
  97.0 1.9 collective-permute-start.6
  98.9 0.1 pad_add_fusion.place
  99.0 1.8 collective-permute-done.6.refs_7_
  100.8 2.5 %norm.1 = (bf16[512,2048]{1,0:T(8,128)(2,1)S(1)}, bf16[8,8,256]{2,1,0:T(8,128)(2,1)S(1)}) custom-call(s32[3]{0:T(128)S(1)} %pad_add_fusion.place, bf16[528,256]{1,0:T(8,128)(2,1)S(1)} %pad_maximum_fusion.1.refs_0_, bf16[528,256]{1,0:T(8,128)(2,1)} %collective-permute-done.refs_1_, bf16[528,256]{1,0:T(8,128)(2,1)} %collective-permute-done.1.refs_2_, ...), custom_call_target="tpu_custom_call" | custom-call | tf_op jit(solution)/shard_map/norm/pallas_call | solution.py:264
  103.3 1.3 copy-done
  104.6 5.6 %all-to-all-done.1 = bf16[4,4,128,768]{3,2,1,0:T(8,128)(2,1)S(1)} async-done(((bf16[4,4,128,768]{3,2,1,0:T(8,128)(2,1)}), bf16[4,4,128,768]{3,2,1,0:T(8,128)(2,1)S(1)}, u32[]{:S(2)}, u32[]{:S(2)}) %all-to-all-start.1) | async-done | bytes 3145760 | tf_op jit(solution)/shard_map/all_to_all | solution.py:30
  110.3 1.6 copy-done.1
  111.9 1.5 stats.1
  113.4 0.8 copy-done.5
  114.2 0.6 broadcast_in_dim.43
  114.8 7.4 %all-to-all-start.2 = ((f32[8,2,512]{2,1,0:T(2,128)}), f32[8,2,512]{2,1,0:T(2,128)S(1)}, u32[]{:S(2)}, u32[]{:S(2)}) async-start(f32[8,2,512]{2,1,0:T(2,128)} %broadcast_in_dim.43), calls=%async_computation.2 | async-start | bytes 65536 | tf_op jit(solution)/shard_map/all_to_all | solution.py:30
  122.3 1.6 copy-done.2
  123.9 1.3 gate.1.act_u
  125.2 0.8 copy-done.3
  126.0 1.0 all-to-all-done.2.stats
  127.0 1.1 copy-done.4
  128.1 1.1 copy-done.6
  129.1 1.6 mix.2
  130.7 2.6 %collective-permute-start.10 = (bf16[4,512,256]{2,1,0:T(8,128)(2,1)S(1)}, bf16[4,512,256]{2,1,0:T(8,128)(2,1)S(1)}, u32[]{:S(2)}, u32[]{:S(2)}) collective-permute-start(bf16[4,512,256]{2,1,0:T(8,128)(2,1)S(1)} %get-tuple-element.18), channel_id=1, source_target_pairs={{0,1},{1,0},{2,3},{3,2},{4,5},{5,4},{6,7},{7,6},{8,9},{9,8},{10,11... | collective-permute-start | bytes 3145736 | tf_op jit(solution)/shard_map/ppermute | solution.py:34
  133.3 2.3 %collective-permute-done.10 = bf16[4,512,256]{2,1,0:T(8,128)(2,1)S(1)} collective-permute-done((bf16[4,512,256]{2,1,0:T(8,128)(2,1)S(1)}, bf16[4,512,256]{2,1,0:T(8,128)(2,1)S(1)}, u32[]{:S(2)}, u32[]{:S(2)}) %collective-permute-start.10) | collective-permute-done | bytes 1048608 | tf_op jit(solution)/shard_map/ppermute | solution.py:34
  135.5 0.2 add_convert_fusion.1
  135.8 0.0 copy-start.12
  135.8 17.0 %all_to_all.30 = bf16[4,512,256]{2,1,0:T(8,128)(2,1)S(1)} all-to-all(bf16[4,512,256]{2,1,0:T(8,128)(2,1)S(1)} %add_convert_fusion.1), channel_id=1, replica_groups=mesh['zh'=4,'zl'=4,'y'=4,'x'=4,'c'=2] {'x'}, dimensions={0} | all-to-all | bytes 2097152 | tf_op jit(solution)/shard_map/all_to_all | solution.py:224
  152.8 0.1 convert_reduce_fusion.1
  153.0 0.0 copy-start.8
  153.0 0.0 copy-start.9
  153.0 0.1 add_convert_fusion.3
  153.1 0.1 broadcast_in_dim.46
  153.1 15.8 %all_to_all.31.mine = bf16[4,512,256]{2,1,0:T(8,128)(2,1)S(1)} all-to-all(bf16[4,512,256]{2,1,0:T(8,128)(2,1)S(1)} %broadcast_in_dim.46), channel_id=1, replica_groups=mesh['zh'=4,'zl'=4,'y'=4,'x'=4,'c'=2] {'x'}, dimensions={0} | all-to-all | bytes 2097152 | tf_op jit(solution)/shard_map/all_to_all | solution.py:30
  168.9 4.6 %collective-permute-start.11 = (bf16[4,512,256]{2,1,0:T(8,128)(2,1)S(1)}, bf16[4,512,256]{2,1,0:T(8,128)(2,1)S(1)}, u32[]{:S(2)}, u32[]{:S(2)}) collective-permute-start(bf16[4,512,256]{2,1,0:T(8,128)(2,1)S(1)} %all_to_all.31.mine), channel_id=1, source_target_pairs={{0,1},{1,0},{2,3},{3,2},{4,5},{5,4},{6,7},{7,6},{8,9},{9,8},{10,11... | collective-permute-start | bytes 3145736 | tf_op jit(solution)/shard_map/ppermute | solution.py:34
  173.5 2.3 %collective-permute-done.11.other = bf16[4,512,256]{2,1,0:T(8,128)(2,1)S(1)} collective-permute-done((bf16[4,512,256]{2,1,0:T(8,128)(2,1)S(1)}, bf16[4,512,256]{2,1,0:T(8,128)(2,1)S(1)}, u32[]{:S(2)}, u32[]{:S(2)}) %collective-permute-start.11) | collective-permute-done | bytes 1048608 | tf_op jit(solution)/shard_map/ppermute | solution.py:34
  175.8 7.0 %ffn.1 = (bf16[4,512,256]{2,1,0:T(8,128)(2,1)S(1)}, bf16[4,512,256]{2,1,0:T(8,128)(2,1)S(1)}) custom-call(s32[3]{0:T(128)S(1)} %pad_add_fusion.place, bf16[4,512,256]{2,1,0:T(8,128)(2,1)S(1)} %all_to_all.31.mine, bf16[4,512,256]{2,1,0:T(8,128)(2,1)S(1)} %collective-permute-done.11.other, bf16[8,8,256]{2,1,0:T(8,128)(2,1)S(1)} %get-tuple-element.19.gain, ...), custom_call_target="tpu_custom_call" | custom-call | tf_op jit(solution)/shard_map/ffn/pallas_call | solution.py:314
  182.8 2.3 %collective-permute-start.15 = (bf16[4,512,256]{2,1,0:T(8,128)(2,1)S(1)}, bf16[4,512,256]{2,1,0:T(8,128)(2,1)S(1)}, u32[]{:S(2)}, u32[]{:S(2)}) collective-permute-start(bf16[4,512,256]{2,1,0:T(8,128)(2,1)S(1)} %get-tuple-element.22), channel_id=1, source_target_pairs={{0,1},{1,0},{2,3},{3,2},{4,5},{5,4},{6,7},{7,6},{8,9},{9,8},{10,11... | collective-permute-start | bytes 3145736 | tf_op jit(solution)/shard_map/ppermute | solution.py:34
  185.1 2.3 %collective-permute-done.15 = bf16[4,512,256]{2,1,0:T(8,128)(2,1)S(1)} collective-permute-done((bf16[4,512,256]{2,1,0:T(8,128)(2,1)S(1)}, bf16[4,512,256]{2,1,0:T(8,128)(2,1)S(1)}, u32[]{:S(2)}, u32[]{:S(2)}) %collective-permute-start.15) | collective-permute-done | bytes 1048608 | tf_op jit(solution)/shard_map/ppermute | solution.py:34
  187.3 0.3 add_convert_fusion
  187.6 17.2 %all_to_all.32 = bf16[4,512,256]{2,1,0:T(8,128)(2,1)S(1)} all-to-all(bf16[4,512,256]{2,1,0:T(8,128)(2,1)S(1)} %add_convert_fusion), channel_id=1, replica_groups=mesh['zh'=4,'zl'=4,'y'=4,'x'=4,'c'=2] {'x'}, dimensions={0} | all-to-all | bytes 2097152 | tf_op jit(solution)/shard_map/all_to_all | solution.py:224
  204.8 0.1 convert_reduce_fusion
  205.0 0.8 add_convert_fusion.2
  (43 shorter events, 0.2 us)
Async XLA Ops:
  7.3 28.0 %collective-permute-start.12 = (bf16[32,1536]{1,0:T(8,128)(2,1)S(1)}, bf16[32,1536]{1,0:T(8,128)(2,1)S(1)}, u32[]{:S(2)}, u32[]{:S(2)}) collective-permute-start(bf16[32,1536]{1,0:T(8,128)(2,1)S(1)} %pad_maximum_fusion.2), channel_id=1, source_target_pairs={{0,8},{8,16},{16,24},{24,0},{1,9},{9,17},{17,25},{25,1},{2,10},{10... | collective-permute-start | bytes 294920 | tf_op jit(solution)/shard_map/ppermute | solution.py:44
  11.4 24.0 %collective-permute-start.13 = (bf16[32,1536]{1,0:T(8,128)(2,1)S(1)}, bf16[32,1536]{1,0:T(8,128)(2,1)S(1)}, u32[]{:S(2)}, u32[]{:S(2)}) collective-permute-start(bf16[32,1536]{1,0:T(8,128)(2,1)S(1)} %pad_maximum_fusion.2), channel_id=1, source_target_pairs={{0,24},{8,0},{16,8},{24,16},{1,25},{9,1},{17,9},{25,17},{2,26},{10... | collective-permute-start | bytes 294920 | tf_op jit(solution)/shard_map/ppermute | solution.py:44
  14.7 45.2 %collective-permute-start.14 = (bf16[32,1536]{1,0:T(8,128)(2,1)S(1)}, bf16[32,1536]{1,0:T(8,128)(2,1)S(1)}, u32[]{:S(2)}, u32[]{:S(2)}) collective-permute-start(bf16[32,1536]{1,0:T(8,128)(2,1)S(1)} %pad_maximum_fusion.2), channel_id=1, source_target_pairs={{0,16},{8,24},{16,0},{24,8},{1,17},{9,25},{17,1},{25,9},{2,18},{10... | collective-permute-start | bytes 294920 | tf_op jit(solution)/shard_map/ppermute | solution.py:44
  19.7 27.5 %all-to-all-start = ((bf16[4,32,768]{2,1,0:T(8,128)(2,1)}), bf16[4,32,768]{2,1,0:T(8,128)(2,1)S(1)}, u32[]{:S(2)}, u32[]{:S(2)}) async-start(bf16[4,32,768]{2,1,0:T(8,128)(2,1)} %broadcast_in_dim.41), calls=%async_computation | async-start | bytes 393216 | tf_op jit(solution)/shard_map/all_to_all | solution.py:30
  34.5 141.3 %all-gather.2.cloned.1.call-start = ((), (), s32[]{:S(2)}) async-start(), calls=%async_computation.6 | async-start | bytes 6684672 | tf_op jit(solution)/shard_map/all_gather | solution.py:256
  47.2 12.8 %collective-permute-start.7 = (bf16[128,768]{1,0:T(8,128)(2,1)S(1)}, bf16[128,768]{1,0:T(8,128)(2,1)S(1)}, u32[]{:S(2)}, u32[]{:S(2)}) collective-permute-start(bf16[128,768]{1,0:T(8,128)(2,1)S(1)} %bitcast.24), channel_id=1, source_target_pairs={{0,32},{32,64},{64,96},{96,128},{128,160},{160,192},{192,224},{224... | collective-permute-start | bytes 589832 | tf_op jit(solution)/shard_map/ppermute | solution.py:44
  54.2 6.4 %collective-permute-start.8 = (bf16[128,768]{1,0:T(8,128)(2,1)S(1)}, bf16[128,768]{1,0:T(8,128)(2,1)S(1)}, u32[]{:S(2)}, u32[]{:S(2)}) collective-permute-start(bf16[128,768]{1,0:T(8,128)(2,1)S(1)} %bitcast.25), channel_id=1, source_target_pairs={{0,480},{32,0},{64,32},{96,64},{128,96},{160,128},{192,160},{224,1... | collective-permute-start | bytes 589832 | tf_op jit(solution)/shard_map/ppermute | solution.py:44
  56.1 12.8 %collective-permute-start.9 = (bf16[128,768]{1,0:T(8,128)(2,1)S(1)}, bf16[128,768]{1,0:T(8,128)(2,1)S(1)}, u32[]{:S(2)}, u32[]{:S(2)}) collective-permute-start(bf16[128,768]{1,0:T(8,128)(2,1)S(1)} %bitcast.26), channel_id=1, source_target_pairs={{0,64},{32,96},{64,128},{96,160},{128,192},{160,224},{192,256},{22... | collective-permute-start | bytes 589832 | tf_op jit(solution)/shard_map/ppermute | solution.py:44
  60.0 9.0 %copy-start.11 = (bf16[4,32,1536]{2,1,0:T(8,128)(2,1)}, bf16[4,32,1536]{2,1,0:T(8,128)(2,1)S(1)}, u32[]{:S(2)}) copy-start(bf16[4,32,1536]{2,1,0:T(8,128)(2,1)S(1)} %bitcast_dynamic-update-slice_fusion) | copy-start | bytes 1179652
  71.1 3.8 %copy-start.13 = (bf16[256]{0:T(256)(128)(2,1)S(1)}, bf16[256]{0:T(256)(128)(2,1)}, u32[]{:S(2)}) copy-start(bf16[256]{0:T(256)(128)(2,1)} %param.16) | copy-start | bytes 1540
  71.1 3.9 %copy-start.14 = (bf16[256]{0:T(256)(128)(2,1)S(1)}, bf16[256]{0:T(256)(128)(2,1)}, u32[]{:S(2)}) copy-start(bf16[256]{0:T(256)(128)(2,1)} %param.24) | copy-start | bytes 1540
  71.1 39.2 %all-to-all-start.1 = ((bf16[4,4,128,768]{3,2,1,0:T(8,128)(2,1)}), bf16[4,4,128,768]{3,2,1,0:T(8,128)(2,1)S(1)}, u32[]{:S(2)}, u32[]{:S(2)}) async-start(bf16[4,4,128,768]{3,2,1,0:T(8,128)(2,1)} %broadcast_in_dim.42), calls=%async_computation.1 | async-start | bytes 6291456 | tf_op jit(solution)/shard_map/all_to_all | solution.py:30
  75.9 15.0 %collective-permute-start = (bf16[528,256]{1,0:T(8,128)(2,1)S(1)}, bf16[528,256]{1,0:T(8,128)(2,1)}, u32[]{:S(2)}, u32[]{:S(2)}) collective-permute-start(bf16[528,256]{1,0:T(8,128)(2,1)S(1)} %pad_maximum_fusion.1.refs_0_), channel_id=1, source_target_pairs={{0,2},{2,4},{4,6},{6,0},{1,3},{3,5},{5,7},{7,1},{8,10},{10,12},{12... | collective-permute-start | bytes 811016 | tf_op jit(solution)/shard_map/ppermute | solution.py:44
  79.1 13.8 %collective-permute-start.1 = (bf16[528,256]{1,0:T(8,128)(2,1)S(1)}, bf16[528,256]{1,0:T(8,128)(2,1)}, u32[]{:S(2)}, u32[]{:S(2)}) collective-permute-start(bf16[528,256]{1,0:T(8,128)(2,1)S(1)} %pad_maximum_fusion.1.refs_0_), channel_id=1, source_target_pairs={{0,6},{2,0},{4,2},{6,4},{1,7},{3,1},{5,3},{7,5},{8,14},{10,8},{12,... | collective-permute-start | bytes 811016 | tf_op jit(solution)/shard_map/ppermute | solution.py:44
  82.4 14.5 %collective-permute-start.2 = (bf16[528,256]{1,0:T(8,128)(2,1)S(1)}, bf16[528,256]{1,0:T(8,128)(2,1)}, u32[]{:S(2)}, u32[]{:S(2)}) collective-permute-start(bf16[528,256]{1,0:T(8,128)(2,1)S(1)} %pad_maximum_fusion.1.refs_0_), channel_id=1, source_target_pairs={{0,4},{2,6},{4,0},{6,2},{1,5},{3,7},{5,1},{7,3},{8,12},{10,14},{12... | collective-permute-start | bytes 811016 | tf_op jit(solution)/shard_map/ppermute | solution.py:44
  85.9 13.1 %collective-permute-start.3 = (bf16[528,256]{1,0:T(8,128)(2,1)S(1)}, bf16[528,256]{1,0:T(8,128)(2,1)}, u32[]{:S(2)}, u32[]{:S(2)}) collective-permute-start(bf16[528,256]{1,0:T(8,128)(2,1)S(1)} %pad_maximum_fusion.1.refs_0_), channel_id=1, source_target_pairs={{0,1},{1,0},{2,3},{3,2},{4,5},{5,4},{6,7},{7,6},{8,9},{9,8},{10,11... | collective-permute-start | bytes 811016 | tf_op jit(solution)/shard_map/ppermute | solution.py:34
  90.9 8.1 %collective-permute-start.4 = (bf16[528,256]{1,0:T(8,128)(2,1)}, bf16[528,256]{1,0:T(8,128)(2,1)}, u32[]{:S(2)}, u32[]{:S(2)}) collective-permute-start(bf16[528,256]{1,0:T(8,128)(2,1)} %collective-permute-done.refs_1_), channel_id=1, source_target_pairs={{0,1},{1,0},{2,3},{3,2},{4,5},{5,4},{6,7},{7,6},{8,9},{9,8},{10,11... | collective-permute-start | bytes 811016 | tf_op jit(solution)/shard_map/ppermute | solution.py:34
  92.9 6.1 %collective-permute-start.5 = (bf16[528,256]{1,0:T(8,128)(2,1)}, bf16[528,256]{1,0:T(8,128)(2,1)}, u32[]{:S(2)}, u32[]{:S(2)}) collective-permute-start(bf16[528,256]{1,0:T(8,128)(2,1)} %collective-permute-done.1.refs_2_), channel_id=1, source_target_pairs={{0,1},{1,0},{2,3},{3,2},{4,5},{5,4},{6,7},{7,6},{8,9},{9,8},{10,11... | collective-permute-start | bytes 811016 | tf_op jit(solution)/shard_map/ppermute | solution.py:34
  97.0 3.8 %collective-permute-start.6 = (bf16[528,256]{1,0:T(8,128)(2,1)}, bf16[528,256]{1,0:T(8,128)(2,1)}, u32[]{:S(2)}, u32[]{:S(2)}) collective-permute-start(bf16[528,256]{1,0:T(8,128)(2,1)} %collective-permute-done.2.refs_3_), channel_id=1, source_target_pairs={{0,1},{1,0},{2,3},{3,2},{4,5},{5,4},{6,7},{7,6},{8,9},{9,8},{10,11... | collective-permute-start | bytes 811016 | tf_op jit(solution)/shard_map/ppermute | solution.py:34
  103.3 1.3 copy-start
  110.3 1.6 copy-start.1
  111.9 10.4 %copy-start.15 = (bf16[256]{0:T(256)(128)(2,1)S(1)}, bf16[256]{0:T(256)(128)(2,1)}, u32[]{:S(2)}) copy-start(bf16[256]{0:T(256)(128)(2,1)} %param.19) | copy-start | bytes 1540
  111.9 10.4 %copy-start.16 = (bf16[256]{0:T(256)(128)(2,1)S(1)}, bf16[256]{0:T(256)(128)(2,1)}, u32[]{:S(2)}) copy-start(bf16[256]{0:T(256)(128)(2,1)} %param.20) | copy-start | bytes 1540
  113.4 0.8 copy-start.5
  114.8 12.2 %all-to-all-start.2 = ((f32[8,2,512]{2,1,0:T(2,128)}), f32[8,2,512]{2,1,0:T(2,128)S(1)}, u32[]{:S(2)}, u32[]{:S(2)}) async-start(f32[8,2,512]{2,1,0:T(2,128)} %broadcast_in_dim.43), calls=%async_computation.2 | async-start | bytes 65536 | tf_op jit(solution)/shard_map/all_to_all | solution.py:30
  122.3 1.6 copy-start.2
  123.9 3.1 %copy-start.7 = (bf16[2,128,128]{2,1,0:T(8,128)(2,1)S(1)}, bf16[2,128,128]{2,1,0:T(8,128)(2,1)}, u32[]{:S(2)}) copy-start(bf16[2,128,128]{2,1,0:T(8,128)(2,1)} %mix.3) | copy-start | bytes 196612
  123.9 3.1 %copy-start.10 = (bf16[2,128]{1,0:T(2,128)(2,1)S(1)}, bf16[2,128]{1,0:T(2,128)(2,1)}, u32[]{:S(2)}) copy-start(bf16[2,128]{1,0:T(2,128)(2,1)} %bias.1) | copy-start | bytes 1540
  125.2 0.8 copy-start.3
  127.0 1.1 copy-start.4
  128.1 1.1 copy-start.6
  130.7 4.8 %collective-permute-start.10 = (bf16[4,512,256]{2,1,0:T(8,128)(2,1)S(1)}, bf16[4,512,256]{2,1,0:T(8,128)(2,1)S(1)}, u32[]{:S(2)}, u32[]{:S(2)}) collective-permute-start(bf16[4,512,256]{2,1,0:T(8,128)(2,1)S(1)} %get-tuple-element.18), channel_id=1, source_target_pairs={{0,1},{1,0},{2,3},{3,2},{4,5},{5,4},{6,7},{7,6},{8,9},{9,8},{10,11... | collective-permute-start | bytes 3145736 | tf_op jit(solution)/shard_map/ppermute | solution.py:34
  135.8 17.2 %copy-start.12 = (bf16[512,256]{1,0:T(8,128)(2,1)S(1)}, bf16[512,256]{1,0:T(8,128)(2,1)}, u32[]{:S(2)}) copy-start(bf16[512,256]{1,0:T(8,128)(2,1)} %param.15) | copy-start | bytes 786436
  153.0 22.8 %copy-start.8 = (bf16[3,512]{1,0:T(4,128)(2,1)S(1)}, bf16[3,512]{1,0:T(4,128)(2,1)}, u32[]{:S(2)}) copy-start(bf16[3,512]{1,0:T(4,128)(2,1)} %conv_gate.1) | copy-start | bytes 9220
  153.0 22.8 %copy-start.9 = (bf16[3,512]{1,0:T(4,128)(2,1)S(1)}, bf16[3,512]{1,0:T(4,128)(2,1)}, u32[]{:S(2)}) copy-start(bf16[3,512]{1,0:T(4,128)(2,1)} %conv_value.1) | copy-start | bytes 9220
  168.9 6.8 %collective-permute-start.11 = (bf16[4,512,256]{2,1,0:T(8,128)(2,1)S(1)}, bf16[4,512,256]{2,1,0:T(8,128)(2,1)S(1)}, u32[]{:S(2)}, u32[]{:S(2)}) collective-permute-start(bf16[4,512,256]{2,1,0:T(8,128)(2,1)S(1)} %all_to_all.31.mine), channel_id=1, source_target_pairs={{0,1},{1,0},{2,3},{3,2},{4,5},{5,4},{6,7},{7,6},{8,9},{9,8},{10,11... | collective-permute-start | bytes 3145736 | tf_op jit(solution)/shard_map/ppermute | solution.py:34
  182.8 4.6 %collective-permute-start.15 = (bf16[4,512,256]{2,1,0:T(8,128)(2,1)S(1)}, bf16[4,512,256]{2,1,0:T(8,128)(2,1)S(1)}, u32[]{:S(2)}, u32[]{:S(2)}) collective-permute-start(bf16[4,512,256]{2,1,0:T(8,128)(2,1)S(1)} %get-tuple-element.22), channel_id=1, source_target_pairs={{0,1},{1,0},{2,3},{3,2},{4,5},{5,4},{6,7},{7,6},{8,9},{9,8},{10,11... | collective-permute-start | bytes 3145736 | tf_op jit(solution)/shard_map/ppermute | solution.py:34
Sparse Core Ops, SparseCore 0:
  69.2 77.1 all-gather.1

commit v5 on v4

--- a/solution.py
+++ b/solution.py
@@ -44,73 +44,68 @@
     return [shard] + [lax.ppermute(shard, axis, [(i, (i + step) % size) for i in range(size)]) for step in steps]
 
 
-def in_order(parts, axis):
-    here = lax.axis_index(axis).astype(jnp.uint32)
-    filled = jnp.zeros((4, *parts[0].shape), parts[0].dtype)
-    for step, part in zip(RING, parts):
-        at = (here + jnp.uint32(4 - step)) & jnp.uint32(3)
-        filled = lax.dynamic_update_slice(filled, part[None], (at, *([jnp.uint32(0)] * part.ndim)))
-    return filled
-
-
-def norm_kernel(place, *refs):
-    parts, (out, gain_two) = refs[:8], refs[8:]
-    count, width = parts[0].shape[0] - 16, parts[0].shape[1]
+def doubled(blocks, step):
+    came = lax.ppermute(blocks, "y", [(i, i ^ step) for i in range(4)])
+    upper = (lax.axis_index("y") & step) != 0
+    return jnp.concatenate([jnp.where(upper, came, blocks), jnp.where(upper, blocks, came)], axis=0)
+
+
+def norm_kernel(place, p0, p1, p2, p3, out, gain_two):
+    parts = (p0, p1, p2, p3)
+    count, width = p0.shape[1] - 16, p0.shape[2]
     x, c = place[0], place[1]
     for part in range(count // BLOCK):
         rows = pl.ds(part * BLOCK, BLOCK)
         squares = jnp.zeros((BLOCK, width), F32)
         for ref in parts:
-            value = ref[rows, :].astype(F32)
-            squares = squares + value * value
+            for side in range(2):
+                value = ref[side, rows, :].astype(F32)
+                squares = squares + value * value
         scale = lax.rsqrt(jnp.sum(squares, axis=1, keepdims=True) / (8 * width) + EPS)
-        for at, ref in enumerate(parts):
-            block = origin(x, RING[at % 4]) * 2 + (c if at < 4 else 1 - c)
-            gain = ref[count : count + 1, :].astype(F32)
-            out[rows, pl.ds(pl.multiple_of(block * width, width), width)] = (
-                ref[rows, :].astype(F32) * scale * gain
-            ).astype(BF16)
-    for at, ref in enumerate(parts):
-        block = origin(x, RING[at % 4]) * 2 + (c if at < 4 else 1 - c)
-        gain_two[block] = ref[count + 8 : count + 16, :]
+        for step, ref in zip(RING, parts):
+            for side in range(2):
+                block = origin(x, step) * 2 + (1 - c if side else c)
+                gain = ref[side, count : count + 1, :].astype(F32)
+                out[rows, pl.ds(pl.multiple_of(block * width, width), width)] = (
+                    ref[side, rows, :].astype(F32) * scale * gain
+                ).astype(BF16)
+    for step, ref in zip(RING, parts):
+        for side in range(2):
+            block = origin(x, step) * 2 + (1 - c if side else c)
+            gain_two[block] = ref[side, count + 8 : count + 16, :]
 
 
 def origin(here, step):
     return (here + (4 - step)) & 3
 
 
-def fill_rows(weight, early, near, cols):
-    for y in range(4):
-        for at, step in enumerate(RING):
+def fill_rows(weight, parts, y, z):
+    for step, part in zip(RING, parts):
+        for at, less in enumerate(RING):
             for far in range(4):
-                start = pl.multiple_of(((far * 4 + origin(near, step)) * 4 + y) * PIECE, PIECE)
+                start = pl.multiple_of(((far * 4 + origin(z, less)) * 4 + origin(y, step)) * PIECE, PIECE)
                 came = (at * 4 + far) * PIECE
-                weight[pl.ds(start, PIECE), :] = early[y, came : came + PIECE, cols]
-
-
-def stats_kernel(place, normed, early, act, sums, weight):
-    width = act.shape[1]
-    fill_rows(weight, early, place[2], slice(width, 2 * width))
+                weight[pl.ds(start, PIECE), :] = part[came : came + PIECE, :]
+
+
+def first_kernel(place, normed, p0, p1, p2, p3, act_u, act_v, sums, weight):
+    width = act_u.shape[1]
+    fill_rows(weight, (p0, p1, p2, p3), place[2], place[3])
     for part in range(normed.shape[0] // SEQ_LEN):
         rows = pl.ds(part * SEQ_LEN, SEQ_LEN)
-        value = gelu(jnp.dot(normed[rows, :], weight[...], preferred_element_type=F32))
-        act[rows, :] = value
+        both = gelu(jnp.dot(normed[rows, :], weight[...], preferred_element_type=F32))
+        act_u[rows, :] = both[:, :width]
+        value = both[:, width:]
+        act_v[rows, :] = value
         once = sum(value[:, k : k + 128] for k in range(0, width, 128))
         twice = sum(value[:, k : k + 128] * value[:, k : k + 128] for k in range(0, width, 128))
         sums[0:1, rows] = jnp.sum(once.T, axis=0, keepdims=True)
         sums[1:2, rows] = jnp.sum(twice.T, axis=0, keepdims=True)
 
 
-def gate_kernel(place, normed, early, act, weight):
-    fill_rows(weight, early, place[2], slice(0, act.shape[1]))
-    for part in range(normed.shape[0] // SEQ_LEN):
-        rows = pl.ds(part * SEQ_LEN, SEQ_LEN)
-        act[rows, :] = gelu(jnp.dot(normed[rows, :], weight[...], preferred_element_type=F32))
-
-
-def mix_kernel(place, act_v, act_u, stats, gain, shift, mix, bias, early, give, keep, weight, gated):
+def mix_kernel(place, act_v, act_u, stats, gain, shift, mix, bias, p0, p1, p2, p3, give, keep, weight, gated):
     width = act_v.shape[1]
-    fill_rows(weight, early, place[2], slice(2 * width, 3 * width))
+    fill_rows(weight, (p0, p1, p2, p3), place[2], place[3])
     full = width * stats.shape[0]
     i = lax.broadcasted_iota(jnp.int32, (BLOCK, BLOCK), 0)
     j = lax.broadcasted_iota(jnp.int32, (BLOCK, BLOCK), 1)
@@ -248,51 +243,44 @@
 
     early = jnp.concatenate([proj_u, proj_v, proj_out.T], axis=1)
     early_far = everyones(early, "zh").reshape(-1, early.shape[1])
-    early_z = jnp.stack(round_ring(early_far, Z))
-    early_all = everyones(early_z, "y").reshape(4, -1, early.shape[1])
+    early_z = round_ring(early_far, Z)
+    early_parts = round_ring(jnp.concatenate([part[:, : 2 * da] for part in early_z], axis=0), "y")
+    out_parts = round_ring(jnp.concatenate([part[:, 2 * da :] for part in early_z], axis=0), "y")
 
     late = jnp.concatenate([ffn_gate, ffn_value, proj_down.T], axis=1)
-    late_y = in_order(round_ring(late, "y"), "y").reshape(-1, late.shape[1])
-    late_all = lax.all_gather(after(late_y, early_z), Z, axis=0, tiled=True)
+    late_pair = doubled(late[None], 1)
+    late_y = doubled(late_pair, 2).reshape(-1, late.shape[1])
+    late_all = lax.all_gather(after(late_y, *early_z), Z, axis=0, tiled=True)
 
     packed = jnp.concatenate([tokens, jnp.broadcast_to(norm_gain, (8, da)), jnp.broadcast_to(ffn_gain, (8, da))], axis=0)
-    mine = round_ring(packed, "x")
-    other = [other_core(part) for part in mine]
-    place = jnp.stack([lax.axis_index(name).astype(jnp.int32) for name in ("x", "c", "zl")])
+    pair = jnp.stack([packed, other_core(packed)])
+    token_parts = round_ring(pair, "x")
+    place = jnp.stack([lax.axis_index(name).astype(jnp.int32) for name in ("x", "c", "y", "zl")])
     model = proj_u.shape[0] * lax.axis_size(FS)
     tp = lax.axis_size(TP)
     normed, gain_two = pl.pallas_call(
         norm_kernel,
-        in_specs=[SMEM] + [VMEM] * 8,
+        in_specs=[SMEM] + [VMEM] * 4,
         out_specs=[VMEM] * 2,
         out_shape=[shape((row_count, model), BF16), shape((tp, 8, da), BF16)],
         name="norm",
         compiler_params=room(12),
-    )(place, *mine, *other)
-
-    act_v, sums = pl.pallas_call(
-        stats_kernel,
-        in_specs=[SMEM] + [VMEM] * 2,
-        out_specs=[VMEM] * 2,
-        out_shape=[shape((row_count, da), F32), shape((2, row_count), F32)],
-        scratch_shapes=[pltpu.VMEM((model, da), BF16)],
-        name="stats",
+    )(place, *token_parts)
+
+    act_u, act_v, sums = pl.pallas_call(
+        first_kernel,
+        in_specs=[SMEM] + [VMEM] * 5,
+        out_specs=[VMEM] * 3,
+        out_shape=[shape((row_count, da), F32)] * 2 + [shape((2, row_count), F32)],
+        scratch_shapes=[pltpu.VMEM((model, 2 * da), BF16)],
+        name="first",
         compiler_params=room(14),
-    )(place, normed, early_all)
+    )(place, normed, *early_parts)
     stats = everyones(sums, TP)
-    act_u = pl.pallas_call(
-        gate_kernel,
-        in_specs=[SMEM] + [VMEM] * 2,
-        out_specs=VMEM,
-        out_shape=shape((row_count, da), F32),
-        scratch_shapes=[pltpu.VMEM((model, da), BF16)],
-        name="gate",
-        compiler_params=room(14),
-    )(place, normed, early_all)
     blocks = [shape((lax.axis_size("x"), row_count, da), BF16)] * 2
     give, keep = pl.pallas_call(
         mix_kernel,
-        in_specs=[SMEM] + [VMEM] * 8,
+        in_specs=[SMEM] + [VMEM] * 11,
         out_specs=[VMEM] * 2,
         out_shape=blocks,
         scratch_shapes=[pltpu.VMEM((model, da), BF16), pltpu.VMEM((row_count, da), BF16)],
@@ -307,7 +295,7 @@
         layer_shift[None],
         mix_weight,
         mix_bias,
-        early_all,
+        *out_parts,
     )
     stream = (tokens.astype(F32) + summed_at_owner(give, keep)).astype(BF16)
     mine = everyones(stream, "x")

time: 214 us -> 216 us (level)
  local copies, waits for them, and re-layouts: 11.7 us -> 4.06 us
  starting transfers between devices: 82 us -> 86.4 us
  waiting for transfers between devices: 36 us -> 39.9 us
    ppermute x0 -> x2, starting transfers between devices: none -> 8.99 us  [doubled(): came = lax.ppermute(blocks, 'y', [(i, i ^ step) for i in range(4)])]
    unnamed x34 -> x26, local copies, waits for them, and re-layouts: 8.26 us -> 0.07 us
    ppermute x7 -> x4, starting transfers between devices: 22.4 us -> 15.2 us  [other_core(): return lax.ppermute(value, 'c', SWAP)]
    ppermute x9 -> x12, starting transfers between devices: 33.6 us -> 37.4 us  [round_ring(): lax.ppermute(shard, axis, [(i, (i + step) % size) for i in range(size)])]
    ppermute x9 -> x12, waiting for transfers between devices: 8.93 us -> 12.7 us  [round_ring(): lax.ppermute(shard, axis, [(i, (i + step) % size) for i in range(size)])]
    slice x0 -> x8, local copies, waits for them, and re-layouts: none -> 2.59 us  [the longest x4 2.54 us: on_device(): part[:, 2 * da:]]
    all_to_all x3 -> x2, starting transfers between devices: 26 us -> 24.8 us  [everyones(): return lax.all_to_all(copies, axis, split_axis=0, concat_axis=0, tiled=True)]
    all_to_all x3 -> x2, waiting for transfers between devices: 18.4 us -> 17.3 us  [everyones(): return lax.all_to_all(copies, axis, split_axis=0, concat_axis=0, tiled=True)]
  transfers between devices with their start and end apart: 20 -> 21, of which waited for: 9 -> 10; matrix products, arithmetic and copies ran while one was open for 3% -> 3% of each run, Pallas kernels for 3% -> 3%
where the time goes in v5:
time: 216 us; the launch traced here: 214 us
  starting transfers between devices  86.4 us (40%)
  blocking collectives  51 us (24%)
  waiting for transfers between devices  39.9 us (18%)
  between operations  13.9 us (6%)
  Pallas kernels  13.6 us (6%)
  other arithmetic  5.14 us (2%)
  local copies, waits for them, and re-layouts  4.06 us (2%)
    ppermute x12, starting transfers between devices, round_ring(): lax.ppermute(shard, axis, [(i, (i + step) % size) for i in range(size)])  37.4 us
    all_to_all x2, blocking collectives, summed_at_owner(): arrived = lax.all_to_all(pair, 'x', split_axis=0, concat_axis=0, tiled=True)  34.6 us
    all_to_all x2, starting transfers between devices, everyones(): return lax.all_to_all(copies, axis, split_axis=0, concat_axis=0, tiled=True)  24.8 us
    all_to_all x2, waiting for transfers between devices, everyones(): return lax.all_to_all(copies, axis, split_axis=0, concat_axis=0, tiled=True)  17.3 us
    all_to_all x1, blocking collectives, everyones(): return lax.all_to_all(copies, axis, split_axis=0, concat_axis=0, tiled=True)  16.4 us
    ppermute x4, starting transfers between devices, other_core(): return lax.ppermute(value, 'c', SWAP)  15.2 us
    ppermute x12, waiting for transfers between devices, round_ring(): lax.ppermute(shard, axis, [(i, (i + step) % size) for i in range(size)])  12.7 us
    ppermute x2, starting transfers between devices, doubled(): came = lax.ppermute(blocks, 'y', [(i, i ^ step) for i in range(4)])  8.99 us
  transfers between devices with their start and end apart: 21, of which 10 were waited for; matrix products, arithmetic and copies ran while one was open for 3% of the time, Pallas kernels for 3%

profile of v5, /device:TPU:1, one launch (start us, length us, event | category | flops | bytes accessed | tf_op | source)
XLA Modules:
  0.0 214.0 jit_solution(9124008001589138345)
XLA Ops:
  6.5 0.8 maximum_bitcast_fusion
  7.4 4.0 %collective-permute-start.15 = (bf16[1,32,1536]{2,1,0:T(8,128)(2,1)S(1)}, bf16[1,32,1536]{2,1,0:T(8,128)(2,1)S(1)}, u32[]{:S(2)}, u32[]{:S(2)}) collective-permute-start(bf16[1,32,1536]{2,1,0:T(8,128)(2,1)S(1)} %maximum_bitcast_fusion), channel_id=1, source_target_pairs={{0,8},{8,0},{16,24},{24,16},{1,9},{9,1},{17,25},{25,17},{2,10},{10... | collective-permute-start | bytes 294920 | tf_op jit(solution)/shard_map/ppermute | solution.py:48
  11.4 2.0 collective-permute-done.15
  13.4 0.8 broadcast_select_fusion.3
  14.3 5.0 %collective-permute-start.16 = (bf16[2,32,1536]{2,1,0:T(8,128)(2,1)S(1)}, bf16[2,32,1536]{2,1,0:T(8,128)(2,1)S(1)}, u32[]{:S(2)}, u32[]{:S(2)}) collective-permute-start(bf16[2,32,1536]{2,1,0:T(8,128)(2,1)S(1)} %pad_maximum_fusion.5), channel_id=1, source_target_pairs={{0,16},{8,24},{16,0},{24,8},{1,17},{9,25},{17,1},{25,9},{2,18},{10... | collective-permute-start | bytes 589832 | tf_op jit(solution)/shard_map/ppermute | solution.py:48
  19.2 0.8 pad_maximum_fusion.6
  20.0 0.7 broadcast_in_dim.26
  20.7 14.8 %all-to-all-start = ((bf16[4,32,768]{2,1,0:T(8,128)(2,1)}), bf16[4,32,768]{2,1,0:T(8,128)(2,1)S(1)}, u32[]{:S(2)}, u32[]{:S(2)}) async-start(bf16[4,32,768]{2,1,0:T(8,128)(2,1)} %broadcast_in_dim.26), calls=%async_computation | async-start | bytes 393216 | tf_op jit(solution)/shard_map/all_to_all | solution.py:30
  35.5 12.6 %all-to-all-done = bf16[4,32,768]{2,1,0:T(8,128)(2,1)S(1)} async-done(((bf16[4,32,768]{2,1,0:T(8,128)(2,1)}), bf16[4,32,768]{2,1,0:T(8,128)(2,1)S(1)}, u32[]{:S(2)}, u32[]{:S(2)}) %all-to-all-start) | async-done | bytes 196640 | tf_op jit(solution)/shard_map/all_to_all | solution.py:30
  48.1 4.2 %collective-permute-start.4 = (bf16[128,768]{1,0:T(8,128)(2,1)S(1)}, bf16[128,768]{1,0:T(8,128)(2,1)S(1)}, u32[]{:S(2)}, u32[]{:S(2)}) collective-permute-start(bf16[128,768]{1,0:T(8,128)(2,1)S(1)} %bitcast.18), channel_id=1, source_target_pairs={{0,32},{32,64},{64,96},{96,128},{128,160},{160,192},{192,224},{224... | collective-permute-start | bytes 589832 | tf_op jit(solution)/shard_map/ppermute | solution.py:44
  52.3 2.3 %collective-permute-start.5 = (bf16[128,768]{1,0:T(8,128)(2,1)S(1)}, bf16[128,768]{1,0:T(8,128)(2,1)S(1)}, u32[]{:S(2)}, u32[]{:S(2)}) collective-permute-start(bf16[128,768]{1,0:T(8,128)(2,1)S(1)} %bitcast.19), channel_id=1, source_target_pairs={{0,480},{32,0},{64,32},{96,64},{128,96},{160,128},{192,160},{224,1... | collective-permute-start | bytes 589832 | tf_op jit(solution)/shard_map/ppermute | solution.py:44
  54.6 3.4 %collective-permute-start.6 = (bf16[128,768]{1,0:T(8,128)(2,1)S(1)}, bf16[128,768]{1,0:T(8,128)(2,1)S(1)}, u32[]{:S(2)}, u32[]{:S(2)}) collective-permute-start(bf16[128,768]{1,0:T(8,128)(2,1)S(1)} %bitcast.20), channel_id=1, source_target_pairs={{0,64},{32,96},{64,128},{96,160},{128,192},{160,224},{192,256},{22... | collective-permute-start | bytes 589832 | tf_op jit(solution)/shard_map/ppermute | solution.py:44
  58.0 0.8 pad_maximum_fusion.2
  58.9 7.8 %collective-permute-done.6 = bf16[128,768]{1,0:T(8,128)(2,1)S(1)} collective-permute-done((bf16[128,768]{1,0:T(8,128)(2,1)S(1)}, bf16[128,768]{1,0:T(8,128)(2,1)S(1)}, u32[]{:S(2)}, u32[]{:S(2)}) %collective-permute-start.6) | collective-permute-done | bytes 196640 | tf_op jit(solution)/shard_map/ppermute | solution.py:44
  66.6 0.0 all-gather.2.cloned.1.call-update
  66.7 6.4 %collective-permute-start = (bf16[528,256]{1,0:T(8,128)(2,1)S(1)}, bf16[528,256]{1,0:T(8,128)(2,1)S(1)}, u32[]{:S(2)}, u32[]{:S(2)}) collective-permute-start(bf16[528,256]{1,0:T(8,128)(2,1)S(1)} %get-tuple-element.28), channel_id=1, source_target_pairs={{0,1},{1,0},{2,3},{3,2},{4,5},{5,4},{6,7},{7,6},{8,9},{9,8},{10,11... | collective-permute-start | bytes 811016 | tf_op jit(solution)/shard_map/ppermute | solution.py:34
  73.1 1.2 collective-permute-done
  74.3 0.1 pad_maximum_fusion.p0
  74.3 3.1 %collective-permute-start.1 = (bf16[2,528,256]{2,1,0:T(8,128)(2,1)S(1)}, bf16[2,528,256]{2,1,0:T(8,128)(2,1)S(1)}, u32[]{:S(2)}, u32[]{:S(2)}) collective-permute-start(bf16[2,528,256]{2,1,0:T(8,128)(2,1)S(1)} %pad_maximum_fusion.p0), channel_id=1, source_target_pairs={{0,2},{2,4},{4,6},{6,0},{1,3},{3,5},{5,7},{7,1},{8,10},{10,12},{12... | collective-permute-start | bytes 1622024 | tf_op jit(solution)/shard_map/ppermute | solution.py:44
  77.5 3.4 %collective-permute-start.2 = (bf16[2,528,256]{2,1,0:T(8,128)(2,1)S(1)}, bf16[2,528,256]{2,1,0:T(8,128)(2,1)S(1)}, u32[]{:S(2)}, u32[]{:S(2)}) collective-permute-start(bf16[2,528,256]{2,1,0:T(8,128)(2,1)S(1)} %pad_maximum_fusion.p0), channel_id=1, source_target_pairs={{0,6},{2,0},{4,2},{6,4},{1,7},{3,1},{5,3},{7,5},{8,14},{10,8},{12,... | collective-permute-start | bytes 1622024 | tf_op jit(solution)/shard_map/ppermute | solution.py:44
  80.8 3.4 %collective-permute-start.3 = (bf16[2,528,256]{2,1,0:T(8,128)(2,1)S(1)}, bf16[2,528,256]{2,1,0:T(8,128)(2,1)S(1)}, u32[]{:S(2)}, u32[]{:S(2)}) collective-permute-start(bf16[2,528,256]{2,1,0:T(8,128)(2,1)S(1)} %pad_maximum_fusion.p0), channel_id=1, source_target_pairs={{0,4},{2,6},{4,0},{6,2},{1,5},{3,7},{5,1},{7,3},{8,12},{10,14},{12... | collective-permute-start | bytes 1622024 | tf_op jit(solution)/shard_map/ppermute | solution.py:44
  84.4 2.3 %collective-permute-start.7 = (bf16[512,512]{1,0:T(8,128)(2,1)S(1)}, bf16[512,512]{1,0:T(8,128)(2,1)S(1)}, u32[]{:S(2)}, u32[]{:S(2)}) collective-permute-start(bf16[512,512]{1,0:T(8,128)(2,1)S(1)} %pad_maximum_fusion.1.p0), channel_id=1, source_target_pairs={{0,8},{8,16},{16,24},{24,0},{1,9},{9,17},{17,25},{25,1},{2,10},{10... | collective-permute-start | bytes 1572872 | tf_op jit(solution)/shard_map/ppermute | solution.py:44
  86.8 4.2 %collective-permute-start.8 = (bf16[512,512]{1,0:T(8,128)(2,1)S(1)}, bf16[512,512]{1,0:T(8,128)(2,1)}, u32[]{:S(2)}, u32[]{:S(2)}) collective-permute-start(bf16[512,512]{1,0:T(8,128)(2,1)S(1)} %pad_maximum_fusion.1.p0), channel_id=1, source_target_pairs={{0,24},{8,0},{16,8},{24,16},{1,25},{9,1},{17,9},{25,17},{2,26},{10... | collective-permute-start | bytes 1572872 | tf_op jit(solution)/shard_map/ppermute | solution.py:44
  90.9 0.1 collective-permute-done.1.p1
  91.0 2.0 collective-permute-start.9
  93.0 0.8 slice.37
  93.8 0.8 slice.38
  94.7 0.8 slice.39
  95.5 0.0 collective-permute-done.2.p2
  95.5 3.2 %collective-permute-start.10 = (bf16[512,256]{1,0:T(8,128)(2,1)S(1)}, bf16[512,256]{1,0:T(8,128)(2,1)}, u32[]{:S(2)}, u32[]{:S(2)}) collective-permute-start(bf16[512,256]{1,0:T(8,128)(2,1)S(1)} %pad_maximum_fusion.4.p0), channel_id=1, source_target_pairs={{0,8},{8,16},{16,24},{24,0},{1,9},{9,17},{17,25},{25,1},{2,10},{10... | collective-permute-start | bytes 786440 | tf_op jit(solution)/shard_map/ppermute | solution.py:44
  98.8 4.8 %collective-permute-done.3.p3 = bf16[2,528,256]{2,1,0:T(8,128)(2,1)S(1)} collective-permute-done((bf16[2,528,256]{2,1,0:T(8,128)(2,1)S(1)}, bf16[2,528,256]{2,1,0:T(8,128)(2,1)S(1)}, u32[]{:S(2)}, u32[]{:S(2)}) %collective-permute-start.3) | collective-permute-done | bytes 540704 | tf_op jit(solution)/shard_map/ppermute | solution.py:44
  103.6 2.6 %collective-permute-start.11 = (bf16[512,256]{1,0:T(8,128)(2,1)S(1)}, bf16[512,256]{1,0:T(8,128)(2,1)}, u32[]{:S(2)}, u32[]{:S(2)}) collective-permute-start(bf16[512,256]{1,0:T(8,128)(2,1)S(1)} %pad_maximum_fusion.4.p0), channel_id=1, source_target_pairs={{0,24},{8,0},{16,8},{24,16},{1,25},{9,1},{17,9},{25,17},{2,26},{10... | collective-permute-start | bytes 786440 | tf_op jit(solution)/shard_map/ppermute | solution.py:44
  106.2 3.3 %collective-permute-start.12 = (bf16[512,256]{1,0:T(8,128)(2,1)S(1)}, bf16[512,256]{1,0:T(8,128)(2,1)}, u32[]{:S(2)}, u32[]{:S(2)}) collective-permute-start(bf16[512,256]{1,0:T(8,128)(2,1)S(1)} %pad_maximum_fusion.4.p0), channel_id=1, source_target_pairs={{0,16},{8,24},{16,0},{24,8},{1,17},{9,25},{17,1},{25,9},{2,18},{10... | collective-permute-start | bytes 786440 | tf_op jit(solution)/shard_map/ppermute | solution.py:44
  109.5 0.1 pad_add_fusion.place
  109.6 1.6 norm.1
  111.2 0.0 copy-start.11
  111.2 0.0 copy-start.12
  111.2 0.0 copy-start
  111.2 0.0 copy-start.3
  111.2 2.9 %first.1 = (f32[512,256]{1,0:T(8,128)S(1)}, f32[512,256]{1,0:T(8,128)S(1)}, f32[2,512]{1,0:T(2,128)S(1)}) custom-call(s32[4]{0:T(128)S(1)} %pad_add_fusion.place, bf16[512,2048]{1,0:T(8,128)(2,1)S(1)} %get-tuple-element.15.normed, bf16[512,512]{1,0:T(8,128)(2,1)S(1)} %pad_maximum_fusion.1.p0, bf16[512,512]{1,0:T(8,128)(2,1)S(1)} %collective-permute-done.7.p1, ...), custom_call_target="tpu_custom_call" | custom-call | tf_op jit(solution)/shard_map/first/pallas_call | solution.py:270
  114.1 0.6 broadcast_in_dim.27
  114.7 10.0 %all-to-all-start.1 = ((f32[8,2,512]{2,1,0:T(2,128)}), f32[8,2,512]{2,1,0:T(2,128)S(1)}, u32[]{:S(2)}, u32[]{:S(2)}) async-start(f32[8,2,512]{2,1,0:T(2,128)} %broadcast_in_dim.27), calls=%async_computation.1 | async-start | bytes 65536 | tf_op jit(solution)/shard_map/all_to_all | solution.py:30
  124.8 4.7 %all-to-all-done.1.stats = f32[8,2,512]{2,1,0:T(2,128)S(1)} async-done(((f32[8,2,512]{2,1,0:T(2,128)}), f32[8,2,512]{2,1,0:T(2,128)S(1)}, u32[]{:S(2)}, u32[]{:S(2)}) %all-to-all-start.1) | async-done | bytes 32800 | tf_op jit(solution)/shard_map/all_to_all | solution.py:30
  129.5 2.1 %mix.2 = (bf16[4,512,256]{2,1,0:T(8,128)(2,1)S(1)}, bf16[4,512,256]{2,1,0:T(8,128)(2,1)S(1)}) custom-call(s32[4]{0:T(128)S(1)} %pad_add_fusion.place, f32[512,256]{1,0:T(8,128)S(1)} %get-tuple-element.16.act_v, f32[512,256]{1,0:T(8,128)S(1)} %get-tuple-element.17.act_u, f32[8,2,512]{2,1,0:T(2,128)S(1)} %all-to-all-done.1.stats, ...), custom_call_target="tpu_custom_call" | custom-call | tf_op jit(solution)/shard_map/mix/pallas_call | solution.py:281
  131.7 2.6 %collective-permute-start.13 = (bf16[4,512,256]{2,1,0:T(8,128)(2,1)S(1)}, bf16[4,512,256]{2,1,0:T(8,128)(2,1)S(1)}, u32[]{:S(2)}, u32[]{:S(2)}) collective-permute-start(bf16[4,512,256]{2,1,0:T(8,128)(2,1)S(1)} %get-tuple-element.20), channel_id=1, source_target_pairs={{0,1},{1,0},{2,3},{3,2},{4,5},{5,4},{6,7},{7,6},{8,9},{9,8},{10,11... | collective-permute-start | bytes 3145736 | tf_op jit(solution)/shard_map/ppermute | solution.py:34
  134.3 2.3 %collective-permute-done.13 = bf16[4,512,256]{2,1,0:T(8,128)(2,1)S(1)} collective-permute-done((bf16[4,512,256]{2,1,0:T(8,128)(2,1)S(1)}, bf16[4,512,256]{2,1,0:T(8,128)(2,1)S(1)}, u32[]{:S(2)}, u32[]{:S(2)}) %collective-permute-start.13) | collective-permute-done | bytes 1048608 | tf_op jit(solution)/shard_map/ppermute | solution.py:34
  136.6 0.2 add_convert_fusion.1
  136.8 0.0 copy-start.5
  136.8 17.4 %all_to_all.25 = bf16[4,512,256]{2,1,0:T(8,128)(2,1)S(1)} all-to-all(bf16[4,512,256]{2,1,0:T(8,128)(2,1)S(1)} %add_convert_fusion.1), channel_id=1, replica_groups=mesh['zh'=4,'zl'=4,'y'=4,'x'=4,'c'=2] {'x'}, dimensions={0} | all-to-all | bytes 2097152 | tf_op jit(solution)/shard_map/all_to_all | solution.py:219
  154.2 0.1 convert_reduce_fusion.1
  154.4 0.0 copy-start.1
  154.4 0.0 copy-start.2
  154.4 0.1 add_convert_fusion.3
  154.5 0.1 broadcast_in_dim.30
  154.5 16.4 %all_to_all.26.mine = bf16[4,512,256]{2,1,0:T(8,128)(2,1)S(1)} all-to-all(bf16[4,512,256]{2,1,0:T(8,128)(2,1)S(1)} %broadcast_in_dim.30), channel_id=1, replica_groups=mesh['zh'=4,'zl'=4,'y'=4,'x'=4,'c'=2] {'x'}, dimensions={0} | all-to-all | bytes 2097152 | tf_op jit(solution)/shard_map/all_to_all | solution.py:30
  170.9 4.0 %collective-permute-start.14 = (bf16[4,512,256]{2,1,0:T(8,128)(2,1)S(1)}, bf16[4,512,256]{2,1,0:T(8,128)(2,1)S(1)}, u32[]{:S(2)}, u32[]{:S(2)}) collective-permute-start(bf16[4,512,256]{2,1,0:T(8,128)(2,1)S(1)} %all_to_all.26.mine), channel_id=1, source_target_pairs={{0,1},{1,0},{2,3},{3,2},{4,5},{5,4},{6,7},{7,6},{8,9},{9,8},{10,11... | collective-permute-start | bytes 3145736 | tf_op jit(solution)/shard_map/ppermute | solution.py:34
  174.9 2.3 %collective-permute-done.14.other = bf16[4,512,256]{2,1,0:T(8,128)(2,1)S(1)} collective-permute-done((bf16[4,512,256]{2,1,0:T(8,128)(2,1)S(1)}, bf16[4,512,256]{2,1,0:T(8,128)(2,1)S(1)}, u32[]{:S(2)}, u32[]{:S(2)}) %collective-permute-start.14) | collective-permute-done | bytes 1048608 | tf_op jit(solution)/shard_map/ppermute | solution.py:34
  177.2 7.0 %ffn.1 = (bf16[4,512,256]{2,1,0:T(8,128)(2,1)S(1)}, bf16[4,512,256]{2,1,0:T(8,128)(2,1)S(1)}) custom-call(s32[4]{0:T(128)S(1)} %pad_add_fusion.place, bf16[4,512,256]{2,1,0:T(8,128)(2,1)S(1)} %all_to_all.26.mine, bf16[4,512,256]{2,1,0:T(8,128)(2,1)S(1)} %collective-permute-done.14.other, bf16[8,8,256]{2,1,0:T(8,128)(2,1)S(1)} %get-tuple-element.21.gain, ...), custom_call_target="tpu_custom_call" | custom-call | tf_op jit(solution)/shard_map/ffn/pallas_call | solution.py:302
  184.2 2.3 %collective-permute-start.17 = (bf16[4,512,256]{2,1,0:T(8,128)(2,1)S(1)}, bf16[4,512,256]{2,1,0:T(8,128)(2,1)S(1)}, u32[]{:S(2)}, u32[]{:S(2)}) collective-permute-start(bf16[4,512,256]{2,1,0:T(8,128)(2,1)S(1)} %get-tuple-element.24), channel_id=1, source_target_pairs={{0,1},{1,0},{2,3},{3,2},{4,5},{5,4},{6,7},{7,6},{8,9},{9,8},{10,11... | collective-permute-start | bytes 3145736 | tf_op jit(solution)/shard_map/ppermute | solution.py:34
  186.5 2.3 %collective-permute-done.17 = bf16[4,512,256]{2,1,0:T(8,128)(2,1)S(1)} collective-permute-done((bf16[4,512,256]{2,1,0:T(8,128)(2,1)S(1)}, bf16[4,512,256]{2,1,0:T(8,128)(2,1)S(1)}, u32[]{:S(2)}, u32[]{:S(2)}) %collective-permute-start.17) | collective-permute-done | bytes 1048608 | tf_op jit(solution)/shard_map/ppermute | solution.py:34
  188.7 0.3 add_convert_fusion
  189.0 17.2 %all_to_all.27 = bf16[4,512,256]{2,1,0:T(8,128)(2,1)S(1)} all-to-all(bf16[4,512,256]{2,1,0:T(8,128)(2,1)S(1)} %add_convert_fusion), channel_id=1, replica_groups=mesh['zh'=4,'zl'=4,'y'=4,'x'=4,'c'=2] {'x'}, dimensions={0} | all-to-all | bytes 2097152 | tf_op jit(solution)/shard_map/all_to_all | solution.py:219
  206.3 0.1 convert_reduce_fusion
  206.4 0.8 add_convert_fusion.2
  (44 shorter events, 0.3 us)
Async XLA Ops:
  6.5 60.1 %copy-start.9 = (bf16[256]{0:T(256)(128)(2,1)S(1)}, bf16[256]{0:T(256)(128)(2,1)}, u32[]{:S(2)}) copy-start(bf16[256]{0:T(256)(128)(2,1)} %param.16) | copy-start | bytes 1540
  6.5 60.1 %copy-start.10 = (bf16[256]{0:T(256)(128)(2,1)S(1)}, bf16[256]{0:T(256)(128)(2,1)}, u32[]{:S(2)}) copy-start(bf16[256]{0:T(256)(128)(2,1)} %param.24) | copy-start | bytes 1540
  6.5 60.2 %copy-start.4 = (bf16[512,256]{1,0:T(8,128)(2,1)S(1)}, bf16[512,256]{1,0:T(8,128)(2,1)}, u32[]{:S(2)}) copy-start(bf16[512,256]{1,0:T(8,128)(2,1)} %param.15) | copy-start | bytes 786436
  7.4 6.0 %collective-permute-start.15 = (bf16[1,32,1536]{2,1,0:T(8,128)(2,1)S(1)}, bf16[1,32,1536]{2,1,0:T(8,128)(2,1)S(1)}, u32[]{:S(2)}, u32[]{:S(2)}) collective-permute-start(bf16[1,32,1536]{2,1,0:T(8,128)(2,1)S(1)} %maximum_bitcast_fusion), channel_id=1, source_target_pairs={{0,8},{8,0},{16,24},{24,16},{1,9},{9,1},{17,25},{25,17},{2,10},{10... | collective-permute-start | bytes 294920 | tf_op jit(solution)/shard_map/ppermute | solution.py:48
  14.3 21.2 %collective-permute-start.16 = (bf16[2,32,1536]{2,1,0:T(8,128)(2,1)S(1)}, bf16[2,32,1536]{2,1,0:T(8,128)(2,1)S(1)}, u32[]{:S(2)}, u32[]{:S(2)}) collective-permute-start(bf16[2,32,1536]{2,1,0:T(8,128)(2,1)S(1)} %pad_maximum_fusion.5), channel_id=1, source_target_pairs={{0,16},{8,24},{16,0},{24,8},{1,17},{9,25},{17,1},{25,9},{2,18},{10... | collective-permute-start | bytes 589832 | tf_op jit(solution)/shard_map/ppermute | solution.py:48
  20.7 27.4 %all-to-all-start = ((bf16[4,32,768]{2,1,0:T(8,128)(2,1)}), bf16[4,32,768]{2,1,0:T(8,128)(2,1)S(1)}, u32[]{:S(2)}, u32[]{:S(2)}) async-start(bf16[4,32,768]{2,1,0:T(8,128)(2,1)} %broadcast_in_dim.26), calls=%async_computation | async-start | bytes 393216 | tf_op jit(solution)/shard_map/all_to_all | solution.py:30
  35.5 141.7 %all-gather.2.cloned.1.call-start = ((), (), s32[]{:S(2)}) async-start(), calls=%async_computation.5 | async-start | bytes 6684672 | tf_op jit(solution)/shard_map/all_gather | solution.py:253
  48.1 10.7 %collective-permute-start.4 = (bf16[128,768]{1,0:T(8,128)(2,1)S(1)}, bf16[128,768]{1,0:T(8,128)(2,1)S(1)}, u32[]{:S(2)}, u32[]{:S(2)}) collective-permute-start(bf16[128,768]{1,0:T(8,128)(2,1)S(1)} %bitcast.18), channel_id=1, source_target_pairs={{0,32},{32,64},{64,96},{96,128},{128,160},{160,192},{192,224},{224... | collective-permute-start | bytes 589832 | tf_op jit(solution)/shard_map/ppermute | solution.py:44
  52.3 6.5 %collective-permute-start.5 = (bf16[128,768]{1,0:T(8,128)(2,1)S(1)}, bf16[128,768]{1,0:T(8,128)(2,1)S(1)}, u32[]{:S(2)}, u32[]{:S(2)}) collective-permute-start(bf16[128,768]{1,0:T(8,128)(2,1)S(1)} %bitcast.19), channel_id=1, source_target_pairs={{0,480},{32,0},{64,32},{96,64},{128,96},{160,128},{192,160},{224,1... | collective-permute-start | bytes 589832 | tf_op jit(solution)/shard_map/ppermute | solution.py:44
  54.6 12.0 %collective-permute-start.6 = (bf16[128,768]{1,0:T(8,128)(2,1)S(1)}, bf16[128,768]{1,0:T(8,128)(2,1)S(1)}, u32[]{:S(2)}, u32[]{:S(2)}) collective-permute-start(bf16[128,768]{1,0:T(8,128)(2,1)S(1)} %bitcast.20), channel_id=1, source_target_pairs={{0,64},{32,96},{64,128},{96,160},{128,192},{160,224},{192,256},{22... | collective-permute-start | bytes 589832 | tf_op jit(solution)/shard_map/ppermute | solution.py:44
  58.8 25.5 %copy-start.6 = (bf16[128,768]{1,0:T(8,128)(2,1)}, bf16[128,768]{1,0:T(8,128)(2,1)S(1)}, u32[]{:S(2)}) copy-start(bf16[128,768]{1,0:T(8,128)(2,1)S(1)} %collective-permute-done.4) | copy-start | bytes 589828
  58.8 25.5 %copy-start.7 = (bf16[128,768]{1,0:T(8,128)(2,1)}, bf16[128,768]{1,0:T(8,128)(2,1)S(1)}, u32[]{:S(2)}) copy-start(bf16[128,768]{1,0:T(8,128)(2,1)S(1)} %collective-permute-done.5) | copy-start | bytes 589828
  66.6 17.8 %copy-start.8 = (bf16[128,768]{1,0:T(8,128)(2,1)}, bf16[128,768]{1,0:T(8,128)(2,1)S(1)}, u32[]{:S(2)}) copy-start(bf16[128,768]{1,0:T(8,128)(2,1)S(1)} %collective-permute-done.6) | copy-start | bytes 589828
  66.7 7.5 %collective-permute-start = (bf16[528,256]{1,0:T(8,128)(2,1)S(1)}, bf16[528,256]{1,0:T(8,128)(2,1)S(1)}, u32[]{:S(2)}, u32[]{:S(2)}) collective-permute-start(bf16[528,256]{1,0:T(8,128)(2,1)S(1)} %get-tuple-element.28), channel_id=1, source_target_pairs={{0,1},{1,0},{2,3},{3,2},{4,5},{5,4},{6,7},{7,6},{8,9},{9,8},{10,11... | collective-permute-start | bytes 811016 | tf_op jit(solution)/shard_map/ppermute | solution.py:34
  74.3 16.7 %collective-permute-start.1 = (bf16[2,528,256]{2,1,0:T(8,128)(2,1)S(1)}, bf16[2,528,256]{2,1,0:T(8,128)(2,1)S(1)}, u32[]{:S(2)}, u32[]{:S(2)}) collective-permute-start(bf16[2,528,256]{2,1,0:T(8,128)(2,1)S(1)} %pad_maximum_fusion.p0), channel_id=1, source_target_pairs={{0,2},{2,4},{4,6},{6,0},{1,3},{3,5},{5,7},{7,1},{8,10},{10,12},{12... | collective-permute-start | bytes 1622024 | tf_op jit(solution)/shard_map/ppermute | solution.py:44
  77.5 18.1 %collective-permute-start.2 = (bf16[2,528,256]{2,1,0:T(8,128)(2,1)S(1)}, bf16[2,528,256]{2,1,0:T(8,128)(2,1)S(1)}, u32[]{:S(2)}, u32[]{:S(2)}) collective-permute-start(bf16[2,528,256]{2,1,0:T(8,128)(2,1)S(1)} %pad_maximum_fusion.p0), channel_id=1, source_target_pairs={{0,6},{2,0},{4,2},{6,4},{1,7},{3,1},{5,3},{7,5},{8,14},{10,8},{12,... | collective-permute-start | bytes 1622024 | tf_op jit(solution)/shard_map/ppermute | solution.py:44
  80.8 22.7 %collective-permute-start.3 = (bf16[2,528,256]{2,1,0:T(8,128)(2,1)S(1)}, bf16[2,528,256]{2,1,0:T(8,128)(2,1)S(1)}, u32[]{:S(2)}, u32[]{:S(2)}) collective-permute-start(bf16[2,528,256]{2,1,0:T(8,128)(2,1)S(1)} %pad_maximum_fusion.p0), channel_id=1, source_target_pairs={{0,4},{2,6},{4,0},{6,2},{1,5},{3,7},{5,1},{7,3},{8,12},{10,14},{12... | collective-permute-start | bytes 1622024 | tf_op jit(solution)/shard_map/ppermute | solution.py:44
  84.4 21.7 %collective-permute-start.7 = (bf16[512,512]{1,0:T(8,128)(2,1)S(1)}, bf16[512,512]{1,0:T(8,128)(2,1)S(1)}, u32[]{:S(2)}, u32[]{:S(2)}) collective-permute-start(bf16[512,512]{1,0:T(8,128)(2,1)S(1)} %pad_maximum_fusion.1.p0), channel_id=1, source_target_pairs={{0,8},{8,16},{16,24},{24,0},{1,9},{9,17},{17,25},{25,1},{2,10},{10... | collective-permute-start | bytes 1572872 | tf_op jit(solution)/shard_map/ppermute | solution.py:44
  86.8 24.4 %collective-permute-start.8 = (bf16[512,512]{1,0:T(8,128)(2,1)S(1)}, bf16[512,512]{1,0:T(8,128)(2,1)}, u32[]{:S(2)}, u32[]{:S(2)}) collective-permute-start(bf16[512,512]{1,0:T(8,128)(2,1)S(1)} %pad_maximum_fusion.1.p0), channel_id=1, source_target_pairs={{0,24},{8,0},{16,8},{24,16},{1,25},{9,1},{17,9},{25,17},{2,26},{10... | collective-permute-start | bytes 1572872 | tf_op jit(solution)/shard_map/ppermute | solution.py:44
  91.0 20.1 %collective-permute-start.9 = (bf16[512,512]{1,0:T(8,128)(2,1)S(1)}, bf16[512,512]{1,0:T(8,128)(2,1)}, u32[]{:S(2)}, u32[]{:S(2)}) collective-permute-start(bf16[512,512]{1,0:T(8,128)(2,1)S(1)} %pad_maximum_fusion.1.p0), channel_id=1, source_target_pairs={{0,16},{8,24},{16,0},{24,8},{1,17},{9,25},{17,1},{25,9},{2,18},{10... | collective-permute-start | bytes 1572872 | tf_op jit(solution)/shard_map/ppermute | solution.py:44
  95.5 29.2 %collective-permute-start.10 = (bf16[512,256]{1,0:T(8,128)(2,1)S(1)}, bf16[512,256]{1,0:T(8,128)(2,1)}, u32[]{:S(2)}, u32[]{:S(2)}) collective-permute-start(bf16[512,256]{1,0:T(8,128)(2,1)S(1)} %pad_maximum_fusion.4.p0), channel_id=1, source_target_pairs={{0,8},{8,16},{16,24},{24,0},{1,9},{9,17},{17,25},{25,1},{2,10},{10... | collective-permute-start | bytes 786440 | tf_op jit(solution)/shard_map/ppermute | solution.py:44
  103.6 21.2 %collective-permute-start.11 = (bf16[512,256]{1,0:T(8,128)(2,1)S(1)}, bf16[512,256]{1,0:T(8,128)(2,1)}, u32[]{:S(2)}, u32[]{:S(2)}) collective-permute-start(bf16[512,256]{1,0:T(8,128)(2,1)S(1)} %pad_maximum_fusion.4.p0), channel_id=1, source_target_pairs={{0,24},{8,0},{16,8},{24,16},{1,25},{9,1},{17,9},{25,17},{2,26},{10... | collective-permute-start | bytes 786440 | tf_op jit(solution)/shard_map/ppermute | solution.py:44
  106.2 18.6 %collective-permute-start.12 = (bf16[512,256]{1,0:T(8,128)(2,1)S(1)}, bf16[512,256]{1,0:T(8,128)(2,1)}, u32[]{:S(2)}, u32[]{:S(2)}) collective-permute-start(bf16[512,256]{1,0:T(8,128)(2,1)S(1)} %pad_maximum_fusion.4.p0), channel_id=1, source_target_pairs={{0,16},{8,24},{16,0},{24,8},{1,17},{9,25},{17,1},{25,9},{2,18},{10... | collective-permute-start | bytes 786440 | tf_op jit(solution)/shard_map/ppermute | solution.py:44
  111.2 13.6 %copy-start.11 = (bf16[256]{0:T(256)(128)(2,1)S(1)}, bf16[256]{0:T(256)(128)(2,1)}, u32[]{:S(2)}) copy-start(bf16[256]{0:T(256)(128)(2,1)} %param.19) | copy-start | bytes 1540
  111.2 13.6 %copy-start.12 = (bf16[256]{0:T(256)(128)(2,1)S(1)}, bf16[256]{0:T(256)(128)(2,1)}, u32[]{:S(2)}) copy-start(bf16[256]{0:T(256)(128)(2,1)} %param.20) | copy-start | bytes 1540
  111.2 18.4 %copy-start = (bf16[2,128,128]{2,1,0:T(8,128)(2,1)S(1)}, bf16[2,128,128]{2,1,0:T(8,128)(2,1)}, u32[]{:S(2)}) copy-start(bf16[2,128,128]{2,1,0:T(8,128)(2,1)} %mix.3) | copy-start | bytes 196612
  111.2 18.4 %copy-start.3 = (bf16[2,128]{1,0:T(2,128)(2,1)S(1)}, bf16[2,128]{1,0:T(2,128)(2,1)}, u32[]{:S(2)}) copy-start(bf16[2,128]{1,0:T(2,128)(2,1)} %bias.1) | copy-start | bytes 1540
  114.7 14.8 %all-to-all-start.1 = ((f32[8,2,512]{2,1,0:T(2,128)}), f32[8,2,512]{2,1,0:T(2,128)S(1)}, u32[]{:S(2)}, u32[]{:S(2)}) async-start(f32[8,2,512]{2,1,0:T(2,128)} %broadcast_in_dim.27), calls=%async_computation.1 | async-start | bytes 65536 | tf_op jit(solution)/shard_map/all_to_all | solution.py:30
  131.7 4.9 %collective-permute-start.13 = (bf16[4,512,256]{2,1,0:T(8,128)(2,1)S(1)}, bf16[4,512,256]{2,1,0:T(8,128)(2,1)S(1)}, u32[]{:S(2)}, u32[]{:S(2)}) collective-permute-start(bf16[4,512,256]{2,1,0:T(8,128)(2,1)S(1)} %get-tuple-element.20), channel_id=1, source_target_pairs={{0,1},{1,0},{2,3},{3,2},{4,5},{5,4},{6,7},{7,6},{8,9},{9,8},{10,11... | collective-permute-start | bytes 3145736 | tf_op jit(solution)/shard_map/ppermute | solution.py:34
  136.8 17.5 %copy-start.5 = (bf16[512,256]{1,0:T(8,128)(2,1)S(1)}, bf16[512,256]{1,0:T(8,128)(2,1)}, u32[]{:S(2)}) copy-start(bf16[512,256]{1,0:T(8,128)(2,1)} %param.15) | copy-start | bytes 786436
  154.4 22.8 %copy-start.1 = (bf16[3,512]{1,0:T(4,128)(2,1)S(1)}, bf16[3,512]{1,0:T(4,128)(2,1)}, u32[]{:S(2)}) copy-start(bf16[3,512]{1,0:T(4,128)(2,1)} %conv_gate.1) | copy-start | bytes 9220
  154.4 22.8 %copy-start.2 = (bf16[3,512]{1,0:T(4,128)(2,1)S(1)}, bf16[3,512]{1,0:T(4,128)(2,1)}, u32[]{:S(2)}) copy-start(bf16[3,512]{1,0:T(4,128)(2,1)} %conv_value.1) | copy-start | bytes 9220
  170.9 6.3 %collective-permute-start.14 = (bf16[4,512,256]{2,1,0:T(8,128)(2,1)S(1)}, bf16[4,512,256]{2,1,0:T(8,128)(2,1)S(1)}, u32[]{:S(2)}, u32[]{:S(2)}) collective-permute-start(bf16[4,512,256]{2,1,0:T(8,128)(2,1)S(1)} %all_to_all.26.mine), channel_id=1, source_target_pairs={{0,1},{1,0},{2,3},{3,2},{4,5},{5,4},{6,7},{7,6},{8,9},{9,8},{10,11... | collective-permute-start | bytes 3145736 | tf_op jit(solution)/shard_map/ppermute | solution.py:34
  184.2 4.6 %collective-permute-start.17 = (bf16[4,512,256]{2,1,0:T(8,128)(2,1)S(1)}, bf16[4,512,256]{2,1,0:T(8,128)(2,1)S(1)}, u32[]{:S(2)}, u32[]{:S(2)}) collective-permute-start(bf16[4,512,256]{2,1,0:T(8,128)(2,1)S(1)} %get-tuple-element.24), channel_id=1, source_target_pairs={{0,1},{1,0},{2,3},{3,2},{4,5},{5,4},{6,7},{7,6},{8,9},{9,8},{10,11... | collective-permute-start | bytes 3145736 | tf_op jit(solution)/shard_map/ppermute | solution.py:34
Sparse Core Ops, SparseCore 0:
  66.8 80.7 all-gather.1

commit v6 on v5

--- a/solution.py
+++ b/solution.py
@@ -44,35 +44,24 @@
     return [shard] + [lax.ppermute(shard, axis, [(i, (i + step) % size) for i in range(size)]) for step in steps]
 
 
-def doubled(blocks, step):
-    came = lax.ppermute(blocks, "y", [(i, i ^ step) for i in range(4)])
-    upper = (lax.axis_index("y") & step) != 0
-    return jnp.concatenate([jnp.where(upper, came, blocks), jnp.where(upper, blocks, came)], axis=0)
-
-
-def norm_kernel(place, p0, p1, p2, p3, out, gain_two):
-    parts = (p0, p1, p2, p3)
-    count, width = p0.shape[1] - 16, p0.shape[2]
-    x, c = place[0], place[1]
+def norm_kernel(place, mine, other, out, gain_two):
+    count, width = mine.shape[1] - 16, mine.shape[2]
+    c = place[0]
+    blocks = [(ref, x, 2 * x + (1 - c if side else c)) for side, ref in enumerate((mine, other)) for x in range(4)]
     for part in range(count // BLOCK):
         rows = pl.ds(part * BLOCK, BLOCK)
         squares = jnp.zeros((BLOCK, width), F32)
-        for ref in parts:
-            for side in range(2):
-                value = ref[side, rows, :].astype(F32)
-                squares = squares + value * value
+        for ref, x, _ in blocks:
+            value = ref[x, rows, :].astype(F32)
+            squares = squares + value * value
         scale = lax.rsqrt(jnp.sum(squares, axis=1, keepdims=True) / (8 * width) + EPS)
-        for step, ref in zip(RING, parts):
-            for side in range(2):
-                block = origin(x, step) * 2 + (1 - c if side else c)
-                gain = ref[side, count : count + 1, :].astype(F32)
-                out[rows, pl.ds(pl.multiple_of(block * width, width), width)] = (
-                    ref[side, rows, :].astype(F32) * scale * gain
-                ).astype(BF16)
-    for step, ref in zip(RING, parts):
-        for side in range(2):
-            block = origin(x, step) * 2 + (1 - c if side else c)
-            gain_two[block] = ref[side, count + 8 : count + 16, :]
+        for ref, x, block in blocks:
+            gain = ref[x, count : count + 1, :].astype(F32)
+            out[rows, pl.ds(pl.multiple_of(block * width, width), width)] = (
+                ref[x, rows, :].astype(F32) * scale * gain
+            ).astype(BF16)
+    for ref, x, block in blocks:
+        gain_two[block] = ref[x, count + 8 : count + 16, :]
 
 
 def origin(here, step):
@@ -90,7 +79,7 @@
 
 def first_kernel(place, normed, p0, p1, p2, p3, act_u, act_v, sums, weight):
     width = act_u.shape[1]
-    fill_rows(weight, (p0, p1, p2, p3), place[2], place[3])
+    fill_rows(weight, (p0, p1, p2, p3), place[1], place[2])
     for part in range(normed.shape[0] // SEQ_LEN):
         rows = pl.ds(part * SEQ_LEN, SEQ_LEN)
         both = gelu(jnp.dot(normed[rows, :], weight[...], preferred_element_type=F32))
@@ -105,7 +94,7 @@
 
 def mix_kernel(place, act_v, act_u, stats, gain, shift, mix, bias, p0, p1, p2, p3, give, keep, weight, gated):
     width = act_v.shape[1]
-    fill_rows(weight, (p0, p1, p2, p3), place[2], place[3])
+    fill_rows(weight, (p0, p1, p2, p3), place[1], place[2])
     full = width * stats.shape[0]
     i = lax.broadcasted_iota(jnp.int32, (BLOCK, BLOCK), 0)
     j = lax.broadcasted_iota(jnp.int32, (BLOCK, BLOCK), 1)
@@ -128,7 +117,7 @@
             seen = jnp.where(visible, mix[g].astype(F32), 0.0).astype(BF16)
             spatial = jnp.dot(seen, mixed, preferred_element_type=F32) + biases[g]
             gated[rows, cols] = (act_u[rows, cols] * spatial).astype(BF16)
-    c = place[1]
+    c = place[0]
     for out, side in ((give, 1 - c), (keep, c)):
         for x in range(out.shape[0]):
             start = pl.multiple_of((2 * x + side) * width, width)
@@ -151,7 +140,7 @@
 def ffn_kernel(place, mine, other, gain, late_hbm, conv_gate, conv_value, give, keep, normed, hidden, late, done):
     width = mine.shape[2]
     ff = conv_gate.shape[1]
-    c = place[1]
+    c = place[0]
     copies = [
         pltpu.make_async_copy(late_hbm.at[:, pl.ds(k * ff, ff)], late.at[:, pl.ds(k * ff, ff)], done.at[k])
         for k in range(3)
@@ -243,29 +232,29 @@
 
     early = jnp.concatenate([proj_u, proj_v, proj_out.T], axis=1)
     early_far = everyones(early, "zh").reshape(-1, early.shape[1])
-    early_z = round_ring(early_far, Z)
-    early_parts = round_ring(jnp.concatenate([part[:, : 2 * da] for part in early_z], axis=0), "y")
-    out_parts = round_ring(jnp.concatenate([part[:, 2 * da :] for part in early_z], axis=0), "y")
+    early_z = jnp.concatenate(round_ring(early_far, Z), axis=0)
+    early_parts = round_ring(early_z[:, : 2 * da], "y")
+    out_parts = round_ring(early_z[:, 2 * da :], "y")
 
     late = jnp.concatenate([ffn_gate, ffn_value, proj_down.T], axis=1)
-    late_pair = doubled(late[None], 1)
-    late_y = doubled(late_pair, 2).reshape(-1, late.shape[1])
-    late_all = lax.all_gather(after(late_y, *early_z), Z, axis=0, tiled=True)
+    padded = jnp.pad(late, ((0, 2 * late.shape[0]), (0, 0)))
+    late_y = lax.all_gather(padded, "y", axis=0)[:, : late.shape[0]].reshape(-1, late.shape[1])
+    late_all = lax.all_gather(after(late_y, early_z), Z, axis=0, tiled=True)
 
     packed = jnp.concatenate([tokens, jnp.broadcast_to(norm_gain, (8, da)), jnp.broadcast_to(ffn_gain, (8, da))], axis=0)
-    pair = jnp.stack([packed, other_core(packed)])
-    token_parts = round_ring(pair, "x")
-    place = jnp.stack([lax.axis_index(name).astype(jnp.int32) for name in ("x", "c", "y", "zl")])
+    mine = lax.all_gather(packed, "x", axis=0)
+    other = other_core(mine)
+    place = jnp.stack([lax.axis_index(name).astype(jnp.int32) for name in ("c", "y", "zl")])
     model = proj_u.shape[0] * lax.axis_size(FS)
     tp = lax.axis_size(TP)
     normed, gain_two = pl.pallas_call(
         norm_kernel,
-        in_specs=[SMEM] + [VMEM] * 4,
+        in_specs=[SMEM] + [VMEM] * 2,
         out_specs=[VMEM] * 2,
         out_shape=[shape((row_count, model), BF16), shape((tp, 8, da), BF16)],
         name="norm",
         compiler_params=room(12),
-    )(place, *token_parts)
+    )(place, mine, other)
 
     act_u, act_v, sums = pl.pallas_call(
         first_kernel,

time: 216 us -> 219 us (1.014)
  starting transfers between devices: 86.4 us -> 55.2 us
  blocking collectives: 51 us -> 79.5 us
  waiting for transfers between devices: 39.9 us -> 43.2 us
    all_to_all x1 -> x2, blocking collectives: 16.4 us -> 44.9 us  [everyones(): return lax.all_to_all(copies, axis, split_axis=0, concat_axis=0, tiled=True)]
    all_gather x1 -> x3, waiting for transfers between devices: 0.01 us -> 16.8 us  [the longest x1 16.8 us: on_device(): mine = lax.all_gather(packed, 'x', axis=0)]
    all_to_all x2 -> x1, starting transfers between devices: 24.8 us -> 10.9 us  [everyones(): return lax.all_to_all(copies, axis, split_axis=0, concat_axis=0, tiled=True)]
    all_to_all x2 -> x1, waiting for transfers between devices: 17.3 us -> 4.71 us  [everyones(): return lax.all_to_all(copies, axis, split_axis=0, concat_axis=0, tiled=True)]
    ppermute x2 -> x0, starting transfers between devices: 8.99 us -> none  [doubled(): came = lax.ppermute(blocks, 'y', [(i, i ^ step) for i in range(4)])]
    ppermute x12 -> x9, starting transfers between devices: 37.4 us -> 30.6 us  [round_ring(): lax.ppermute(shard, axis, [(i, (i + step) % size) for i in range(size)])]
    concatenate x4 -> x3, other arithmetic: 0.87 us -> 4.2 us  [the longest x1 1.68 us: on_device(): jnp.concatenate([tokens, jnp.broadcast_to(norm_gain, (8, da)), jnp.broadc...]
    ppermute x12 -> x9, waiting for transfers between devices: 12.7 us -> 14.8 us  [round_ring(): lax.ppermute(shard, axis, [(i, (i + step) % size) for i in range(size)])]
  transfers between devices with their start and end apart: 21 -> 17, of which waited for: 10 -> 9; matrix products, arithmetic and copies ran while one was open for 3% -> 5% of each run, Pallas kernels for 3% -> 3%
where the time goes in v6:
time: 219 us; the launch traced here: 218 us
  blocking collectives  79.5 us (36%)
  starting transfers between devices  55.2 us (25%)
  waiting for transfers between devices  43.2 us (20%)
  Pallas kernels  13.6 us (6%)
  between operations  13.4 us (6%)
  other arithmetic  6.66 us (3%)
  local copies, waits for them, and re-layouts  5.9 us (3%)
    all_to_all x2, blocking collectives, everyones(): return lax.all_to_all(copies, axis, split_axis=0, concat_axis=0, tiled=True)  44.9 us
    all_to_all x2, blocking collectives, summed_at_owner(): arrived = lax.all_to_all(pair, 'x', split_axis=0, concat_axis=0, tiled=True)  34.6 us
    ppermute x9, starting transfers between devices, round_ring(): lax.ppermute(shard, axis, [(i, (i + step) % size) for i in range(size)])  30.6 us
    all_gather x1, waiting for transfers between devices, on_device(): mine = lax.all_gather(packed, 'x', axis=0)  16.8 us
    ppermute x9, waiting for transfers between devices, round_ring(): lax.ppermute(shard, axis, [(i, (i + step) % size) for i in range(size)])  14.8 us
    ppermute x4, starting transfers between devices, other_core(): return lax.ppermute(value, 'c', SWAP)  13.6 us
    all_to_all x1, starting transfers between devices, everyones(): return lax.all_to_all(copies, axis, split_axis=0, concat_axis=0, tiled=True)  10.9 us
    pallas_call x1, Pallas kernels, on_device(): pl.pallas_call(ffn_kernel, in_specs=[SMEM] + [VMEM] * 3 + [HBM] + [VMEM]...  7 us
  transfers between devices with their start and end apart: 17, of which 9 were waited for; matrix products, arithmetic and copies ran while one was open for 5% of the time, Pallas kernels for 3%

profile of v6, /device:TPU:1, one launch (start us, length us, event | category | flops | bytes accessed | tf_op | source)
XLA Modules:
  0.0 217.5 jit_solution(11833254514501657080)
XLA Ops:
  6.5 1.5 fusion.4
  8.0 0.0 all-gather.10.cloned.1.call-update
  8.1 0.0 all-gather.8.cloned.1.call-start
  8.1 0.7 broadcast_in_dim.21
  8.8 0.7 broadcast_in_dim.22
  9.4 1.7 pad_maximum_fusion.1
  11.1 0.0 all-gather.8.cloned.1.call-update
  11.1 0.0 all-gather.6.cloned.1.call-start
  11.2 0.8 pad_maximum_fusion.2
  12.0 28.5 %all_to_all.25 = bf16[4,32,768]{2,1,0:T(8,128)(2,1)S(1)} all-to-all(bf16[4,32,768]{2,1,0:T(8,128)(2,1)S(1)} %broadcast_in_dim.23), channel_id=1, replica_groups=mesh['zh'=4,'zl'=4,'y'=4,'x'=4,'c'=2] {'zh'}, dimensions={0} | all-to-all | bytes 393216 | tf_op jit(solution)/shard_map/all_to_all | solution.py:30
  40.5 6.9 %collective-permute-start.1 = (bf16[128,768]{1,0:T(8,128)(2,1)S(1)}, bf16[128,768]{1,0:T(8,128)(2,1)S(1)}, u32[]{:S(2)}, u32[]{:S(2)}) collective-permute-start(bf16[128,768]{1,0:T(8,128)(2,1)S(1)} %bitcast.12), channel_id=1, source_target_pairs={{0,32},{32,64},{64,96},{96,128},{128,160},{160,192},{192,224},{224... | collective-permute-start | bytes 589832 | tf_op jit(solution)/shard_map/ppermute | solution.py:44
  47.4 1.9 collective-permute-start.2
  49.4 3.9 %collective-permute-start.3 = (bf16[128,768]{1,0:T(8,128)(2,1)S(1)}, bf16[128,768]{1,0:T(8,128)(2,1)S(1)}, u32[]{:S(2)}, u32[]{:S(2)}) collective-permute-start(bf16[128,768]{1,0:T(8,128)(2,1)S(1)} %bitcast.14), channel_id=1, source_target_pairs={{0,64},{32,96},{64,128},{96,160},{128,192},{160,224},{192,256},{22... | collective-permute-start | bytes 589832 | tf_op jit(solution)/shard_map/ppermute | solution.py:44
  53.3 0.0 collective-permute-done.1
  53.3 0.6 collective-permute-done.2
  53.8 5.8 %collective-permute-done.3 = bf16[128,768]{1,0:T(8,128)(2,1)S(1)} collective-permute-done((bf16[128,768]{1,0:T(8,128)(2,1)S(1)}, bf16[128,768]{1,0:T(8,128)(2,1)S(1)}, u32[]{:S(2)}, u32[]{:S(2)}) %collective-permute-start.3) | collective-permute-done | bytes 196640 | tf_op jit(solution)/shard_map/ppermute | solution.py:44
  59.7 1.0 pad_maximum_fusion
  60.7 1.8 slice.14
  62.5 0.0 all-gather.6.cloned.1.call-update
  62.5 16.8 %all-gather.8.cloned.1.call-done = bf16[2112,256]{1,0:T(8,128)(2,1)} async-done(((bf16[528,256]{1,0:T(8,128)(2,1)}), bf16[2112,256]{1,0:T(8,128)(2,1)}) %all-gather.8.cloned.1.call-update) | async-done | bytes 1081360 | tf_op jit(solution)/shard_map/all_gather | solution.py:245
  79.3 4.8 %collective-permute-start = (bf16[4,528,256]{2,1,0:T(8,128)(2,1)}, bf16[4,528,256]{2,1,0:T(8,128)(2,1)S(1)}, u32[]{:S(2)}, u32[]{:S(2)}) collective-permute-start(bf16[4,528,256]{2,1,0:T(8,128)(2,1)} %bitcast.9), channel_id=1, source_target_pairs={{0,1},{1,0},{2,3},{3,2},{4,5},{5,4},{6,7},{7,6},{8,9},{9,8},{10,11... | collective-permute-start | bytes 3244040 | tf_op jit(solution)/shard_map/ppermute | solution.py:34
  84.1 1.1 slice.12.p0
  85.2 3.1 %collective-permute-start.4 = (bf16[512,512]{1,0:T(8,128)(2,1)S(1)}, bf16[512,512]{1,0:T(8,128)(2,1)S(1)}, u32[]{:S(2)}, u32[]{:S(2)}) collective-permute-start(bf16[512,512]{1,0:T(8,128)(2,1)S(1)} %slice.12.p0), channel_id=1, source_target_pairs={{0,8},{8,16},{16,24},{24,0},{1,9},{9,17},{17,25},{25,1},{2,10},{10... | collective-permute-start | bytes 1572872 | tf_op jit(solution)/shard_map/ppermute | solution.py:44
  88.3 3.4 %collective-permute-start.5 = (bf16[512,512]{1,0:T(8,128)(2,1)S(1)}, bf16[512,512]{1,0:T(8,128)(2,1)}, u32[]{:S(2)}, u32[]{:S(2)}) collective-permute-start(bf16[512,512]{1,0:T(8,128)(2,1)S(1)} %slice.12.p0), channel_id=1, source_target_pairs={{0,24},{8,0},{16,8},{24,16},{1,25},{9,1},{17,9},{25,17},{2,26},{10... | collective-permute-start | bytes 1572872 | tf_op jit(solution)/shard_map/ppermute | solution.py:44
  91.7 3.4 %collective-permute-start.6 = (bf16[512,512]{1,0:T(8,128)(2,1)S(1)}, bf16[512,512]{1,0:T(8,128)(2,1)}, u32[]{:S(2)}, u32[]{:S(2)}) collective-permute-start(bf16[512,512]{1,0:T(8,128)(2,1)S(1)} %slice.12.p0), channel_id=1, source_target_pairs={{0,16},{8,24},{16,0},{24,8},{1,17},{9,25},{17,1},{25,9},{2,18},{10... | collective-permute-start | bytes 1572872 | tf_op jit(solution)/shard_map/ppermute | solution.py:44
  95.2 1.0 slice.13.p0
  96.1 2.2 %collective-permute-start.7 = (bf16[512,256]{1,0:T(8,128)(2,1)S(1)}, bf16[512,256]{1,0:T(8,128)(2,1)}, u32[]{:S(2)}, u32[]{:S(2)}) collective-permute-start(bf16[512,256]{1,0:T(8,128)(2,1)S(1)} %slice.13.p0), channel_id=1, source_target_pairs={{0,8},{8,16},{16,24},{24,0},{1,9},{9,17},{17,25},{25,1},{2,10},{10... | collective-permute-start | bytes 786440 | tf_op jit(solution)/shard_map/ppermute | solution.py:44
  98.4 3.4 %collective-permute-done.4.p1 = bf16[512,512]{1,0:T(8,128)(2,1)S(1)} collective-permute-done((bf16[512,512]{1,0:T(8,128)(2,1)S(1)}, bf16[512,512]{1,0:T(8,128)(2,1)S(1)}, u32[]{:S(2)}, u32[]{:S(2)}) %collective-permute-start.4) | collective-permute-done | bytes 524320 | tf_op jit(solution)/shard_map/ppermute | solution.py:44
  101.8 3.3 %collective-permute-start.8 = (bf16[512,256]{1,0:T(8,128)(2,1)S(1)}, bf16[512,256]{1,0:T(8,128)(2,1)}, u32[]{:S(2)}, u32[]{:S(2)}) collective-permute-start(bf16[512,256]{1,0:T(8,128)(2,1)S(1)} %slice.13.p0), channel_id=1, source_target_pairs={{0,24},{8,0},{16,8},{24,16},{1,25},{9,1},{17,9},{25,17},{2,26},{10... | collective-permute-start | bytes 786440 | tf_op jit(solution)/shard_map/ppermute | solution.py:44
  105.0 0.0 collective-permute-done.other
  105.1 2.4 %collective-permute-start.9 = (bf16[512,256]{1,0:T(8,128)(2,1)S(1)}, bf16[512,256]{1,0:T(8,128)(2,1)}, u32[]{:S(2)}, u32[]{:S(2)}) collective-permute-start(bf16[512,256]{1,0:T(8,128)(2,1)S(1)} %slice.13.p0), channel_id=1, source_target_pairs={{0,16},{8,24},{16,0},{24,8},{1,17},{9,25},{17,1},{25,9},{2,18},{10... | collective-permute-start | bytes 786440 | tf_op jit(solution)/shard_map/ppermute | solution.py:44
  107.5 0.1 pad_add_fusion.place
  107.6 1.6 norm.1
  109.2 0.0 collective-permute-done.5.p2
  109.2 5.0 %collective-permute-done.6.p3 = bf16[512,512]{1,0:T(8,128)(2,1)} collective-permute-done((bf16[512,512]{1,0:T(8,128)(2,1)S(1)}, bf16[512,512]{1,0:T(8,128)(2,1)}, u32[]{:S(2)}, u32[]{:S(2)}) %collective-permute-start.6) | collective-permute-done | bytes 524320 | tf_op jit(solution)/shard_map/ppermute | solution.py:44
  114.1 2.9 %first.1 = (f32[512,256]{1,0:T(8,128)S(1)}, f32[512,256]{1,0:T(8,128)S(1)}, f32[2,512]{1,0:T(2,128)S(1)}) custom-call(s32[3]{0:T(128)S(1)} %pad_add_fusion.place, bf16[512,2048]{1,0:T(8,128)(2,1)S(1)} %get-tuple-element.15.normed, bf16[512,512]{1,0:T(8,128)(2,1)S(1)} %slice.12.p0, bf16[512,512]{1,0:T(8,128)(2,1)S(1)} %collective-permute-done.4.p1, ...), custom_call_target="tpu_custom_call" | custom-call | tf_op jit(solution)/shard_map/first/pallas_call | solution.py:259
  117.0 0.6 broadcast_in_dim.24
  117.7 10.9 %all-to-all-start.1 = ((f32[8,2,512]{2,1,0:T(2,128)}), f32[8,2,512]{2,1,0:T(2,128)S(1)}, u32[]{:S(2)}, u32[]{:S(2)}) async-start(f32[8,2,512]{2,1,0:T(2,128)} %broadcast_in_dim.24), calls=%async_computation.1 | async-start | bytes 65536 | tf_op jit(solution)/shard_map/all_to_all | solution.py:30
  128.6 0.0 copy-done.6
  128.6 0.0 collective-permute-done.7.p1
  128.6 0.0 collective-permute-done.8.p2
  128.6 0.0 collective-permute-done.9.p3
  128.7 4.7 %all-to-all-done.1.stats = f32[8,2,512]{2,1,0:T(2,128)S(1)} async-done(((f32[8,2,512]{2,1,0:T(2,128)}), f32[8,2,512]{2,1,0:T(2,128)S(1)}, u32[]{:S(2)}, u32[]{:S(2)}) %all-to-all-start.1) | async-done | bytes 32800 | tf_op jit(solution)/shard_map/all_to_all | solution.py:30
  133.4 2.2 mix.2
  135.6 2.6 %collective-permute-start.10 = (bf16[4,512,256]{2,1,0:T(8,128)(2,1)S(1)}, bf16[4,512,256]{2,1,0:T(8,128)(2,1)S(1)}, u32[]{:S(2)}, u32[]{:S(2)}) collective-permute-start(bf16[4,512,256]{2,1,0:T(8,128)(2,1)S(1)} %get-tuple-element.20), channel_id=1, source_target_pairs={{0,1},{1,0},{2,3},{3,2},{4,5},{5,4},{6,7},{7,6},{8,9},{9,8},{10,11... | collective-permute-start | bytes 3145736 | tf_op jit(solution)/shard_map/ppermute | solution.py:34
  138.2 2.3 %collective-permute-done.10 = bf16[4,512,256]{2,1,0:T(8,128)(2,1)S(1)} collective-permute-done((bf16[4,512,256]{2,1,0:T(8,128)(2,1)S(1)}, bf16[4,512,256]{2,1,0:T(8,128)(2,1)S(1)}, u32[]{:S(2)}, u32[]{:S(2)}) %collective-permute-start.10) | collective-permute-done | bytes 1048608 | tf_op jit(solution)/shard_map/ppermute | solution.py:34
  140.4 0.3 add_convert_fusion.1
  140.7 0.0 copy-start.5
  140.7 17.4 %all_to_all.26 = bf16[4,512,256]{2,1,0:T(8,128)(2,1)S(1)} all-to-all(bf16[4,512,256]{2,1,0:T(8,128)(2,1)S(1)} %add_convert_fusion.1), channel_id=1, replica_groups=mesh['zh'=4,'zl'=4,'y'=4,'x'=4,'c'=2] {'x'}, dimensions={0} | all-to-all | bytes 2097152 | tf_op jit(solution)/shard_map/all_to_all | solution.py:208
  158.1 0.1 convert_reduce_fusion.1
  158.2 0.0 copy-start.2
  158.2 0.0 copy-start.3
  158.3 0.1 add_convert_fusion.3
  158.3 0.1 broadcast_in_dim.27
  158.4 16.4 %all_to_all.27.mine = bf16[4,512,256]{2,1,0:T(8,128)(2,1)S(1)} all-to-all(bf16[4,512,256]{2,1,0:T(8,128)(2,1)S(1)} %broadcast_in_dim.27), channel_id=1, replica_groups=mesh['zh'=4,'zl'=4,'y'=4,'x'=4,'c'=2] {'x'}, dimensions={0} | all-to-all | bytes 2097152 | tf_op jit(solution)/shard_map/all_to_all | solution.py:30
  174.8 4.0 %collective-permute-start.11 = (bf16[4,512,256]{2,1,0:T(8,128)(2,1)S(1)}, bf16[4,512,256]{2,1,0:T(8,128)(2,1)S(1)}, u32[]{:S(2)}, u32[]{:S(2)}) collective-permute-start(bf16[4,512,256]{2,1,0:T(8,128)(2,1)S(1)} %all_to_all.27.mine), channel_id=1, source_target_pairs={{0,1},{1,0},{2,3},{3,2},{4,5},{5,4},{6,7},{7,6},{8,9},{9,8},{10,11... | collective-permute-start | bytes 3145736 | tf_op jit(solution)/shard_map/ppermute | solution.py:34
  178.8 2.3 %collective-permute-done.11.other = bf16[4,512,256]{2,1,0:T(8,128)(2,1)S(1)} collective-permute-done((bf16[4,512,256]{2,1,0:T(8,128)(2,1)S(1)}, bf16[4,512,256]{2,1,0:T(8,128)(2,1)S(1)}, u32[]{:S(2)}, u32[]{:S(2)}) %collective-permute-start.11) | collective-permute-done | bytes 1048608 | tf_op jit(solution)/shard_map/ppermute | solution.py:34
  181.1 7.0 %ffn.1 = (bf16[4,512,256]{2,1,0:T(8,128)(2,1)S(1)}, bf16[4,512,256]{2,1,0:T(8,128)(2,1)S(1)}) custom-call(s32[3]{0:T(128)S(1)} %pad_add_fusion.place, bf16[4,512,256]{2,1,0:T(8,128)(2,1)S(1)} %all_to_all.27.mine, bf16[4,512,256]{2,1,0:T(8,128)(2,1)S(1)} %collective-permute-done.11.other, bf16[8,8,256]{2,1,0:T(8,128)(2,1)S(1)} %get-tuple-element.21.gain, ...), custom_call_target="tpu_custom_call" | custom-call | tf_op jit(solution)/shard_map/ffn/pallas_call | solution.py:291
  188.1 2.3 %collective-permute-start.12 = (bf16[4,512,256]{2,1,0:T(8,128)(2,1)S(1)}, bf16[4,512,256]{2,1,0:T(8,128)(2,1)S(1)}, u32[]{:S(2)}, u32[]{:S(2)}) collective-permute-start(bf16[4,512,256]{2,1,0:T(8,128)(2,1)S(1)} %get-tuple-element.24), channel_id=1, source_target_pairs={{0,1},{1,0},{2,3},{3,2},{4,5},{5,4},{6,7},{7,6},{8,9},{9,8},{10,11... | collective-permute-start | bytes 3145736 | tf_op jit(solution)/shard_map/ppermute | solution.py:34
  190.3 2.3 %collective-permute-done.12 = bf16[4,512,256]{2,1,0:T(8,128)(2,1)S(1)} collective-permute-done((bf16[4,512,256]{2,1,0:T(8,128)(2,1)S(1)}, bf16[4,512,256]{2,1,0:T(8,128)(2,1)S(1)}, u32[]{:S(2)}, u32[]{:S(2)}) %collective-permute-start.12) | collective-permute-done | bytes 1048608 | tf_op jit(solution)/shard_map/ppermute | solution.py:34
  192.6 0.2 add_convert_fusion
  192.9 17.2 %all_to_all.28 = bf16[4,512,256]{2,1,0:T(8,128)(2,1)S(1)} all-to-all(bf16[4,512,256]{2,1,0:T(8,128)(2,1)S(1)} %add_convert_fusion), channel_id=1, replica_groups=mesh['zh'=4,'zl'=4,'y'=4,'x'=4,'c'=2] {'x'}, dimensions={0} | all-to-all | bytes 2097152 | tf_op jit(solution)/shard_map/all_to_all | solution.py:208
  210.1 0.1 convert_reduce_fusion
  210.3 0.8 add_convert_fusion.2
  (18 shorter events, 0.1 us)
Async XLA Ops:
  6.5 54.2 %all-gather.10.cloned.1.call-start = ((), (), s32[]{:S(2)}) async-start(), calls=%async_computation.7 | async-start | bytes 1474560 | tf_op jit(solution)/shard_map/all_gather | solution.py:241
  8.1 71.3 %all-gather.8.cloned.1.call-start = ((), (), s32[]{:S(2)}) async-start(), calls=%async_computation.6 | async-start | bytes 1351680 | tf_op jit(solution)/shard_map/all_gather | solution.py:245
  11.1 169.9 %all-gather.6.cloned.1.call-start = ((), (), s32[]{:S(2)}) async-start(), calls=%async_computation.5 | async-start | bytes 6684672 | tf_op jit(solution)/shard_map/all_gather | solution.py:242
  40.5 12.8 %collective-permute-start.1 = (bf16[128,768]{1,0:T(8,128)(2,1)S(1)}, bf16[128,768]{1,0:T(8,128)(2,1)S(1)}, u32[]{:S(2)}, u32[]{:S(2)}) collective-permute-start(bf16[128,768]{1,0:T(8,128)(2,1)S(1)} %bitcast.12), channel_id=1, source_target_pairs={{0,32},{32,64},{64,96},{96,128},{128,160},{160,192},{192,224},{224... | collective-permute-start | bytes 589832 | tf_op jit(solution)/shard_map/ppermute | solution.py:44
  47.4 6.4 %collective-permute-start.2 = (bf16[128,768]{1,0:T(8,128)(2,1)S(1)}, bf16[128,768]{1,0:T(8,128)(2,1)S(1)}, u32[]{:S(2)}, u32[]{:S(2)}) collective-permute-start(bf16[128,768]{1,0:T(8,128)(2,1)S(1)} %bitcast.13), channel_id=1, source_target_pairs={{0,480},{32,0},{64,32},{96,64},{128,96},{160,128},{192,160},{224,1... | collective-permute-start | bytes 589832 | tf_op jit(solution)/shard_map/ppermute | solution.py:44
  49.4 10.3 %collective-permute-start.3 = (bf16[128,768]{1,0:T(8,128)(2,1)S(1)}, bf16[128,768]{1,0:T(8,128)(2,1)S(1)}, u32[]{:S(2)}, u32[]{:S(2)}) collective-permute-start(bf16[128,768]{1,0:T(8,128)(2,1)S(1)} %bitcast.14), channel_id=1, source_target_pairs={{0,64},{32,96},{64,128},{96,160},{128,192},{160,224},{192,256},{22... | collective-permute-start | bytes 589832 | tf_op jit(solution)/shard_map/ppermute | solution.py:44
  79.3 28.3 %copy-start = (bf16[2112,256]{1,0:T(8,128)(2,1)S(1)}, bf16[2112,256]{1,0:T(8,128)(2,1)}, u32[]{:S(2)}) copy-start(bf16[2112,256]{1,0:T(8,128)(2,1)} %all-gather.8.cloned.1.call-done) | copy-start | bytes 3244036
  79.3 25.7 %collective-permute-start = (bf16[4,528,256]{2,1,0:T(8,128)(2,1)}, bf16[4,528,256]{2,1,0:T(8,128)(2,1)S(1)}, u32[]{:S(2)}, u32[]{:S(2)}) collective-permute-start(bf16[4,528,256]{2,1,0:T(8,128)(2,1)} %bitcast.9), channel_id=1, source_target_pairs={{0,1},{1,0},{2,3},{3,2},{4,5},{5,4},{6,7},{7,6},{8,9},{9,8},{10,11... | collective-permute-start | bytes 3244040 | tf_op jit(solution)/shard_map/ppermute | solution.py:34
  85.2 16.6 %collective-permute-start.4 = (bf16[512,512]{1,0:T(8,128)(2,1)S(1)}, bf16[512,512]{1,0:T(8,128)(2,1)S(1)}, u32[]{:S(2)}, u32[]{:S(2)}) collective-permute-start(bf16[512,512]{1,0:T(8,128)(2,1)S(1)} %slice.12.p0), channel_id=1, source_target_pairs={{0,8},{8,16},{16,24},{24,0},{1,9},{9,17},{17,25},{25,1},{2,10},{10... | collective-permute-start | bytes 1572872 | tf_op jit(solution)/shard_map/ppermute | solution.py:44
  88.3 20.8 %collective-permute-start.5 = (bf16[512,512]{1,0:T(8,128)(2,1)S(1)}, bf16[512,512]{1,0:T(8,128)(2,1)}, u32[]{:S(2)}, u32[]{:S(2)}) collective-permute-start(bf16[512,512]{1,0:T(8,128)(2,1)S(1)} %slice.12.p0), channel_id=1, source_target_pairs={{0,24},{8,0},{16,8},{24,16},{1,25},{9,1},{17,9},{25,17},{2,26},{10... | collective-permute-start | bytes 1572872 | tf_op jit(solution)/shard_map/ppermute | solution.py:44
  91.7 22.4 %collective-permute-start.6 = (bf16[512,512]{1,0:T(8,128)(2,1)S(1)}, bf16[512,512]{1,0:T(8,128)(2,1)}, u32[]{:S(2)}, u32[]{:S(2)}) collective-permute-start(bf16[512,512]{1,0:T(8,128)(2,1)S(1)} %slice.12.p0), channel_id=1, source_target_pairs={{0,16},{8,24},{16,0},{24,8},{1,17},{9,25},{17,1},{25,9},{2,18},{10... | collective-permute-start | bytes 1572872 | tf_op jit(solution)/shard_map/ppermute | solution.py:44
  96.1 32.5 %collective-permute-start.7 = (bf16[512,256]{1,0:T(8,128)(2,1)S(1)}, bf16[512,256]{1,0:T(8,128)(2,1)}, u32[]{:S(2)}, u32[]{:S(2)}) collective-permute-start(bf16[512,256]{1,0:T(8,128)(2,1)S(1)} %slice.13.p0), channel_id=1, source_target_pairs={{0,8},{8,16},{16,24},{24,0},{1,9},{9,17},{17,25},{25,1},{2,10},{10... | collective-permute-start | bytes 786440 | tf_op jit(solution)/shard_map/ppermute | solution.py:44
  101.8 26.9 %collective-permute-start.8 = (bf16[512,256]{1,0:T(8,128)(2,1)S(1)}, bf16[512,256]{1,0:T(8,128)(2,1)}, u32[]{:S(2)}, u32[]{:S(2)}) collective-permute-start(bf16[512,256]{1,0:T(8,128)(2,1)S(1)} %slice.13.p0), channel_id=1, source_target_pairs={{0,24},{8,0},{16,8},{24,16},{1,25},{9,1},{17,9},{25,17},{2,26},{10... | collective-permute-start | bytes 786440 | tf_op jit(solution)/shard_map/ppermute | solution.py:44
  105.1 23.6 %collective-permute-start.9 = (bf16[512,256]{1,0:T(8,128)(2,1)S(1)}, bf16[512,256]{1,0:T(8,128)(2,1)}, u32[]{:S(2)}, u32[]{:S(2)}) collective-permute-start(bf16[512,256]{1,0:T(8,128)(2,1)S(1)} %slice.13.p0), channel_id=1, source_target_pairs={{0,16},{8,24},{16,0},{24,8},{1,17},{9,25},{17,1},{25,9},{2,18},{10... | collective-permute-start | bytes 786440 | tf_op jit(solution)/shard_map/ppermute | solution.py:44
  114.1 14.5 %copy-start.6 = (bf16[256]{0:T(256)(128)(2,1)S(1)}, bf16[256]{0:T(256)(128)(2,1)}, u32[]{:S(2)}) copy-start(bf16[256]{0:T(256)(128)(2,1)} %param.19) | copy-start | bytes 1540
  114.1 14.5 %copy-start.7 = (bf16[256]{0:T(256)(128)(2,1)S(1)}, bf16[256]{0:T(256)(128)(2,1)}, u32[]{:S(2)}) copy-start(bf16[256]{0:T(256)(128)(2,1)} %param.20) | copy-start | bytes 1540
  114.1 19.2 %copy-start.1 = (bf16[2,128,128]{2,1,0:T(8,128)(2,1)S(1)}, bf16[2,128,128]{2,1,0:T(8,128)(2,1)}, u32[]{:S(2)}) copy-start(bf16[2,128,128]{2,1,0:T(8,128)(2,1)} %mix.3) | copy-start | bytes 196612
  114.1 19.2 %copy-start.4 = (bf16[2,128]{1,0:T(2,128)(2,1)S(1)}, bf16[2,128]{1,0:T(2,128)(2,1)}, u32[]{:S(2)}) copy-start(bf16[2,128]{1,0:T(2,128)(2,1)} %bias.1) | copy-start | bytes 1540
  117.7 15.7 %all-to-all-start.1 = ((f32[8,2,512]{2,1,0:T(2,128)}), f32[8,2,512]{2,1,0:T(2,128)S(1)}, u32[]{:S(2)}, u32[]{:S(2)}) async-start(f32[8,2,512]{2,1,0:T(2,128)} %broadcast_in_dim.24), calls=%async_computation.1 | async-start | bytes 65536 | tf_op jit(solution)/shard_map/all_to_all | solution.py:30
  135.6 4.9 %collective-permute-start.10 = (bf16[4,512,256]{2,1,0:T(8,128)(2,1)S(1)}, bf16[4,512,256]{2,1,0:T(8,128)(2,1)S(1)}, u32[]{:S(2)}, u32[]{:S(2)}) collective-permute-start(bf16[4,512,256]{2,1,0:T(8,128)(2,1)S(1)} %get-tuple-element.20), channel_id=1, source_target_pairs={{0,1},{1,0},{2,3},{3,2},{4,5},{5,4},{6,7},{7,6},{8,9},{9,8},{10,11... | collective-permute-start | bytes 3145736 | tf_op jit(solution)/shard_map/ppermute | solution.py:34
  140.7 17.5 %copy-start.5 = (bf16[512,256]{1,0:T(8,128)(2,1)S(1)}, bf16[512,256]{1,0:T(8,128)(2,1)}, u32[]{:S(2)}) copy-start(bf16[512,256]{1,0:T(8,128)(2,1)} %param.15) | copy-start | bytes 786436
  158.2 22.8 %copy-start.2 = (bf16[3,512]{1,0:T(4,128)(2,1)S(1)}, bf16[3,512]{1,0:T(4,128)(2,1)}, u32[]{:S(2)}) copy-start(bf16[3,512]{1,0:T(4,128)(2,1)} %conv_gate.1) | copy-start | bytes 9220
  158.2 22.8 %copy-start.3 = (bf16[3,512]{1,0:T(4,128)(2,1)S(1)}, bf16[3,512]{1,0:T(4,128)(2,1)}, u32[]{:S(2)}) copy-start(bf16[3,512]{1,0:T(4,128)(2,1)} %conv_value.1) | copy-start | bytes 9220
  174.8 6.3 %collective-permute-start.11 = (bf16[4,512,256]{2,1,0:T(8,128)(2,1)S(1)}, bf16[4,512,256]{2,1,0:T(8,128)(2,1)S(1)}, u32[]{:S(2)}, u32[]{:S(2)}) collective-permute-start(bf16[4,512,256]{2,1,0:T(8,128)(2,1)S(1)} %all_to_all.27.mine), channel_id=1, source_target_pairs={{0,1},{1,0},{2,3},{3,2},{4,5},{5,4},{6,7},{7,6},{8,9},{9,8},{10,11... | collective-permute-start | bytes 3145736 | tf_op jit(solution)/shard_map/ppermute | solution.py:34
  188.1 4.6 %collective-permute-start.12 = (bf16[4,512,256]{2,1,0:T(8,128)(2,1)S(1)}, bf16[4,512,256]{2,1,0:T(8,128)(2,1)S(1)}, u32[]{:S(2)}, u32[]{:S(2)}) collective-permute-start(bf16[4,512,256]{2,1,0:T(8,128)(2,1)S(1)} %get-tuple-element.24), channel_id=1, source_target_pairs={{0,1},{1,0},{2,3},{3,2},{4,5},{5,4},{6,7},{7,6},{8,9},{9,8},{10,11... | collective-permute-start | bytes 3145736 | tf_op jit(solution)/shard_map/ppermute | solution.py:34
Sparse Core Ops, SparseCore 0:
  9.4 35.3 all-gather.9
  46.9 32.3 all-gather.7
  81.4 85.6 all-gather.5

commit v7 on v5

--- a/solution.py
+++ b/solution.py
@@ -42,12 +42,6 @@
     size = lax.axis_size(axis)
     steps = (1, size - 1, 2)
     return [shard] + [lax.ppermute(shard, axis, [(i, (i + step) % size) for i in range(size)]) for step in steps]
-
-
-def doubled(blocks, step):
-    came = lax.ppermute(blocks, "y", [(i, i ^ step) for i in range(4)])
-    upper = (lax.axis_index("y") & step) != 0
-    return jnp.concatenate([jnp.where(upper, came, blocks), jnp.where(upper, blocks, came)], axis=0)
 
 
 def norm_kernel(place, p0, p1, p2, p3, out, gain_two):
@@ -243,14 +237,14 @@
 
     early = jnp.concatenate([proj_u, proj_v, proj_out.T], axis=1)
     early_far = everyones(early, "zh").reshape(-1, early.shape[1])
-    early_z = round_ring(early_far, Z)
-    early_parts = round_ring(jnp.concatenate([part[:, : 2 * da] for part in early_z], axis=0), "y")
-    out_parts = round_ring(jnp.concatenate([part[:, 2 * da :] for part in early_z], axis=0), "y")
+    early_z = jnp.concatenate(round_ring(early_far, Z), axis=0)
+    early_parts = round_ring(early_z[:, : 2 * da], "y")
+    out_parts = round_ring(early_z[:, 2 * da :], "y")
 
     late = jnp.concatenate([ffn_gate, ffn_value, proj_down.T], axis=1)
-    late_pair = doubled(late[None], 1)
-    late_y = doubled(late_pair, 2).reshape(-1, late.shape[1])
-    late_all = lax.all_gather(after(late_y, *early_z), Z, axis=0, tiled=True)
+    padded = jnp.pad(late, ((0, 2 * late.shape[0]), (0, 0)))
+    late_y = lax.all_gather(padded, "y", axis=0)[:, : late.shape[0]].reshape(-1, late.shape[1])
+    late_all = lax.all_gather(after(late_y, early_z), Z, axis=0, tiled=True)
 
     packed = jnp.concatenate([tokens, jnp.broadcast_to(norm_gain, (8, da)), jnp.broadcast_to(ffn_gain, (8, da))], axis=0)
     pair = jnp.stack([packed, other_core(packed)])

time: 216 us -> 210 us (0.972)
  blocking collectives: 51 us -> 79.5 us
  starting transfers between devices: 86.4 us -> 69.8 us
  waiting for transfers between devices: 39.9 us -> 24.8 us
    all_to_all x1 -> x2, blocking collectives: 16.4 us -> 44.9 us  [everyones(): return lax.all_to_all(copies, axis, split_axis=0, concat_axis=0, tiled=True)]
    all_to_all x2 -> x1, starting transfers between devices: 24.8 us -> 11.2 us  [everyones(): return lax.all_to_all(copies, axis, split_axis=0, concat_axis=0, tiled=True)]
    all_to_all x2 -> x1, waiting for transfers between devices: 17.3 us -> 4.73 us  [everyones(): return lax.all_to_all(copies, axis, split_axis=0, concat_axis=0, tiled=True)]
    ppermute x2 -> x0, starting transfers between devices: 8.99 us -> none  [doubled(): came = lax.ppermute(blocks, 'y', [(i, i ^ step) for i in range(4)])]
    ppermute x12, starting transfers between devices: 37.4 us -> 43.2 us  [round_ring(): lax.ppermute(shard, axis, [(i, (i + step) % size) for i in range(size)])]
  transfers between devices with their start and end apart: 21 -> 19, of which waited for: 10 -> 10; matrix products, arithmetic and copies ran while one was open for 3% -> 1% of each run, Pallas kernels for 3% -> 3%
where the time goes in v7:
time: 210 us; the launch traced here: 209 us
  blocking collectives  79.5 us (38%)
  starting transfers between devices  69.8 us (33%)
  waiting for transfers between devices  24.8 us (12%)
  between operations  13.8 us (7%)
  Pallas kernels  13.6 us (6%)
  other arithmetic  5.08 us (2%)
  local copies, waits for them, and re-layouts  2.61 us (1%)
    all_to_all x2, blocking collectives, everyones(): return lax.all_to_all(copies, axis, split_axis=0, concat_axis=0, tiled=True)  44.9 us
    ppermute x12, starting transfers between devices, round_ring(): lax.ppermute(shard, axis, [(i, (i + step) % size) for i in range(size)])  43.2 us
    all_to_all x2, blocking collectives, summed_at_owner(): arrived = lax.all_to_all(pair, 'x', split_axis=0, concat_axis=0, tiled=True)  34.6 us
    ppermute x4, starting transfers between devices, other_core(): return lax.ppermute(value, 'c', SWAP)  15.3 us
    ppermute x12, waiting for transfers between devices, round_ring(): lax.ppermute(shard, axis, [(i, (i + step) % size) for i in range(size)])  12.1 us
    all_to_all x1, starting transfers between devices, everyones(): return lax.all_to_all(copies, axis, split_axis=0, concat_axis=0, tiled=True)  11.2 us
    ppermute x4, waiting for transfers between devices, other_core(): return lax.ppermute(value, 'c', SWAP)  7.95 us
    pallas_call x1, Pallas kernels, on_device(): pl.pallas_call(ffn_kernel, in_specs=[SMEM] + [VMEM] * 3 + [HBM] + [VMEM]...  6.98 us
  transfers between devices with their start and end apart: 19, of which 10 were waited for; matrix products, arithmetic and copies ran while one was open for 1% of the time, Pallas kernels for 3%

profile of v7, /device:TPU:1, one launch (start us, length us, event | category | flops | bytes accessed | tf_op | source)
XLA Modules:
  0.0 209.2 jit_solution(14048409091949048424)
XLA Ops:
  6.5 1.6 fusion.4
  8.1 0.0 all-gather.6.cloned.1.call-update
  8.1 0.0 all-gather.4.cloned.1.call-start
  8.2 0.8 pad_maximum_fusion.3
  9.0 28.5 %all_to_all.25 = bf16[4,32,768]{2,1,0:T(8,128)(2,1)S(1)} all-to-all(bf16[4,32,768]{2,1,0:T(8,128)(2,1)S(1)} %broadcast_in_dim.23), channel_id=1, replica_groups=mesh['zh'=4,'zl'=4,'y'=4,'x'=4,'c'=2] {'zh'}, dimensions={0} | all-to-all | bytes 393216 | tf_op jit(solution)/shard_map/all_to_all | solution.py:30
  37.5 6.9 %collective-permute-start.4 = (bf16[128,768]{1,0:T(8,128)(2,1)S(1)}, bf16[128,768]{1,0:T(8,128)(2,1)S(1)}, u32[]{:S(2)}, u32[]{:S(2)}) collective-permute-start(bf16[128,768]{1,0:T(8,128)(2,1)S(1)} %bitcast.13), channel_id=1, source_target_pairs={{0,32},{32,64},{64,96},{96,128},{128,160},{160,192},{192,224},{224... | collective-permute-start | bytes 589832 | tf_op jit(solution)/shard_map/ppermute | solution.py:44
  44.4 1.9 collective-permute-start.5
  46.4 3.9 %collective-permute-start.6 = (bf16[128,768]{1,0:T(8,128)(2,1)S(1)}, bf16[128,768]{1,0:T(8,128)(2,1)S(1)}, u32[]{:S(2)}, u32[]{:S(2)}) collective-permute-start(bf16[128,768]{1,0:T(8,128)(2,1)S(1)} %bitcast.15), channel_id=1, source_target_pairs={{0,64},{32,96},{64,128},{96,160},{128,192},{160,224},{192,256},{22... | collective-permute-start | bytes 589832 | tf_op jit(solution)/shard_map/ppermute | solution.py:44
  50.2 0.0 collective-permute-done.4
  50.3 0.6 collective-permute-done.5
  50.8 5.8 %collective-permute-done.6 = bf16[128,768]{1,0:T(8,128)(2,1)S(1)} collective-permute-done((bf16[128,768]{1,0:T(8,128)(2,1)S(1)}, bf16[128,768]{1,0:T(8,128)(2,1)S(1)}, u32[]{:S(2)}, u32[]{:S(2)}) %collective-permute-start.6) | collective-permute-done | bytes 196640 | tf_op jit(solution)/shard_map/ppermute | solution.py:44
  56.7 0.9 pad_maximum_fusion
  57.6 1.8 slice.14
  59.4 0.0 all-gather.4.cloned.1.call-update
  59.5 6.5 %collective-permute-start = (bf16[528,256]{1,0:T(8,128)(2,1)S(1)}, bf16[528,256]{1,0:T(8,128)(2,1)S(1)}, u32[]{:S(2)}, u32[]{:S(2)}) collective-permute-start(bf16[528,256]{1,0:T(8,128)(2,1)S(1)} %get-tuple-element.26), channel_id=1, source_target_pairs={{0,1},{1,0},{2,3},{3,2},{4,5},{5,4},{6,7},{7,6},{8,9},{9,8},{10,11... | collective-permute-start | bytes 811016 | tf_op jit(solution)/shard_map/ppermute | solution.py:34
  66.0 1.2 collective-permute-done
  67.1 0.1 pad_maximum_fusion.1.p0
  67.2 3.1 %collective-permute-start.1 = (bf16[2,528,256]{2,1,0:T(8,128)(2,1)S(1)}, bf16[2,528,256]{2,1,0:T(8,128)(2,1)S(1)}, u32[]{:S(2)}, u32[]{:S(2)}) collective-permute-start(bf16[2,528,256]{2,1,0:T(8,128)(2,1)S(1)} %pad_maximum_fusion.1.p0), channel_id=1, source_target_pairs={{0,2},{2,4},{4,6},{6,0},{1,3},{3,5},{5,7},{7,1},{8,10},{10,12},{12... | collective-permute-start | bytes 1622024 | tf_op jit(solution)/shard_map/ppermute | solution.py:44
  70.3 3.4 %collective-permute-start.2 = (bf16[2,528,256]{2,1,0:T(8,128)(2,1)S(1)}, bf16[2,528,256]{2,1,0:T(8,128)(2,1)S(1)}, u32[]{:S(2)}, u32[]{:S(2)}) collective-permute-start(bf16[2,528,256]{2,1,0:T(8,128)(2,1)S(1)} %pad_maximum_fusion.1.p0), channel_id=1, source_target_pairs={{0,6},{2,0},{4,2},{6,4},{1,7},{3,1},{5,3},{7,5},{8,14},{10,8},{12,... | collective-permute-start | bytes 1622024 | tf_op jit(solution)/shard_map/ppermute | solution.py:44
  73.7 3.4 %collective-permute-start.3 = (bf16[2,528,256]{2,1,0:T(8,128)(2,1)S(1)}, bf16[2,528,256]{2,1,0:T(8,128)(2,1)S(1)}, u32[]{:S(2)}, u32[]{:S(2)}) collective-permute-start(bf16[2,528,256]{2,1,0:T(8,128)(2,1)S(1)} %pad_maximum_fusion.1.p0), channel_id=1, source_target_pairs={{0,4},{2,6},{4,0},{6,2},{1,5},{3,7},{5,1},{7,3},{8,12},{10,14},{12... | collective-permute-start | bytes 1622024 | tf_op jit(solution)/shard_map/ppermute | solution.py:44
  77.2 3.2 %collective-permute-start.7 = (bf16[512,512]{1,0:T(8,128)(2,1)S(1)}, bf16[512,512]{1,0:T(8,128)(2,1)S(1)}, u32[]{:S(2)}, u32[]{:S(2)}) collective-permute-start(bf16[512,512]{1,0:T(8,128)(2,1)S(1)} %slice.12.p0), channel_id=1, source_target_pairs={{0,8},{8,16},{16,24},{24,0},{1,9},{9,17},{17,25},{25,1},{2,10},{10... | collective-permute-start | bytes 1572872 | tf_op jit(solution)/shard_map/ppermute | solution.py:44
  80.4 3.4 %collective-permute-start.8 = (bf16[512,512]{1,0:T(8,128)(2,1)S(1)}, bf16[512,512]{1,0:T(8,128)(2,1)}, u32[]{:S(2)}, u32[]{:S(2)}) collective-permute-start(bf16[512,512]{1,0:T(8,128)(2,1)S(1)} %slice.12.p0), channel_id=1, source_target_pairs={{0,24},{8,0},{16,8},{24,16},{1,25},{9,1},{17,9},{25,17},{2,26},{10... | collective-permute-start | bytes 1572872 | tf_op jit(solution)/shard_map/ppermute | solution.py:44
  83.8 0.1 collective-permute-done.1.p1
  83.9 4.8 %collective-permute-start.9 = (bf16[512,512]{1,0:T(8,128)(2,1)S(1)}, bf16[512,512]{1,0:T(8,128)(2,1)}, u32[]{:S(2)}, u32[]{:S(2)}) collective-permute-start(bf16[512,512]{1,0:T(8,128)(2,1)S(1)} %slice.12.p0), channel_id=1, source_target_pairs={{0,16},{8,24},{16,0},{24,8},{1,17},{9,25},{17,1},{25,9},{2,18},{10... | collective-permute-start | bytes 1572872 | tf_op jit(solution)/shard_map/ppermute | solution.py:44
  88.7 0.0 collective-permute-done.2.p2
  88.7 2.3 %collective-permute-start.10 = (bf16[512,256]{1,0:T(8,128)(2,1)S(1)}, bf16[512,256]{1,0:T(8,128)(2,1)}, u32[]{:S(2)}, u32[]{:S(2)}) collective-permute-start(bf16[512,256]{1,0:T(8,128)(2,1)S(1)} %slice.13.p0), channel_id=1, source_target_pairs={{0,8},{8,16},{16,24},{24,0},{1,9},{9,17},{17,25},{25,1},{2,10},{10... | collective-permute-start | bytes 786440 | tf_op jit(solution)/shard_map/ppermute | solution.py:44
  91.0 5.3 %collective-permute-done.3.p3 = bf16[2,528,256]{2,1,0:T(8,128)(2,1)S(1)} collective-permute-done((bf16[2,528,256]{2,1,0:T(8,128)(2,1)S(1)}, bf16[2,528,256]{2,1,0:T(8,128)(2,1)S(1)}, u32[]{:S(2)}, u32[]{:S(2)}) %collective-permute-start.3) | collective-permute-done | bytes 540704 | tf_op jit(solution)/shard_map/ppermute | solution.py:44
  96.3 4.6 %collective-permute-start.11 = (bf16[512,256]{1,0:T(8,128)(2,1)S(1)}, bf16[512,256]{1,0:T(8,128)(2,1)}, u32[]{:S(2)}, u32[]{:S(2)}) collective-permute-start(bf16[512,256]{1,0:T(8,128)(2,1)S(1)} %slice.13.p0), channel_id=1, source_target_pairs={{0,24},{8,0},{16,8},{24,16},{1,25},{9,1},{17,9},{25,17},{2,26},{10... | collective-permute-start | bytes 786440 | tf_op jit(solution)/shard_map/ppermute | solution.py:44
  101.0 0.0 collective-permute-done.7.p1
  101.0 2.3 %collective-permute-start.12 = (bf16[512,256]{1,0:T(8,128)(2,1)S(1)}, bf16[512,256]{1,0:T(8,128)(2,1)}, u32[]{:S(2)}, u32[]{:S(2)}) collective-permute-start(bf16[512,256]{1,0:T(8,128)(2,1)S(1)} %slice.13.p0), channel_id=1, source_target_pairs={{0,16},{8,24},{16,0},{24,8},{1,17},{9,25},{17,1},{25,9},{2,18},{10... | collective-permute-start | bytes 786440 | tf_op jit(solution)/shard_map/ppermute | solution.py:44
  103.2 0.1 pad_add_fusion.place
  103.3 1.6 norm.1
  104.9 0.0 collective-permute-done.8.p2
  104.9 0.3 collective-permute-done.9.p3
  105.2 2.9 %first.1 = (f32[512,256]{1,0:T(8,128)S(1)}, f32[512,256]{1,0:T(8,128)S(1)}, f32[2,512]{1,0:T(2,128)S(1)}) custom-call(s32[4]{0:T(128)S(1)} %pad_add_fusion.place, bf16[512,2048]{1,0:T(8,128)(2,1)S(1)} %get-tuple-element.15.normed, bf16[512,512]{1,0:T(8,128)(2,1)S(1)} %slice.12.p0, bf16[512,512]{1,0:T(8,128)(2,1)S(1)} %collective-permute-done.7.p1, ...), custom_call_target="tpu_custom_call" | custom-call | tf_op jit(solution)/shard_map/first/pallas_call | solution.py:264
  108.1 0.6 broadcast_in_dim.24
  108.8 11.2 %all-to-all-start.1 = ((f32[8,2,512]{2,1,0:T(2,128)}), f32[8,2,512]{2,1,0:T(2,128)S(1)}, u32[]{:S(2)}, u32[]{:S(2)}) async-start(f32[8,2,512]{2,1,0:T(2,128)} %broadcast_in_dim.24), calls=%async_computation.1 | async-start | bytes 65536 | tf_op jit(solution)/shard_map/all_to_all | solution.py:30
  120.0 0.0 copy-done.10
  120.0 0.0 collective-permute-done.10.p1
  120.0 0.0 collective-permute-done.11.p2
  120.0 0.0 collective-permute-done.12.p3
  120.0 4.7 %all-to-all-done.1.stats = f32[8,2,512]{2,1,0:T(2,128)S(1)} async-done(((f32[8,2,512]{2,1,0:T(2,128)}), f32[8,2,512]{2,1,0:T(2,128)S(1)}, u32[]{:S(2)}, u32[]{:S(2)}) %all-to-all-start.1) | async-done | bytes 32800 | tf_op jit(solution)/shard_map/all_to_all | solution.py:30
  124.7 0.0 copy-done
  124.7 2.2 %mix.2 = (bf16[4,512,256]{2,1,0:T(8,128)(2,1)S(1)}, bf16[4,512,256]{2,1,0:T(8,128)(2,1)S(1)}) custom-call(s32[4]{0:T(128)S(1)} %pad_add_fusion.place, f32[512,256]{1,0:T(8,128)S(1)} %get-tuple-element.16.act_v, f32[512,256]{1,0:T(8,128)S(1)} %get-tuple-element.17.act_u, f32[8,2,512]{2,1,0:T(2,128)S(1)} %all-to-all-done.1.stats, ...), custom_call_target="tpu_custom_call" | custom-call | tf_op jit(solution)/shard_map/mix/pallas_call | solution.py:275
  126.9 2.6 %collective-permute-start.13 = (bf16[4,512,256]{2,1,0:T(8,128)(2,1)S(1)}, bf16[4,512,256]{2,1,0:T(8,128)(2,1)S(1)}, u32[]{:S(2)}, u32[]{:S(2)}) collective-permute-start(bf16[4,512,256]{2,1,0:T(8,128)(2,1)S(1)} %get-tuple-element.20), channel_id=1, source_target_pairs={{0,1},{1,0},{2,3},{3,2},{4,5},{5,4},{6,7},{7,6},{8,9},{9,8},{10,11... | collective-permute-start | bytes 3145736 | tf_op jit(solution)/shard_map/ppermute | solution.py:34
  129.5 2.3 %collective-permute-done.13 = bf16[4,512,256]{2,1,0:T(8,128)(2,1)S(1)} collective-permute-done((bf16[4,512,256]{2,1,0:T(8,128)(2,1)S(1)}, bf16[4,512,256]{2,1,0:T(8,128)(2,1)S(1)}, u32[]{:S(2)}, u32[]{:S(2)}) %collective-permute-start.13) | collective-permute-done | bytes 1048608 | tf_op jit(solution)/shard_map/ppermute | solution.py:34
  131.8 0.2 add_convert_fusion.1
  132.0 0.0 copy-start.6
  132.0 17.4 %all_to_all.26 = bf16[4,512,256]{2,1,0:T(8,128)(2,1)S(1)} all-to-all(bf16[4,512,256]{2,1,0:T(8,128)(2,1)S(1)} %add_convert_fusion.1), channel_id=1, replica_groups=mesh['zh'=4,'zl'=4,'y'=4,'x'=4,'c'=2] {'x'}, dimensions={0} | all-to-all | bytes 2097152 | tf_op jit(solution)/shard_map/all_to_all | solution.py:213
  149.4 0.1 convert_reduce_fusion.1
  149.6 0.0 copy-start.1
  149.6 0.0 copy-start.2
  149.6 0.1 add_convert_fusion.3
  149.6 0.1 broadcast_in_dim.27
  149.7 16.4 %all_to_all.27.mine = bf16[4,512,256]{2,1,0:T(8,128)(2,1)S(1)} all-to-all(bf16[4,512,256]{2,1,0:T(8,128)(2,1)S(1)} %broadcast_in_dim.27), channel_id=1, replica_groups=mesh['zh'=4,'zl'=4,'y'=4,'x'=4,'c'=2] {'x'}, dimensions={0} | all-to-all | bytes 2097152 | tf_op jit(solution)/shard_map/all_to_all | solution.py:30
  166.1 4.0 %collective-permute-start.14 = (bf16[4,512,256]{2,1,0:T(8,128)(2,1)S(1)}, bf16[4,512,256]{2,1,0:T(8,128)(2,1)S(1)}, u32[]{:S(2)}, u32[]{:S(2)}) collective-permute-start(bf16[4,512,256]{2,1,0:T(8,128)(2,1)S(1)} %all_to_all.27.mine), channel_id=1, source_target_pairs={{0,1},{1,0},{2,3},{3,2},{4,5},{5,4},{6,7},{7,6},{8,9},{9,8},{10,11... | collective-permute-start | bytes 3145736 | tf_op jit(solution)/shard_map/ppermute | solution.py:34
  170.1 2.3 %collective-permute-done.14.other = bf16[4,512,256]{2,1,0:T(8,128)(2,1)S(1)} collective-permute-done((bf16[4,512,256]{2,1,0:T(8,128)(2,1)S(1)}, bf16[4,512,256]{2,1,0:T(8,128)(2,1)S(1)}, u32[]{:S(2)}, u32[]{:S(2)}) %collective-permute-start.14) | collective-permute-done | bytes 1048608 | tf_op jit(solution)/shard_map/ppermute | solution.py:34
  172.4 7.0 %ffn.1 = (bf16[4,512,256]{2,1,0:T(8,128)(2,1)S(1)}, bf16[4,512,256]{2,1,0:T(8,128)(2,1)S(1)}) custom-call(s32[4]{0:T(128)S(1)} %pad_add_fusion.place, bf16[4,512,256]{2,1,0:T(8,128)(2,1)S(1)} %all_to_all.27.mine, bf16[4,512,256]{2,1,0:T(8,128)(2,1)S(1)} %collective-permute-done.14.other, bf16[8,8,256]{2,1,0:T(8,128)(2,1)S(1)} %get-tuple-element.21.gain, ...), custom_call_target="tpu_custom_call" | custom-call | tf_op jit(solution)/shard_map/ffn/pallas_call | solution.py:296
  179.4 2.3 %collective-permute-start.15 = (bf16[4,512,256]{2,1,0:T(8,128)(2,1)S(1)}, bf16[4,512,256]{2,1,0:T(8,128)(2,1)S(1)}, u32[]{:S(2)}, u32[]{:S(2)}) collective-permute-start(bf16[4,512,256]{2,1,0:T(8,128)(2,1)S(1)} %get-tuple-element.24), channel_id=1, source_target_pairs={{0,1},{1,0},{2,3},{3,2},{4,5},{5,4},{6,7},{7,6},{8,9},{9,8},{10,11... | collective-permute-start | bytes 3145736 | tf_op jit(solution)/shard_map/ppermute | solution.py:34
  181.6 2.3 %collective-permute-done.15 = bf16[4,512,256]{2,1,0:T(8,128)(2,1)S(1)} collective-permute-done((bf16[4,512,256]{2,1,0:T(8,128)(2,1)S(1)}, bf16[4,512,256]{2,1,0:T(8,128)(2,1)S(1)}, u32[]{:S(2)}, u32[]{:S(2)}) %collective-permute-start.15) | collective-permute-done | bytes 1048608 | tf_op jit(solution)/shard_map/ppermute | solution.py:34
  183.9 0.3 add_convert_fusion
  184.2 17.2 %all_to_all.28 = bf16[4,512,256]{2,1,0:T(8,128)(2,1)S(1)} all-to-all(bf16[4,512,256]{2,1,0:T(8,128)(2,1)S(1)} %add_convert_fusion), channel_id=1, replica_groups=mesh['zh'=4,'zl'=4,'y'=4,'x'=4,'c'=2] {'x'}, dimensions={0} | all-to-all | bytes 2097152 | tf_op jit(solution)/shard_map/all_to_all | solution.py:213
  201.4 0.1 convert_reduce_fusion
  201.6 0.8 add_convert_fusion.2
  (28 shorter events, 0.2 us)
Async XLA Ops:
  6.5 51.1 %all-gather.6.cloned.1.call-start = ((), (), s32[]{:S(2)}) async-start(), calls=%async_computation.6 | async-start | bytes 1474560 | tf_op jit(solution)/shard_map/all_gather | solution.py:246
  6.5 52.9 %copy-start.7 = (bf16[256]{0:T(256)(128)(2,1)S(1)}, bf16[256]{0:T(256)(128)(2,1)}, u32[]{:S(2)}) copy-start(bf16[256]{0:T(256)(128)(2,1)} %param.16) | copy-start | bytes 1540
  6.5 52.9 %copy-start.8 = (bf16[256]{0:T(256)(128)(2,1)S(1)}, bf16[256]{0:T(256)(128)(2,1)}, u32[]{:S(2)}) copy-start(bf16[256]{0:T(256)(128)(2,1)} %param.24) | copy-start | bytes 1540
  6.5 52.9 %copy-start.5 = (bf16[512,256]{1,0:T(8,128)(2,1)S(1)}, bf16[512,256]{1,0:T(8,128)(2,1)}, u32[]{:S(2)}) copy-start(bf16[512,256]{1,0:T(8,128)(2,1)} %param.15) | copy-start | bytes 786436
  8.1 164.2 %all-gather.4.cloned.1.call-start = ((), (), s32[]{:S(2)}) async-start(), calls=%async_computation.5 | async-start | bytes 6684672 | tf_op jit(solution)/shard_map/all_gather | solution.py:247
  37.5 12.8 %collective-permute-start.4 = (bf16[128,768]{1,0:T(8,128)(2,1)S(1)}, bf16[128,768]{1,0:T(8,128)(2,1)S(1)}, u32[]{:S(2)}, u32[]{:S(2)}) collective-permute-start(bf16[128,768]{1,0:T(8,128)(2,1)S(1)} %bitcast.13), channel_id=1, source_target_pairs={{0,32},{32,64},{64,96},{96,128},{128,160},{160,192},{192,224},{224... | collective-permute-start | bytes 589832 | tf_op jit(solution)/shard_map/ppermute | solution.py:44
  44.4 6.4 %collective-permute-start.5 = (bf16[128,768]{1,0:T(8,128)(2,1)S(1)}, bf16[128,768]{1,0:T(8,128)(2,1)S(1)}, u32[]{:S(2)}, u32[]{:S(2)}) collective-permute-start(bf16[128,768]{1,0:T(8,128)(2,1)S(1)} %bitcast.14), channel_id=1, source_target_pairs={{0,480},{32,0},{64,32},{96,64},{128,96},{160,128},{192,160},{224,1... | collective-permute-start | bytes 589832 | tf_op jit(solution)/shard_map/ppermute | solution.py:44
  46.4 10.3 %collective-permute-start.6 = (bf16[128,768]{1,0:T(8,128)(2,1)S(1)}, bf16[128,768]{1,0:T(8,128)(2,1)S(1)}, u32[]{:S(2)}, u32[]{:S(2)}) collective-permute-start(bf16[128,768]{1,0:T(8,128)(2,1)S(1)} %bitcast.15), channel_id=1, source_target_pairs={{0,64},{32,96},{64,128},{96,160},{128,192},{160,224},{192,256},{22... | collective-permute-start | bytes 589832 | tf_op jit(solution)/shard_map/ppermute | solution.py:44
  59.4 17.7 %copy-start.4 = (bf16[512,768]{1,0:T(8,128)(2,1)S(1)}, bf16[512,768]{1,0:T(8,128)(2,1)}, u32[]{:S(2)}) copy-start(bf16[512,768]{1,0:T(8,128)(2,1)} %pad_maximum_fusion) | copy-start | bytes 2359300
  59.5 7.6 %collective-permute-start = (bf16[528,256]{1,0:T(8,128)(2,1)S(1)}, bf16[528,256]{1,0:T(8,128)(2,1)S(1)}, u32[]{:S(2)}, u32[]{:S(2)}) collective-permute-start(bf16[528,256]{1,0:T(8,128)(2,1)S(1)} %get-tuple-element.26), channel_id=1, source_target_pairs={{0,1},{1,0},{2,3},{3,2},{4,5},{5,4},{6,7},{7,6},{8,9},{9,8},{10,11... | collective-permute-start | bytes 811016 | tf_op jit(solution)/shard_map/ppermute | solution.py:34
  67.2 16.7 %collective-permute-start.1 = (bf16[2,528,256]{2,1,0:T(8,128)(2,1)S(1)}, bf16[2,528,256]{2,1,0:T(8,128)(2,1)S(1)}, u32[]{:S(2)}, u32[]{:S(2)}) collective-permute-start(bf16[2,528,256]{2,1,0:T(8,128)(2,1)S(1)} %pad_maximum_fusion.1.p0), channel_id=1, source_target_pairs={{0,2},{2,4},{4,6},{6,0},{1,3},{3,5},{5,7},{7,1},{8,10},{10,12},{12... | collective-permute-start | bytes 1622024 | tf_op jit(solution)/shard_map/ppermute | solution.py:44
  70.3 18.4 %collective-permute-start.2 = (bf16[2,528,256]{2,1,0:T(8,128)(2,1)S(1)}, bf16[2,528,256]{2,1,0:T(8,128)(2,1)S(1)}, u32[]{:S(2)}, u32[]{:S(2)}) collective-permute-start(bf16[2,528,256]{2,1,0:T(8,128)(2,1)S(1)} %pad_maximum_fusion.1.p0), channel_id=1, source_target_pairs={{0,6},{2,0},{4,2},{6,4},{1,7},{3,1},{5,3},{7,5},{8,14},{10,8},{12,... | collective-permute-start | bytes 1622024 | tf_op jit(solution)/shard_map/ppermute | solution.py:44
  73.7 22.6 %collective-permute-start.3 = (bf16[2,528,256]{2,1,0:T(8,128)(2,1)S(1)}, bf16[2,528,256]{2,1,0:T(8,128)(2,1)S(1)}, u32[]{:S(2)}, u32[]{:S(2)}) collective-permute-start(bf16[2,528,256]{2,1,0:T(8,128)(2,1)S(1)} %pad_maximum_fusion.1.p0), channel_id=1, source_target_pairs={{0,4},{2,6},{4,0},{6,2},{1,5},{3,7},{5,1},{7,3},{8,12},{10,14},{12... | collective-permute-start | bytes 1622024 | tf_op jit(solution)/shard_map/ppermute | solution.py:44
  77.2 23.8 %collective-permute-start.7 = (bf16[512,512]{1,0:T(8,128)(2,1)S(1)}, bf16[512,512]{1,0:T(8,128)(2,1)S(1)}, u32[]{:S(2)}, u32[]{:S(2)}) collective-permute-start(bf16[512,512]{1,0:T(8,128)(2,1)S(1)} %slice.12.p0), channel_id=1, source_target_pairs={{0,8},{8,16},{16,24},{24,0},{1,9},{9,17},{17,25},{25,1},{2,10},{10... | collective-permute-start | bytes 1572872 | tf_op jit(solution)/shard_map/ppermute | solution.py:44
  80.4 24.5 %collective-permute-start.8 = (bf16[512,512]{1,0:T(8,128)(2,1)S(1)}, bf16[512,512]{1,0:T(8,128)(2,1)}, u32[]{:S(2)}, u32[]{:S(2)}) collective-permute-start(bf16[512,512]{1,0:T(8,128)(2,1)S(1)} %slice.12.p0), channel_id=1, source_target_pairs={{0,24},{8,0},{16,8},{24,16},{1,25},{9,1},{17,9},{25,17},{2,26},{10... | collective-permute-start | bytes 1572872 | tf_op jit(solution)/shard_map/ppermute | solution.py:44
  83.9 21.3 %collective-permute-start.9 = (bf16[512,512]{1,0:T(8,128)(2,1)S(1)}, bf16[512,512]{1,0:T(8,128)(2,1)}, u32[]{:S(2)}, u32[]{:S(2)}) collective-permute-start(bf16[512,512]{1,0:T(8,128)(2,1)S(1)} %slice.12.p0), channel_id=1, source_target_pairs={{0,16},{8,24},{16,0},{24,8},{1,17},{9,25},{17,1},{25,9},{2,18},{10... | collective-permute-start | bytes 1572872 | tf_op jit(solution)/shard_map/ppermute | solution.py:44
  88.7 31.3 %collective-permute-start.10 = (bf16[512,256]{1,0:T(8,128)(2,1)S(1)}, bf16[512,256]{1,0:T(8,128)(2,1)}, u32[]{:S(2)}, u32[]{:S(2)}) collective-permute-start(bf16[512,256]{1,0:T(8,128)(2,1)S(1)} %slice.13.p0), channel_id=1, source_target_pairs={{0,8},{8,16},{16,24},{24,0},{1,9},{9,17},{17,25},{25,1},{2,10},{10... | collective-permute-start | bytes 786440 | tf_op jit(solution)/shard_map/ppermute | solution.py:44
  96.3 23.7 %collective-permute-start.11 = (bf16[512,256]{1,0:T(8,128)(2,1)S(1)}, bf16[512,256]{1,0:T(8,128)(2,1)}, u32[]{:S(2)}, u32[]{:S(2)}) collective-permute-start(bf16[512,256]{1,0:T(8,128)(2,1)S(1)} %slice.13.p0), channel_id=1, source_target_pairs={{0,24},{8,0},{16,8},{24,16},{1,25},{9,1},{17,9},{25,17},{2,26},{10... | collective-permute-start | bytes 786440 | tf_op jit(solution)/shard_map/ppermute | solution.py:44
  101.0 19.0 %collective-permute-start.12 = (bf16[512,256]{1,0:T(8,128)(2,1)S(1)}, bf16[512,256]{1,0:T(8,128)(2,1)}, u32[]{:S(2)}, u32[]{:S(2)}) collective-permute-start(bf16[512,256]{1,0:T(8,128)(2,1)S(1)} %slice.13.p0), channel_id=1, source_target_pairs={{0,16},{8,24},{16,0},{24,8},{1,17},{9,25},{17,1},{25,9},{2,18},{10... | collective-permute-start | bytes 786440 | tf_op jit(solution)/shard_map/ppermute | solution.py:44
  105.2 14.7 %copy-start.9 = (bf16[256]{0:T(256)(128)(2,1)S(1)}, bf16[256]{0:T(256)(128)(2,1)}, u32[]{:S(2)}) copy-start(bf16[256]{0:T(256)(128)(2,1)} %param.19) | copy-start | bytes 1540
  105.2 14.8 %copy-start.10 = (bf16[256]{0:T(256)(128)(2,1)S(1)}, bf16[256]{0:T(256)(128)(2,1)}, u32[]{:S(2)}) copy-start(bf16[256]{0:T(256)(128)(2,1)} %param.20) | copy-start | bytes 1540
  105.2 19.5 %copy-start = (bf16[2,128,128]{2,1,0:T(8,128)(2,1)S(1)}, bf16[2,128,128]{2,1,0:T(8,128)(2,1)}, u32[]{:S(2)}) copy-start(bf16[2,128,128]{2,1,0:T(8,128)(2,1)} %mix.3) | copy-start | bytes 196612
  105.2 19.5 %copy-start.3 = (bf16[2,128]{1,0:T(2,128)(2,1)S(1)}, bf16[2,128]{1,0:T(2,128)(2,1)}, u32[]{:S(2)}) copy-start(bf16[2,128]{1,0:T(2,128)(2,1)} %bias.1) | copy-start | bytes 1540
  108.8 16.0 %all-to-all-start.1 = ((f32[8,2,512]{2,1,0:T(2,128)}), f32[8,2,512]{2,1,0:T(2,128)S(1)}, u32[]{:S(2)}, u32[]{:S(2)}) async-start(f32[8,2,512]{2,1,0:T(2,128)} %broadcast_in_dim.24), calls=%async_computation.1 | async-start | bytes 65536 | tf_op jit(solution)/shard_map/all_to_all | solution.py:30
  126.9 4.8 %collective-permute-start.13 = (bf16[4,512,256]{2,1,0:T(8,128)(2,1)S(1)}, bf16[4,512,256]{2,1,0:T(8,128)(2,1)S(1)}, u32[]{:S(2)}, u32[]{:S(2)}) collective-permute-start(bf16[4,512,256]{2,1,0:T(8,128)(2,1)S(1)} %get-tuple-element.20), channel_id=1, source_target_pairs={{0,1},{1,0},{2,3},{3,2},{4,5},{5,4},{6,7},{7,6},{8,9},{9,8},{10,11... | collective-permute-start | bytes 3145736 | tf_op jit(solution)/shard_map/ppermute | solution.py:34
  132.0 17.5 %copy-start.6 = (bf16[512,256]{1,0:T(8,128)(2,1)S(1)}, bf16[512,256]{1,0:T(8,128)(2,1)}, u32[]{:S(2)}) copy-start(bf16[512,256]{1,0:T(8,128)(2,1)} %param.15) | copy-start | bytes 786436
  149.6 22.8 %copy-start.1 = (bf16[3,512]{1,0:T(4,128)(2,1)S(1)}, bf16[3,512]{1,0:T(4,128)(2,1)}, u32[]{:S(2)}) copy-start(bf16[3,512]{1,0:T(4,128)(2,1)} %conv_gate.1) | copy-start | bytes 9220
  149.6 22.8 %copy-start.2 = (bf16[3,512]{1,0:T(4,128)(2,1)S(1)}, bf16[3,512]{1,0:T(4,128)(2,1)}, u32[]{:S(2)}) copy-start(bf16[3,512]{1,0:T(4,128)(2,1)} %conv_value.1) | copy-start | bytes 9220
  166.1 6.3 %collective-permute-start.14 = (bf16[4,512,256]{2,1,0:T(8,128)(2,1)S(1)}, bf16[4,512,256]{2,1,0:T(8,128)(2,1)S(1)}, u32[]{:S(2)}, u32[]{:S(2)}) collective-permute-start(bf16[4,512,256]{2,1,0:T(8,128)(2,1)S(1)} %all_to_all.27.mine), channel_id=1, source_target_pairs={{0,1},{1,0},{2,3},{3,2},{4,5},{5,4},{6,7},{7,6},{8,9},{9,8},{10,11... | collective-permute-start | bytes 3145736 | tf_op jit(solution)/shard_map/ppermute | solution.py:34
  179.4 4.6 %collective-permute-start.15 = (bf16[4,512,256]{2,1,0:T(8,128)(2,1)S(1)}, bf16[4,512,256]{2,1,0:T(8,128)(2,1)S(1)}, u32[]{:S(2)}, u32[]{:S(2)}) collective-permute-start(bf16[4,512,256]{2,1,0:T(8,128)(2,1)S(1)} %get-tuple-element.24), channel_id=1, source_target_pairs={{0,1},{1,0},{2,3},{3,2},{4,5},{5,4},{6,7},{7,6},{8,9},{9,8},{10,11... | collective-permute-start | bytes 3145736 | tf_op jit(solution)/shard_map/ppermute | solution.py:34
Sparse Core Ops, SparseCore 0:
  9.4 35.2 all-gather.5
  59.5 81.1 all-gather.3

commit v8 on v7

--- a/solution.py
+++ b/solution.py
@@ -17,7 +17,7 @@
 F32 = jnp.float32
 BF16 = jnp.bfloat16
 SWAP = [(0, 1), (1, 0)]
-RING = (0, 1, 3, 2)
+RING = (0, 2, 1, 3)
 PIECE = 32
 HBM = pl.BlockSpec(memory_space=pltpu.HBM)
 SQRT_HALF = 0.7071067811865476
@@ -40,7 +40,7 @@
 
 def round_ring(shard, axis):
     size = lax.axis_size(axis)
-    steps = (1, size - 1, 2)
+    steps = (2, 1, size - 1)
     return [shard] + [lax.ppermute(shard, axis, [(i, (i + step) % size) for i in range(size)]) for step in steps]
 
 
@@ -152,37 +152,29 @@
     ]
     for copy in copies:
         copy.start()
+    for part in range(mine.shape[1] // BLOCK):
+        rows = pl.ds(part * BLOCK, BLOCK)
+        squares = jnp.zeros((BLOCK, width), F32)
+        for ref in (mine, other):
+            for x in range(4):
+                value = ref[x, rows, :].astype(F32)
+                squares = squares + value * value
+        scale = lax.rsqrt(jnp.sum(squares, axis=1, keepdims=True) / (8 * width) + EPS)
+        for side, ref in ((c, mine), (1 - c, other)):
+            for x in range(4):
+                block = 2 * x + side
+                row = gain[block, 0:1, :].astype(F32)
+                normed[rows, pl.ds(pl.multiple_of(block * width, width), width)] = (
+                    ref[x, rows, :].astype(F32) * scale * row
+                ).astype(BF16)
     for part in range(mine.shape[1] // SEQ_LEN):
         rows = pl.ds(part * SEQ_LEN, SEQ_LEN)
-        squares = jnp.zeros((SEQ_LEN, 1), F32)
-        for x in range(mine.shape[0]):
-            for ref in (mine, other):
-                value = ref[x, rows, :].astype(F32)
-                squares = squares + jnp.sum(value * value, axis=1, keepdims=True)
-        scale = lax.rsqrt(squares / (2 * mine.shape[0] * width) + EPS)
-
-        def fill(ref, side):
-            for x in range(mine.shape[0]):
-                at = pl.ds((2 * x + side) * width, width)
-                row = gain[2 * x + side, 0:1, :].astype(F32)
-                normed[:, at] = (ref[x, rows, :].astype(F32) * scale * row).astype(BF16)
-
-        @pl.when(c == 0)
-        def _():
-            fill(mine, 0)
-            fill(other, 1)
-
-        @pl.when(c == 1)
-        def _():
-            fill(other, 0)
-            fill(mine, 1)
-
         if part == 0:
             copies[0].wait()
-        gate = jnp.dot(normed[...], late[:, 0:ff], preferred_element_type=F32)
+        gate = jnp.dot(normed[rows, :], late[:, 0:ff], preferred_element_type=F32)
         if part == 0:
             copies[1].wait()
-        value = jnp.dot(normed[...], late[:, ff : 2 * ff], preferred_element_type=F32)
+        value = jnp.dot(normed[rows, :], late[:, ff : 2 * ff], preferred_element_type=F32)
         conv_g = taps(gate, conv_gate[...].astype(F32))
         conv_v = taps(value, conv_value[...].astype(F32))
         hidden[rows, :] = (conv_g * jax.nn.sigmoid(conv_g) * conv_v).astype(BF16)
@@ -244,7 +236,7 @@
     late = jnp.concatenate([ffn_gate, ffn_value, proj_down.T], axis=1)
     padded = jnp.pad(late, ((0, 2 * late.shape[0]), (0, 0)))
     late_y = lax.all_gather(padded, "y", axis=0)[:, : late.shape[0]].reshape(-1, late.shape[1])
-    late_all = lax.all_gather(after(late_y, early_z), Z, axis=0, tiled=True)
+    late_all = lax.all_gather(after(late_y, early_far), Z, axis=0, tiled=True)
 
     packed = jnp.concatenate([tokens, jnp.broadcast_to(norm_gain, (8, da)), jnp.broadcast_to(ffn_gain, (8, da))], axis=0)
     pair = jnp.stack([packed, other_core(packed)])
@@ -298,7 +290,7 @@
         in_specs=[SMEM] + [VMEM] * 3 + [HBM] + [VMEM] * 2,
         out_specs=[VMEM] * 2,
         out_shape=blocks,
-        scratch_shapes=[pltpu.VMEM((SEQ_LEN, model), BF16), pltpu.VMEM((row_count, ff), BF16), pltpu.VMEM(late_all.shape, BF16), pltpu.SemaphoreType.DMA((3,))],
+        scratch_shapes=[pltpu.VMEM((row_count, model), BF16), pltpu.VMEM((row_count, ff), BF16), pltpu.VMEM(late_all.shape, BF16), pltpu.SemaphoreType.DMA((3,))],
         name="ffn",
         compiler_params=room(47),
     )(

time: 210 us -> 203 us (0.967)
  blocking collectives: 79.5 us -> 51 us
  waiting for transfers between devices: 24.8 us -> 38.2 us
  starting transfers between devices: 69.8 us -> 76.9 us
    all_to_all x2 -> x1, blocking collectives: 44.9 us -> 16.4 us  [everyones(): return lax.all_to_all(copies, axis, split_axis=0, concat_axis=0, tiled=True)]
    all_gather x1, waiting for transfers between devices: 0.01 us -> 19.5 us  [on_device(): lax.all_gather(padded, 'y', axis=0)[:, :late.shape[0]]]
    all_to_all x1 -> x2, starting transfers between devices: 11.2 us -> 20.7 us  [everyones(): return lax.all_to_all(copies, axis, split_axis=0, concat_axis=0, tiled=True)]
    ppermute x12, waiting for transfers between devices: 12.1 us -> 7.71 us  [round_ring(): lax.ppermute(shard, axis, [(i, (i + step) % size) for i in range(size)])]
    all_to_all x1 -> x2, waiting for transfers between devices: 4.73 us -> 4.18 us  [everyones(): return lax.all_to_all(copies, axis, split_axis=0, concat_axis=0, tiled=True)]
  transfers between devices with their start and end apart: 19 -> 20, of which waited for: 10 -> 8; matrix products, arithmetic and copies ran while one was open for 1% -> 3% of each run, Pallas kernels for 3% -> 3%
where the time goes in v8:
time: 203 us; the launch traced here: 202 us
  starting transfers between devices  76.9 us (38%)
  blocking collectives  51 us (25%)
  waiting for transfers between devices  38.2 us (19%)
  Pallas kernels  14.1 us (7%)
  between operations  13.8 us (7%)
  other arithmetic  5.07 us (2%)
  local copies, waits for them, and re-layouts  3.27 us (2%)
    ppermute x12, starting transfers between devices, round_ring(): lax.ppermute(shard, axis, [(i, (i + step) % size) for i in range(size)])  42.6 us
    all_to_all x2, blocking collectives, summed_at_owner(): arrived = lax.all_to_all(pair, 'x', split_axis=0, concat_axis=0, tiled=True)  34.6 us
    all_to_all x2, starting transfers between devices, everyones(): return lax.all_to_all(copies, axis, split_axis=0, concat_axis=0, tiled=True)  20.7 us
    all_gather x1, waiting for transfers between devices, on_device(): lax.all_gather(padded, 'y', axis=0)[:, :late.shape[0]]  19.5 us
    all_to_all x1, blocking collectives, everyones(): return lax.all_to_all(copies, axis, split_axis=0, concat_axis=0, tiled=True)  16.4 us
    ppermute x4, starting transfers between devices, other_core(): return lax.ppermute(value, 'c', SWAP)  13.6 us
    ppermute x12, waiting for transfers between devices, round_ring(): lax.ppermute(shard, axis, [(i, (i + step) % size) for i in range(size)])  7.71 us
    pallas_call x1, Pallas kernels, on_device(): pl.pallas_call(ffn_kernel, in_specs=[SMEM] + [VMEM] * 3 + [HBM] + [VMEM]...  7.45 us
  transfers between devices with their start and end apart: 20, of which 8 were waited for; matrix products, arithmetic and copies ran while one was open for 3% of the time, Pallas kernels for 3%

profile of v8, /device:TPU:1, one launch (start us, length us, event | category | flops | bytes accessed | tf_op | source)
XLA Modules:
  0.0 202.3 jit_solution(11676909633810179757)
XLA Ops:
  6.5 1.6 fusion.4
  8.1 0.0 all-gather.6.cloned.1.call-update
  8.2 0.8 pad_maximum_fusion.4
  8.9 0.7 broadcast_in_dim.23
  9.6 15.6 %all-to-all-start = ((bf16[4,32,768]{2,1,0:T(8,128)(2,1)}), bf16[4,32,768]{2,1,0:T(8,128)(2,1)S(1)}, u32[]{:S(2)}, u32[]{:S(2)}) async-start(bf16[4,32,768]{2,1,0:T(8,128)(2,1)} %broadcast_in_dim.23), calls=%async_computation | async-start | bytes 393216 | tf_op jit(solution)/shard_map/all_to_all | solution.py:30
  25.2 19.5 %all-gather.6.cloned.1.call-done = bf16[384,1536]{1,0:T(8,128)(2,1)} async-done(((bf16[96,1536]{1,0:T(8,128)(2,1)}), bf16[384,1536]{1,0:T(8,128)(2,1)}) %all-gather.6.cloned.1.call-update) | async-done | bytes 1179664 | tf_op jit(solution)/shard_map/all_gather | solution.py:238
  44.7 1.8 slice.13
  46.5 0.0 all-to-all-done
  46.5 0.0 all-gather.4.cloned.1.call-update
  46.6 4.7 %collective-permute-start = (bf16[528,256]{1,0:T(8,128)(2,1)S(1)}, bf16[528,256]{1,0:T(8,128)(2,1)S(1)}, u32[]{:S(2)}, u32[]{:S(2)}) collective-permute-start(bf16[528,256]{1,0:T(8,128)(2,1)S(1)} %get-tuple-element.26), channel_id=1, source_target_pairs={{0,1},{1,0},{2,3},{3,2},{4,5},{5,4},{6,7},{7,6},{8,9},{9,8},{10,11... | collective-permute-start | bytes 811016 | tf_op jit(solution)/shard_map/ppermute | solution.py:34
  51.3 4.2 %collective-permute-start.4 = (bf16[128,768]{1,0:T(8,128)(2,1)S(1)}, bf16[128,768]{1,0:T(8,128)(2,1)S(1)}, u32[]{:S(2)}, u32[]{:S(2)}) collective-permute-start(bf16[128,768]{1,0:T(8,128)(2,1)S(1)} %bitcast.12), channel_id=1, source_target_pairs={{0,64},{32,96},{64,128},{96,160},{128,192},{160,224},{192,256},{22... | collective-permute-start | bytes 589832 | tf_op jit(solution)/shard_map/ppermute | solution.py:44
  55.5 3.2 %collective-permute-start.5 = (bf16[128,768]{1,0:T(8,128)(2,1)S(1)}, bf16[128,768]{1,0:T(8,128)(2,1)S(1)}, u32[]{:S(2)}, u32[]{:S(2)}) collective-permute-start(bf16[128,768]{1,0:T(8,128)(2,1)S(1)} %bitcast.13), channel_id=1, source_target_pairs={{0,32},{32,64},{64,96},{96,128},{128,160},{160,192},{192,224},{224... | collective-permute-start | bytes 589832 | tf_op jit(solution)/shard_map/ppermute | solution.py:44
  58.7 3.3 %collective-permute-start.6 = (bf16[128,768]{1,0:T(8,128)(2,1)S(1)}, bf16[128,768]{1,0:T(8,128)(2,1)S(1)}, u32[]{:S(2)}, u32[]{:S(2)}) collective-permute-start(bf16[128,768]{1,0:T(8,128)(2,1)S(1)} %bitcast.14), channel_id=1, source_target_pairs={{0,480},{32,0},{64,32},{96,64},{128,96},{160,128},{192,160},{224,1... | collective-permute-start | bytes 589832 | tf_op jit(solution)/shard_map/ppermute | solution.py:44
  62.0 0.0 collective-permute-done
  62.0 0.1 pad_maximum_fusion.1.p0
  62.1 4.6 %collective-permute-start.1 = (bf16[2,528,256]{2,1,0:T(8,128)(2,1)S(1)}, bf16[2,528,256]{2,1,0:T(8,128)(2,1)S(1)}, u32[]{:S(2)}, u32[]{:S(2)}) collective-permute-start(bf16[2,528,256]{2,1,0:T(8,128)(2,1)S(1)} %pad_maximum_fusion.1.p0), channel_id=1, source_target_pairs={{0,4},{2,6},{4,0},{6,2},{1,5},{3,7},{5,1},{7,3},{8,12},{10,14},{12... | collective-permute-start | bytes 1622024 | tf_op jit(solution)/shard_map/ppermute | solution.py:44
  66.7 2.2 %collective-permute-start.2 = (bf16[2,528,256]{2,1,0:T(8,128)(2,1)S(1)}, bf16[2,528,256]{2,1,0:T(8,128)(2,1)S(1)}, u32[]{:S(2)}, u32[]{:S(2)}) collective-permute-start(bf16[2,528,256]{2,1,0:T(8,128)(2,1)S(1)} %pad_maximum_fusion.1.p0), channel_id=1, source_target_pairs={{0,2},{2,4},{4,6},{6,0},{1,3},{3,5},{5,7},{7,1},{8,10},{10,12},{12... | collective-permute-start | bytes 1622024 | tf_op jit(solution)/shard_map/ppermute | solution.py:44
  68.9 0.0 collective-permute-done.4
  68.9 4.3 %collective-permute-start.3 = (bf16[2,528,256]{2,1,0:T(8,128)(2,1)S(1)}, bf16[2,528,256]{2,1,0:T(8,128)(2,1)S(1)}, u32[]{:S(2)}, u32[]{:S(2)}) collective-permute-start(bf16[2,528,256]{2,1,0:T(8,128)(2,1)S(1)} %pad_maximum_fusion.1.p0), channel_id=1, source_target_pairs={{0,6},{2,0},{4,2},{6,4},{1,7},{3,1},{5,3},{7,5},{8,14},{10,8},{12,... | collective-permute-start | bytes 1622024 | tf_op jit(solution)/shard_map/ppermute | solution.py:44
  73.2 0.0 collective-permute-done.5
  73.3 0.1 pad_maximum_fusion
  73.4 3.9 %collective-permute-start.7 = (bf16[512,512]{1,0:T(8,128)(2,1)S(1)}, bf16[512,512]{1,0:T(8,128)(2,1)S(1)}, u32[]{:S(2)}, u32[]{:S(2)}) collective-permute-start(bf16[512,512]{1,0:T(8,128)(2,1)S(1)} %slice.12.p0), channel_id=1, source_target_pairs={{0,16},{8,24},{16,0},{24,8},{1,17},{9,25},{17,1},{25,9},{2,18},{10... | collective-permute-start | bytes 1572872 | tf_op jit(solution)/shard_map/ppermute | solution.py:44
  77.3 1.9 collective-permute-start.8
  79.3 0.0 collective-permute-done.1.p1
  79.3 4.6 %collective-permute-start.9 = (bf16[512,512]{1,0:T(8,128)(2,1)S(1)}, bf16[512,512]{1,0:T(8,128)(2,1)}, u32[]{:S(2)}, u32[]{:S(2)}) collective-permute-start(bf16[512,512]{1,0:T(8,128)(2,1)S(1)} %slice.12.p0), channel_id=1, source_target_pairs={{0,24},{8,0},{16,8},{24,16},{1,25},{9,1},{17,9},{25,17},{2,26},{10... | collective-permute-start | bytes 1572872 | tf_op jit(solution)/shard_map/ppermute | solution.py:44
  83.8 0.9 pad_maximum_fusion.3.p0
  84.7 6.7 %collective-permute-done.2.p2 = bf16[2,528,256]{2,1,0:T(8,128)(2,1)S(1)} collective-permute-done((bf16[2,528,256]{2,1,0:T(8,128)(2,1)S(1)}, bf16[2,528,256]{2,1,0:T(8,128)(2,1)S(1)}, u32[]{:S(2)}, u32[]{:S(2)}) %collective-permute-start.2) | collective-permute-done | bytes 540704 | tf_op jit(solution)/shard_map/ppermute | solution.py:44
  91.4 3.9 %collective-permute-start.10 = (bf16[512,256]{1,0:T(8,128)(2,1)S(1)}, bf16[512,256]{1,0:T(8,128)(2,1)}, u32[]{:S(2)}, u32[]{:S(2)}) collective-permute-start(bf16[512,256]{1,0:T(8,128)(2,1)S(1)} %pad_maximum_fusion.3.p0), channel_id=1, source_target_pairs={{0,16},{8,24},{16,0},{24,8},{1,17},{9,25},{17,1},{25,9},{2,18},{10... | collective-permute-start | bytes 786440 | tf_op jit(solution)/shard_map/ppermute | solution.py:44
  95.3 0.0 collective-permute-done.3.p3
  95.3 1.9 collective-permute-start.11
  97.3 4.6 %collective-permute-start.12 = (bf16[512,256]{1,0:T(8,128)(2,1)S(1)}, bf16[512,256]{1,0:T(8,128)(2,1)}, u32[]{:S(2)}, u32[]{:S(2)}) collective-permute-start(bf16[512,256]{1,0:T(8,128)(2,1)S(1)} %pad_maximum_fusion.3.p0), channel_id=1, source_target_pairs={{0,24},{8,0},{16,8},{24,16},{1,25},{9,1},{17,9},{25,17},{2,26},{10... | collective-permute-start | bytes 786440 | tf_op jit(solution)/shard_map/ppermute | solution.py:44
  101.9 0.1 pad_add_fusion.place
  101.9 1.6 norm.1
  103.5 0.5 collective-permute-done.8.p2
  104.0 0.0 collective-permute-done.9.p3
  104.0 0.0 copy-start.3
  104.0 2.9 %first.1 = (f32[512,256]{1,0:T(8,128)S(1)}, f32[512,256]{1,0:T(8,128)S(1)}, f32[2,512]{1,0:T(2,128)S(1)}) custom-call(s32[4]{0:T(128)S(1)} %pad_add_fusion.place, bf16[512,2048]{1,0:T(8,128)(2,1)S(1)} %get-tuple-element.15.normed, bf16[512,512]{1,0:T(8,128)(2,1)S(1)} %slice.12.p0, bf16[512,512]{1,0:T(8,128)(2,1)S(1)} %collective-permute-done.7.p1, ...), custom_call_target="tpu_custom_call" | custom-call | tf_op jit(solution)/shard_map/first/pallas_call | solution.py:256
  106.9 0.6 broadcast_in_dim.24
  107.5 5.1 %all-to-all-start.1 = ((f32[8,2,512]{2,1,0:T(2,128)}), f32[8,2,512]{2,1,0:T(2,128)S(1)}, u32[]{:S(2)}, u32[]{:S(2)}) async-start(f32[8,2,512]{2,1,0:T(2,128)} %broadcast_in_dim.24), calls=%async_computation.1 | async-start | bytes 65536 | tf_op jit(solution)/shard_map/all_to_all | solution.py:30
  112.6 0.0 collective-permute-done.10.p1
  112.6 0.6 collective-permute-done.11.p2
  113.2 0.0 collective-permute-done.12.p3
  113.2 4.2 %all-to-all-done.1.stats = f32[8,2,512]{2,1,0:T(2,128)S(1)} async-done(((f32[8,2,512]{2,1,0:T(2,128)}), f32[8,2,512]{2,1,0:T(2,128)S(1)}, u32[]{:S(2)}, u32[]{:S(2)}) %all-to-all-start.1) | async-done | bytes 32800 | tf_op jit(solution)/shard_map/all_to_all | solution.py:30
  117.4 2.2 %mix.2 = (bf16[4,512,256]{2,1,0:T(8,128)(2,1)S(1)}, bf16[4,512,256]{2,1,0:T(8,128)(2,1)S(1)}) custom-call(s32[4]{0:T(128)S(1)} %pad_add_fusion.place, f32[512,256]{1,0:T(8,128)S(1)} %get-tuple-element.16.act_v, f32[512,256]{1,0:T(8,128)S(1)} %get-tuple-element.17.act_u, f32[8,2,512]{2,1,0:T(2,128)S(1)} %all-to-all-done.1.stats, ...), custom_call_target="tpu_custom_call" | custom-call | tf_op jit(solution)/shard_map/mix/pallas_call | solution.py:267
  119.5 2.6 %collective-permute-start.13 = (bf16[4,512,256]{2,1,0:T(8,128)(2,1)S(1)}, bf16[4,512,256]{2,1,0:T(8,128)(2,1)S(1)}, u32[]{:S(2)}, u32[]{:S(2)}) collective-permute-start(bf16[4,512,256]{2,1,0:T(8,128)(2,1)S(1)} %get-tuple-element.20), channel_id=1, source_target_pairs={{0,1},{1,0},{2,3},{3,2},{4,5},{5,4},{6,7},{7,6},{8,9},{9,8},{10,11... | collective-permute-start | bytes 3145736 | tf_op jit(solution)/shard_map/ppermute | solution.py:34
  122.1 2.3 %collective-permute-done.13 = bf16[4,512,256]{2,1,0:T(8,128)(2,1)S(1)} collective-permute-done((bf16[4,512,256]{2,1,0:T(8,128)(2,1)S(1)}, bf16[4,512,256]{2,1,0:T(8,128)(2,1)S(1)}, u32[]{:S(2)}, u32[]{:S(2)}) %collective-permute-start.13) | collective-permute-done | bytes 1048608 | tf_op jit(solution)/shard_map/ppermute | solution.py:34
  124.4 0.2 add_convert_fusion.1
  124.6 0.0 copy-start.6
  124.6 17.4 %all_to_all.25 = bf16[4,512,256]{2,1,0:T(8,128)(2,1)S(1)} all-to-all(bf16[4,512,256]{2,1,0:T(8,128)(2,1)S(1)} %add_convert_fusion.1), channel_id=1, replica_groups=mesh['zh'=4,'zl'=4,'y'=4,'x'=4,'c'=2] {'x'}, dimensions={0} | all-to-all | bytes 2097152 | tf_op jit(solution)/shard_map/all_to_all | solution.py:205
  142.0 0.1 convert_reduce_fusion.1
  142.2 0.0 copy-start.1
  142.2 0.0 copy-start.2
  142.2 0.1 add_convert_fusion.3
  142.3 0.1 broadcast_in_dim.27
  142.3 16.4 %all_to_all.26.mine = bf16[4,512,256]{2,1,0:T(8,128)(2,1)S(1)} all-to-all(bf16[4,512,256]{2,1,0:T(8,128)(2,1)S(1)} %broadcast_in_dim.27), channel_id=1, replica_groups=mesh['zh'=4,'zl'=4,'y'=4,'x'=4,'c'=2] {'x'}, dimensions={0} | all-to-all | bytes 2097152 | tf_op jit(solution)/shard_map/all_to_all | solution.py:30
  158.7 4.0 %collective-permute-start.14 = (bf16[4,512,256]{2,1,0:T(8,128)(2,1)S(1)}, bf16[4,512,256]{2,1,0:T(8,128)(2,1)S(1)}, u32[]{:S(2)}, u32[]{:S(2)}) collective-permute-start(bf16[4,512,256]{2,1,0:T(8,128)(2,1)S(1)} %all_to_all.26.mine), channel_id=1, source_target_pairs={{0,1},{1,0},{2,3},{3,2},{4,5},{5,4},{6,7},{7,6},{8,9},{9,8},{10,11... | collective-permute-start | bytes 3145736 | tf_op jit(solution)/shard_map/ppermute | solution.py:34
  162.7 2.3 %collective-permute-done.14.other = bf16[4,512,256]{2,1,0:T(8,128)(2,1)S(1)} collective-permute-done((bf16[4,512,256]{2,1,0:T(8,128)(2,1)S(1)}, bf16[4,512,256]{2,1,0:T(8,128)(2,1)S(1)}, u32[]{:S(2)}, u32[]{:S(2)}) %collective-permute-start.14) | collective-permute-done | bytes 1048608 | tf_op jit(solution)/shard_map/ppermute | solution.py:34
  165.0 7.4 %ffn.1 = (bf16[4,512,256]{2,1,0:T(8,128)(2,1)S(1)}, bf16[4,512,256]{2,1,0:T(8,128)(2,1)S(1)}) custom-call(s32[4]{0:T(128)S(1)} %pad_add_fusion.place, bf16[4,512,256]{2,1,0:T(8,128)(2,1)S(1)} %all_to_all.26.mine, bf16[4,512,256]{2,1,0:T(8,128)(2,1)S(1)} %collective-permute-done.14.other, bf16[8,8,256]{2,1,0:T(8,128)(2,1)S(1)} %get-tuple-element.21.gain, ...), custom_call_target="tpu_custom_call" | custom-call | tf_op jit(solution)/shard_map/ffn/pallas_call | solution.py:288
  172.4 2.3 %collective-permute-start.15 = (bf16[4,512,256]{2,1,0:T(8,128)(2,1)S(1)}, bf16[4,512,256]{2,1,0:T(8,128)(2,1)S(1)}, u32[]{:S(2)}, u32[]{:S(2)}) collective-permute-start(bf16[4,512,256]{2,1,0:T(8,128)(2,1)S(1)} %get-tuple-element.24), channel_id=1, source_target_pairs={{0,1},{1,0},{2,3},{3,2},{4,5},{5,4},{6,7},{7,6},{8,9},{9,8},{10,11... | collective-permute-start | bytes 3145736 | tf_op jit(solution)/shard_map/ppermute | solution.py:34
  174.7 2.3 %collective-permute-done.15 = bf16[4,512,256]{2,1,0:T(8,128)(2,1)S(1)} collective-permute-done((bf16[4,512,256]{2,1,0:T(8,128)(2,1)S(1)}, bf16[4,512,256]{2,1,0:T(8,128)(2,1)S(1)}, u32[]{:S(2)}, u32[]{:S(2)}) %collective-permute-start.15) | collective-permute-done | bytes 1048608 | tf_op jit(solution)/shard_map/ppermute | solution.py:34
  177.0 0.3 add_convert_fusion
  177.3 17.2 %all_to_all.27 = bf16[4,512,256]{2,1,0:T(8,128)(2,1)S(1)} all-to-all(bf16[4,512,256]{2,1,0:T(8,128)(2,1)S(1)} %add_convert_fusion), channel_id=1, replica_groups=mesh['zh'=4,'zl'=4,'y'=4,'x'=4,'c'=2] {'x'}, dimensions={0} | all-to-all | bytes 2097152 | tf_op jit(solution)/shard_map/all_to_all | solution.py:205
  194.5 0.1 convert_reduce_fusion
  194.7 0.8 add_convert_fusion.2
  (29 shorter events, 0.1 us)
Async XLA Ops:
  6.5 40.0 %copy-start.7 = (bf16[256]{0:T(256)(128)(2,1)S(1)}, bf16[256]{0:T(256)(128)(2,1)}, u32[]{:S(2)}) copy-start(bf16[256]{0:T(256)(128)(2,1)} %param.16) | copy-start | bytes 1540
  6.5 40.0 %copy-start.8 = (bf16[256]{0:T(256)(128)(2,1)S(1)}, bf16[256]{0:T(256)(128)(2,1)}, u32[]{:S(2)}) copy-start(bf16[256]{0:T(256)(128)(2,1)} %param.24) | copy-start | bytes 1540
  6.5 40.0 %copy-start.5 = (bf16[512,256]{1,0:T(8,128)(2,1)S(1)}, bf16[512,256]{1,0:T(8,128)(2,1)}, u32[]{:S(2)}) copy-start(bf16[512,256]{1,0:T(8,128)(2,1)} %param.15) | copy-start | bytes 786436
  6.5 38.2 %all-gather.6.cloned.1.call-start = ((), (), s32[]{:S(2)}) async-start(), calls=%async_computation.6 | async-start | bytes 1474560 | tf_op jit(solution)/shard_map/all_gather | solution.py:238
  9.6 36.9 %all-to-all-start = ((bf16[4,32,768]{2,1,0:T(8,128)(2,1)}), bf16[4,32,768]{2,1,0:T(8,128)(2,1)S(1)}, u32[]{:S(2)}, u32[]{:S(2)}) async-start(bf16[4,32,768]{2,1,0:T(8,128)(2,1)} %broadcast_in_dim.23), calls=%async_computation | async-start | bytes 393216 | tf_op jit(solution)/shard_map/all_to_all | solution.py:30
  25.2 139.8 %all-gather.4.cloned.1.call-start = ((), (), s32[]{:S(2)}) async-start(), calls=%async_computation.5 | async-start | bytes 6684672 | tf_op jit(solution)/shard_map/all_gather | solution.py:239
  46.5 26.7 %copy-start.4 = (bf16[4,32,768]{2,1,0:T(8,128)(2,1)}, bf16[4,32,768]{2,1,0:T(8,128)(2,1)S(1)}, u32[]{:S(2)}) copy-start(bf16[4,32,768]{2,1,0:T(8,128)(2,1)S(1)} %all-to-all-done) | copy-start | bytes 589828
  46.6 15.4 %collective-permute-start = (bf16[528,256]{1,0:T(8,128)(2,1)S(1)}, bf16[528,256]{1,0:T(8,128)(2,1)S(1)}, u32[]{:S(2)}, u32[]{:S(2)}) collective-permute-start(bf16[528,256]{1,0:T(8,128)(2,1)S(1)} %get-tuple-element.26), channel_id=1, source_target_pairs={{0,1},{1,0},{2,3},{3,2},{4,5},{5,4},{6,7},{7,6},{8,9},{9,8},{10,11... | collective-permute-start | bytes 811016 | tf_op jit(solution)/shard_map/ppermute | solution.py:34
  51.3 17.6 %collective-permute-start.4 = (bf16[128,768]{1,0:T(8,128)(2,1)S(1)}, bf16[128,768]{1,0:T(8,128)(2,1)S(1)}, u32[]{:S(2)}, u32[]{:S(2)}) collective-permute-start(bf16[128,768]{1,0:T(8,128)(2,1)S(1)} %bitcast.12), channel_id=1, source_target_pairs={{0,64},{32,96},{64,128},{96,160},{128,192},{160,224},{192,256},{22... | collective-permute-start | bytes 589832 | tf_op jit(solution)/shard_map/ppermute | solution.py:44
  55.5 17.7 %collective-permute-start.5 = (bf16[128,768]{1,0:T(8,128)(2,1)S(1)}, bf16[128,768]{1,0:T(8,128)(2,1)S(1)}, u32[]{:S(2)}, u32[]{:S(2)}) collective-permute-start(bf16[128,768]{1,0:T(8,128)(2,1)S(1)} %bitcast.13), channel_id=1, source_target_pairs={{0,32},{32,64},{64,96},{96,128},{128,160},{160,192},{192,224},{224... | collective-permute-start | bytes 589832 | tf_op jit(solution)/shard_map/ppermute | solution.py:44
  58.7 14.5 %collective-permute-start.6 = (bf16[128,768]{1,0:T(8,128)(2,1)S(1)}, bf16[128,768]{1,0:T(8,128)(2,1)S(1)}, u32[]{:S(2)}, u32[]{:S(2)}) collective-permute-start(bf16[128,768]{1,0:T(8,128)(2,1)S(1)} %bitcast.14), channel_id=1, source_target_pairs={{0,480},{32,0},{64,32},{96,64},{128,96},{160,128},{192,160},{224,1... | collective-permute-start | bytes 589832 | tf_op jit(solution)/shard_map/ppermute | solution.py:44
  62.1 17.2 %collective-permute-start.1 = (bf16[2,528,256]{2,1,0:T(8,128)(2,1)S(1)}, bf16[2,528,256]{2,1,0:T(8,128)(2,1)S(1)}, u32[]{:S(2)}, u32[]{:S(2)}) collective-permute-start(bf16[2,528,256]{2,1,0:T(8,128)(2,1)S(1)} %pad_maximum_fusion.1.p0), channel_id=1, source_target_pairs={{0,4},{2,6},{4,0},{6,2},{1,5},{3,7},{5,1},{7,3},{8,12},{10,14},{12... | collective-permute-start | bytes 1622024 | tf_op jit(solution)/shard_map/ppermute | solution.py:44
  66.7 24.7 %collective-permute-start.2 = (bf16[2,528,256]{2,1,0:T(8,128)(2,1)S(1)}, bf16[2,528,256]{2,1,0:T(8,128)(2,1)S(1)}, u32[]{:S(2)}, u32[]{:S(2)}) collective-permute-start(bf16[2,528,256]{2,1,0:T(8,128)(2,1)S(1)} %pad_maximum_fusion.1.p0), channel_id=1, source_target_pairs={{0,2},{2,4},{4,6},{6,0},{1,3},{3,5},{5,7},{7,1},{8,10},{10,12},{12... | collective-permute-start | bytes 1622024 | tf_op jit(solution)/shard_map/ppermute | solution.py:44
  68.9 26.4 %collective-permute-start.3 = (bf16[2,528,256]{2,1,0:T(8,128)(2,1)S(1)}, bf16[2,528,256]{2,1,0:T(8,128)(2,1)S(1)}, u32[]{:S(2)}, u32[]{:S(2)}) collective-permute-start(bf16[2,528,256]{2,1,0:T(8,128)(2,1)S(1)} %pad_maximum_fusion.1.p0), channel_id=1, source_target_pairs={{0,6},{2,0},{4,2},{6,4},{1,7},{3,1},{5,3},{7,5},{8,14},{10,8},{12,... | collective-permute-start | bytes 1622024 | tf_op jit(solution)/shard_map/ppermute | solution.py:44
  73.4 23.9 %collective-permute-start.7 = (bf16[512,512]{1,0:T(8,128)(2,1)S(1)}, bf16[512,512]{1,0:T(8,128)(2,1)S(1)}, u32[]{:S(2)}, u32[]{:S(2)}) collective-permute-start(bf16[512,512]{1,0:T(8,128)(2,1)S(1)} %slice.12.p0), channel_id=1, source_target_pairs={{0,16},{8,24},{16,0},{24,8},{1,17},{9,25},{17,1},{25,9},{2,18},{10... | collective-permute-start | bytes 1572872 | tf_op jit(solution)/shard_map/ppermute | solution.py:44
  77.3 26.6 %collective-permute-start.8 = (bf16[512,512]{1,0:T(8,128)(2,1)S(1)}, bf16[512,512]{1,0:T(8,128)(2,1)}, u32[]{:S(2)}, u32[]{:S(2)}) collective-permute-start(bf16[512,512]{1,0:T(8,128)(2,1)S(1)} %slice.12.p0), channel_id=1, source_target_pairs={{0,8},{8,16},{16,24},{24,0},{1,9},{9,17},{17,25},{25,1},{2,10},{10... | collective-permute-start | bytes 1572872 | tf_op jit(solution)/shard_map/ppermute | solution.py:44
  79.3 24.7 %collective-permute-start.9 = (bf16[512,512]{1,0:T(8,128)(2,1)S(1)}, bf16[512,512]{1,0:T(8,128)(2,1)}, u32[]{:S(2)}, u32[]{:S(2)}) collective-permute-start(bf16[512,512]{1,0:T(8,128)(2,1)S(1)} %slice.12.p0), channel_id=1, source_target_pairs={{0,24},{8,0},{16,8},{24,16},{1,25},{9,1},{17,9},{25,17},{2,26},{10... | collective-permute-start | bytes 1572872 | tf_op jit(solution)/shard_map/ppermute | solution.py:44
  91.4 21.2 %collective-permute-start.10 = (bf16[512,256]{1,0:T(8,128)(2,1)S(1)}, bf16[512,256]{1,0:T(8,128)(2,1)}, u32[]{:S(2)}, u32[]{:S(2)}) collective-permute-start(bf16[512,256]{1,0:T(8,128)(2,1)S(1)} %pad_maximum_fusion.3.p0), channel_id=1, source_target_pairs={{0,16},{8,24},{16,0},{24,8},{1,17},{9,25},{17,1},{25,9},{2,18},{10... | collective-permute-start | bytes 786440 | tf_op jit(solution)/shard_map/ppermute | solution.py:44
  95.3 17.8 %collective-permute-start.11 = (bf16[512,256]{1,0:T(8,128)(2,1)S(1)}, bf16[512,256]{1,0:T(8,128)(2,1)}, u32[]{:S(2)}, u32[]{:S(2)}) collective-permute-start(bf16[512,256]{1,0:T(8,128)(2,1)S(1)} %pad_maximum_fusion.3.p0), channel_id=1, source_target_pairs={{0,8},{8,16},{16,24},{24,0},{1,9},{9,17},{17,25},{25,1},{2,10},{10... | collective-permute-start | bytes 786440 | tf_op jit(solution)/shard_map/ppermute | solution.py:44
  97.3 15.9 %collective-permute-start.12 = (bf16[512,256]{1,0:T(8,128)(2,1)S(1)}, bf16[512,256]{1,0:T(8,128)(2,1)}, u32[]{:S(2)}, u32[]{:S(2)}) collective-permute-start(bf16[512,256]{1,0:T(8,128)(2,1)S(1)} %pad_maximum_fusion.3.p0), channel_id=1, source_target_pairs={{0,24},{8,0},{16,8},{24,16},{1,25},{9,1},{17,9},{25,17},{2,26},{10... | collective-permute-start | bytes 786440 | tf_op jit(solution)/shard_map/ppermute | solution.py:44
  104.0 8.6 %copy-start.9 = (bf16[256]{0:T(256)(128)(2,1)S(1)}, bf16[256]{0:T(256)(128)(2,1)}, u32[]{:S(2)}) copy-start(bf16[256]{0:T(256)(128)(2,1)} %param.19) | copy-start | bytes 1540
  104.0 8.6 %copy-start.10 = (bf16[256]{0:T(256)(128)(2,1)S(1)}, bf16[256]{0:T(256)(128)(2,1)}, u32[]{:S(2)}) copy-start(bf16[256]{0:T(256)(128)(2,1)} %param.20) | copy-start | bytes 1540
  104.0 13.4 %copy-start = (bf16[2,128,128]{2,1,0:T(8,128)(2,1)S(1)}, bf16[2,128,128]{2,1,0:T(8,128)(2,1)}, u32[]{:S(2)}) copy-start(bf16[2,128,128]{2,1,0:T(8,128)(2,1)} %mix.3) | copy-start | bytes 196612
  104.0 13.4 %copy-start.3 = (bf16[2,128]{1,0:T(2,128)(2,1)S(1)}, bf16[2,128]{1,0:T(2,128)(2,1)}, u32[]{:S(2)}) copy-start(bf16[2,128]{1,0:T(2,128)(2,1)} %bias.1) | copy-start | bytes 1540
  107.5 9.8 %all-to-all-start.1 = ((f32[8,2,512]{2,1,0:T(2,128)}), f32[8,2,512]{2,1,0:T(2,128)S(1)}, u32[]{:S(2)}, u32[]{:S(2)}) async-start(f32[8,2,512]{2,1,0:T(2,128)} %broadcast_in_dim.24), calls=%async_computation.1 | async-start | bytes 65536 | tf_op jit(solution)/shard_map/all_to_all | solution.py:30
  119.5 4.9 %collective-permute-start.13 = (bf16[4,512,256]{2,1,0:T(8,128)(2,1)S(1)}, bf16[4,512,256]{2,1,0:T(8,128)(2,1)S(1)}, u32[]{:S(2)}, u32[]{:S(2)}) collective-permute-start(bf16[4,512,256]{2,1,0:T(8,128)(2,1)S(1)} %get-tuple-element.20), channel_id=1, source_target_pairs={{0,1},{1,0},{2,3},{3,2},{4,5},{5,4},{6,7},{7,6},{8,9},{9,8},{10,11... | collective-permute-start | bytes 3145736 | tf_op jit(solution)/shard_map/ppermute | solution.py:34
  124.6 17.5 %copy-start.6 = (bf16[512,256]{1,0:T(8,128)(2,1)S(1)}, bf16[512,256]{1,0:T(8,128)(2,1)}, u32[]{:S(2)}) copy-start(bf16[512,256]{1,0:T(8,128)(2,1)} %param.15) | copy-start | bytes 786436
  142.2 22.8 %copy-start.1 = (bf16[3,512]{1,0:T(4,128)(2,1)S(1)}, bf16[3,512]{1,0:T(4,128)(2,1)}, u32[]{:S(2)}) copy-start(bf16[3,512]{1,0:T(4,128)(2,1)} %conv_gate.1) | copy-start | bytes 9220
  142.2 22.8 %copy-start.2 = (bf16[3,512]{1,0:T(4,128)(2,1)S(1)}, bf16[3,512]{1,0:T(4,128)(2,1)}, u32[]{:S(2)}) copy-start(bf16[3,512]{1,0:T(4,128)(2,1)} %conv_value.1) | copy-start | bytes 9220
  158.7 6.3 %collective-permute-start.14 = (bf16[4,512,256]{2,1,0:T(8,128)(2,1)S(1)}, bf16[4,512,256]{2,1,0:T(8,128)(2,1)S(1)}, u32[]{:S(2)}, u32[]{:S(2)}) collective-permute-start(bf16[4,512,256]{2,1,0:T(8,128)(2,1)S(1)} %all_to_all.26.mine), channel_id=1, source_target_pairs={{0,1},{1,0},{2,3},{3,2},{4,5},{5,4},{6,7},{7,6},{8,9},{9,8},{10,11... | collective-permute-start | bytes 3145736 | tf_op jit(solution)/shard_map/ppermute | solution.py:34
  172.4 4.6 %collective-permute-start.15 = (bf16[4,512,256]{2,1,0:T(8,128)(2,1)S(1)}, bf16[4,512,256]{2,1,0:T(8,128)(2,1)S(1)}, u32[]{:S(2)}, u32[]{:S(2)}) collective-permute-start(bf16[4,512,256]{2,1,0:T(8,128)(2,1)S(1)} %get-tuple-element.24), channel_id=1, source_target_pairs={{0,1},{1,0},{2,3},{3,2},{4,5},{5,4},{6,7},{7,6},{8,9},{9,8},{10,11... | collective-permute-start | bytes 3145736 | tf_op jit(solution)/shard_map/ppermute | solution.py:34
Sparse Core Ops, SparseCore 0:
  9.4 35.2 all-gather.5
  46.8 86.6 all-gather.3

commit v9 on v8

--- a/solution.py
+++ b/solution.py
@@ -82,14 +82,12 @@
                 weight[pl.ds(start, PIECE), :] = part[came : came + PIECE, :]
 
 
-def first_kernel(place, normed, p0, p1, p2, p3, act_u, act_v, sums, weight):
-    width = act_u.shape[1]
+def first_kernel(place, normed, p0, p1, p2, p3, act_v, sums, weight):
+    width = act_v.shape[1]
     fill_rows(weight, (p0, p1, p2, p3), place[2], place[3])
     for part in range(normed.shape[0] // SEQ_LEN):
         rows = pl.ds(part * SEQ_LEN, SEQ_LEN)
-        both = gelu(jnp.dot(normed[rows, :], weight[...], preferred_element_type=F32))
-        act_u[rows, :] = both[:, :width]
-        value = both[:, width:]
+        value = gelu(jnp.dot(normed[rows, :], weight[...], preferred_element_type=F32))
         act_v[rows, :] = value
         once = sum(value[:, k : k + 128] for k in range(0, width, 128))
         twice = sum(value[:, k : k + 128] * value[:, k : k + 128] for k in range(0, width, 128))
@@ -97,9 +95,12 @@
         sums[1:2, rows] = jnp.sum(twice.T, axis=0, keepdims=True)
 
 
-def mix_kernel(place, act_v, act_u, stats, gain, shift, mix, bias, p0, p1, p2, p3, give, keep, weight, gated):
+def mix_kernel(place, normed, act_v, stats, gain, shift, mix, bias, p0, p1, p2, p3, give, keep, weight, act_u, gated):
     width = act_v.shape[1]
     fill_rows(weight, (p0, p1, p2, p3), place[2], place[3])
+    for part in range(normed.shape[0] // SEQ_LEN):
+        rows = pl.ds(part * SEQ_LEN, SEQ_LEN)
+        act_u[rows, :] = gelu(jnp.dot(normed[rows, :], weight[:, :width], preferred_element_type=F32))
     full = width * stats.shape[0]
     i = lax.broadcasted_iota(jnp.int32, (BLOCK, BLOCK), 0)
     j = lax.broadcasted_iota(jnp.int32, (BLOCK, BLOCK), 1)
@@ -126,7 +127,7 @@
     for out, side in ((give, 1 - c), (keep, c)):
         for x in range(out.shape[0]):
             start = pl.multiple_of((2 * x + side) * width, width)
-            columns = weight[pl.ds(start, width), :]
+            columns = weight[pl.ds(start, width), width : 2 * width]
             out[x] = lax.dot_general(
                 gated[...], columns, (((1,), (1,)), ((), ())), preferred_element_type=F32
             ).astype(BF16)
@@ -150,9 +151,10 @@
         pltpu.make_async_copy(late_hbm.at[:, pl.ds(k * ff, ff)], late.at[:, pl.ds(k * ff, ff)], done.at[k])
         for k in range(3)
     ]
-    for copy in copies:
-        copy.start()
+    copies[0].start()
     for part in range(mine.shape[1] // BLOCK):
+        if part == 3:
+            copies[1].start()
         rows = pl.ds(part * BLOCK, BLOCK)
         squares = jnp.zeros((BLOCK, width), F32)
         for ref in (mine, other):
@@ -173,6 +175,7 @@
             copies[0].wait()
         gate = jnp.dot(normed[rows, :], late[:, 0:ff], preferred_element_type=F32)
         if part == 0:
+            copies[2].start()
             copies[1].wait()
         value = jnp.dot(normed[rows, :], late[:, ff : 2 * ff], preferred_element_type=F32)
         conv_g = taps(gate, conv_gate[...].astype(F32))
@@ -227,11 +230,12 @@
     ff = ffn_gate.shape[1]
     row_count = tokens.shape[0]
 
-    early = jnp.concatenate([proj_u, proj_v, proj_out.T], axis=1)
+    early = jnp.concatenate([proj_v, proj_u, proj_out.T], axis=1)
     early_far = everyones(early, "zh").reshape(-1, early.shape[1])
     early_z = jnp.concatenate(round_ring(early_far, Z), axis=0)
-    early_parts = round_ring(early_z[:, : 2 * da], "y")
-    out_parts = round_ring(early_z[:, 2 * da :], "y")
+    early_v, early_rest = lax.optimization_barrier((early_z[:, :da], early_z[:, da:]))
+    early_parts = round_ring(early_v, "y")
+    out_parts = round_ring(early_rest, "y")
 
     late = jnp.concatenate([ffn_gate, ffn_value, proj_down.T], axis=1)
     padded = jnp.pad(late, ((0, 2 * late.shape[0]), (0, 0)))
@@ -253,12 +257,12 @@
         compiler_params=room(12),
     )(place, *token_parts)
 
-    act_u, act_v, sums = pl.pallas_call(
+    act_v, sums = pl.pallas_call(
         first_kernel,
         in_specs=[SMEM] + [VMEM] * 5,
-        out_specs=[VMEM] * 3,
-        out_shape=[shape((row_count, da), F32)] * 2 + [shape((2, row_count), F32)],
-        scratch_shapes=[pltpu.VMEM((model, 2 * da), BF16)],
+        out_specs=[VMEM] * 2,
+        out_shape=[shape((row_count, da), F32), shape((2, row_count), F32)],
+        scratch_shapes=[pltpu.VMEM((model, da), BF16)],
         name="first",
         compiler_params=room(14),
     )(place, normed, *early_parts)
@@ -269,13 +273,17 @@
         in_specs=[SMEM] + [VMEM] * 11,
         out_specs=[VMEM] * 2,
         out_shape=blocks,
-        scratch_shapes=[pltpu.VMEM((model, da), BF16), pltpu.VMEM((row_count, da), BF16)],
+        scratch_shapes=[
+            pltpu.VMEM((model, 2 * da), BF16),
+            pltpu.VMEM((row_count, da), F32),
+            pltpu.VMEM((row_count, da), BF16),
+        ],
         name="mix",
         compiler_params=room(16),
     )(
         place,
+        normed,
         act_v,
-        act_u,
         stats,
         layer_gain[None],
         layer_shift[None],

time: 203 us -> 224 us (1.10)
  waiting for transfers between devices: 38.2 us -> 54.5 us
  local copies, waits for them, and re-layouts: 3.27 us -> 9.48 us
    ppermute x12, waiting for transfers between devices: 7.71 us -> 22.2 us  [round_ring(): lax.ppermute(shard, axis, [(i, (i + step) % size) for i in range(size)])]
    unnamed x22 -> x36, local copies, waits for them, and re-layouts: 0.05 us -> 6.31 us
  transfers between devices with their start and end apart: 20 -> 20, of which waited for: 8 -> 9; matrix products, arithmetic and copies ran while one was open for 3% -> 2% of each run, Pallas kernels for 3% -> 3%
where the time goes in v9:
time: 224 us; the launch traced here: 222 us
  starting transfers between devices  75.1 us (34%)
  waiting for transfers between devices  54.5 us (24%)
  blocking collectives  51 us (23%)
  Pallas kernels  14 us (6%)
  between operations  13.8 us (6%)
  local copies, waits for them, and re-layouts  9.48 us (4%)
  other arithmetic  4.21 us (2%)
    ppermute x12, starting transfers between devices, round_ring(): lax.ppermute(shard, axis, [(i, (i + step) % size) for i in range(size)])  41.5 us
    all_to_all x2, blocking collectives, summed_at_owner(): arrived = lax.all_to_all(pair, 'x', split_axis=0, concat_axis=0, tiled=True)  34.6 us
    ppermute x12, waiting for transfers between devices, round_ring(): lax.ppermute(shard, axis, [(i, (i + step) % size) for i in range(size)])  22.2 us
    all_to_all x2, starting transfers between devices, everyones(): return lax.all_to_all(copies, axis, split_axis=0, concat_axis=0, tiled=True)  20 us
    all_gather x1, waiting for transfers between devices, on_device(): lax.all_gather(padded, 'y', axis=0)[:, :late.shape[0]]  19.5 us
    all_to_all x1, blocking collectives, everyones(): return lax.all_to_all(copies, axis, split_axis=0, concat_axis=0, tiled=True)  16.4 us
    ppermute x4, starting transfers between devices, other_core(): return lax.ppermute(value, 'c', SWAP)  13.6 us
    ppermute x4, waiting for transfers between devices, other_core(): return lax.ppermute(value, 'c', SWAP)  7.95 us
  transfers between devices with their start and end apart: 20, of which 9 were waited for; matrix products, arithmetic and copies ran while one was open for 2% of the time, Pallas kernels for 3%

profile of v9, /device:TPU:1, one launch (start us, length us, event | category | flops | bytes accessed | tf_op | source)
XLA Modules:
  0.0 222.1 jit_solution(4913182664264858112)
XLA Ops:
  6.5 1.6 fusion.4
  8.1 0.0 all-gather.6.cloned.1.call-update
  8.1 0.8 pad_maximum_fusion.6
  8.9 0.7 broadcast_in_dim.23
  9.6 15.6 %all-to-all-start = ((bf16[4,32,768]{2,1,0:T(8,128)(2,1)}), bf16[4,32,768]{2,1,0:T(8,128)(2,1)S(1)}, u32[]{:S(2)}, u32[]{:S(2)}) async-start(bf16[4,32,768]{2,1,0:T(8,128)(2,1)} %broadcast_in_dim.23), calls=%async_computation | async-start | bytes 393216 | tf_op jit(solution)/shard_map/all_to_all | solution.py:30
  25.2 19.5 %all-gather.6.cloned.1.call-done = bf16[384,1536]{1,0:T(8,128)(2,1)} async-done(((bf16[96,1536]{1,0:T(8,128)(2,1)}), bf16[384,1536]{1,0:T(8,128)(2,1)}) %all-gather.6.cloned.1.call-update) | async-done | bytes 1179664 | tf_op jit(solution)/shard_map/all_gather | solution.py:242
  44.7 1.8 slice.12
  46.5 0.0 all-gather.4.cloned.1.call-update
  46.6 4.7 %collective-permute-start = (bf16[528,256]{1,0:T(8,128)(2,1)S(1)}, bf16[528,256]{1,0:T(8,128)(2,1)S(1)}, u32[]{:S(2)}, u32[]{:S(2)}) collective-permute-start(bf16[528,256]{1,0:T(8,128)(2,1)S(1)} %get-tuple-element.28), channel_id=1, source_target_pairs={{0,1},{1,0},{2,3},{3,2},{4,5},{5,4},{6,7},{7,6},{8,9},{9,8},{10,11... | collective-permute-start | bytes 811016 | tf_op jit(solution)/shard_map/ppermute | solution.py:34
  51.3 1.2 collective-permute-done
  52.5 0.1 pad_maximum_fusion.p0
  52.5 4.6 %collective-permute-start.1 = (bf16[2,528,256]{2,1,0:T(8,128)(2,1)S(1)}, bf16[2,528,256]{2,1,0:T(8,128)(2,1)S(1)}, u32[]{:S(2)}, u32[]{:S(2)}) collective-permute-start(bf16[2,528,256]{2,1,0:T(8,128)(2,1)S(1)} %pad_maximum_fusion.p0), channel_id=1, source_target_pairs={{0,4},{2,6},{4,0},{6,2},{1,5},{3,7},{5,1},{7,3},{8,12},{10,14},{12... | collective-permute-start | bytes 1622024 | tf_op jit(solution)/shard_map/ppermute | solution.py:44
  57.1 2.2 collective-permute-start.2
  59.3 4.2 %collective-permute-start.4 = (bf16[128,768]{1,0:T(8,128)(2,1)S(1)}, bf16[128,768]{1,0:T(8,128)(2,1)S(1)}, u32[]{:S(2)}, u32[]{:S(2)}) collective-permute-start(bf16[128,768]{1,0:T(8,128)(2,1)S(1)} %bitcast.12), channel_id=1, source_target_pairs={{0,64},{32,96},{64,128},{96,160},{128,192},{160,224},{192,256},{22... | collective-permute-start | bytes 589832 | tf_op jit(solution)/shard_map/ppermute | solution.py:44
  63.5 3.2 %collective-permute-start.5 = (bf16[128,768]{1,0:T(8,128)(2,1)S(1)}, bf16[128,768]{1,0:T(8,128)(2,1)S(1)}, u32[]{:S(2)}, u32[]{:S(2)}) collective-permute-start(bf16[128,768]{1,0:T(8,128)(2,1)S(1)} %bitcast.13), channel_id=1, source_target_pairs={{0,32},{32,64},{64,96},{96,128},{128,160},{160,192},{192,224},{224... | collective-permute-start | bytes 589832 | tf_op jit(solution)/shard_map/ppermute | solution.py:44
  66.7 3.3 %collective-permute-start.6 = (bf16[128,768]{1,0:T(8,128)(2,1)S(1)}, bf16[128,768]{1,0:T(8,128)(2,1)S(1)}, u32[]{:S(2)}, u32[]{:S(2)}) collective-permute-start(bf16[128,768]{1,0:T(8,128)(2,1)S(1)} %bitcast.14), channel_id=1, source_target_pairs={{0,480},{32,0},{64,32},{96,64},{128,96},{160,128},{192,160},{224,1... | collective-permute-start | bytes 589832 | tf_op jit(solution)/shard_map/ppermute | solution.py:44
  70.0 1.1 collective-permute-done.4
  71.2 4.3 %collective-permute-start.3 = (bf16[2,528,256]{2,1,0:T(8,128)(2,1)S(1)}, bf16[2,528,256]{2,1,0:T(8,128)(2,1)S(1)}, u32[]{:S(2)}, u32[]{:S(2)}) collective-permute-start(bf16[2,528,256]{2,1,0:T(8,128)(2,1)S(1)} %pad_maximum_fusion.p0), channel_id=1, source_target_pairs={{0,6},{2,0},{4,2},{6,4},{1,7},{3,1},{5,3},{7,5},{8,14},{10,8},{12,... | collective-permute-start | bytes 1622024 | tf_op jit(solution)/shard_map/ppermute | solution.py:44
  75.5 8.4 %collective-permute-done.5 = bf16[128,768]{1,0:T(8,128)(2,1)S(1)} collective-permute-done((bf16[128,768]{1,0:T(8,128)(2,1)S(1)}, bf16[128,768]{1,0:T(8,128)(2,1)S(1)}, u32[]{:S(2)}, u32[]{:S(2)}) %collective-permute-start.5) | collective-permute-done | bytes 196640 | tf_op jit(solution)/shard_map/ppermute | solution.py:44
  83.9 3.9 %collective-permute-start.7 = (bf16[512,256]{1,0:T(8,128)(2,1)S(1)}, bf16[512,256]{1,0:T(8,128)(2,1)S(1)}, u32[]{:S(2)}, u32[]{:S(2)}) collective-permute-start(bf16[512,256]{1,0:T(8,128)(2,1)S(1)} %pad_maximum_fusion.5.p0), channel_id=1, source_target_pairs={{0,16},{8,24},{16,0},{24,8},{1,17},{9,25},{17,1},{25,9},{2,18},{10... | collective-permute-start | bytes 786440 | tf_op jit(solution)/shard_map/ppermute | solution.py:44
  87.8 2.9 %collective-permute-start.10 = (bf16[512,512]{1,0:T(8,128)(2,1)S(1)}, bf16[512,512]{1,0:T(8,128)(2,1)}, u32[]{:S(2)}, u32[]{:S(2)}) collective-permute-start(bf16[512,512]{1,0:T(8,128)(2,1)S(1)} %pad_maximum_fusion.1.p0), channel_id=1, source_target_pairs={{0,16},{8,24},{16,0},{24,8},{1,17},{9,25},{17,1},{25,9},{2,18},{10... | collective-permute-start | bytes 1572872 | tf_op jit(solution)/shard_map/ppermute | solution.py:44
  90.7 0.8 copy-done
  91.5 1.9 collective-permute-start.11
  93.5 0.8 copy-done.2
  94.2 4.6 %collective-permute-start.12 = (bf16[512,512]{1,0:T(8,128)(2,1)S(1)}, bf16[512,512]{1,0:T(8,128)(2,1)}, u32[]{:S(2)}, u32[]{:S(2)}) collective-permute-start(bf16[512,512]{1,0:T(8,128)(2,1)S(1)} %pad_maximum_fusion.1.p0), channel_id=1, source_target_pairs={{0,24},{8,0},{16,8},{24,16},{1,25},{9,1},{17,9},{25,17},{2,26},{10... | collective-permute-start | bytes 1572872 | tf_op jit(solution)/shard_map/ppermute | solution.py:44
  98.8 0.8 copy-done.4
  99.7 1.9 collective-permute-start.8
  101.6 0.0 copy-start.6
  101.6 0.7 copy-done.6
  102.3 4.6 %collective-permute-start.9 = (bf16[512,256]{1,0:T(8,128)(2,1)S(1)}, bf16[512,256]{1,0:T(8,128)(2,1)}, u32[]{:S(2)}, u32[]{:S(2)}) collective-permute-start(bf16[512,256]{1,0:T(8,128)(2,1)S(1)} %pad_maximum_fusion.5.p0), channel_id=1, source_target_pairs={{0,24},{8,0},{16,8},{24,16},{1,25},{9,1},{17,9},{25,17},{2,26},{10... | collective-permute-start | bytes 786440 | tf_op jit(solution)/shard_map/ppermute | solution.py:44
  106.9 0.1 pad_add_fusion.place
  106.9 1.1 copy-done.1
  108.0 1.1 copy-done.3
  109.1 1.0 copy-done.5
  110.1 1.6 norm.1
  111.7 0.0 copy-start.16
  111.7 0.0 copy-start.17
  111.7 0.0 copy-start.8
  111.7 0.0 copy-start.11
  111.7 12.7 %collective-permute-done.8.p2 = bf16[512,256]{1,0:T(8,128)(2,1)} collective-permute-done((bf16[512,256]{1,0:T(8,128)(2,1)S(1)}, bf16[512,256]{1,0:T(8,128)(2,1)}, u32[]{:S(2)}, u32[]{:S(2)}) %collective-permute-start.8) | collective-permute-done | bytes 262176 | tf_op jit(solution)/shard_map/ppermute | solution.py:44
  124.4 2.0 first.1
  126.4 0.6 broadcast_in_dim.24
  127.1 4.4 %all-to-all-start.1 = ((f32[8,2,512]{2,1,0:T(2,128)}), f32[8,2,512]{2,1,0:T(2,128)S(1)}, u32[]{:S(2)}, u32[]{:S(2)}) async-start(f32[8,2,512]{2,1,0:T(2,128)} %broadcast_in_dim.24), calls=%async_computation.1 | async-start | bytes 65536 | tf_op jit(solution)/shard_map/all_to_all | solution.py:30
  131.5 4.7 %all-to-all-done.1.stats = f32[8,2,512]{2,1,0:T(2,128)S(1)} async-done(((f32[8,2,512]{2,1,0:T(2,128)}), f32[8,2,512]{2,1,0:T(2,128)S(1)}, u32[]{:S(2)}, u32[]{:S(2)}) %all-to-all-start.1) | async-done | bytes 32800 | tf_op jit(solution)/shard_map/all_to_all | solution.py:30
  136.3 3.0 %mix.2 = (bf16[4,512,256]{2,1,0:T(8,128)(2,1)S(1)}, bf16[4,512,256]{2,1,0:T(8,128)(2,1)S(1)}) custom-call(s32[4]{0:T(128)S(1)} %pad_add_fusion.place, bf16[512,2048]{1,0:T(8,128)(2,1)S(1)} %get-tuple-element.16.normed, f32[512,256]{1,0:T(8,128)S(1)} %get-tuple-element.18.act_v, f32[8,2,512]{2,1,0:T(2,128)S(1)} %all-to-all-done.1.stats, ...), custom_call_target="tpu_custom_call" | custom-call | tf_op jit(solution)/shard_map/mix/pallas_call | solution.py:271
  139.3 2.6 %collective-permute-start.13 = (bf16[4,512,256]{2,1,0:T(8,128)(2,1)S(1)}, bf16[4,512,256]{2,1,0:T(8,128)(2,1)S(1)}, u32[]{:S(2)}, u32[]{:S(2)}) collective-permute-start(bf16[4,512,256]{2,1,0:T(8,128)(2,1)S(1)} %get-tuple-element.22), channel_id=1, source_target_pairs={{0,1},{1,0},{2,3},{3,2},{4,5},{5,4},{6,7},{7,6},{8,9},{9,8},{10,11... | collective-permute-start | bytes 3145736 | tf_op jit(solution)/shard_map/ppermute | solution.py:34
  141.9 2.3 %collective-permute-done.13 = bf16[4,512,256]{2,1,0:T(8,128)(2,1)S(1)} collective-permute-done((bf16[4,512,256]{2,1,0:T(8,128)(2,1)S(1)}, bf16[4,512,256]{2,1,0:T(8,128)(2,1)S(1)}, u32[]{:S(2)}, u32[]{:S(2)}) %collective-permute-start.13) | collective-permute-done | bytes 1048608 | tf_op jit(solution)/shard_map/ppermute | solution.py:34
  144.2 0.3 add_convert_fusion.1
  144.4 0.0 copy-start.13
  144.5 17.4 %all_to_all.25 = bf16[4,512,256]{2,1,0:T(8,128)(2,1)S(1)} all-to-all(bf16[4,512,256]{2,1,0:T(8,128)(2,1)S(1)} %add_convert_fusion.1), channel_id=1, replica_groups=mesh['zh'=4,'zl'=4,'y'=4,'x'=4,'c'=2] {'x'}, dimensions={0} | all-to-all | bytes 2097152 | tf_op jit(solution)/shard_map/all_to_all | solution.py:208
  161.8 0.1 convert_reduce_fusion.1
  162.0 0.0 copy-start.9
  162.0 0.1 add_convert_fusion.3
  162.1 0.1 broadcast_in_dim.27
  162.2 16.4 %all_to_all.26.mine = bf16[4,512,256]{2,1,0:T(8,128)(2,1)S(1)} all-to-all(bf16[4,512,256]{2,1,0:T(8,128)(2,1)S(1)} %broadcast_in_dim.27), channel_id=1, replica_groups=mesh['zh'=4,'zl'=4,'y'=4,'x'=4,'c'=2] {'x'}, dimensions={0} | all-to-all | bytes 2097152 | tf_op jit(solution)/shard_map/all_to_all | solution.py:30
  178.5 4.0 %collective-permute-start.14 = (bf16[4,512,256]{2,1,0:T(8,128)(2,1)S(1)}, bf16[4,512,256]{2,1,0:T(8,128)(2,1)S(1)}, u32[]{:S(2)}, u32[]{:S(2)}) collective-permute-start(bf16[4,512,256]{2,1,0:T(8,128)(2,1)S(1)} %all_to_all.26.mine), channel_id=1, source_target_pairs={{0,1},{1,0},{2,3},{3,2},{4,5},{5,4},{6,7},{7,6},{8,9},{9,8},{10,11... | collective-permute-start | bytes 3145736 | tf_op jit(solution)/shard_map/ppermute | solution.py:34
  182.5 2.3 %collective-permute-done.14.other = bf16[4,512,256]{2,1,0:T(8,128)(2,1)S(1)} collective-permute-done((bf16[4,512,256]{2,1,0:T(8,128)(2,1)S(1)}, bf16[4,512,256]{2,1,0:T(8,128)(2,1)S(1)}, u32[]{:S(2)}, u32[]{:S(2)}) %collective-permute-start.14) | collective-permute-done | bytes 1048608 | tf_op jit(solution)/shard_map/ppermute | solution.py:34
  184.8 7.5 %ffn.1 = (bf16[4,512,256]{2,1,0:T(8,128)(2,1)S(1)}, bf16[4,512,256]{2,1,0:T(8,128)(2,1)S(1)}) custom-call(s32[4]{0:T(128)S(1)} %pad_add_fusion.place, bf16[4,512,256]{2,1,0:T(8,128)(2,1)S(1)} %all_to_all.26.mine, bf16[4,512,256]{2,1,0:T(8,128)(2,1)S(1)} %collective-permute-done.14.other, bf16[8,8,256]{2,1,0:T(8,128)(2,1)S(1)} %get-tuple-element.23.gain, ...), custom_call_target="tpu_custom_call" | custom-call | tf_op jit(solution)/shard_map/ffn/pallas_call | solution.py:296
  192.3 2.3 %collective-permute-start.15 = (bf16[4,512,256]{2,1,0:T(8,128)(2,1)S(1)}, bf16[4,512,256]{2,1,0:T(8,128)(2,1)S(1)}, u32[]{:S(2)}, u32[]{:S(2)}) collective-permute-start(bf16[4,512,256]{2,1,0:T(8,128)(2,1)S(1)} %get-tuple-element.26), channel_id=1, source_target_pairs={{0,1},{1,0},{2,3},{3,2},{4,5},{5,4},{6,7},{7,6},{8,9},{9,8},{10,11... | collective-permute-start | bytes 3145736 | tf_op jit(solution)/shard_map/ppermute | solution.py:34
  194.6 2.3 %collective-permute-done.15 = bf16[4,512,256]{2,1,0:T(8,128)(2,1)S(1)} collective-permute-done((bf16[4,512,256]{2,1,0:T(8,128)(2,1)S(1)}, bf16[4,512,256]{2,1,0:T(8,128)(2,1)S(1)}, u32[]{:S(2)}, u32[]{:S(2)}) %collective-permute-start.15) | collective-permute-done | bytes 1048608 | tf_op jit(solution)/shard_map/ppermute | solution.py:34
  196.8 0.3 add_convert_fusion
  197.1 17.2 %all_to_all.27 = bf16[4,512,256]{2,1,0:T(8,128)(2,1)S(1)} all-to-all(bf16[4,512,256]{2,1,0:T(8,128)(2,1)S(1)} %add_convert_fusion), channel_id=1, replica_groups=mesh['zh'=4,'zl'=4,'y'=4,'x'=4,'c'=2] {'x'}, dimensions={0} | all-to-all | bytes 2097152 | tf_op jit(solution)/shard_map/all_to_all | solution.py:208
  214.4 0.1 convert_reduce_fusion
  214.5 0.8 add_convert_fusion.2
  (42 shorter events, 0.2 us)
Async XLA Ops:
  6.5 40.0 %copy-start.14 = (bf16[256]{0:T(256)(128)(2,1)S(1)}, bf16[256]{0:T(256)(128)(2,1)}, u32[]{:S(2)}) copy-start(bf16[256]{0:T(256)(128)(2,1)} %param.16) | copy-start | bytes 1540
  6.5 40.0 %copy-start.15 = (bf16[256]{0:T(256)(128)(2,1)S(1)}, bf16[256]{0:T(256)(128)(2,1)}, u32[]{:S(2)}) copy-start(bf16[256]{0:T(256)(128)(2,1)} %param.24) | copy-start | bytes 1540
  6.5 40.0 %copy-start.12 = (bf16[512,256]{1,0:T(8,128)(2,1)S(1)}, bf16[512,256]{1,0:T(8,128)(2,1)}, u32[]{:S(2)}) copy-start(bf16[512,256]{1,0:T(8,128)(2,1)} %param.15) | copy-start | bytes 786436
  6.5 38.2 %all-gather.6.cloned.1.call-start = ((), (), s32[]{:S(2)}) async-start(), calls=%async_computation.6 | async-start | bytes 1474560 | tf_op jit(solution)/shard_map/all_gather | solution.py:242
  9.6 36.9 %all-to-all-start = ((bf16[4,32,768]{2,1,0:T(8,128)(2,1)}), bf16[4,32,768]{2,1,0:T(8,128)(2,1)S(1)}, u32[]{:S(2)}, u32[]{:S(2)}) async-start(bf16[4,32,768]{2,1,0:T(8,128)(2,1)} %broadcast_in_dim.23), calls=%async_computation | async-start | bytes 393216 | tf_op jit(solution)/shard_map/all_to_all | solution.py:30
  25.2 159.6 %all-gather.4.cloned.1.call-start = ((), (), s32[]{:S(2)}) async-start(), calls=%async_computation.5 | async-start | bytes 6684672 | tf_op jit(solution)/shard_map/all_gather | solution.py:243
  46.6 5.9 %collective-permute-start = (bf16[528,256]{1,0:T(8,128)(2,1)S(1)}, bf16[528,256]{1,0:T(8,128)(2,1)S(1)}, u32[]{:S(2)}, u32[]{:S(2)}) collective-permute-start(bf16[528,256]{1,0:T(8,128)(2,1)S(1)} %get-tuple-element.28), channel_id=1, source_target_pairs={{0,1},{1,0},{2,3},{3,2},{4,5},{5,4},{6,7},{7,6},{8,9},{9,8},{10,11... | collective-permute-start | bytes 811016 | tf_op jit(solution)/shard_map/ppermute | solution.py:34
  52.5 38.2 %collective-permute-start.1 = (bf16[2,528,256]{2,1,0:T(8,128)(2,1)S(1)}, bf16[2,528,256]{2,1,0:T(8,128)(2,1)S(1)}, u32[]{:S(2)}, u32[]{:S(2)}) collective-permute-start(bf16[2,528,256]{2,1,0:T(8,128)(2,1)S(1)} %pad_maximum_fusion.p0), channel_id=1, source_target_pairs={{0,4},{2,6},{4,0},{6,2},{1,5},{3,7},{5,1},{7,3},{8,12},{10,14},{12... | collective-permute-start | bytes 1622024 | tf_op jit(solution)/shard_map/ppermute | solution.py:44
  57.1 36.3 %collective-permute-start.2 = (bf16[2,528,256]{2,1,0:T(8,128)(2,1)S(1)}, bf16[2,528,256]{2,1,0:T(8,128)(2,1)S(1)}, u32[]{:S(2)}, u32[]{:S(2)}) collective-permute-start(bf16[2,528,256]{2,1,0:T(8,128)(2,1)S(1)} %pad_maximum_fusion.p0), channel_id=1, source_target_pairs={{0,2},{2,4},{4,6},{6,0},{1,3},{3,5},{5,7},{7,1},{8,10},{10,12},{12... | collective-permute-start | bytes 1622024 | tf_op jit(solution)/shard_map/ppermute | solution.py:44
  59.3 11.8 %collective-permute-start.4 = (bf16[128,768]{1,0:T(8,128)(2,1)S(1)}, bf16[128,768]{1,0:T(8,128)(2,1)S(1)}, u32[]{:S(2)}, u32[]{:S(2)}) collective-permute-start(bf16[128,768]{1,0:T(8,128)(2,1)S(1)} %bitcast.12), channel_id=1, source_target_pairs={{0,64},{32,96},{64,128},{96,160},{128,192},{160,224},{192,256},{22... | collective-permute-start | bytes 589832 | tf_op jit(solution)/shard_map/ppermute | solution.py:44
  63.5 20.3 %collective-permute-start.5 = (bf16[128,768]{1,0:T(8,128)(2,1)S(1)}, bf16[128,768]{1,0:T(8,128)(2,1)S(1)}, u32[]{:S(2)}, u32[]{:S(2)}) collective-permute-start(bf16[128,768]{1,0:T(8,128)(2,1)S(1)} %bitcast.13), channel_id=1, source_target_pairs={{0,32},{32,64},{64,96},{96,128},{128,160},{160,192},{192,224},{224... | collective-permute-start | bytes 589832 | tf_op jit(solution)/shard_map/ppermute | solution.py:44
  66.7 17.1 %collective-permute-start.6 = (bf16[128,768]{1,0:T(8,128)(2,1)S(1)}, bf16[128,768]{1,0:T(8,128)(2,1)S(1)}, u32[]{:S(2)}, u32[]{:S(2)}) collective-permute-start(bf16[128,768]{1,0:T(8,128)(2,1)S(1)} %bitcast.14), channel_id=1, source_target_pairs={{0,480},{32,0},{64,32},{96,64},{128,96},{160,128},{192,160},{224,1... | collective-permute-start | bytes 589832 | tf_op jit(solution)/shard_map/ppermute | solution.py:44
  71.2 27.7 %collective-permute-start.3 = (bf16[2,528,256]{2,1,0:T(8,128)(2,1)S(1)}, bf16[2,528,256]{2,1,0:T(8,128)(2,1)S(1)}, u32[]{:S(2)}, u32[]{:S(2)}) collective-permute-start(bf16[2,528,256]{2,1,0:T(8,128)(2,1)S(1)} %pad_maximum_fusion.p0), channel_id=1, source_target_pairs={{0,6},{2,0},{4,2},{6,4},{1,7},{3,1},{5,3},{7,5},{8,14},{10,8},{12,... | collective-permute-start | bytes 1622024 | tf_op jit(solution)/shard_map/ppermute | solution.py:44
  83.9 17.7 %collective-permute-start.7 = (bf16[512,256]{1,0:T(8,128)(2,1)S(1)}, bf16[512,256]{1,0:T(8,128)(2,1)S(1)}, u32[]{:S(2)}, u32[]{:S(2)}) collective-permute-start(bf16[512,256]{1,0:T(8,128)(2,1)S(1)} %pad_maximum_fusion.5.p0), channel_id=1, source_target_pairs={{0,16},{8,24},{16,0},{24,8},{1,17},{9,25},{17,1},{25,9},{2,18},{10... | collective-permute-start | bytes 786440 | tf_op jit(solution)/shard_map/ppermute | solution.py:44
  87.8 48.5 %collective-permute-start.10 = (bf16[512,512]{1,0:T(8,128)(2,1)S(1)}, bf16[512,512]{1,0:T(8,128)(2,1)}, u32[]{:S(2)}, u32[]{:S(2)}) collective-permute-start(bf16[512,512]{1,0:T(8,128)(2,1)S(1)} %pad_maximum_fusion.1.p0), channel_id=1, source_target_pairs={{0,16},{8,24},{16,0},{24,8},{1,17},{9,25},{17,1},{25,9},{2,18},{10... | collective-permute-start | bytes 1572872 | tf_op jit(solution)/shard_map/ppermute | solution.py:44
  90.7 0.8 copy-start
  91.5 44.8 %collective-permute-start.11 = (bf16[512,512]{1,0:T(8,128)(2,1)S(1)}, bf16[512,512]{1,0:T(8,128)(2,1)}, u32[]{:S(2)}, u32[]{:S(2)}) collective-permute-start(bf16[512,512]{1,0:T(8,128)(2,1)S(1)} %pad_maximum_fusion.1.p0), channel_id=1, source_target_pairs={{0,8},{8,16},{16,24},{24,0},{1,9},{9,17},{17,25},{25,1},{2,10},{10... | collective-permute-start | bytes 1572872 | tf_op jit(solution)/shard_map/ppermute | solution.py:44
  93.4 0.8 copy-start.2
  94.2 42.0 %collective-permute-start.12 = (bf16[512,512]{1,0:T(8,128)(2,1)S(1)}, bf16[512,512]{1,0:T(8,128)(2,1)}, u32[]{:S(2)}, u32[]{:S(2)}) collective-permute-start(bf16[512,512]{1,0:T(8,128)(2,1)S(1)} %pad_maximum_fusion.1.p0), channel_id=1, source_target_pairs={{0,24},{8,0},{16,8},{24,16},{1,25},{9,1},{17,9},{25,17},{2,26},{10... | collective-permute-start | bytes 1572872 | tf_op jit(solution)/shard_map/ppermute | solution.py:44
  98.8 0.8 copy-start.4
  99.7 24.7 %collective-permute-start.8 = (bf16[512,256]{1,0:T(8,128)(2,1)S(1)}, bf16[512,256]{1,0:T(8,128)(2,1)}, u32[]{:S(2)}, u32[]{:S(2)}) collective-permute-start(bf16[512,256]{1,0:T(8,128)(2,1)S(1)} %pad_maximum_fusion.5.p0), channel_id=1, source_target_pairs={{0,8},{8,16},{16,24},{24,0},{1,9},{9,17},{17,25},{25,1},{2,10},{10... | collective-permute-start | bytes 786440 | tf_op jit(solution)/shard_map/ppermute | solution.py:44
  101.6 0.7 copy-start.6
  102.3 22.1 %collective-permute-start.9 = (bf16[512,256]{1,0:T(8,128)(2,1)S(1)}, bf16[512,256]{1,0:T(8,128)(2,1)}, u32[]{:S(2)}, u32[]{:S(2)}) collective-permute-start(bf16[512,256]{1,0:T(8,128)(2,1)S(1)} %pad_maximum_fusion.5.p0), channel_id=1, source_target_pairs={{0,24},{8,0},{16,8},{24,16},{1,25},{9,1},{17,9},{25,17},{2,26},{10... | collective-permute-start | bytes 786440 | tf_op jit(solution)/shard_map/ppermute | solution.py:44
  106.9 1.1 copy-start.1
  108.0 1.1 copy-start.3
  109.1 1.0 copy-start.5
  110.1 14.3 %copy-start.7 = (bf16[512,256]{1,0:T(8,128)(2,1)S(1)}, bf16[512,256]{1,0:T(8,128)(2,1)}, u32[]{:S(2)}) copy-start(bf16[512,256]{1,0:T(8,128)(2,1)} %copy-done.6) | copy-start | bytes 786436
  111.7 19.8 %copy-start.16 = (bf16[256]{0:T(256)(128)(2,1)S(1)}, bf16[256]{0:T(256)(128)(2,1)}, u32[]{:S(2)}) copy-start(bf16[256]{0:T(256)(128)(2,1)} %param.19) | copy-start | bytes 1540
  111.7 19.8 %copy-start.17 = (bf16[256]{0:T(256)(128)(2,1)S(1)}, bf16[256]{0:T(256)(128)(2,1)}, u32[]{:S(2)}) copy-start(bf16[256]{0:T(256)(128)(2,1)} %param.20) | copy-start | bytes 1540
  111.7 24.6 %copy-start.8 = (bf16[2,128,128]{2,1,0:T(8,128)(2,1)S(1)}, bf16[2,128,128]{2,1,0:T(8,128)(2,1)}, u32[]{:S(2)}) copy-start(bf16[2,128,128]{2,1,0:T(8,128)(2,1)} %mix.3) | copy-start | bytes 196612
  111.7 24.6 %copy-start.11 = (bf16[2,128]{1,0:T(2,128)(2,1)S(1)}, bf16[2,128]{1,0:T(2,128)(2,1)}, u32[]{:S(2)}) copy-start(bf16[2,128]{1,0:T(2,128)(2,1)} %bias.1) | copy-start | bytes 1540
  127.1 9.2 %all-to-all-start.1 = ((f32[8,2,512]{2,1,0:T(2,128)}), f32[8,2,512]{2,1,0:T(2,128)S(1)}, u32[]{:S(2)}, u32[]{:S(2)}) async-start(f32[8,2,512]{2,1,0:T(2,128)} %broadcast_in_dim.24), calls=%async_computation.1 | async-start | bytes 65536 | tf_op jit(solution)/shard_map/all_to_all | solution.py:30
  139.3 4.9 %collective-permute-start.13 = (bf16[4,512,256]{2,1,0:T(8,128)(2,1)S(1)}, bf16[4,512,256]{2,1,0:T(8,128)(2,1)S(1)}, u32[]{:S(2)}, u32[]{:S(2)}) collective-permute-start(bf16[4,512,256]{2,1,0:T(8,128)(2,1)S(1)} %get-tuple-element.22), channel_id=1, source_target_pairs={{0,1},{1,0},{2,3},{3,2},{4,5},{5,4},{6,7},{7,6},{8,9},{9,8},{10,11... | collective-permute-start | bytes 3145736 | tf_op jit(solution)/shard_map/ppermute | solution.py:34
  144.4 17.5 %copy-start.13 = (bf16[512,256]{1,0:T(8,128)(2,1)S(1)}, bf16[512,256]{1,0:T(8,128)(2,1)}, u32[]{:S(2)}) copy-start(bf16[512,256]{1,0:T(8,128)(2,1)} %param.15) | copy-start | bytes 786436
  162.0 22.8 %copy-start.9 = (bf16[3,512]{1,0:T(4,128)(2,1)S(1)}, bf16[3,512]{1,0:T(4,128)(2,1)}, u32[]{:S(2)}) copy-start(bf16[3,512]{1,0:T(4,128)(2,1)} %conv_gate.1) | copy-start | bytes 9220
  162.0 22.8 %copy-start.10 = (bf16[3,512]{1,0:T(4,128)(2,1)S(1)}, bf16[3,512]{1,0:T(4,128)(2,1)}, u32[]{:S(2)}) copy-start(bf16[3,512]{1,0:T(4,128)(2,1)} %conv_value.1) | copy-start | bytes 9220
  178.5 6.3 %collective-permute-start.14 = (bf16[4,512,256]{2,1,0:T(8,128)(2,1)S(1)}, bf16[4,512,256]{2,1,0:T(8,128)(2,1)S(1)}, u32[]{:S(2)}, u32[]{:S(2)}) collective-permute-start(bf16[4,512,256]{2,1,0:T(8,128)(2,1)S(1)} %all_to_all.26.mine), channel_id=1, source_target_pairs={{0,1},{1,0},{2,3},{3,2},{4,5},{5,4},{6,7},{7,6},{8,9},{9,8},{10,11... | collective-permute-start | bytes 3145736 | tf_op jit(solution)/shard_map/ppermute | solution.py:34
  192.3 4.6 %collective-permute-start.15 = (bf16[4,512,256]{2,1,0:T(8,128)(2,1)S(1)}, bf16[4,512,256]{2,1,0:T(8,128)(2,1)S(1)}, u32[]{:S(2)}, u32[]{:S(2)}) collective-permute-start(bf16[4,512,256]{2,1,0:T(8,128)(2,1)S(1)} %get-tuple-element.26), channel_id=1, source_target_pairs={{0,1},{1,0},{2,3},{3,2},{4,5},{5,4},{6,7},{7,6},{8,9},{9,8},{10,11... | collective-permute-start | bytes 3145736 | tf_op jit(solution)/shard_map/ppermute | solution.py:34
Sparse Core Ops, SparseCore 0:
  9.4 35.2 all-gather.5
  46.8 94.8 all-gather.3

commit v10 on v7

--- a/solution.py
+++ b/solution.py
@@ -17,7 +17,7 @@
 F32 = jnp.float32
 BF16 = jnp.bfloat16
 SWAP = [(0, 1), (1, 0)]
-RING = (0, 1, 3, 2)
+RING = (0, 2, 1, 3)
 PIECE = 32
 HBM = pl.BlockSpec(memory_space=pltpu.HBM)
 SQRT_HALF = 0.7071067811865476
@@ -40,7 +40,7 @@
 
 def round_ring(shard, axis):
     size = lax.axis_size(axis)
-    steps = (1, size - 1, 2)
+    steps = (2, 1, size - 1)
     return [shard] + [lax.ppermute(shard, axis, [(i, (i + step) % size) for i in range(size)]) for step in steps]
 
 
@@ -82,14 +82,12 @@
                 weight[pl.ds(start, PIECE), :] = part[came : came + PIECE, :]
 
 
-def first_kernel(place, normed, p0, p1, p2, p3, act_u, act_v, sums, weight):
-    width = act_u.shape[1]
+def first_kernel(place, normed, p0, p1, p2, p3, act_v, sums, weight):
+    width = act_v.shape[1]
     fill_rows(weight, (p0, p1, p2, p3), place[2], place[3])
     for part in range(normed.shape[0] // SEQ_LEN):
         rows = pl.ds(part * SEQ_LEN, SEQ_LEN)
-        both = gelu(jnp.dot(normed[rows, :], weight[...], preferred_element_type=F32))
-        act_u[rows, :] = both[:, :width]
-        value = both[:, width:]
+        value = gelu(jnp.dot(normed[rows, :], weight[...], preferred_element_type=F32))
         act_v[rows, :] = value
         once = sum(value[:, k : k + 128] for k in range(0, width, 128))
         twice = sum(value[:, k : k + 128] * value[:, k : k + 128] for k in range(0, width, 128))
@@ -97,9 +95,12 @@
         sums[1:2, rows] = jnp.sum(twice.T, axis=0, keepdims=True)
 
 
-def mix_kernel(place, act_v, act_u, stats, gain, shift, mix, bias, p0, p1, p2, p3, give, keep, weight, gated):
+def mix_kernel(place, normed, act_v, stats, gain, shift, mix, bias, p0, p1, p2, p3, give, keep, weight, act_u, gated):
     width = act_v.shape[1]
     fill_rows(weight, (p0, p1, p2, p3), place[2], place[3])
+    for part in range(normed.shape[0] // SEQ_LEN):
+        rows = pl.ds(part * SEQ_LEN, SEQ_LEN)
+        act_u[rows, :] = gelu(jnp.dot(normed[rows, :], weight[:, :width], preferred_element_type=F32))
     full = width * stats.shape[0]
     i = lax.broadcasted_iota(jnp.int32, (BLOCK, BLOCK), 0)
     j = lax.broadcasted_iota(jnp.int32, (BLOCK, BLOCK), 1)
@@ -126,7 +127,7 @@
     for out, side in ((give, 1 - c), (keep, c)):
         for x in range(out.shape[0]):
             start = pl.multiple_of((2 * x + side) * width, width)
-            columns = weight[pl.ds(start, width), :]
+            columns = weight[pl.ds(start, width), width : 2 * width]
             out[x] = lax.dot_general(
                 gated[...], columns, (((1,), (1,)), ((), ())), preferred_element_type=F32
             ).astype(BF16)
@@ -235,16 +236,17 @@
     ff = ffn_gate.shape[1]
     row_count = tokens.shape[0]
 
-    early = jnp.concatenate([proj_u, proj_v, proj_out.T], axis=1)
+    early = jnp.concatenate([proj_v, proj_u, proj_out.T], axis=1)
     early_far = everyones(early, "zh").reshape(-1, early.shape[1])
     early_z = jnp.concatenate(round_ring(early_far, Z), axis=0)
-    early_parts = round_ring(early_z[:, : 2 * da], "y")
-    out_parts = round_ring(early_z[:, 2 * da :], "y")
+    early_v, early_rest = lax.optimization_barrier((early_z[:, :da], early_z[:, da:]))
+    early_parts = round_ring(early_v, "y")
+    out_parts = round_ring(early_rest, "y")
 
     late = jnp.concatenate([ffn_gate, ffn_value, proj_down.T], axis=1)
     padded = jnp.pad(late, ((0, 2 * late.shape[0]), (0, 0)))
     late_y = lax.all_gather(padded, "y", axis=0)[:, : late.shape[0]].reshape(-1, late.shape[1])
-    late_all = lax.all_gather(after(late_y, early_z), Z, axis=0, tiled=True)
+    late_all = lax.all_gather(after(late_y, early_far), Z, axis=0, tiled=True)
 
     packed = jnp.concatenate([tokens, jnp.broadcast_to(norm_gain, (8, da)), jnp.broadcast_to(ffn_gain, (8, da))], axis=0)
     pair = jnp.stack([packed, other_core(packed)])
@@ -261,12 +263,12 @@
         compiler_params=room(12),
     )(place, *token_parts)
 
-    act_u, act_v, sums = pl.pallas_call(
+    act_v, sums = pl.pallas_call(
         first_kernel,
         in_specs=[SMEM] + [VMEM] * 5,
-        out_specs=[VMEM] * 3,
-        out_shape=[shape((row_count, da), F32)] * 2 + [shape((2, row_count), F32)],
-        scratch_shapes=[pltpu.VMEM((model, 2 * da), BF16)],
+        out_specs=[VMEM] * 2,
+        out_shape=[shape((row_count, da), F32), shape((2, row_count), F32)],
+        scratch_shapes=[pltpu.VMEM((model, da), BF16)],
         name="first",
         compiler_params=room(14),
     )(place, normed, *early_parts)
@@ -277,13 +279,17 @@
         in_specs=[SMEM] + [VMEM] * 11,
         out_specs=[VMEM] * 2,
         out_shape=blocks,
-        scratch_shapes=[pltpu.VMEM((model, da), BF16), pltpu.VMEM((row_count, da), BF16)],
+        scratch_shapes=[
+            pltpu.VMEM((model, 2 * da), BF16),
+            pltpu.VMEM((row_count, da), F32),
+            pltpu.VMEM((row_count, da), BF16),
+        ],
         name="mix",
         compiler_params=room(16),
     )(
         place,
+        normed,
         act_v,
-        act_u,
         stats,
         layer_gain[None],
         layer_shift[None],

time: 210 us -> 224 us (1.067)
  waiting for transfers between devices: 24.8 us -> 54.5 us
  blocking collectives: 79.5 us -> 51 us
  local copies, waits for them, and re-layouts: 2.61 us -> 9.48 us
  starting transfers between devices: 69.8 us -> 75.1 us
    all_to_all x2 -> x1, blocking collectives: 44.9 us -> 16.4 us  [everyones(): return lax.all_to_all(copies, axis, split_axis=0, concat_axis=0, tiled=True)]
    all_gather x1, waiting for transfers between devices: 0.01 us -> 19.5 us  [on_device(): lax.all_gather(padded, 'y', axis=0)[:, :late.shape[0]]]
    ppermute x12, waiting for transfers between devices: 12.1 us -> 22.2 us  [round_ring(): lax.ppermute(shard, axis, [(i, (i + step) % size) for i in range(size)])]
    all_to_all x1 -> x2, starting transfers between devices: 11.2 us -> 20 us  [everyones(): return lax.all_to_all(copies, axis, split_axis=0, concat_axis=0, tiled=True)]
    unnamed x22 -> x36, local copies, waits for them, and re-layouts: 0.05 us -> 6.31 us
    all_to_all x1 -> x2, waiting for transfers between devices: 4.73 us -> 4.75 us  [everyones(): return lax.all_to_all(copies, axis, split_axis=0, concat_axis=0, tiled=True)]
  transfers between devices with their start and end apart: 19 -> 20, of which waited for: 10 -> 9; matrix products, arithmetic and copies ran while one was open for 1% -> 2% of each run, Pallas kernels for 3% -> 3%
where the time goes in v10:
time: 224 us; the launch traced here: 222 us
  starting transfers between devices  75.1 us (34%)
  waiting for transfers between devices  54.5 us (24%)
  blocking collectives  51 us (23%)
  between operations  13.8 us (6%)
  Pallas kernels  13.6 us (6%)
  local copies, waits for them, and re-layouts  9.48 us (4%)
  other arithmetic  4.21 us (2%)
    ppermute x12, starting transfers between devices, round_ring(): lax.ppermute(shard, axis, [(i, (i + step) % size) for i in range(size)])  41.5 us
    all_to_all x2, blocking collectives, summed_at_owner(): arrived = lax.all_to_all(pair, 'x', split_axis=0, concat_axis=0, tiled=True)  34.6 us
    ppermute x12, waiting for transfers between devices, round_ring(): lax.ppermute(shard, axis, [(i, (i + step) % size) for i in range(size)])  22.2 us
    all_to_all x2, starting transfers between devices, everyones(): return lax.all_to_all(copies, axis, split_axis=0, concat_axis=0, tiled=True)  20 us
    all_gather x1, waiting for transfers between devices, on_device(): lax.all_gather(padded, 'y', axis=0)[:, :late.shape[0]]  19.5 us
    all_to_all x1, blocking collectives, everyones(): return lax.all_to_all(copies, axis, split_axis=0, concat_axis=0, tiled=True)  16.4 us
    ppermute x4, starting transfers between devices, other_core(): return lax.ppermute(value, 'c', SWAP)  13.5 us
    ppermute x4, waiting for transfers between devices, other_core(): return lax.ppermute(value, 'c', SWAP)  7.96 us
  transfers between devices with their start and end apart: 20, of which 9 were waited for; matrix products, arithmetic and copies ran while one was open for 2% of the time, Pallas kernels for 3%

profile of v10, /device:TPU:1, one launch (start us, length us, event | category | flops | bytes accessed | tf_op | source)
XLA Modules:
  0.0 221.6 jit_solution(6006081899911986926)
XLA Ops:
  6.5 1.6 fusion.4
  8.1 0.0 all-gather.6.cloned.1.call-update
  8.1 0.8 pad_maximum_fusion.6
  8.9 0.7 broadcast_in_dim.23
  9.6 15.6 %all-to-all-start = ((bf16[4,32,768]{2,1,0:T(8,128)(2,1)}), bf16[4,32,768]{2,1,0:T(8,128)(2,1)S(1)}, u32[]{:S(2)}, u32[]{:S(2)}) async-start(bf16[4,32,768]{2,1,0:T(8,128)(2,1)} %broadcast_in_dim.23), calls=%async_computation | async-start | bytes 393216 | tf_op jit(solution)/shard_map/all_to_all | solution.py:30
  25.2 19.5 %all-gather.6.cloned.1.call-done = bf16[384,1536]{1,0:T(8,128)(2,1)} async-done(((bf16[96,1536]{1,0:T(8,128)(2,1)}), bf16[384,1536]{1,0:T(8,128)(2,1)}) %all-gather.6.cloned.1.call-update) | async-done | bytes 1179664 | tf_op jit(solution)/shard_map/all_gather | solution.py:248
  44.7 1.8 slice.12
  46.5 0.0 all-gather.4.cloned.1.call-update
  46.6 4.7 %collective-permute-start = (bf16[528,256]{1,0:T(8,128)(2,1)S(1)}, bf16[528,256]{1,0:T(8,128)(2,1)S(1)}, u32[]{:S(2)}, u32[]{:S(2)}) collective-permute-start(bf16[528,256]{1,0:T(8,128)(2,1)S(1)} %get-tuple-element.28), channel_id=1, source_target_pairs={{0,1},{1,0},{2,3},{3,2},{4,5},{5,4},{6,7},{7,6},{8,9},{9,8},{10,11... | collective-permute-start | bytes 811016 | tf_op jit(solution)/shard_map/ppermute | solution.py:34
  51.3 1.2 collective-permute-done
  52.5 0.1 pad_maximum_fusion.p0
  52.5 4.6 %collective-permute-start.1 = (bf16[2,528,256]{2,1,0:T(8,128)(2,1)S(1)}, bf16[2,528,256]{2,1,0:T(8,128)(2,1)S(1)}, u32[]{:S(2)}, u32[]{:S(2)}) collective-permute-start(bf16[2,528,256]{2,1,0:T(8,128)(2,1)S(1)} %pad_maximum_fusion.p0), channel_id=1, source_target_pairs={{0,4},{2,6},{4,0},{6,2},{1,5},{3,7},{5,1},{7,3},{8,12},{10,14},{12... | collective-permute-start | bytes 1622024 | tf_op jit(solution)/shard_map/ppermute | solution.py:44
  57.1 2.2 collective-permute-start.2
  59.3 4.2 %collective-permute-start.4 = (bf16[128,768]{1,0:T(8,128)(2,1)S(1)}, bf16[128,768]{1,0:T(8,128)(2,1)S(1)}, u32[]{:S(2)}, u32[]{:S(2)}) collective-permute-start(bf16[128,768]{1,0:T(8,128)(2,1)S(1)} %bitcast.12), channel_id=1, source_target_pairs={{0,64},{32,96},{64,128},{96,160},{128,192},{160,224},{192,256},{22... | collective-permute-start | bytes 589832 | tf_op jit(solution)/shard_map/ppermute | solution.py:44
  63.5 3.2 %collective-permute-start.5 = (bf16[128,768]{1,0:T(8,128)(2,1)S(1)}, bf16[128,768]{1,0:T(8,128)(2,1)S(1)}, u32[]{:S(2)}, u32[]{:S(2)}) collective-permute-start(bf16[128,768]{1,0:T(8,128)(2,1)S(1)} %bitcast.13), channel_id=1, source_target_pairs={{0,32},{32,64},{64,96},{96,128},{128,160},{160,192},{192,224},{224... | collective-permute-start | bytes 589832 | tf_op jit(solution)/shard_map/ppermute | solution.py:44
  66.7 3.3 %collective-permute-start.6 = (bf16[128,768]{1,0:T(8,128)(2,1)S(1)}, bf16[128,768]{1,0:T(8,128)(2,1)S(1)}, u32[]{:S(2)}, u32[]{:S(2)}) collective-permute-start(bf16[128,768]{1,0:T(8,128)(2,1)S(1)} %bitcast.14), channel_id=1, source_target_pairs={{0,480},{32,0},{64,32},{96,64},{128,96},{160,128},{192,160},{224,1... | collective-permute-start | bytes 589832 | tf_op jit(solution)/shard_map/ppermute | solution.py:44
  70.0 1.1 collective-permute-done.4
  71.2 4.3 %collective-permute-start.3 = (bf16[2,528,256]{2,1,0:T(8,128)(2,1)S(1)}, bf16[2,528,256]{2,1,0:T(8,128)(2,1)S(1)}, u32[]{:S(2)}, u32[]{:S(2)}) collective-permute-start(bf16[2,528,256]{2,1,0:T(8,128)(2,1)S(1)} %pad_maximum_fusion.p0), channel_id=1, source_target_pairs={{0,6},{2,0},{4,2},{6,4},{1,7},{3,1},{5,3},{7,5},{8,14},{10,8},{12,... | collective-permute-start | bytes 1622024 | tf_op jit(solution)/shard_map/ppermute | solution.py:44
  75.5 8.4 %collective-permute-done.5 = bf16[128,768]{1,0:T(8,128)(2,1)S(1)} collective-permute-done((bf16[128,768]{1,0:T(8,128)(2,1)S(1)}, bf16[128,768]{1,0:T(8,128)(2,1)S(1)}, u32[]{:S(2)}, u32[]{:S(2)}) %collective-permute-start.5) | collective-permute-done | bytes 196640 | tf_op jit(solution)/shard_map/ppermute | solution.py:44
  83.9 3.9 %collective-permute-start.7 = (bf16[512,256]{1,0:T(8,128)(2,1)S(1)}, bf16[512,256]{1,0:T(8,128)(2,1)S(1)}, u32[]{:S(2)}, u32[]{:S(2)}) collective-permute-start(bf16[512,256]{1,0:T(8,128)(2,1)S(1)} %pad_maximum_fusion.5.p0), channel_id=1, source_target_pairs={{0,16},{8,24},{16,0},{24,8},{1,17},{9,25},{17,1},{25,9},{2,18},{10... | collective-permute-start | bytes 786440 | tf_op jit(solution)/shard_map/ppermute | solution.py:44
  87.8 2.9 %collective-permute-start.10 = (bf16[512,512]{1,0:T(8,128)(2,1)S(1)}, bf16[512,512]{1,0:T(8,128)(2,1)}, u32[]{:S(2)}, u32[]{:S(2)}) collective-permute-start(bf16[512,512]{1,0:T(8,128)(2,1)S(1)} %pad_maximum_fusion.1.p0), channel_id=1, source_target_pairs={{0,16},{8,24},{16,0},{24,8},{1,17},{9,25},{17,1},{25,9},{2,18},{10... | collective-permute-start | bytes 1572872 | tf_op jit(solution)/shard_map/ppermute | solution.py:44
  90.7 0.8 copy-done
  91.5 1.9 collective-permute-start.11
  93.5 0.8 copy-done.2
  94.2 4.6 %collective-permute-start.12 = (bf16[512,512]{1,0:T(8,128)(2,1)S(1)}, bf16[512,512]{1,0:T(8,128)(2,1)}, u32[]{:S(2)}, u32[]{:S(2)}) collective-permute-start(bf16[512,512]{1,0:T(8,128)(2,1)S(1)} %pad_maximum_fusion.1.p0), channel_id=1, source_target_pairs={{0,24},{8,0},{16,8},{24,16},{1,25},{9,1},{17,9},{25,17},{2,26},{10... | collective-permute-start | bytes 1572872 | tf_op jit(solution)/shard_map/ppermute | solution.py:44
  98.8 0.8 copy-done.4
  99.7 1.9 collective-permute-start.8
  101.6 0.0 copy-start.6
  101.6 0.7 copy-done.6
  102.3 4.6 %collective-permute-start.9 = (bf16[512,256]{1,0:T(8,128)(2,1)S(1)}, bf16[512,256]{1,0:T(8,128)(2,1)}, u32[]{:S(2)}, u32[]{:S(2)}) collective-permute-start(bf16[512,256]{1,0:T(8,128)(2,1)S(1)} %pad_maximum_fusion.5.p0), channel_id=1, source_target_pairs={{0,24},{8,0},{16,8},{24,16},{1,25},{9,1},{17,9},{25,17},{2,26},{10... | collective-permute-start | bytes 786440 | tf_op jit(solution)/shard_map/ppermute | solution.py:44
  106.9 0.1 pad_add_fusion.place
  106.9 1.1 copy-done.1
  108.0 1.1 copy-done.3
  109.1 1.0 copy-done.5
  110.1 1.6 norm.1
  111.7 0.0 copy-start.16
  111.7 0.0 copy-start.17
  111.7 0.0 copy-start.8
  111.7 0.0 copy-start.11
  111.7 12.7 %collective-permute-done.8.p2 = bf16[512,256]{1,0:T(8,128)(2,1)} collective-permute-done((bf16[512,256]{1,0:T(8,128)(2,1)S(1)}, bf16[512,256]{1,0:T(8,128)(2,1)}, u32[]{:S(2)}, u32[]{:S(2)}) %collective-permute-start.8) | collective-permute-done | bytes 262176 | tf_op jit(solution)/shard_map/ppermute | solution.py:44
  124.4 2.0 first.1
  126.4 0.6 broadcast_in_dim.24
  127.1 4.4 %all-to-all-start.1 = ((f32[8,2,512]{2,1,0:T(2,128)}), f32[8,2,512]{2,1,0:T(2,128)S(1)}, u32[]{:S(2)}, u32[]{:S(2)}) async-start(f32[8,2,512]{2,1,0:T(2,128)} %broadcast_in_dim.24), calls=%async_computation.1 | async-start | bytes 65536 | tf_op jit(solution)/shard_map/all_to_all | solution.py:30
  131.5 4.7 %all-to-all-done.1.stats = f32[8,2,512]{2,1,0:T(2,128)S(1)} async-done(((f32[8,2,512]{2,1,0:T(2,128)}), f32[8,2,512]{2,1,0:T(2,128)S(1)}, u32[]{:S(2)}, u32[]{:S(2)}) %all-to-all-start.1) | async-done | bytes 32800 | tf_op jit(solution)/shard_map/all_to_all | solution.py:30
  136.3 3.0 %mix.2 = (bf16[4,512,256]{2,1,0:T(8,128)(2,1)S(1)}, bf16[4,512,256]{2,1,0:T(8,128)(2,1)S(1)}) custom-call(s32[4]{0:T(128)S(1)} %pad_add_fusion.place, bf16[512,2048]{1,0:T(8,128)(2,1)S(1)} %get-tuple-element.16.normed, f32[512,256]{1,0:T(8,128)S(1)} %get-tuple-element.18.act_v, f32[8,2,512]{2,1,0:T(2,128)S(1)} %all-to-all-done.1.stats, ...), custom_call_target="tpu_custom_call" | custom-call | tf_op jit(solution)/shard_map/mix/pallas_call | solution.py:277
  139.3 2.6 %collective-permute-start.13 = (bf16[4,512,256]{2,1,0:T(8,128)(2,1)S(1)}, bf16[4,512,256]{2,1,0:T(8,128)(2,1)S(1)}, u32[]{:S(2)}, u32[]{:S(2)}) collective-permute-start(bf16[4,512,256]{2,1,0:T(8,128)(2,1)S(1)} %get-tuple-element.22), channel_id=1, source_target_pairs={{0,1},{1,0},{2,3},{3,2},{4,5},{5,4},{6,7},{7,6},{8,9},{9,8},{10,11... | collective-permute-start | bytes 3145736 | tf_op jit(solution)/shard_map/ppermute | solution.py:34
  141.9 2.3 %collective-permute-done.13 = bf16[4,512,256]{2,1,0:T(8,128)(2,1)S(1)} collective-permute-done((bf16[4,512,256]{2,1,0:T(8,128)(2,1)S(1)}, bf16[4,512,256]{2,1,0:T(8,128)(2,1)S(1)}, u32[]{:S(2)}, u32[]{:S(2)}) %collective-permute-start.13) | collective-permute-done | bytes 1048608 | tf_op jit(solution)/shard_map/ppermute | solution.py:34
  144.2 0.3 add_convert_fusion.1
  144.4 0.0 copy-start.13
  144.5 17.4 %all_to_all.25 = bf16[4,512,256]{2,1,0:T(8,128)(2,1)S(1)} all-to-all(bf16[4,512,256]{2,1,0:T(8,128)(2,1)S(1)} %add_convert_fusion.1), channel_id=1, replica_groups=mesh['zh'=4,'zl'=4,'y'=4,'x'=4,'c'=2] {'x'}, dimensions={0} | all-to-all | bytes 2097152 | tf_op jit(solution)/shard_map/all_to_all | solution.py:214
  161.8 0.1 convert_reduce_fusion.1
  162.0 0.0 copy-start.9
  162.0 0.1 add_convert_fusion.3
  162.1 0.1 broadcast_in_dim.27
  162.2 16.4 %all_to_all.26.mine = bf16[4,512,256]{2,1,0:T(8,128)(2,1)S(1)} all-to-all(bf16[4,512,256]{2,1,0:T(8,128)(2,1)S(1)} %broadcast_in_dim.27), channel_id=1, replica_groups=mesh['zh'=4,'zl'=4,'y'=4,'x'=4,'c'=2] {'x'}, dimensions={0} | all-to-all | bytes 2097152 | tf_op jit(solution)/shard_map/all_to_all | solution.py:30
  178.5 4.0 %collective-permute-start.14 = (bf16[4,512,256]{2,1,0:T(8,128)(2,1)S(1)}, bf16[4,512,256]{2,1,0:T(8,128)(2,1)S(1)}, u32[]{:S(2)}, u32[]{:S(2)}) collective-permute-start(bf16[4,512,256]{2,1,0:T(8,128)(2,1)S(1)} %all_to_all.26.mine), channel_id=1, source_target_pairs={{0,1},{1,0},{2,3},{3,2},{4,5},{5,4},{6,7},{7,6},{8,9},{9,8},{10,11... | collective-permute-start | bytes 3145736 | tf_op jit(solution)/shard_map/ppermute | solution.py:34
  182.5 2.3 %collective-permute-done.14.other = bf16[4,512,256]{2,1,0:T(8,128)(2,1)S(1)} collective-permute-done((bf16[4,512,256]{2,1,0:T(8,128)(2,1)S(1)}, bf16[4,512,256]{2,1,0:T(8,128)(2,1)S(1)}, u32[]{:S(2)}, u32[]{:S(2)}) %collective-permute-start.14) | collective-permute-done | bytes 1048608 | tf_op jit(solution)/shard_map/ppermute | solution.py:34
  184.8 7.0 %ffn.1 = (bf16[4,512,256]{2,1,0:T(8,128)(2,1)S(1)}, bf16[4,512,256]{2,1,0:T(8,128)(2,1)S(1)}) custom-call(s32[4]{0:T(128)S(1)} %pad_add_fusion.place, bf16[4,512,256]{2,1,0:T(8,128)(2,1)S(1)} %all_to_all.26.mine, bf16[4,512,256]{2,1,0:T(8,128)(2,1)S(1)} %collective-permute-done.14.other, bf16[8,8,256]{2,1,0:T(8,128)(2,1)S(1)} %get-tuple-element.23.gain, ...), custom_call_target="tpu_custom_call" | custom-call | tf_op jit(solution)/shard_map/ffn/pallas_call | solution.py:302
  191.8 2.3 %collective-permute-start.15 = (bf16[4,512,256]{2,1,0:T(8,128)(2,1)S(1)}, bf16[4,512,256]{2,1,0:T(8,128)(2,1)S(1)}, u32[]{:S(2)}, u32[]{:S(2)}) collective-permute-start(bf16[4,512,256]{2,1,0:T(8,128)(2,1)S(1)} %get-tuple-element.26), channel_id=1, source_target_pairs={{0,1},{1,0},{2,3},{3,2},{4,5},{5,4},{6,7},{7,6},{8,9},{9,8},{10,11... | collective-permute-start | bytes 3145736 | tf_op jit(solution)/shard_map/ppermute | solution.py:34
  194.1 2.3 %collective-permute-done.15 = bf16[4,512,256]{2,1,0:T(8,128)(2,1)S(1)} collective-permute-done((bf16[4,512,256]{2,1,0:T(8,128)(2,1)S(1)}, bf16[4,512,256]{2,1,0:T(8,128)(2,1)S(1)}, u32[]{:S(2)}, u32[]{:S(2)}) %collective-permute-start.15) | collective-permute-done | bytes 1048608 | tf_op jit(solution)/shard_map/ppermute | solution.py:34
  196.3 0.3 add_convert_fusion
  196.6 17.3 %all_to_all.27 = bf16[4,512,256]{2,1,0:T(8,128)(2,1)S(1)} all-to-all(bf16[4,512,256]{2,1,0:T(8,128)(2,1)S(1)} %add_convert_fusion), channel_id=1, replica_groups=mesh['zh'=4,'zl'=4,'y'=4,'x'=4,'c'=2] {'x'}, dimensions={0} | all-to-all | bytes 2097152 | tf_op jit(solution)/shard_map/all_to_all | solution.py:214
  213.9 0.1 convert_reduce_fusion
  214.0 0.8 add_convert_fusion.2
  (42 shorter events, 0.2 us)
Async XLA Ops:
  6.5 40.0 %copy-start.14 = (bf16[256]{0:T(256)(128)(2,1)S(1)}, bf16[256]{0:T(256)(128)(2,1)}, u32[]{:S(2)}) copy-start(bf16[256]{0:T(256)(128)(2,1)} %param.16) | copy-start | bytes 1540
  6.5 40.0 %copy-start.15 = (bf16[256]{0:T(256)(128)(2,1)S(1)}, bf16[256]{0:T(256)(128)(2,1)}, u32[]{:S(2)}) copy-start(bf16[256]{0:T(256)(128)(2,1)} %param.24) | copy-start | bytes 1540
  6.5 40.0 %copy-start.12 = (bf16[512,256]{1,0:T(8,128)(2,1)S(1)}, bf16[512,256]{1,0:T(8,128)(2,1)}, u32[]{:S(2)}) copy-start(bf16[512,256]{1,0:T(8,128)(2,1)} %param.15) | copy-start | bytes 786436
  6.5 38.2 %all-gather.6.cloned.1.call-start = ((), (), s32[]{:S(2)}) async-start(), calls=%async_computation.6 | async-start | bytes 1474560 | tf_op jit(solution)/shard_map/all_gather | solution.py:248
  9.6 36.9 %all-to-all-start = ((bf16[4,32,768]{2,1,0:T(8,128)(2,1)}), bf16[4,32,768]{2,1,0:T(8,128)(2,1)S(1)}, u32[]{:S(2)}, u32[]{:S(2)}) async-start(bf16[4,32,768]{2,1,0:T(8,128)(2,1)} %broadcast_in_dim.23), calls=%async_computation | async-start | bytes 393216 | tf_op jit(solution)/shard_map/all_to_all | solution.py:30
  25.2 159.6 %all-gather.4.cloned.1.call-start = ((), (), s32[]{:S(2)}) async-start(), calls=%async_computation.5 | async-start | bytes 6684672 | tf_op jit(solution)/shard_map/all_gather | solution.py:249
  46.6 5.9 %collective-permute-start = (bf16[528,256]{1,0:T(8,128)(2,1)S(1)}, bf16[528,256]{1,0:T(8,128)(2,1)S(1)}, u32[]{:S(2)}, u32[]{:S(2)}) collective-permute-start(bf16[528,256]{1,0:T(8,128)(2,1)S(1)} %get-tuple-element.28), channel_id=1, source_target_pairs={{0,1},{1,0},{2,3},{3,2},{4,5},{5,4},{6,7},{7,6},{8,9},{9,8},{10,11... | collective-permute-start | bytes 811016 | tf_op jit(solution)/shard_map/ppermute | solution.py:34
  52.5 38.2 %collective-permute-start.1 = (bf16[2,528,256]{2,1,0:T(8,128)(2,1)S(1)}, bf16[2,528,256]{2,1,0:T(8,128)(2,1)S(1)}, u32[]{:S(2)}, u32[]{:S(2)}) collective-permute-start(bf16[2,528,256]{2,1,0:T(8,128)(2,1)S(1)} %pad_maximum_fusion.p0), channel_id=1, source_target_pairs={{0,4},{2,6},{4,0},{6,2},{1,5},{3,7},{5,1},{7,3},{8,12},{10,14},{12... | collective-permute-start | bytes 1622024 | tf_op jit(solution)/shard_map/ppermute | solution.py:44
  57.1 36.3 %collective-permute-start.2 = (bf16[2,528,256]{2,1,0:T(8,128)(2,1)S(1)}, bf16[2,528,256]{2,1,0:T(8,128)(2,1)S(1)}, u32[]{:S(2)}, u32[]{:S(2)}) collective-permute-start(bf16[2,528,256]{2,1,0:T(8,128)(2,1)S(1)} %pad_maximum_fusion.p0), channel_id=1, source_target_pairs={{0,2},{2,4},{4,6},{6,0},{1,3},{3,5},{5,7},{7,1},{8,10},{10,12},{12... | collective-permute-start | bytes 1622024 | tf_op jit(solution)/shard_map/ppermute | solution.py:44
  59.3 11.8 %collective-permute-start.4 = (bf16[128,768]{1,0:T(8,128)(2,1)S(1)}, bf16[128,768]{1,0:T(8,128)(2,1)S(1)}, u32[]{:S(2)}, u32[]{:S(2)}) collective-permute-start(bf16[128,768]{1,0:T(8,128)(2,1)S(1)} %bitcast.12), channel_id=1, source_target_pairs={{0,64},{32,96},{64,128},{96,160},{128,192},{160,224},{192,256},{22... | collective-permute-start | bytes 589832 | tf_op jit(solution)/shard_map/ppermute | solution.py:44
  63.5 20.3 %collective-permute-start.5 = (bf16[128,768]{1,0:T(8,128)(2,1)S(1)}, bf16[128,768]{1,0:T(8,128)(2,1)S(1)}, u32[]{:S(2)}, u32[]{:S(2)}) collective-permute-start(bf16[128,768]{1,0:T(8,128)(2,1)S(1)} %bitcast.13), channel_id=1, source_target_pairs={{0,32},{32,64},{64,96},{96,128},{128,160},{160,192},{192,224},{224... | collective-permute-start | bytes 589832 | tf_op jit(solution)/shard_map/ppermute | solution.py:44
  66.7 17.1 %collective-permute-start.6 = (bf16[128,768]{1,0:T(8,128)(2,1)S(1)}, bf16[128,768]{1,0:T(8,128)(2,1)S(1)}, u32[]{:S(2)}, u32[]{:S(2)}) collective-permute-start(bf16[128,768]{1,0:T(8,128)(2,1)S(1)} %bitcast.14), channel_id=1, source_target_pairs={{0,480},{32,0},{64,32},{96,64},{128,96},{160,128},{192,160},{224,1... | collective-permute-start | bytes 589832 | tf_op jit(solution)/shard_map/ppermute | solution.py:44
  71.2 27.7 %collective-permute-start.3 = (bf16[2,528,256]{2,1,0:T(8,128)(2,1)S(1)}, bf16[2,528,256]{2,1,0:T(8,128)(2,1)S(1)}, u32[]{:S(2)}, u32[]{:S(2)}) collective-permute-start(bf16[2,528,256]{2,1,0:T(8,128)(2,1)S(1)} %pad_maximum_fusion.p0), channel_id=1, source_target_pairs={{0,6},{2,0},{4,2},{6,4},{1,7},{3,1},{5,3},{7,5},{8,14},{10,8},{12,... | collective-permute-start | bytes 1622024 | tf_op jit(solution)/shard_map/ppermute | solution.py:44
  83.9 17.7 %collective-permute-start.7 = (bf16[512,256]{1,0:T(8,128)(2,1)S(1)}, bf16[512,256]{1,0:T(8,128)(2,1)S(1)}, u32[]{:S(2)}, u32[]{:S(2)}) collective-permute-start(bf16[512,256]{1,0:T(8,128)(2,1)S(1)} %pad_maximum_fusion.5.p0), channel_id=1, source_target_pairs={{0,16},{8,24},{16,0},{24,8},{1,17},{9,25},{17,1},{25,9},{2,18},{10... | collective-permute-start | bytes 786440 | tf_op jit(solution)/shard_map/ppermute | solution.py:44
  87.8 48.5 %collective-permute-start.10 = (bf16[512,512]{1,0:T(8,128)(2,1)S(1)}, bf16[512,512]{1,0:T(8,128)(2,1)}, u32[]{:S(2)}, u32[]{:S(2)}) collective-permute-start(bf16[512,512]{1,0:T(8,128)(2,1)S(1)} %pad_maximum_fusion.1.p0), channel_id=1, source_target_pairs={{0,16},{8,24},{16,0},{24,8},{1,17},{9,25},{17,1},{25,9},{2,18},{10... | collective-permute-start | bytes 1572872 | tf_op jit(solution)/shard_map/ppermute | solution.py:44
  90.7 0.8 copy-start
  91.5 44.8 %collective-permute-start.11 = (bf16[512,512]{1,0:T(8,128)(2,1)S(1)}, bf16[512,512]{1,0:T(8,128)(2,1)}, u32[]{:S(2)}, u32[]{:S(2)}) collective-permute-start(bf16[512,512]{1,0:T(8,128)(2,1)S(1)} %pad_maximum_fusion.1.p0), channel_id=1, source_target_pairs={{0,8},{8,16},{16,24},{24,0},{1,9},{9,17},{17,25},{25,1},{2,10},{10... | collective-permute-start | bytes 1572872 | tf_op jit(solution)/shard_map/ppermute | solution.py:44
  93.4 0.8 copy-start.2
  94.2 42.0 %collective-permute-start.12 = (bf16[512,512]{1,0:T(8,128)(2,1)S(1)}, bf16[512,512]{1,0:T(8,128)(2,1)}, u32[]{:S(2)}, u32[]{:S(2)}) collective-permute-start(bf16[512,512]{1,0:T(8,128)(2,1)S(1)} %pad_maximum_fusion.1.p0), channel_id=1, source_target_pairs={{0,24},{8,0},{16,8},{24,16},{1,25},{9,1},{17,9},{25,17},{2,26},{10... | collective-permute-start | bytes 1572872 | tf_op jit(solution)/shard_map/ppermute | solution.py:44
  98.8 0.8 copy-start.4
  99.7 24.7 %collective-permute-start.8 = (bf16[512,256]{1,0:T(8,128)(2,1)S(1)}, bf16[512,256]{1,0:T(8,128)(2,1)}, u32[]{:S(2)}, u32[]{:S(2)}) collective-permute-start(bf16[512,256]{1,0:T(8,128)(2,1)S(1)} %pad_maximum_fusion.5.p0), channel_id=1, source_target_pairs={{0,8},{8,16},{16,24},{24,0},{1,9},{9,17},{17,25},{25,1},{2,10},{10... | collective-permute-start | bytes 786440 | tf_op jit(solution)/shard_map/ppermute | solution.py:44
  101.6 0.7 copy-start.6
  102.3 22.1 %collective-permute-start.9 = (bf16[512,256]{1,0:T(8,128)(2,1)S(1)}, bf16[512,256]{1,0:T(8,128)(2,1)}, u32[]{:S(2)}, u32[]{:S(2)}) collective-permute-start(bf16[512,256]{1,0:T(8,128)(2,1)S(1)} %pad_maximum_fusion.5.p0), channel_id=1, source_target_pairs={{0,24},{8,0},{16,8},{24,16},{1,25},{9,1},{17,9},{25,17},{2,26},{10... | collective-permute-start | bytes 786440 | tf_op jit(solution)/shard_map/ppermute | solution.py:44
  106.9 1.1 copy-start.1
  108.0 1.1 copy-start.3
  109.1 1.0 copy-start.5
  110.1 14.3 %copy-start.7 = (bf16[512,256]{1,0:T(8,128)(2,1)S(1)}, bf16[512,256]{1,0:T(8,128)(2,1)}, u32[]{:S(2)}) copy-start(bf16[512,256]{1,0:T(8,128)(2,1)} %copy-done.6) | copy-start | bytes 786436
  111.7 19.8 %copy-start.16 = (bf16[256]{0:T(256)(128)(2,1)S(1)}, bf16[256]{0:T(256)(128)(2,1)}, u32[]{:S(2)}) copy-start(bf16[256]{0:T(256)(128)(2,1)} %param.19) | copy-start | bytes 1540
  111.7 19.8 %copy-start.17 = (bf16[256]{0:T(256)(128)(2,1)S(1)}, bf16[256]{0:T(256)(128)(2,1)}, u32[]{:S(2)}) copy-start(bf16[256]{0:T(256)(128)(2,1)} %param.20) | copy-start | bytes 1540
  111.7 24.6 %copy-start.8 = (bf16[2,128,128]{2,1,0:T(8,128)(2,1)S(1)}, bf16[2,128,128]{2,1,0:T(8,128)(2,1)}, u32[]{:S(2)}) copy-start(bf16[2,128,128]{2,1,0:T(8,128)(2,1)} %mix.3) | copy-start | bytes 196612
  111.7 24.6 %copy-start.11 = (bf16[2,128]{1,0:T(2,128)(2,1)S(1)}, bf16[2,128]{1,0:T(2,128)(2,1)}, u32[]{:S(2)}) copy-start(bf16[2,128]{1,0:T(2,128)(2,1)} %bias.1) | copy-start | bytes 1540
  127.1 9.2 %all-to-all-start.1 = ((f32[8,2,512]{2,1,0:T(2,128)}), f32[8,2,512]{2,1,0:T(2,128)S(1)}, u32[]{:S(2)}, u32[]{:S(2)}) async-start(f32[8,2,512]{2,1,0:T(2,128)} %broadcast_in_dim.24), calls=%async_computation.1 | async-start | bytes 65536 | tf_op jit(solution)/shard_map/all_to_all | solution.py:30
  139.3 4.9 %collective-permute-start.13 = (bf16[4,512,256]{2,1,0:T(8,128)(2,1)S(1)}, bf16[4,512,256]{2,1,0:T(8,128)(2,1)S(1)}, u32[]{:S(2)}, u32[]{:S(2)}) collective-permute-start(bf16[4,512,256]{2,1,0:T(8,128)(2,1)S(1)} %get-tuple-element.22), channel_id=1, source_target_pairs={{0,1},{1,0},{2,3},{3,2},{4,5},{5,4},{6,7},{7,6},{8,9},{9,8},{10,11... | collective-permute-start | bytes 3145736 | tf_op jit(solution)/shard_map/ppermute | solution.py:34
  144.4 17.5 %copy-start.13 = (bf16[512,256]{1,0:T(8,128)(2,1)S(1)}, bf16[512,256]{1,0:T(8,128)(2,1)}, u32[]{:S(2)}) copy-start(bf16[512,256]{1,0:T(8,128)(2,1)} %param.15) | copy-start | bytes 786436
  162.0 22.8 %copy-start.9 = (bf16[3,512]{1,0:T(4,128)(2,1)S(1)}, bf16[3,512]{1,0:T(4,128)(2,1)}, u32[]{:S(2)}) copy-start(bf16[3,512]{1,0:T(4,128)(2,1)} %conv_gate.1) | copy-start | bytes 9220
  162.0 22.8 %copy-start.10 = (bf16[3,512]{1,0:T(4,128)(2,1)S(1)}, bf16[3,512]{1,0:T(4,128)(2,1)}, u32[]{:S(2)}) copy-start(bf16[3,512]{1,0:T(4,128)(2,1)} %conv_value.1) | copy-start | bytes 9220
  178.5 6.3 %collective-permute-start.14 = (bf16[4,512,256]{2,1,0:T(8,128)(2,1)S(1)}, bf16[4,512,256]{2,1,0:T(8,128)(2,1)S(1)}, u32[]{:S(2)}, u32[]{:S(2)}) collective-permute-start(bf16[4,512,256]{2,1,0:T(8,128)(2,1)S(1)} %all_to_all.26.mine), channel_id=1, source_target_pairs={{0,1},{1,0},{2,3},{3,2},{4,5},{5,4},{6,7},{7,6},{8,9},{9,8},{10,11... | collective-permute-start | bytes 3145736 | tf_op jit(solution)/shard_map/ppermute | solution.py:34
  191.8 4.6 %collective-permute-start.15 = (bf16[4,512,256]{2,1,0:T(8,128)(2,1)S(1)}, bf16[4,512,256]{2,1,0:T(8,128)(2,1)S(1)}, u32[]{:S(2)}, u32[]{:S(2)}) collective-permute-start(bf16[4,512,256]{2,1,0:T(8,128)(2,1)S(1)} %get-tuple-element.26), channel_id=1, source_target_pairs={{0,1},{1,0},{2,3},{3,2},{4,5},{5,4},{6,7},{7,6},{8,9},{9,8},{10,11... | collective-permute-start | bytes 3145736 | tf_op jit(solution)/shard_map/ppermute | solution.py:34
Sparse Core Ops, SparseCore 0:
  9.4 35.2 all-gather.5
  46.8 94.8 all-gather.3

commit v11 on v7

--- a/solution.py
+++ b/solution.py
@@ -17,7 +17,7 @@
 F32 = jnp.float32
 BF16 = jnp.bfloat16
 SWAP = [(0, 1), (1, 0)]
-RING = (0, 1, 3, 2)
+RING = (0, 2, 1, 3)
 PIECE = 32
 HBM = pl.BlockSpec(memory_space=pltpu.HBM)
 SQRT_HALF = 0.7071067811865476
@@ -40,7 +40,7 @@
 
 def round_ring(shard, axis):
     size = lax.axis_size(axis)
-    steps = (1, size - 1, 2)
+    steps = (2, 1, size - 1)
     return [shard] + [lax.ppermute(shard, axis, [(i, (i + step) % size) for i in range(size)]) for step in steps]
 
 
@@ -238,13 +238,14 @@
     early = jnp.concatenate([proj_u, proj_v, proj_out.T], axis=1)
     early_far = everyones(early, "zh").reshape(-1, early.shape[1])
     early_z = jnp.concatenate(round_ring(early_far, Z), axis=0)
-    early_parts = round_ring(early_z[:, : 2 * da], "y")
-    out_parts = round_ring(early_z[:, 2 * da :], "y")
+    early_uv, early_out = lax.optimization_barrier((early_z[:, : 2 * da], early_z[:, 2 * da :]))
+    early_parts = round_ring(early_uv, "y")
+    out_parts = round_ring(early_out, "y")
 
     late = jnp.concatenate([ffn_gate, ffn_value, proj_down.T], axis=1)
     padded = jnp.pad(late, ((0, 2 * late.shape[0]), (0, 0)))
     late_y = lax.all_gather(padded, "y", axis=0)[:, : late.shape[0]].reshape(-1, late.shape[1])
-    late_all = lax.all_gather(after(late_y, early_z), Z, axis=0, tiled=True)
+    late_all = lax.all_gather(after(late_y, early_far), Z, axis=0, tiled=True)
 
     packed = jnp.concatenate([tokens, jnp.broadcast_to(norm_gain, (8, da)), jnp.broadcast_to(ffn_gain, (8, da))], axis=0)
     pair = jnp.stack([packed, other_core(packed)])

time: 210 us -> 203 us (0.967)
  blocking collectives: 79.5 us -> 51 us
  waiting for transfers between devices: 24.8 us -> 39.1 us
  starting transfers between devices: 69.8 us -> 76.8 us
    all_to_all x2 -> x1, blocking collectives: 44.9 us -> 16.4 us  [everyones(): return lax.all_to_all(copies, axis, split_axis=0, concat_axis=0, tiled=True)]
    all_gather x1, waiting for transfers between devices: 0.01 us -> 19.5 us  [on_device(): lax.all_gather(padded, 'y', axis=0)[:, :late.shape[0]]]
    all_to_all x1 -> x2, starting transfers between devices: 11.2 us -> 20.7 us  [everyones(): return lax.all_to_all(copies, axis, split_axis=0, concat_axis=0, tiled=True)]
    ppermute x12, waiting for transfers between devices: 12.1 us -> 8.59 us  [round_ring(): lax.ppermute(shard, axis, [(i, (i + step) % size) for i in range(size)])]
    all_to_all x1 -> x2, waiting for transfers between devices: 4.73 us -> 4.16 us  [everyones(): return lax.all_to_all(copies, axis, split_axis=0, concat_axis=0, tiled=True)]
  transfers between devices with their start and end apart: 19 -> 20, of which waited for: 10 -> 8; matrix products, arithmetic and copies ran while one was open for 1% -> 2% of each run, Pallas kernels for 3% -> 3%
where the time goes in v11:
time: 203 us; the launch traced here: 202 us
  starting transfers between devices  76.8 us (38%)
  blocking collectives  51 us (25%)
  waiting for transfers between devices  39.1 us (19%)
  between operations  13.8 us (7%)
  Pallas kernels  13.6 us (7%)
  other arithmetic  4.22 us (2%)
  local copies, waits for them, and re-layouts  3.27 us (2%)
    ppermute x12, starting transfers between devices, round_ring(): lax.ppermute(shard, axis, [(i, (i + step) % size) for i in range(size)])  42.6 us
    all_to_all x2, blocking collectives, summed_at_owner(): arrived = lax.all_to_all(pair, 'x', split_axis=0, concat_axis=0, tiled=True)  34.6 us
    all_to_all x2, starting transfers between devices, everyones(): return lax.all_to_all(copies, axis, split_axis=0, concat_axis=0, tiled=True)  20.7 us
    all_gather x1, waiting for transfers between devices, on_device(): lax.all_gather(padded, 'y', axis=0)[:, :late.shape[0]]  19.5 us
    all_to_all x1, blocking collectives, everyones(): return lax.all_to_all(copies, axis, split_axis=0, concat_axis=0, tiled=True)  16.4 us
    ppermute x4, starting transfers between devices, other_core(): return lax.ppermute(value, 'c', SWAP)  13.5 us
    ppermute x12, waiting for transfers between devices, round_ring(): lax.ppermute(shard, axis, [(i, (i + step) % size) for i in range(size)])  8.59 us
    pallas_call x1, Pallas kernels, on_device(): pl.pallas_call(ffn_kernel, in_specs=[SMEM] + [VMEM] * 3 + [HBM] + [VMEM]...  6.98 us
  transfers between devices with their start and end apart: 20, of which 8 were waited for; matrix products, arithmetic and copies ran while one was open for 2% of the time, Pallas kernels for 3%

profile of v11, /device:TPU:1, one launch (start us, length us, event | category | flops | bytes accessed | tf_op | source)
XLA Modules:
  0.0 201.8 jit_solution(4631333800376848891)
XLA Ops:
  6.5 1.6 fusion.4
  8.1 0.0 all-gather.6.cloned.1.call-update
  8.1 0.8 pad_maximum_fusion.4
  8.9 0.7 broadcast_in_dim.23
  9.6 15.6 %all-to-all-start = ((bf16[4,32,768]{2,1,0:T(8,128)(2,1)}), bf16[4,32,768]{2,1,0:T(8,128)(2,1)S(1)}, u32[]{:S(2)}, u32[]{:S(2)}) async-start(bf16[4,32,768]{2,1,0:T(8,128)(2,1)} %broadcast_in_dim.23), calls=%async_computation | async-start | bytes 393216 | tf_op jit(solution)/shard_map/all_to_all | solution.py:30
  25.2 19.5 %all-gather.6.cloned.1.call-done = bf16[384,1536]{1,0:T(8,128)(2,1)} async-done(((bf16[96,1536]{1,0:T(8,128)(2,1)}), bf16[384,1536]{1,0:T(8,128)(2,1)}) %all-gather.6.cloned.1.call-update) | async-done | bytes 1179664 | tf_op jit(solution)/shard_map/all_gather | solution.py:247
  44.7 1.8 slice.13
  46.5 0.0 all-to-all-done
  46.5 0.0 all-gather.4.cloned.1.call-update
  46.6 4.7 %collective-permute-start = (bf16[528,256]{1,0:T(8,128)(2,1)S(1)}, bf16[528,256]{1,0:T(8,128)(2,1)S(1)}, u32[]{:S(2)}, u32[]{:S(2)}) collective-permute-start(bf16[528,256]{1,0:T(8,128)(2,1)S(1)} %get-tuple-element.30), channel_id=1, source_target_pairs={{0,1},{1,0},{2,3},{3,2},{4,5},{5,4},{6,7},{7,6},{8,9},{9,8},{10,11... | collective-permute-start | bytes 811016 | tf_op jit(solution)/shard_map/ppermute | solution.py:34
  51.3 4.2 %collective-permute-start.4 = (bf16[128,768]{1,0:T(8,128)(2,1)S(1)}, bf16[128,768]{1,0:T(8,128)(2,1)S(1)}, u32[]{:S(2)}, u32[]{:S(2)}) collective-permute-start(bf16[128,768]{1,0:T(8,128)(2,1)S(1)} %bitcast.12), channel_id=1, source_target_pairs={{0,64},{32,96},{64,128},{96,160},{128,192},{160,224},{192,256},{22... | collective-permute-start | bytes 589832 | tf_op jit(solution)/shard_map/ppermute | solution.py:44
  55.5 3.2 %collective-permute-start.5 = (bf16[128,768]{1,0:T(8,128)(2,1)S(1)}, bf16[128,768]{1,0:T(8,128)(2,1)S(1)}, u32[]{:S(2)}, u32[]{:S(2)}) collective-permute-start(bf16[128,768]{1,0:T(8,128)(2,1)S(1)} %bitcast.13), channel_id=1, source_target_pairs={{0,32},{32,64},{64,96},{96,128},{128,160},{160,192},{192,224},{224... | collective-permute-start | bytes 589832 | tf_op jit(solution)/shard_map/ppermute | solution.py:44
  58.7 3.3 %collective-permute-start.6 = (bf16[128,768]{1,0:T(8,128)(2,1)S(1)}, bf16[128,768]{1,0:T(8,128)(2,1)S(1)}, u32[]{:S(2)}, u32[]{:S(2)}) collective-permute-start(bf16[128,768]{1,0:T(8,128)(2,1)S(1)} %bitcast.14), channel_id=1, source_target_pairs={{0,480},{32,0},{64,32},{96,64},{128,96},{160,128},{192,160},{224,1... | collective-permute-start | bytes 589832 | tf_op jit(solution)/shard_map/ppermute | solution.py:44
  62.0 0.0 collective-permute-done
  62.0 0.1 pad_maximum_fusion.1.p0
  62.1 4.6 %collective-permute-start.1 = (bf16[2,528,256]{2,1,0:T(8,128)(2,1)S(1)}, bf16[2,528,256]{2,1,0:T(8,128)(2,1)S(1)}, u32[]{:S(2)}, u32[]{:S(2)}) collective-permute-start(bf16[2,528,256]{2,1,0:T(8,128)(2,1)S(1)} %pad_maximum_fusion.1.p0), channel_id=1, source_target_pairs={{0,4},{2,6},{4,0},{6,2},{1,5},{3,7},{5,1},{7,3},{8,12},{10,14},{12... | collective-permute-start | bytes 1622024 | tf_op jit(solution)/shard_map/ppermute | solution.py:44
  66.7 2.2 %collective-permute-start.2 = (bf16[2,528,256]{2,1,0:T(8,128)(2,1)S(1)}, bf16[2,528,256]{2,1,0:T(8,128)(2,1)S(1)}, u32[]{:S(2)}, u32[]{:S(2)}) collective-permute-start(bf16[2,528,256]{2,1,0:T(8,128)(2,1)S(1)} %pad_maximum_fusion.1.p0), channel_id=1, source_target_pairs={{0,2},{2,4},{4,6},{6,0},{1,3},{3,5},{5,7},{7,1},{8,10},{10,12},{12... | collective-permute-start | bytes 1622024 | tf_op jit(solution)/shard_map/ppermute | solution.py:44
  68.9 0.0 collective-permute-done.4
  68.9 4.3 %collective-permute-start.3 = (bf16[2,528,256]{2,1,0:T(8,128)(2,1)S(1)}, bf16[2,528,256]{2,1,0:T(8,128)(2,1)S(1)}, u32[]{:S(2)}, u32[]{:S(2)}) collective-permute-start(bf16[2,528,256]{2,1,0:T(8,128)(2,1)S(1)} %pad_maximum_fusion.1.p0), channel_id=1, source_target_pairs={{0,6},{2,0},{4,2},{6,4},{1,7},{3,1},{5,3},{7,5},{8,14},{10,8},{12,... | collective-permute-start | bytes 1622024 | tf_op jit(solution)/shard_map/ppermute | solution.py:44
  73.2 0.0 collective-permute-done.5
  73.2 0.0 collective-permute-done.6
  73.2 0.1 pad_maximum_fusion
  73.4 3.9 %collective-permute-start.7 = (bf16[512,512]{1,0:T(8,128)(2,1)S(1)}, bf16[512,512]{1,0:T(8,128)(2,1)S(1)}, u32[]{:S(2)}, u32[]{:S(2)}) collective-permute-start(bf16[512,512]{1,0:T(8,128)(2,1)S(1)} %slice.12.p0), channel_id=1, source_target_pairs={{0,16},{8,24},{16,0},{24,8},{1,17},{9,25},{17,1},{25,9},{2,18},{10... | collective-permute-start | bytes 1572872 | tf_op jit(solution)/shard_map/ppermute | solution.py:44
  77.3 1.9 collective-permute-start.8
  79.3 0.0 collective-permute-done.1.p1
  79.3 4.6 %collective-permute-start.9 = (bf16[512,512]{1,0:T(8,128)(2,1)S(1)}, bf16[512,512]{1,0:T(8,128)(2,1)}, u32[]{:S(2)}, u32[]{:S(2)}) collective-permute-start(bf16[512,512]{1,0:T(8,128)(2,1)S(1)} %slice.12.p0), channel_id=1, source_target_pairs={{0,24},{8,0},{16,8},{24,16},{1,25},{9,1},{17,9},{25,17},{2,26},{10... | collective-permute-start | bytes 1572872 | tf_op jit(solution)/shard_map/ppermute | solution.py:44
  83.8 7.5 %collective-permute-done.2.p2 = bf16[2,528,256]{2,1,0:T(8,128)(2,1)S(1)} collective-permute-done((bf16[2,528,256]{2,1,0:T(8,128)(2,1)S(1)}, bf16[2,528,256]{2,1,0:T(8,128)(2,1)S(1)}, u32[]{:S(2)}, u32[]{:S(2)}) %collective-permute-start.2) | collective-permute-done | bytes 540704 | tf_op jit(solution)/shard_map/ppermute | solution.py:44
  91.4 3.9 %collective-permute-start.10 = (bf16[512,256]{1,0:T(8,128)(2,1)S(1)}, bf16[512,256]{1,0:T(8,128)(2,1)}, u32[]{:S(2)}, u32[]{:S(2)}) collective-permute-start(bf16[512,256]{1,0:T(8,128)(2,1)S(1)} %pad_maximum_fusion.3.p0), channel_id=1, source_target_pairs={{0,16},{8,24},{16,0},{24,8},{1,17},{9,25},{17,1},{25,9},{2,18},{10... | collective-permute-start | bytes 786440 | tf_op jit(solution)/shard_map/ppermute | solution.py:44
  95.3 0.0 collective-permute-done.3.p3
  95.3 1.9 collective-permute-start.11
  97.3 4.6 %collective-permute-start.12 = (bf16[512,256]{1,0:T(8,128)(2,1)S(1)}, bf16[512,256]{1,0:T(8,128)(2,1)}, u32[]{:S(2)}, u32[]{:S(2)}) collective-permute-start(bf16[512,256]{1,0:T(8,128)(2,1)S(1)} %pad_maximum_fusion.3.p0), channel_id=1, source_target_pairs={{0,24},{8,0},{16,8},{24,16},{1,25},{9,1},{17,9},{25,17},{2,26},{10... | collective-permute-start | bytes 786440 | tf_op jit(solution)/shard_map/ppermute | solution.py:44
  101.9 0.1 pad_add_fusion.place
  101.9 1.6 norm.1
  103.5 0.5 collective-permute-done.8.p2
  104.0 0.0 collective-permute-done.9.p3
  104.0 0.0 copy-start.3
  104.0 2.9 %first.1 = (f32[512,256]{1,0:T(8,128)S(1)}, f32[512,256]{1,0:T(8,128)S(1)}, f32[2,512]{1,0:T(2,128)S(1)}) custom-call(s32[4]{0:T(128)S(1)} %pad_add_fusion.place, bf16[512,2048]{1,0:T(8,128)(2,1)S(1)} %get-tuple-element.17.normed, bf16[512,512]{1,0:T(8,128)(2,1)S(1)} %slice.12.p0, bf16[512,512]{1,0:T(8,128)(2,1)S(1)} %collective-permute-done.7.p1, ...), custom_call_target="tpu_custom_call" | custom-call | tf_op jit(solution)/shard_map/first/pallas_call | solution.py:265
  106.9 0.6 broadcast_in_dim.24
  107.5 5.0 %all-to-all-start.1 = ((f32[8,2,512]{2,1,0:T(2,128)}), f32[8,2,512]{2,1,0:T(2,128)S(1)}, u32[]{:S(2)}, u32[]{:S(2)}) async-start(f32[8,2,512]{2,1,0:T(2,128)} %broadcast_in_dim.24), calls=%async_computation.1 | async-start | bytes 65536 | tf_op jit(solution)/shard_map/all_to_all | solution.py:30
  112.6 0.0 collective-permute-done.10.p1
  112.6 0.6 collective-permute-done.11.p2
  113.2 0.0 collective-permute-done.12.p3
  113.2 4.2 %all-to-all-done.1.stats = f32[8,2,512]{2,1,0:T(2,128)S(1)} async-done(((f32[8,2,512]{2,1,0:T(2,128)}), f32[8,2,512]{2,1,0:T(2,128)S(1)}, u32[]{:S(2)}, u32[]{:S(2)}) %all-to-all-start.1) | async-done | bytes 32800 | tf_op jit(solution)/shard_map/all_to_all | solution.py:30
  117.4 2.2 %mix.2 = (bf16[4,512,256]{2,1,0:T(8,128)(2,1)S(1)}, bf16[4,512,256]{2,1,0:T(8,128)(2,1)S(1)}) custom-call(s32[4]{0:T(128)S(1)} %pad_add_fusion.place, f32[512,256]{1,0:T(8,128)S(1)} %get-tuple-element.19.act_v, f32[512,256]{1,0:T(8,128)S(1)} %get-tuple-element.20.act_u, f32[8,2,512]{2,1,0:T(2,128)S(1)} %all-to-all-done.1.stats, ...), custom_call_target="tpu_custom_call" | custom-call | tf_op jit(solution)/shard_map/mix/pallas_call | solution.py:276
  119.5 2.6 %collective-permute-start.13 = (bf16[4,512,256]{2,1,0:T(8,128)(2,1)S(1)}, bf16[4,512,256]{2,1,0:T(8,128)(2,1)S(1)}, u32[]{:S(2)}, u32[]{:S(2)}) collective-permute-start(bf16[4,512,256]{2,1,0:T(8,128)(2,1)S(1)} %get-tuple-element.24), channel_id=1, source_target_pairs={{0,1},{1,0},{2,3},{3,2},{4,5},{5,4},{6,7},{7,6},{8,9},{9,8},{10,11... | collective-permute-start | bytes 3145736 | tf_op jit(solution)/shard_map/ppermute | solution.py:34
  122.1 2.3 %collective-permute-done.13 = bf16[4,512,256]{2,1,0:T(8,128)(2,1)S(1)} collective-permute-done((bf16[4,512,256]{2,1,0:T(8,128)(2,1)S(1)}, bf16[4,512,256]{2,1,0:T(8,128)(2,1)S(1)}, u32[]{:S(2)}, u32[]{:S(2)}) %collective-permute-start.13) | collective-permute-done | bytes 1048608 | tf_op jit(solution)/shard_map/ppermute | solution.py:34
  124.4 0.2 add_convert_fusion.1
  124.6 0.0 copy-start.5
  124.6 17.4 %all_to_all.25 = bf16[4,512,256]{2,1,0:T(8,128)(2,1)S(1)} all-to-all(bf16[4,512,256]{2,1,0:T(8,128)(2,1)S(1)} %add_convert_fusion.1), channel_id=1, replica_groups=mesh['zh'=4,'zl'=4,'y'=4,'x'=4,'c'=2] {'x'}, dimensions={0} | all-to-all | bytes 2097152 | tf_op jit(solution)/shard_map/all_to_all | solution.py:213
  142.0 0.1 convert_reduce_fusion.1
  142.2 0.0 copy-start.1
  142.2 0.0 copy-start.2
  142.2 0.1 add_convert_fusion.3
  142.3 0.1 broadcast_in_dim.27
  142.3 16.4 %all_to_all.26.mine = bf16[4,512,256]{2,1,0:T(8,128)(2,1)S(1)} all-to-all(bf16[4,512,256]{2,1,0:T(8,128)(2,1)S(1)} %broadcast_in_dim.27), channel_id=1, replica_groups=mesh['zh'=4,'zl'=4,'y'=4,'x'=4,'c'=2] {'x'}, dimensions={0} | all-to-all | bytes 2097152 | tf_op jit(solution)/shard_map/all_to_all | solution.py:30
  158.7 4.0 %collective-permute-start.14 = (bf16[4,512,256]{2,1,0:T(8,128)(2,1)S(1)}, bf16[4,512,256]{2,1,0:T(8,128)(2,1)S(1)}, u32[]{:S(2)}, u32[]{:S(2)}) collective-permute-start(bf16[4,512,256]{2,1,0:T(8,128)(2,1)S(1)} %all_to_all.26.mine), channel_id=1, source_target_pairs={{0,1},{1,0},{2,3},{3,2},{4,5},{5,4},{6,7},{7,6},{8,9},{9,8},{10,11... | collective-permute-start | bytes 3145736 | tf_op jit(solution)/shard_map/ppermute | solution.py:34
  162.7 2.3 %collective-permute-done.14.other = bf16[4,512,256]{2,1,0:T(8,128)(2,1)S(1)} collective-permute-done((bf16[4,512,256]{2,1,0:T(8,128)(2,1)S(1)}, bf16[4,512,256]{2,1,0:T(8,128)(2,1)S(1)}, u32[]{:S(2)}, u32[]{:S(2)}) %collective-permute-start.14) | collective-permute-done | bytes 1048608 | tf_op jit(solution)/shard_map/ppermute | solution.py:34
  165.0 7.0 %ffn.1 = (bf16[4,512,256]{2,1,0:T(8,128)(2,1)S(1)}, bf16[4,512,256]{2,1,0:T(8,128)(2,1)S(1)}) custom-call(s32[4]{0:T(128)S(1)} %pad_add_fusion.place, bf16[4,512,256]{2,1,0:T(8,128)(2,1)S(1)} %all_to_all.26.mine, bf16[4,512,256]{2,1,0:T(8,128)(2,1)S(1)} %collective-permute-done.14.other, bf16[8,8,256]{2,1,0:T(8,128)(2,1)S(1)} %get-tuple-element.25.gain, ...), custom_call_target="tpu_custom_call" | custom-call | tf_op jit(solution)/shard_map/ffn/pallas_call | solution.py:297
  172.0 2.3 %collective-permute-start.15 = (bf16[4,512,256]{2,1,0:T(8,128)(2,1)S(1)}, bf16[4,512,256]{2,1,0:T(8,128)(2,1)S(1)}, u32[]{:S(2)}, u32[]{:S(2)}) collective-permute-start(bf16[4,512,256]{2,1,0:T(8,128)(2,1)S(1)} %get-tuple-element.28), channel_id=1, source_target_pairs={{0,1},{1,0},{2,3},{3,2},{4,5},{5,4},{6,7},{7,6},{8,9},{9,8},{10,11... | collective-permute-start | bytes 3145736 | tf_op jit(solution)/shard_map/ppermute | solution.py:34
  174.3 2.3 %collective-permute-done.15 = bf16[4,512,256]{2,1,0:T(8,128)(2,1)S(1)} collective-permute-done((bf16[4,512,256]{2,1,0:T(8,128)(2,1)S(1)}, bf16[4,512,256]{2,1,0:T(8,128)(2,1)S(1)}, u32[]{:S(2)}, u32[]{:S(2)}) %collective-permute-start.15) | collective-permute-done | bytes 1048608 | tf_op jit(solution)/shard_map/ppermute | solution.py:34
  176.5 0.3 add_convert_fusion
  176.8 17.2 %all_to_all.27 = bf16[4,512,256]{2,1,0:T(8,128)(2,1)S(1)} all-to-all(bf16[4,512,256]{2,1,0:T(8,128)(2,1)S(1)} %add_convert_fusion), channel_id=1, replica_groups=mesh['zh'=4,'zl'=4,'y'=4,'x'=4,'c'=2] {'x'}, dimensions={0} | all-to-all | bytes 2097152 | tf_op jit(solution)/shard_map/all_to_all | solution.py:213
  194.1 0.1 convert_reduce_fusion
  194.2 0.8 add_convert_fusion.2
  (27 shorter events, 0.2 us)
Async XLA Ops:
  6.5 40.0 %copy-start.6 = (bf16[256]{0:T(256)(128)(2,1)S(1)}, bf16[256]{0:T(256)(128)(2,1)}, u32[]{:S(2)}) copy-start(bf16[256]{0:T(256)(128)(2,1)} %param.16) | copy-start | bytes 1540
  6.5 40.0 %copy-start.7 = (bf16[256]{0:T(256)(128)(2,1)S(1)}, bf16[256]{0:T(256)(128)(2,1)}, u32[]{:S(2)}) copy-start(bf16[256]{0:T(256)(128)(2,1)} %param.24) | copy-start | bytes 1540
  6.5 40.0 %copy-start.4 = (bf16[512,256]{1,0:T(8,128)(2,1)S(1)}, bf16[512,256]{1,0:T(8,128)(2,1)}, u32[]{:S(2)}) copy-start(bf16[512,256]{1,0:T(8,128)(2,1)} %param.15) | copy-start | bytes 786436
  6.5 38.2 %all-gather.6.cloned.1.call-start = ((), (), s32[]{:S(2)}) async-start(), calls=%async_computation.6 | async-start | bytes 1474560 | tf_op jit(solution)/shard_map/all_gather | solution.py:247
  9.6 36.9 %all-to-all-start = ((bf16[4,32,768]{2,1,0:T(8,128)(2,1)}), bf16[4,32,768]{2,1,0:T(8,128)(2,1)S(1)}, u32[]{:S(2)}, u32[]{:S(2)}) async-start(bf16[4,32,768]{2,1,0:T(8,128)(2,1)} %broadcast_in_dim.23), calls=%async_computation | async-start | bytes 393216 | tf_op jit(solution)/shard_map/all_to_all | solution.py:30
  25.2 139.8 %all-gather.4.cloned.1.call-start = ((), (), s32[]{:S(2)}) async-start(), calls=%async_computation.5 | async-start | bytes 6684672 | tf_op jit(solution)/shard_map/all_gather | solution.py:248
  46.6 15.4 %collective-permute-start = (bf16[528,256]{1,0:T(8,128)(2,1)S(1)}, bf16[528,256]{1,0:T(8,128)(2,1)S(1)}, u32[]{:S(2)}, u32[]{:S(2)}) collective-permute-start(bf16[528,256]{1,0:T(8,128)(2,1)S(1)} %get-tuple-element.30), channel_id=1, source_target_pairs={{0,1},{1,0},{2,3},{3,2},{4,5},{5,4},{6,7},{7,6},{8,9},{9,8},{10,11... | collective-permute-start | bytes 811016 | tf_op jit(solution)/shard_map/ppermute | solution.py:34
  51.3 17.6 %collective-permute-start.4 = (bf16[128,768]{1,0:T(8,128)(2,1)S(1)}, bf16[128,768]{1,0:T(8,128)(2,1)S(1)}, u32[]{:S(2)}, u32[]{:S(2)}) collective-permute-start(bf16[128,768]{1,0:T(8,128)(2,1)S(1)} %bitcast.12), channel_id=1, source_target_pairs={{0,64},{32,96},{64,128},{96,160},{128,192},{160,224},{192,256},{22... | collective-permute-start | bytes 589832 | tf_op jit(solution)/shard_map/ppermute | solution.py:44
  55.5 17.7 %collective-permute-start.5 = (bf16[128,768]{1,0:T(8,128)(2,1)S(1)}, bf16[128,768]{1,0:T(8,128)(2,1)S(1)}, u32[]{:S(2)}, u32[]{:S(2)}) collective-permute-start(bf16[128,768]{1,0:T(8,128)(2,1)S(1)} %bitcast.13), channel_id=1, source_target_pairs={{0,32},{32,64},{64,96},{96,128},{128,160},{160,192},{192,224},{224... | collective-permute-start | bytes 589832 | tf_op jit(solution)/shard_map/ppermute | solution.py:44
  58.7 14.5 %collective-permute-start.6 = (bf16[128,768]{1,0:T(8,128)(2,1)S(1)}, bf16[128,768]{1,0:T(8,128)(2,1)S(1)}, u32[]{:S(2)}, u32[]{:S(2)}) collective-permute-start(bf16[128,768]{1,0:T(8,128)(2,1)S(1)} %bitcast.14), channel_id=1, source_target_pairs={{0,480},{32,0},{64,32},{96,64},{128,96},{160,128},{192,160},{224,1... | collective-permute-start | bytes 589832 | tf_op jit(solution)/shard_map/ppermute | solution.py:44
  62.1 17.2 %collective-permute-start.1 = (bf16[2,528,256]{2,1,0:T(8,128)(2,1)S(1)}, bf16[2,528,256]{2,1,0:T(8,128)(2,1)S(1)}, u32[]{:S(2)}, u32[]{:S(2)}) collective-permute-start(bf16[2,528,256]{2,1,0:T(8,128)(2,1)S(1)} %pad_maximum_fusion.1.p0), channel_id=1, source_target_pairs={{0,4},{2,6},{4,0},{6,2},{1,5},{3,7},{5,1},{7,3},{8,12},{10,14},{12... | collective-permute-start | bytes 1622024 | tf_op jit(solution)/shard_map/ppermute | solution.py:44
  66.7 24.7 %collective-permute-start.2 = (bf16[2,528,256]{2,1,0:T(8,128)(2,1)S(1)}, bf16[2,528,256]{2,1,0:T(8,128)(2,1)S(1)}, u32[]{:S(2)}, u32[]{:S(2)}) collective-permute-start(bf16[2,528,256]{2,1,0:T(8,128)(2,1)S(1)} %pad_maximum_fusion.1.p0), channel_id=1, source_target_pairs={{0,2},{2,4},{4,6},{6,0},{1,3},{3,5},{5,7},{7,1},{8,10},{10,12},{12... | collective-permute-start | bytes 1622024 | tf_op jit(solution)/shard_map/ppermute | solution.py:44
  68.9 26.4 %collective-permute-start.3 = (bf16[2,528,256]{2,1,0:T(8,128)(2,1)S(1)}, bf16[2,528,256]{2,1,0:T(8,128)(2,1)S(1)}, u32[]{:S(2)}, u32[]{:S(2)}) collective-permute-start(bf16[2,528,256]{2,1,0:T(8,128)(2,1)S(1)} %pad_maximum_fusion.1.p0), channel_id=1, source_target_pairs={{0,6},{2,0},{4,2},{6,4},{1,7},{3,1},{5,3},{7,5},{8,14},{10,8},{12,... | collective-permute-start | bytes 1622024 | tf_op jit(solution)/shard_map/ppermute | solution.py:44
  73.4 23.9 %collective-permute-start.7 = (bf16[512,512]{1,0:T(8,128)(2,1)S(1)}, bf16[512,512]{1,0:T(8,128)(2,1)S(1)}, u32[]{:S(2)}, u32[]{:S(2)}) collective-permute-start(bf16[512,512]{1,0:T(8,128)(2,1)S(1)} %slice.12.p0), channel_id=1, source_target_pairs={{0,16},{8,24},{16,0},{24,8},{1,17},{9,25},{17,1},{25,9},{2,18},{10... | collective-permute-start | bytes 1572872 | tf_op jit(solution)/shard_map/ppermute | solution.py:44
  77.3 26.6 %collective-permute-start.8 = (bf16[512,512]{1,0:T(8,128)(2,1)S(1)}, bf16[512,512]{1,0:T(8,128)(2,1)}, u32[]{:S(2)}, u32[]{:S(2)}) collective-permute-start(bf16[512,512]{1,0:T(8,128)(2,1)S(1)} %slice.12.p0), channel_id=1, source_target_pairs={{0,8},{8,16},{16,24},{24,0},{1,9},{9,17},{17,25},{25,1},{2,10},{10... | collective-permute-start | bytes 1572872 | tf_op jit(solution)/shard_map/ppermute | solution.py:44
  79.3 24.7 %collective-permute-start.9 = (bf16[512,512]{1,0:T(8,128)(2,1)S(1)}, bf16[512,512]{1,0:T(8,128)(2,1)}, u32[]{:S(2)}, u32[]{:S(2)}) collective-permute-start(bf16[512,512]{1,0:T(8,128)(2,1)S(1)} %slice.12.p0), channel_id=1, source_target_pairs={{0,24},{8,0},{16,8},{24,16},{1,25},{9,1},{17,9},{25,17},{2,26},{10... | collective-permute-start | bytes 1572872 | tf_op jit(solution)/shard_map/ppermute | solution.py:44
  91.4 21.2 %collective-permute-start.10 = (bf16[512,256]{1,0:T(8,128)(2,1)S(1)}, bf16[512,256]{1,0:T(8,128)(2,1)}, u32[]{:S(2)}, u32[]{:S(2)}) collective-permute-start(bf16[512,256]{1,0:T(8,128)(2,1)S(1)} %pad_maximum_fusion.3.p0), channel_id=1, source_target_pairs={{0,16},{8,24},{16,0},{24,8},{1,17},{9,25},{17,1},{25,9},{2,18},{10... | collective-permute-start | bytes 786440 | tf_op jit(solution)/shard_map/ppermute | solution.py:44
  95.3 17.9 %collective-permute-start.11 = (bf16[512,256]{1,0:T(8,128)(2,1)S(1)}, bf16[512,256]{1,0:T(8,128)(2,1)}, u32[]{:S(2)}, u32[]{:S(2)}) collective-permute-start(bf16[512,256]{1,0:T(8,128)(2,1)S(1)} %pad_maximum_fusion.3.p0), channel_id=1, source_target_pairs={{0,8},{8,16},{16,24},{24,0},{1,9},{9,17},{17,25},{25,1},{2,10},{10... | collective-permute-start | bytes 786440 | tf_op jit(solution)/shard_map/ppermute | solution.py:44
  97.3 15.9 %collective-permute-start.12 = (bf16[512,256]{1,0:T(8,128)(2,1)S(1)}, bf16[512,256]{1,0:T(8,128)(2,1)}, u32[]{:S(2)}, u32[]{:S(2)}) collective-permute-start(bf16[512,256]{1,0:T(8,128)(2,1)S(1)} %pad_maximum_fusion.3.p0), channel_id=1, source_target_pairs={{0,24},{8,0},{16,8},{24,16},{1,25},{9,1},{17,9},{25,17},{2,26},{10... | collective-permute-start | bytes 786440 | tf_op jit(solution)/shard_map/ppermute | solution.py:44
  104.0 8.6 %copy-start.8 = (bf16[256]{0:T(256)(128)(2,1)S(1)}, bf16[256]{0:T(256)(128)(2,1)}, u32[]{:S(2)}) copy-start(bf16[256]{0:T(256)(128)(2,1)} %param.19) | copy-start | bytes 1540
  104.0 8.6 %copy-start.9 = (bf16[256]{0:T(256)(128)(2,1)S(1)}, bf16[256]{0:T(256)(128)(2,1)}, u32[]{:S(2)}) copy-start(bf16[256]{0:T(256)(128)(2,1)} %param.20) | copy-start | bytes 1540
  104.0 13.4 %copy-start = (bf16[2,128,128]{2,1,0:T(8,128)(2,1)S(1)}, bf16[2,128,128]{2,1,0:T(8,128)(2,1)}, u32[]{:S(2)}) copy-start(bf16[2,128,128]{2,1,0:T(8,128)(2,1)} %mix.3) | copy-start | bytes 196612
  104.0 13.4 %copy-start.3 = (bf16[2,128]{1,0:T(2,128)(2,1)S(1)}, bf16[2,128]{1,0:T(2,128)(2,1)}, u32[]{:S(2)}) copy-start(bf16[2,128]{1,0:T(2,128)(2,1)} %bias.1) | copy-start | bytes 1540
  107.5 9.8 %all-to-all-start.1 = ((f32[8,2,512]{2,1,0:T(2,128)}), f32[8,2,512]{2,1,0:T(2,128)S(1)}, u32[]{:S(2)}, u32[]{:S(2)}) async-start(f32[8,2,512]{2,1,0:T(2,128)} %broadcast_in_dim.24), calls=%async_computation.1 | async-start | bytes 65536 | tf_op jit(solution)/shard_map/all_to_all | solution.py:30
  119.5 4.9 %collective-permute-start.13 = (bf16[4,512,256]{2,1,0:T(8,128)(2,1)S(1)}, bf16[4,512,256]{2,1,0:T(8,128)(2,1)S(1)}, u32[]{:S(2)}, u32[]{:S(2)}) collective-permute-start(bf16[4,512,256]{2,1,0:T(8,128)(2,1)S(1)} %get-tuple-element.24), channel_id=1, source_target_pairs={{0,1},{1,0},{2,3},{3,2},{4,5},{5,4},{6,7},{7,6},{8,9},{9,8},{10,11... | collective-permute-start | bytes 3145736 | tf_op jit(solution)/shard_map/ppermute | solution.py:34
  124.6 17.5 %copy-start.5 = (bf16[512,256]{1,0:T(8,128)(2,1)S(1)}, bf16[512,256]{1,0:T(8,128)(2,1)}, u32[]{:S(2)}) copy-start(bf16[512,256]{1,0:T(8,128)(2,1)} %param.15) | copy-start | bytes 786436
  142.2 22.8 %copy-start.1 = (bf16[3,512]{1,0:T(4,128)(2,1)S(1)}, bf16[3,512]{1,0:T(4,128)(2,1)}, u32[]{:S(2)}) copy-start(bf16[3,512]{1,0:T(4,128)(2,1)} %conv_gate.1) | copy-start | bytes 9220
  142.2 22.8 %copy-start.2 = (bf16[3,512]{1,0:T(4,128)(2,1)S(1)}, bf16[3,512]{1,0:T(4,128)(2,1)}, u32[]{:S(2)}) copy-start(bf16[3,512]{1,0:T(4,128)(2,1)} %conv_value.1) | copy-start | bytes 9220
  158.7 6.3 %collective-permute-start.14 = (bf16[4,512,256]{2,1,0:T(8,128)(2,1)S(1)}, bf16[4,512,256]{2,1,0:T(8,128)(2,1)S(1)}, u32[]{:S(2)}, u32[]{:S(2)}) collective-permute-start(bf16[4,512,256]{2,1,0:T(8,128)(2,1)S(1)} %all_to_all.26.mine), channel_id=1, source_target_pairs={{0,1},{1,0},{2,3},{3,2},{4,5},{5,4},{6,7},{7,6},{8,9},{9,8},{10,11... | collective-permute-start | bytes 3145736 | tf_op jit(solution)/shard_map/ppermute | solution.py:34
  172.0 4.6 %collective-permute-start.15 = (bf16[4,512,256]{2,1,0:T(8,128)(2,1)S(1)}, bf16[4,512,256]{2,1,0:T(8,128)(2,1)S(1)}, u32[]{:S(2)}, u32[]{:S(2)}) collective-permute-start(bf16[4,512,256]{2,1,0:T(8,128)(2,1)S(1)} %get-tuple-element.28), channel_id=1, source_target_pairs={{0,1},{1,0},{2,3},{3,2},{4,5},{5,4},{6,7},{7,6},{8,9},{9,8},{10,11... | collective-permute-start | bytes 3145736 | tf_op jit(solution)/shard_map/ppermute | solution.py:34
Sparse Core Ops, SparseCore 0:
  9.4 35.2 all-gather.5
  46.8 86.7 all-gather.3
